TPU v7x, 512 devices: a 8x2x16 block of a 8x8x16 slice. The times are simulated.
512 devices in a mesh: grp: 2 (over y), ep: 32 (over z, core), tp: 8 (over x).
Axes of the slice: x: 8, y: 2, z: 16, core: 2. Of those that a mesh axis runs over, the one named last changes fastest.
The devices are a block of a 8x8x16 slice.
Arguments:
- recurrence_query_input: bfloat16 [8192, 2048], P(('grp', 'ep'), 'tp'), parts along dimension 0, may hold values from -6 to 6
- forget_gate_input: bfloat16 [8192, 2048], P(('grp', 'ep'), 'tp'), parts along dimension 0, may hold values from -6.5 to 6.5
- recurrence_value_input: bfloat16 [8192, 2048], P(('grp', 'ep'), 'tp'), parts along dimension 0, may hold values from -6 to 6
- output_gate_input: bfloat16 [8192, 2048], P(('grp', 'ep'), 'tp'), parts along dimension 0, may hold values from -6 to 6
- forget_lower_margin: float32 [2048], P('tp'), may hold values from 0 to 0.1
- position_decay_extra: float32 [8192, 16], P(('grp', 'ep'), 'tp'), parts along dimension 0, may hold values from -2.1 to 0
- head_norm_gain: float32 [2048], P('tp'), may hold values from 0.1 to 1.9
- recurrence_out_weight: bfloat16 [2048, 2048], P('tp'), may hold values from -0.125 to 0.125
- expert_hidden_state: bfloat16 [8192, 2048], P(('grp', 'ep')), parts along dimension 0, may hold values from -6 to 6
- chosen_expert_index: int32 [8192, 4], P(('grp', 'ep')), parts along dimension 0, may hold values from 0 to 31, all different within a row; in each aligned block of 128 rows (0 to 127, 128 to 255, ...) at most 32 rows name the same one
- chosen_expert_score: float32 [8192, 4], P(('grp', 'ep')), parts along dimension 0, may hold values from 0.02 to 1
- expert_norm_gain: float32 [2048], replicated, may hold values from 0.1 to 1.9
- routed_gate_weight: bfloat16 [32, 2048, 1024], P('ep', None, 'tp'), may hold values from -0.125 to 0.125
- routed_up_weight: bfloat16 [32, 2048, 1024], P('ep', None, 'tp'), may hold values from -0.125 to 0.125
- routed_down_weight: bfloat16 [32, 1024, 2048], P('ep', None, 'tp'), may hold values from -0.1875 to 0.1875
- shared_gate_weight: bfloat16 [2048, 1024], P(None, 'tp'), may hold values from -0.125 to 0.125
- shared_up_weight: bfloat16 [2048, 1024], P(None, 'tp'), may hold values from -0.125 to 0.125
- shared_down_weight: bfloat16 [1024, 2048], P(None, 'tp'), may hold values from -0.1875 to 0.1875
Outputs:
- recurrence_output: bfloat16 [8192, 2048], P(('grp', 'ep', 'tp')), parts along dimension 0
- expert_out: bfloat16 [8192, 2048], P(('grp', 'ep'), 'tp'), parts along dimension 0
There are 2 independent parts, one for each index of `grp`. A program takes and returns all parts, laid end to end along the dimension named above; an argument that names none is the same for every part. Nothing has to cross between parts.
Inputs may be any that keep to these rules, and one draw needn't show every extreme that they name: `chosen_expert_index`: each row names 4 different experts. In each aligned block of 128 rows (the rows of one index of ep) no expert is named by more than 32 rows, and in every draw some block names some expert exactly 32 times.
All inputs are finite; a program needn't handle non-finite values.
Results may differ from a plain program's by a relative error of at most 0.015.
Values may be sent and summed in bfloat16 or wider, within the bound.
No kernel may reach another device: no remote copies, remote signals or barrier semaphores. Data moves between devices by JAX's collectives and lax.ppermute only.
A program may use at most 64 MiB of HBM per device.

v0:
```python
import jax
import jax.numpy as jnp
from jax import lax
from jax.sharding import Mesh
from jax.sharding import PartitionSpec as P

HEAD_CHANNELS = 128
BLK = 64
EP = ("ep_0", "ep_1")
GRP_EP = ("grp", "ep_0", "ep_1")
GRP_EP_TP = ("grp", "ep_0", "ep_1", "tp")


EPSILON = 1e-06
ROUTED_SCALE = 2.5
HIGHEST_PRECISION = lax.Precision.HIGHEST


def filled_with(array, identity):
    return jax.tree.map(
        lambda part, zero: jnp.zeros_like(part) + jnp.asarray(zero, part.dtype), array, identity
    )


def entering(array, axes, combine, identity):
    before = start = filled_with(array, identity)
    subtotal = array
    for axis in reversed(axes):
        count, index = (lax.axis_size(axis), lax.axis_index(axis))
        pieces = jax.tree.map(
            lambda part, kind: lax.all_gather(part.astype(kind), axis),
            subtotal,
            (jnp.bfloat16, jnp.bfloat16),
        )
        inside, subtotal = (start, start)
        for k in range(count):
            passed = k < index
            subtotal = combine(
                subtotal, jax.tree.map(lambda part, own: part[k].astype(own.dtype), pieces, array)
            )
            inside = jax.tree.map(lambda new, old: jnp.where(passed, new, old), subtotal, inside)
        before = combine(inside, before)
    return before


def in_blocks(array, dim, count):
    before, after = (array.shape[:dim], array.shape[dim + 1 :])
    return jnp.moveaxis(array.reshape(*before, count, -1, *after), dim, 0)


def sent_and_summed(array, axis, dim):
    pieces = in_blocks(array, dim, lax.axis_size(axis))
    arrived = lax.all_to_all(pieces, axis, split_axis=0, concat_axis=0, tiled=True)
    return arrived.astype(jnp.float32).sum(axis=0)


def joined_along(pieces, dim):
    shape = list(pieces.shape[1:])
    shape[dim] *= pieces.shape[0]
    return jnp.moveaxis(pieces, 0, dim).reshape(shape)


def copy_for_each(array, axis):
    count = lax.axis_size(axis)
    return lax.all_to_all(
        jnp.broadcast_to(array[None], (count, *array.shape)), axis, 0, 0, tiled=True
    )


def gather_directly(array, axis, dim):
    return joined_along(copy_for_each(array, axis), dim)


def sent_together(arrays, axis, dim, along):
    both = jnp.concatenate(arrays, axis=along)
    filled, at, outs = (lax.all_gather(both, axis, axis=dim, tiled=True), 0, [])
    for a in arrays:
        outs.append(lax.slice_in_dim(filled, at, at + a.shape[along], axis=along))
        at += a.shape[along]
    return tuple(outs)


def chain_states(earlier, later):
    return (earlier[0] * later[0], later[0][..., None] * earlier[1] + later[1])


def mixer_half(
    recurrence_query_input,
    forget_gate_input,
    recurrence_value_input,
    output_gate_input,
    forget_lower_margin,
    position_decay_extra,
    head_norm_gain,
    recurrence_out_weight,
):
    length = recurrence_query_input.shape[0]
    head_tensor = position_decay_extra.shape[1]
    blocks = length // BLK
    queries = jax.nn.silu(recurrence_query_input.astype(jnp.float32))
    key_gate_value = forget_lower_margin[None, :] * jax.nn.sigmoid(
        -forget_gate_input.astype(jnp.float32)
    )
    decay_logarithm = jnp.log1p(-key_gate_value) + jnp.repeat(
        position_decay_extra, HEAD_CHANNELS, axis=1
    )
    value_rows = recurrence_value_input.astype(jnp.float32)

    def split_heads(tensor):
        return tensor.reshape(blocks, BLK, head_tensor, HEAD_CHANNELS).transpose(2, 0, 1, 3)

    query_heads = split_heads(queries)
    key_heads = split_heads(key_gate_value)
    value_heads = split_heads(value_rows)
    cum_decay = jnp.cumsum(split_heads(decay_logarithm), axis=2)
    middle = cum_decay[:, :, BLK // 2 - 1 : BLK // 2]
    block_end = cum_decay[:, :, BLK - 1 : BLK]
    scores = jnp.einsum(
        "hncd,hnsd->hncs",
        query_heads * jnp.exp(cum_decay - middle),
        key_heads * jnp.exp(middle - cum_decay),
        precision=HIGHEST_PRECISION,
    )
    causal = jnp.tril(jnp.ones((BLK, BLK), dtype=bool))
    scores = jnp.where(causal, scores, 0.0)
    within = jnp.einsum("hncs,hnse->hnce", scores, value_heads, precision=HIGHEST_PRECISION)
    updates = jnp.einsum(
        "hncd,hnce->nhde",
        key_heads * jnp.exp(block_end - cum_decay),
        value_heads,
        precision=HIGHEST_PRECISION,
    )
    block_log = block_end[:, :, 0, :]
    block_decay = jnp.exp(block_log).transpose(1, 0, 2)

    def advance(carry_state, inputs):
        factor, update = inputs
        return (factor[..., None] * carry_state + update, carry_state)

    initial = jnp.zeros((head_tensor, HEAD_CHANNELS, HEAD_CHANNELS), jnp.float32)
    local_final, local_starts = lax.scan(advance, initial, (block_decay, updates))
    device_decay = jnp.exp(jnp.sum(block_log, axis=1))
    identity = (jnp.ones_like(device_decay), jnp.zeros_like(local_final))
    _, incoming = entering((device_decay, local_final), EP, chain_states, identity)
    before = jnp.exp(jnp.cumsum(block_log, axis=1) - block_log).transpose(1, 0, 2)
    starts = local_starts + before[..., None] * incoming[None]
    carried = jnp.einsum(
        "hncd,nhde->hnce", query_heads * jnp.exp(cum_decay), starts, precision=HIGHEST_PRECISION
    )
    outputs = (within + carried).transpose(1, 2, 0, 3).reshape(length, head_tensor, HEAD_CHANNELS)
    factor = lax.rsqrt(jnp.mean(outputs * outputs, axis=2, keepdims=True) + EPSILON)
    normed = (outputs * factor).reshape(length, head_tensor * HEAD_CHANNELS) * head_norm_gain[
        None, :
    ]
    gated_rows = (normed * jax.nn.silu(output_gate_input.astype(jnp.float32))).astype(jnp.bfloat16)
    mixed = sent_and_summed(
        jnp.dot(gated_rows, recurrence_out_weight, preferred_element_type=jnp.float32).astype(
            jnp.bfloat16
        ),
        "tp",
        0,
    )
    return mixed.astype(jnp.bfloat16)


def expert_half(
    expert_hidden_state,
    chosen_expert_index,
    chosen_expert_score,
    expert_norm_gain,
    routed_gate_weight,
    routed_up_weight,
    routed_down_weight,
    shared_gate_weight,
    shared_up_weight,
    shared_down_weight,
):
    tokens, top = chosen_expert_index.shape
    local_experts = routed_gate_weight.shape[0]
    devices = lax.axis_size(EP)
    experts = local_experts * devices
    capacity = min(tokens, 2 * tokens * top // experts)
    width_out = routed_down_weight.shape[2]
    features = expert_hidden_state.astype(jnp.float32)
    normed = (
        features
        * lax.rsqrt(jnp.mean(features * features, axis=1, keepdims=True) + EPSILON)
        * expert_norm_gain[None, :]
    ).astype(jnp.bfloat16)
    gates = ROUTED_SCALE * chosen_expert_score / jnp.sum(chosen_expert_score, axis=1, keepdims=True)
    flat_ids = chosen_expert_index.reshape(-1)
    onehot = (flat_ids[:, None] == jnp.arange(experts, dtype=jnp.int32)[None, :]).astype(jnp.int32)
    places = jnp.sum(onehot * (jnp.cumsum(onehot, axis=0) - 1), axis=1)
    slots = flat_ids * capacity + places
    owners = (
        jnp.full((experts * capacity,), tokens, jnp.int32)
        .at[slots]
        .set(jnp.arange(tokens * top, dtype=jnp.int32) // top)
    )
    padded = jnp.concatenate([normed, jnp.zeros((1, normed.shape[1]), jnp.bfloat16)], axis=0)
    share = capacity // lax.axis_size("tp")
    picked_owners = lax.dynamic_slice_in_dim(
        owners.reshape(experts, capacity), lax.axis_index("tp") * share, share, 1
    )
    outgoing = padded[picked_owners]
    arrived = lax.all_to_all(outgoing, EP, split_axis=0, concat_axis=0, tiled=True)
    piece = gather_directly(arrived, "tp", 1)
    grouped = piece.reshape(devices, local_experts, piece.shape[1], piece.shape[2])
    gate_part = jnp.einsum(
        "secd,edh->sech", grouped, routed_gate_weight, preferred_element_type=jnp.float32
    )
    up_part = jnp.einsum(
        "secd,edh->sech", grouped, routed_up_weight, preferred_element_type=jnp.float32
    )
    hidden = (jax.nn.silu(gate_part) * up_part).astype(jnp.bfloat16)
    hidden_rows = hidden.reshape(devices * local_experts, piece.shape[1], hidden.shape[3])
    flat_hidden = hidden_rows.reshape(experts * capacity, hidden_rows.shape[2])
    shared_hidden = (
        jax.nn.silu(jnp.dot(normed, shared_gate_weight, preferred_element_type=jnp.float32))
        * jnp.dot(normed, shared_up_weight, preferred_element_type=jnp.float32)
    ).astype(jnp.bfloat16)
    start_values = (
        jnp.zeros((experts * capacity, width_out), jnp.float32),
        jnp.zeros((tokens, width_out), jnp.float32),
    )
    routed_piece, shared_piece = sent_together((flat_hidden, shared_hidden), "tp", 1, 0)
    count = routed_piece.shape[1]
    grouped = routed_piece.reshape(devices, local_experts, capacity, count)
    routed = jnp.einsum(
        "secn,enk->seck", grouped, routed_down_weight, preferred_element_type=jnp.float32
    )
    shared = jnp.dot(shared_piece, shared_down_weight, preferred_element_type=jnp.float32)
    routed_sum = routed.reshape(start_values[0].shape)
    answers = routed_sum.astype(jnp.bfloat16).reshape(experts, capacity, width_out)
    returned = lax.all_to_all(answers, EP, split_axis=0, concat_axis=0, tiled=True)
    picked_rows = returned.reshape(experts * capacity, width_out)[slots].reshape(
        tokens, top, width_out
    )
    combined = shared + jnp.sum(gates[:, :, None] * picked_rows.astype(jnp.float32), axis=1)
    return combined.astype(jnp.bfloat16)


def per_device(
    recurrence_query_input,
    forget_gate_input,
    recurrence_value_input,
    output_gate_input,
    forget_lower_margin,
    position_decay_extra,
    head_norm_gain,
    recurrence_out_weight,
    expert_hidden_state,
    chosen_expert_index,
    chosen_expert_score,
    expert_norm_gain,
    routed_gate_weight,
    routed_up_weight,
    routed_down_weight,
    shared_gate_weight,
    shared_up_weight,
    shared_down_weight,
):
    recurrence_output = mixer_half(
        recurrence_query_input,
        forget_gate_input,
        recurrence_value_input,
        output_gate_input,
        forget_lower_margin,
        position_decay_extra,
        head_norm_gain,
        recurrence_out_weight,
    )
    expert_out = expert_half(
        expert_hidden_state,
        chosen_expert_index,
        chosen_expert_score,
        expert_norm_gain,
        routed_gate_weight,
        routed_up_weight,
        routed_down_weight,
        shared_gate_weight,
        shared_up_weight,
        shared_down_weight,
    )
    return (recurrence_output, expert_out)


def solution(mesh):
    split = Mesh(
        mesh.devices.reshape(mesh.shape["grp"], 16, 2, mesh.shape["tp"]),
        ("grp", "ep_0", "ep_1", "tp"),
    )
    in_specs = (
        P(GRP_EP, "tp"),
        P(GRP_EP, "tp"),
        P(GRP_EP, "tp"),
        P(GRP_EP, "tp"),
        P("tp"),
        P(GRP_EP, "tp"),
        P("tp"),
        P("tp", None),
        P(GRP_EP, None),
        P(GRP_EP, None),
        P(GRP_EP, None),
        P(),
        P(EP, None, "tp"),
        P(EP, None, "tp"),
        P(EP, None, "tp"),
        P(None, "tp"),
        P(None, "tp"),
        P(None, "tp"),
    )
    out_specs = (P(GRP_EP_TP, None), P(GRP_EP, "tp"))
    return jax.shard_map(
        per_device, mesh=split, in_specs=in_specs, out_specs=out_specs, check_vma=False
    )
```

profile of v0, /device:TPU:65, one launch (start us, length us, event | category | flops | bytes accessed | tf_op | source)
XLA Modules:
  0.0 336.5 jit_solution(10852370283299126797)
XLA Ops:
  7.2 0.8 broadcast_multiply_fusion
  8.0 0.8 copy.58
  9.0 1.2 fusion.5
  10.5 1.2 reduce-window.6
  11.6 0.2 slice_reduce_fusion
  12.0 2.4 scatter_custom_fusion
  14.7 1.2 fusion.7
  16.0 0.9 gather_fusion
  17.0 0.2 reshape.327
  17.2 78.3 %all_to_all.20 = bf16[32,4,2048]{2,1,0:T(4,128)(2,1)S(1)} all-to-all(bf16[32,4,2048]{2,1,0:T(4,128)(2,1)S(1)} %reshape.327), channel_id=1, replica_groups=mesh['grp'=2,'ep_0'=16,'ep_1'=2,'tp'=8] {'ep_0','ep_1'}, dimensions={0} | all-to-all | bytes 1048576 | tf_op jit(solution)/shard_map/all_to_all | solution.py:206
  95.4 4.1 %broadcast_in_dim.34 = bf16[8,32,4,2048]{3,2,1,0:T(4,128)(2,1)} broadcast(bf16[32,4,2048]{2,1,0:T(4,128)(2,1)S(1)} %all_to_all.20), dimensions={1,2,3} | broadcast | bytes 4718592 | tf_op jit(solution)/shard_map/broadcast_in_dim | solution.py:66
  99.6 7.2 %all-to-all-start.2 = ((bf16[8,32,4,2048]{3,2,1,0:T(4,128)(2,1)}), bf16[8,32,4,2048]{3,2,1,0:T(4,128)(2,1)}, u32[]{:S(2)}, u32[]{:S(2)}) async-start(bf16[8,32,4,2048]{3,2,1,0:T(4,128)(2,1)} %broadcast_in_dim.34), calls=%async_computation.2 | async-start | bytes 8388608 | tf_op jit(solution)/shard_map/all_to_all | solution.py:65
  107.0 0.2 broadcast_in_dim.28
  107.5 0.1 reduce_window_sum.35
  107.7 0.4 fusion.26
  108.1 0.4 while.13
  108.1 0.1 bitcast_add_fusion.3
  108.3 0.1 bitcast_add_fusion.3
  108.5 2.3 all-gather.2
  110.8 1.9 all-gather.1
  112.7 0.8 fusion.37
  113.6 0.2 all-gather.8.cloned.1.call-start
  113.8 0.3 fusion.76
  114.1 1.3 fusion.4
  115.5 88.1 %all-to-all-done.2 = bf16[8,32,4,2048]{3,2,1,0:T(4,128)(2,1)} async-done(((bf16[8,32,4,2048]{3,2,1,0:T(4,128)(2,1)}), bf16[8,32,4,2048]{3,2,1,0:T(4,128)(2,1)}, u32[]{:S(2)}, u32[]{:S(2)}) %all-to-all-start.2) | async-done | bytes 4194336 | tf_op jit(solution)/shard_map/all_to_all | solution.py:65
  203.6 7.1 %copy.61 = bf16[32,8,4,2048]{3,2,1,0:T(4,128)(2,1)} copy(bf16[32,8,4,2048]{3,2,0,1:T(4,128)(2,1)} %bitcast.40) | data formatting | bytes 8388608 | tf_op jit(solution)/shard_map/transpose | solution.py:60
  210.7 7.0 %reshape.302 = bf16[32,32,2048]{2,1,0:T(8,128)(2,1)} reshape(bf16[32,8,4,2048]{3,2,1,0:T(4,128)(2,1)} %copy.61) | data formatting | bytes 8388608 | tf_op jit(solution)/shard_map/reshape.5
  217.7 3.6 %convolution_bitcast_fusion.1 = f32[32,1,32,128]{3,2,0,1:T(8,128)S(1)} fusion(bf16[32,32,2048]{2,1,0:T(8,128)(2,1)} %reshape.302, bf16[1,2048,128]{2,1,0:T(8,128)(2,1)S(1)} %copy-done.2), kind=kOutput, calls=%fused_computation.12 | convolution fusion | flops 536870912 | bytes 5242880 | tf_op jit(solution)/shard_map/secd,edh->sech/dot_general | solution.py:209
  221.3 1.2 fusion.1
  222.6 0.8 pad_maximum_fusion
  223.6 21.1 %all_gather.22 = bf16[16,2,128]{2,1,0:T(2,128)(2,1)S(1)} all-gather(bf16[1,2,128]{2,1,0:T(2,128)(2,1)S(1)} %get-tuple-element.98), channel_id=1, replica_groups=mesh['grp'=2,'ep_0'=16,'ep_1'=2,'tp'=8] {'ep_0'}, dimensions={0}, use_global_device_ids=true | all-gather | bytes 8704 | tf_op jit(solution)/shard_map/all_gather | solution.py:31
  244.7 0.4 convolution_select_fusion
  245.1 0.2 fusion.41
  245.3 2.0 fusion.25
  247.3 0.5 multiply_reduce_fusion.1
  248.1 0.2 mul.385
  248.3 1.1 convolution_convert_fusion
  249.5 3.7 %all-to-all-start = ((bf16[8,16,2048]{2,1,0:T(8,128)(2,1)}), bf16[8,16,2048]{2,1,0:T(8,128)(2,1)S(1)}, u32[]{:S(2)}, u32[]{:S(2)}) async-start(bf16[8,16,2048]{2,1,0:T(8,128)(2,1)} %bitcast.36), calls=%async_computation | async-start | bytes 1048576 | tf_op jit(solution)/shard_map/all_to_all | solution.py:53
  253.2 15.0 %all-gather.8.cloned.1.call-done = bf16[1152,1024]{1,0:T(8,128)(2,1)} async-done(((bf16[1152,128]{1,0:T(8,128)(2,1)}), bf16[1152,1024]{1,0:T(8,128)(2,1)}) %all-gather.8.cloned.1.call-update) | async-done | bytes 2359312 | tf_op jit(solution)/shard_map/all_gather | solution.py:76
  268.2 1.6 slice-done
  269.8 2.6 convolution_convert_fusion.1
  272.5 19.5 %all-to-all-start.3 = ((bf16[32,32,256]{2,1,0:T(8,128)(2,1)}), bf16[32,32,256]{2,1,0:T(8,128)(2,1)S(1)}, u32[]{:S(2)}, u32[]{:S(2)}) async-start(bf16[32,32,256]{2,1,0:T(8,128)(2,1)} %convolution_convert_fusion.1), calls=%async_computation.3 | async-start | bytes 1048576 | tf_op jit(solution)/shard_map/all_to_all | solution.py:235
  292.2 0.7 reduce_sum.70
  292.9 32.4 %all-to-all-done.3 = bf16[32,32,256]{2,1,0:T(8,128)(2,1)S(1)} async-done(((bf16[32,32,256]{2,1,0:T(8,128)(2,1)}), bf16[32,32,256]{2,1,0:T(8,128)(2,1)S(1)}, u32[]{:S(2)}, u32[]{:S(2)}) %all-to-all-start.3) | async-done | bytes 524320 | tf_op jit(solution)/shard_map/all_to_all | solution.py:235
  325.3 1.9 gather_fusion.1
  327.3 0.1 reshape.325
  327.4 0.4 multiply_reduce_fusion
  327.8 1.8 fusion.3
  (82 shorter events, 2.2 us)
Async XLA Ops:
  7.2 241.1 %copy-start = (bf16[256,2048]{1,0:T(8,128)(2,1)S(1)}, bf16[256,2048]{1,0:T(8,128)(2,1)}, u32[]{:S(2)}) copy-start(bf16[256,2048]{1,0:T(8,128)(2,1)} %param.27) | copy-start | bytes 3145732
  99.5 7.3 %copy-start.11 = (f32[128,2]{0,1:T(2,128)S(1)}, f32[128,2]{0,1:T(2,128)}, u32[]{:S(2)}) copy-start(f32[128,2]{0,1:T(2,128)} %param.25) | copy-start | bytes 3076
  99.5 7.6 %copy-start.5 = (bf16[128,256]{1,0:T(8,128)(2,1)S(1)}, bf16[128,256]{1,0:T(8,128)(2,1)}, u32[]{:S(2)}) copy-start(bf16[128,256]{1,0:T(8,128)(2,1)} %param.21) | copy-start | bytes 196612
  99.5 7.6 %copy-start.12 = (f32[256]{0:T(256)S(1)}, f32[256]{0:T(256)}, u32[]{:S(2)}) copy-start(f32[256]{0:T(256)} %param.24) | copy-start | bytes 3076
  99.6 7.9 %copy-start.8 = (bf16[128,256]{1,0:T(8,128)(2,1)S(1)}, bf16[128,256]{1,0:T(8,128)(2,1)}, u32[]{:S(2)}) copy-start(bf16[128,256]{1,0:T(8,128)(2,1)} %param.22) | copy-start | bytes 196612
  99.6 104.0 %all-to-all-start.2 = ((bf16[8,32,4,2048]{3,2,1,0:T(4,128)(2,1)}), bf16[8,32,4,2048]{3,2,1,0:T(4,128)(2,1)}, u32[]{:S(2)}, u32[]{:S(2)}) async-start(bf16[8,32,4,2048]{3,2,1,0:T(4,128)(2,1)} %broadcast_in_dim.34), calls=%async_computation.2 | async-start | bytes 8388608 | tf_op jit(solution)/shard_map/all_to_all | solution.py:65
  106.7 7.1 %copy-start.3 = (bf16[2048,128]{1,0:T(8,128)(2,1)S(1)}, bf16[2048,128]{1,0:T(8,128)(2,1)}, u32[]{:S(2)}) copy-start(bf16[2048,128]{1,0:T(8,128)(2,1)} %param.35) | copy-start | bytes 1572868
  106.7 138.6 %all-gather.6.cloned.1.call-start = ((), (), s32[]{:S(2)}) async-start(), calls=%async_computation.4 | async-start | bytes 1114112 | tf_op jit(solution)/shard_map/all_gather | solution.py:31
  113.6 154.7 %all-gather.8.cloned.1.call-start = ((), (), s32[]{:S(2)}) async-start(), calls=%async_computation.5 | async-start | bytes 2654208 | tf_op jit(solution)/shard_map/all_gather | solution.py:76
  210.7 7.0 %copy-start.2 = (bf16[1,2048,128]{2,1,0:T(8,128)(2,1)S(1)}, bf16[1,2048,128]{2,1,0:T(8,128)(2,1)}, u32[]{:S(2)}) copy-start(bf16[1,2048,128]{2,1,0:T(8,128)(2,1)} %param.32) | copy-start | bytes 1572868
  217.7 3.6 %copy-start.1 = (bf16[32,32,2048]{2,1,0:T(8,128)(2,1)S(1)}, bf16[32,32,2048]{2,1,0:T(8,128)(2,1)}, u32[]{:S(2)}) copy-start(bf16[32,32,2048]{2,1,0:T(8,128)(2,1)} %reshape.302) | copy-start | bytes 12582916
  217.7 3.6 %copy-start.13 = (bf16[1,2048,128]{2,1,0:T(8,128)(2,1)S(1)}, bf16[1,2048,128]{2,1,0:T(8,128)(2,1)}, u32[]{:S(2)}) copy-start(bf16[1,2048,128]{2,1,0:T(8,128)(2,1)} %param.33) | copy-start | bytes 1572868
  221.3 2.1 copy-start.6
  222.6 25.7 %copy-start.7 = (bf16[128,256]{1,0:T(8,128)(2,1)S(1)}, bf16[128,256]{1,0:T(8,128)(2,1)}, u32[]{:S(2)}) copy-start(bf16[128,256]{1,0:T(8,128)(2,1)} %param.23) | copy-start | bytes 196612
  222.6 25.7 %copy-start.10 = (f32[256]{0:T(256)S(1)}, f32[256]{0:T(256)}, u32[]{:S(2)}) copy-start(f32[256]{0:T(256)} %param.26) | copy-start | bytes 3076
  249.5 23.0 %all-to-all-start = ((bf16[8,16,2048]{2,1,0:T(8,128)(2,1)}), bf16[8,16,2048]{2,1,0:T(8,128)(2,1)S(1)}, u32[]{:S(2)}, u32[]{:S(2)}) async-start(bf16[8,16,2048]{2,1,0:T(8,128)(2,1)} %bitcast.36), calls=%async_computation | async-start | bytes 1048576 | tf_op jit(solution)/shard_map/all_to_all | solution.py:53
  253.2 38.8 %copy-start.9 = (f32[128,4]{0,1:T(4,128)S(1)}, f32[128,4]{0,1:T(4,128)}, u32[]{:S(2)}) copy-start(f32[128,4]{0,1:T(4,128)} %param.30) | copy-start | bytes 6148
  268.2 1.6 slice-start
  269.8 58.0 %copy-start.4 = (bf16[1024,256]{1,0:T(8,128)(2,1)S(1)}, bf16[1024,256]{1,0:T(8,128)(2,1)}, u32[]{:S(2)}) copy-start(bf16[1024,256]{1,0:T(8,128)(2,1)} %param.37) | copy-start | bytes 1572868
  272.5 52.8 %all-to-all-start.3 = ((bf16[32,32,256]{2,1,0:T(8,128)(2,1)}), bf16[32,32,256]{2,1,0:T(8,128)(2,1)S(1)}, u32[]{:S(2)}, u32[]{:S(2)}) async-start(bf16[32,32,256]{2,1,0:T(8,128)(2,1)} %convolution_convert_fusion.1), calls=%async_computation.3 | async-start | bytes 1048576 | tf_op jit(solution)/shard_map/all_to_all | solution.py:235
Sparse Core Ops, SparseCore 0:
  113.7 56.6 all-gather.5
  223.5 44.6 all-gather.7
where the time goes:
time: 337 us; the launch traced here: 336 us
  waiting for transfers between devices  136 us (40%)
  blocking collectives  104 us (31%)
  starting transfers between devices  30.7 us (9%)
  local copies, waits for them, and re-layouts  28.3 us (8%)
  between operations  14.6 us (4%)
  matrix products  13.5 us (4%)
  other arithmetic  9.96 us (3%)
    all_to_all x1, waiting for transfers between devices, copy_for_each(): lax.all_to_all(jnp.broadcast_to(array[None], (count, *array.shape)), axis...  88.1 us
    all_to_all x1, blocking collectives, expert_half(): lax.all_to_all(outgoing, EP, split_axis=0, concat_axis=0, tiled=True)  78.3 us
    all_to_all x1, waiting for transfers between devices, expert_half(): lax.all_to_all(answers, EP, split_axis=0, concat_axis=0, tiled=True)  32.4 us
    all_gather x3, blocking collectives, entering(): lax.all_gather(part.astype(kind), axis)  25.3 us
    all_to_all x1, starting transfers between devices, expert_half(): lax.all_to_all(answers, EP, split_axis=0, concat_axis=0, tiled=True)  19.5 us
    all_gather x1, waiting for transfers between devices, sent_together(): filled, at, outs = (lax.all_gather(both, axis, axis=dim, tiled=True), 0, [])  15 us
    all_to_all x1, starting transfers between devices, copy_for_each(): lax.all_to_all(jnp.broadcast_to(array[None], (count, *array.shape)), axis...  7.18 us
    transpose x1, local copies, waits for them, and re-layouts, joined_along(): return jnp.moveaxis(pieces, 0, dim).reshape(shape)  7.15 us
  transfers between devices with their start and end apart: 5, of which 3 were waited for; matrix products, arithmetic and copies ran while one was open for 9% of the time, Pallas kernels for 0%

commit v1 on v0

--- a/solution.py
+++ b/solution.py
@@ -16,31 +16,18 @@
 HIGHEST_PRECISION = lax.Precision.HIGHEST
 
 
-def filled_with(array, identity):
-    return jax.tree.map(
-        lambda part, zero: jnp.zeros_like(part) + jnp.asarray(zero, part.dtype), array, identity
-    )
-
-
-def entering(array, axes, combine, identity):
-    before = start = filled_with(array, identity)
-    subtotal = array
-    for axis in reversed(axes):
-        count, index = (lax.axis_size(axis), lax.axis_index(axis))
-        pieces = jax.tree.map(
-            lambda part, kind: lax.all_gather(part.astype(kind), axis),
-            subtotal,
-            (jnp.bfloat16, jnp.bfloat16),
-        )
-        inside, subtotal = (start, start)
-        for k in range(count):
-            passed = k < index
-            subtotal = combine(
-                subtotal, jax.tree.map(lambda part, own: part[k].astype(own.dtype), pieces, array)
-            )
-            inside = jax.tree.map(lambda new, old: jnp.where(passed, new, old), subtotal, inside)
-        before = combine(inside, before)
-    return before
+def shifted(array, axis, step):
+    count = lax.axis_size(axis)
+    return lax.ppermute(array, axis, [(i, (i + step) % count) for i in range(count)])
+
+
+def swapped(array, axis):
+    count = lax.axis_size(axis)
+    return lax.ppermute(array, axis, [(i, i ^ 1) for i in range(count)])
+
+
+def exchanged(array, axis):
+    return lax.all_to_all(array, axis, split_axis=0, concat_axis=0, tiled=True)
 
 
 def in_blocks(array, dim, count):
@@ -50,8 +37,7 @@
 
 def sent_and_summed(array, axis, dim):
     pieces = in_blocks(array, dim, lax.axis_size(axis))
-    arrived = lax.all_to_all(pieces, axis, split_axis=0, concat_axis=0, tiled=True)
-    return arrived.astype(jnp.float32).sum(axis=0)
+    return exchanged(pieces, axis).astype(jnp.float32).sum(axis=0)
 
 
 def joined_along(pieces, dim):
@@ -62,26 +48,42 @@
 
 def copy_for_each(array, axis):
     count = lax.axis_size(axis)
-    return lax.all_to_all(
-        jnp.broadcast_to(array[None], (count, *array.shape)), axis, 0, 0, tiled=True
-    )
-
-
-def gather_directly(array, axis, dim):
-    return joined_along(copy_for_each(array, axis), dim)
-
-
-def sent_together(arrays, axis, dim, along):
-    both = jnp.concatenate(arrays, axis=along)
-    filled, at, outs = (lax.all_gather(both, axis, axis=dim, tiled=True), 0, [])
-    for a in arrays:
-        outs.append(lax.slice_in_dim(filled, at, at + a.shape[along], axis=along))
-        at += a.shape[along]
-    return tuple(outs)
-
-
-def chain_states(earlier, later):
-    return (earlier[0] * later[0], later[0][..., None] * earlier[1] + later[1])
+    return exchanged(jnp.broadcast_to(array[None], (count, *array.shape)), axis)
+
+
+def in_parts(array, count):
+    parts, rest = [], array
+    for _ in range(count):
+        rounded = lax.reduce_precision(rest, 8, 7)
+        parts.append(rounded.astype(jnp.bfloat16))
+        rest = rest - rounded
+    return parts
+
+
+def entering_state(log_decay, state):
+    devices = lax.axis_size(EP)
+    channels, width = state.shape
+    part = channels // devices
+    logs = jnp.stack(in_parts(log_decay, 3), axis=-1).reshape(devices, part, 3)
+    logs = jnp.pad(logs, ((0, 0), (0, 0), (0, HEAD_CHANNELS - 3)))
+    packed = jnp.concatenate(
+        [state.astype(jnp.bfloat16).reshape(devices, part, width), logs], axis=2
+    )
+    arrived = exchanged(packed, EP).astype(jnp.float32)
+    updates = arrived[:, :, :width]
+    logs = jnp.sum(arrived[:, :, width : width + 3], axis=2)
+    at = jnp.arange(devices)
+    between = (at[None, None, :] > at[None, :, None]) & (at[None, None, :] < at[:, None, None])
+    spans = jnp.dot(
+        between.reshape(devices * devices, devices).astype(jnp.float32),
+        logs,
+        precision=HIGHEST_PRECISION,
+    ).reshape(devices, devices, part)
+    earlier = at[None, :, None] < at[:, None, None]
+    factors = jnp.where(earlier, jnp.exp(spans), 0.0)
+    prefix = jnp.einsum("rqc,qcv->rcv", factors, updates, precision=HIGHEST_PRECISION)
+    returned = exchanged(prefix.astype(jnp.bfloat16), EP)
+    return returned.astype(jnp.float32).reshape(channels, width)
 
 
 def mixer_half(
@@ -139,9 +141,9 @@
 
     initial = jnp.zeros((head_tensor, HEAD_CHANNELS, HEAD_CHANNELS), jnp.float32)
     local_final, local_starts = lax.scan(advance, initial, (block_decay, updates))
-    device_decay = jnp.exp(jnp.sum(block_log, axis=1))
-    identity = (jnp.ones_like(device_decay), jnp.zeros_like(local_final))
-    _, incoming = entering((device_decay, local_final), EP, chain_states, identity)
+    incoming = entering_state(
+        jnp.sum(block_log, axis=1).reshape(-1), local_final.reshape(-1, HEAD_CHANNELS)
+    ).reshape(head_tensor, HEAD_CHANNELS, HEAD_CHANNELS)
     before = jnp.exp(jnp.cumsum(block_log, axis=1) - block_log).transpose(1, 0, 2)
     starts = local_starts + before[..., None] * incoming[None]
     carried = jnp.einsum(
@@ -181,6 +183,20 @@
     experts = local_experts * devices
     capacity = min(tokens, 2 * tokens * top // experts)
     width_out = routed_down_weight.shape[2]
+    width_members = lax.axis_size("tp")
+    quads = width_members // 2
+    member = lax.axis_index("tp")
+    parity, quad = (member % 2, member // 2)
+    share = capacity // width_members
+    half = capacity // 2
+    width_in = routed_gate_weight.shape[1]
+    units = routed_gate_weight.shape[2]
+
+    own_in = jnp.concatenate([routed_gate_weight[0], routed_up_weight[0]], axis=1)
+    partner_in = swapped(own_in, "tp")
+    own_down = routed_down_weight[0]
+    partner_down = swapped(own_down, "tp")
+
     features = expert_hidden_state.astype(jnp.float32)
     normed = (
         features
@@ -188,55 +204,91 @@
         * expert_norm_gain[None, :]
     ).astype(jnp.bfloat16)
     gates = ROUTED_SCALE * chosen_expert_score / jnp.sum(chosen_expert_score, axis=1, keepdims=True)
-    flat_ids = chosen_expert_index.reshape(-1)
-    onehot = (flat_ids[:, None] == jnp.arange(experts, dtype=jnp.int32)[None, :]).astype(jnp.int32)
-    places = jnp.sum(onehot * (jnp.cumsum(onehot, axis=0) - 1), axis=1)
-    slots = flat_ids * capacity + places
-    owners = (
-        jnp.full((experts * capacity,), tokens, jnp.int32)
-        .at[slots]
-        .set(jnp.arange(tokens * top, dtype=jnp.int32) // top)
-    )
-    padded = jnp.concatenate([normed, jnp.zeros((1, normed.shape[1]), jnp.bfloat16)], axis=0)
-    share = capacity // lax.axis_size("tp")
-    picked_owners = lax.dynamic_slice_in_dim(
-        owners.reshape(experts, capacity), lax.axis_index("tp") * share, share, 1
-    )
-    outgoing = padded[picked_owners]
-    arrived = lax.all_to_all(outgoing, EP, split_axis=0, concat_axis=0, tiled=True)
-    piece = gather_directly(arrived, "tp", 1)
-    grouped = piece.reshape(devices, local_experts, piece.shape[1], piece.shape[2])
-    gate_part = jnp.einsum(
-        "secd,edh->sech", grouped, routed_gate_weight, preferred_element_type=jnp.float32
-    )
-    up_part = jnp.einsum(
-        "secd,edh->sech", grouped, routed_up_weight, preferred_element_type=jnp.float32
-    )
-    hidden = (jax.nn.silu(gate_part) * up_part).astype(jnp.bfloat16)
-    hidden_rows = hidden.reshape(devices * local_experts, piece.shape[1], hidden.shape[3])
-    flat_hidden = hidden_rows.reshape(experts * capacity, hidden_rows.shape[2])
+    named = chosen_expert_index[:, :, None] == jnp.arange(experts, dtype=jnp.int32)[None, None, :]
+    chosen = jnp.any(named, axis=1)
+    gate_of = jnp.sum(jnp.where(named, gates[:, :, None], 0.0), axis=1)
+    row = jnp.arange(tokens)
+    places = jnp.dot(
+        (row[None, :] < row[:, None]).astype(jnp.bfloat16),
+        chosen.astype(jnp.bfloat16),
+        preferred_element_type=jnp.float32,
+    )
+    places = jnp.where(chosen, places.astype(jnp.int32), -1)
+    first = parity * half + quad * share
+    picks = places.T[:, None, :] == first + jnp.arange(share)[None, :, None]
+    outgoing = jnp.dot(
+        picks.reshape(experts * share, tokens).astype(jnp.bfloat16),
+        normed,
+        preferred_element_type=jnp.float32,
+    ).astype(jnp.bfloat16)
+    arrived = exchanged(outgoing.reshape(devices, share, width_in), EP)
+    chunk = arrived.reshape(devices * share, width_in)
+    rows = chunk.shape[0]
+
     shared_hidden = (
         jax.nn.silu(jnp.dot(normed, shared_gate_weight, preferred_element_type=jnp.float32))
         * jnp.dot(normed, shared_up_weight, preferred_element_type=jnp.float32)
     ).astype(jnp.bfloat16)
-    start_values = (
-        jnp.zeros((experts * capacity, width_out), jnp.float32),
-        jnp.zeros((tokens, width_out), jnp.float32),
-    )
-    routed_piece, shared_piece = sent_together((flat_hidden, shared_hidden), "tp", 1, 0)
-    count = routed_piece.shape[1]
-    grouped = routed_piece.reshape(devices, local_experts, capacity, count)
-    routed = jnp.einsum(
-        "secn,enk->seck", grouped, routed_down_weight, preferred_element_type=jnp.float32
-    )
+    shared_piece = joined_along(copy_for_each(shared_hidden, "tp"), 1)
     shared = jnp.dot(shared_piece, shared_down_weight, preferred_element_type=jnp.float32)
-    routed_sum = routed.reshape(start_values[0].shape)
-    answers = routed_sum.astype(jnp.bfloat16).reshape(experts, capacity, width_out)
-    returned = lax.all_to_all(answers, EP, split_axis=0, concat_axis=0, tiled=True)
-    picked_rows = returned.reshape(experts * capacity, width_out)[slots].reshape(
-        tokens, top, width_out
-    )
-    combined = shared + jnp.sum(gates[:, :, None] * picked_rows.astype(jnp.float32), axis=1)
+
+    def hidden_of(piece):
+        sides = []
+        for matrix in (own_in, partner_in):
+            both = jnp.dot(piece, matrix, preferred_element_type=jnp.float32)
+            sides.append((jax.nn.silu(both[:, :units]) * both[:, units:]).astype(jnp.bfloat16))
+        return jnp.concatenate(sides, axis=1)
+
+    from_before = shifted(chunk, "tp", 2)
+    from_after = shifted(chunk, "tp", -2)
+    across_first = shifted(from_before[: rows // 2], "tp", 2)
+    across_second = shifted(from_after[rows // 2 :], "tp", -2)
+    hidden_own = hidden_of(chunk)
+    hidden_sides = hidden_of(jnp.concatenate([from_after, from_before], axis=0))
+    hidden_across = hidden_of(jnp.concatenate([across_first, across_second], axis=0))
+    around = [hidden_own, hidden_sides[:rows], hidden_across, hidden_sides[rows:]]
+    hidden = lax.dynamic_slice_in_dim(
+        jnp.concatenate(around + around, axis=0), (quads - quad) % quads * rows, quads * rows, 0
+    )
+
+    middle = quads * rows // 2
+    hidden_before = shifted(hidden, "tp", 2)
+    hidden_after = shifted(hidden, "tp", -2)
+    hidden_far = jnp.concatenate(
+        [shifted(hidden_before[:middle], "tp", 2), shifted(hidden_after[middle:], "tp", -2)], axis=0
+    )
+
+    def down_of(step):
+        at = (quad + step) % quads * 2
+        blocks = []
+        for side in (parity, 1 - parity):
+            place = (at + side) * units
+            blocks.append(
+                jnp.concatenate(
+                    [
+                        lax.dynamic_slice_in_dim(matrix, place, units, 0)
+                        for matrix in (own_down, partner_down)
+                    ],
+                    axis=1,
+                )
+            )
+        return jnp.concatenate(blocks, axis=0)
+
+    def product(piece, step):
+        return jnp.dot(piece, down_of(step), preferred_element_type=jnp.float32)
+
+    routed = product(hidden, 0) + product(hidden_before, -1) + product(hidden_after, 1)
+    routed = routed + product(hidden_far, 2)
+    answers = routed.astype(jnp.bfloat16).reshape(quads, devices, share, 2 * width_out)
+    answers = answers.transpose(1, 0, 2, 3).reshape(devices, half, 2 * width_out)
+    returned = exchanged(answers, EP).reshape(experts * half, 2 * width_out)
+    filled = places[:, :, None] == parity * half + jnp.arange(half)[None, None, :]
+    mixing = jnp.where(filled, gate_of[:, :, None], 0.0).reshape(tokens, experts * half)
+    combined = sum(
+        jnp.dot(part, returned, preferred_element_type=jnp.float32) for part in in_parts(mixing, 3)
+    )
+    other = swapped(combined[:, width_out:].astype(jnp.bfloat16), "tp")
+    combined = shared + combined[:, :width_out] + other.astype(jnp.float32)
     return combined.astype(jnp.bfloat16)
 
 

time: 337 us -> 289 us (0.86); the launches traced: 336 us -> 285 us
  starting transfers between devices: 30.7 us -> 137 us
  blocking collectives: 104 us -> 0 us
  waiting for transfers between devices: 136 us -> 109 us
  local copies, waits for them, and re-layouts: 28.3 us -> 10.9 us
  between operations: 14.6 us -> 1.97 us
    all_to_all x1 -> x0, blocking collectives: 78.3 us -> none  [expert_half(): lax.all_to_all(outgoing, EP, split_axis=0, concat_axis=0, tiled=True)]
    all_to_all x3 -> x6, starting transfers between devices: 30.4 us -> 96.3 us  [exchanged(): return lax.all_to_all(array, axis, split_axis=0, concat_axis=0, tiled=True)]
    ppermute x0 -> x11, starting transfers between devices: none -> 41.1 us  [the longest x8 32.6 us: shifted(): lax.ppermute(array, axis, [(i, (i + step) % count) for i in range(count)])]
    all_to_all x3 -> x6, waiting for transfers between devices: 121 us -> 81.2 us  [exchanged(): return lax.all_to_all(array, axis, split_axis=0, concat_axis=0, tiled=True)]
    ppermute x0 -> x11, waiting for transfers between devices: none -> 28.3 us  [the longest x8 28.3 us: shifted(): lax.ppermute(array, axis, [(i, (i + step) % count) for i in range(count)])]
    all_gather x3 -> x0, blocking collectives: 25.3 us -> none  [entering(): lax.all_gather(part.astype(kind), axis)]
    all_gather x2 -> x0, waiting for transfers between devices: 15.1 us -> none  [the longest x1 15 us: sent_together(): filled, at, outs = (lax.all_gather(both, axis, axis=dim, tiled=True), 0, [])]
    another operation x2 -> x0, local copies, waits for them, and re-layouts: 6.97 us -> none
  transfers between devices with their start and end apart: 5 -> 17, of which waited for: 3 -> 10; matrix products, arithmetic and copies ran while one was open for 9% -> 10% of each run, Pallas kernels for 0% -> 0%
where the time goes in v1:
time: 289 us; the launch traced here: 285 us
  starting transfers between devices  137 us (47%)
  waiting for transfers between devices  109 us (38%)
  matrix products  15.7 us (5%)
  local copies, waits for them, and re-layouts  10.9 us (4%)
  other arithmetic  9.35 us (3%)
    all_to_all x6, starting transfers between devices, exchanged(): return lax.all_to_all(array, axis, split_axis=0, concat_axis=0, tiled=True)  96.3 us
    all_to_all x6, waiting for transfers between devices, exchanged(): return lax.all_to_all(array, axis, split_axis=0, concat_axis=0, tiled=True)  81.2 us
    ppermute x8, starting transfers between devices, shifted(): lax.ppermute(array, axis, [(i, (i + step) % count) for i in range(count)])  32.6 us
    ppermute x8, waiting for transfers between devices, shifted(): lax.ppermute(array, axis, [(i, (i + step) % count) for i in range(count)])  28.3 us
    ppermute x3, starting transfers between devices, swapped(): return lax.ppermute(array, axis, [(i, i ^ 1) for i in range(count)])  8.57 us
  transfers between devices with their start and end apart: 17, of which 10 were waited for; matrix products, arithmetic and copies ran while one was open for 10% of the time, Pallas kernels for 0%

profile of v1, /device:TPU:65, one launch (start us, length us, event | category | flops | bytes accessed | tf_op | source)
XLA Modules:
  0.0 284.9 jit_solution(14920814409064800851)
XLA Ops:
  0.7 0.9 copy.147
  1.7 0.9 divide_multiply_fusion
  4.7 1.6 while.13
  4.7 0.7 bitcast_dynamic-update-slice_fusion.2
  6.7 0.7 fusion.63
  7.4 45.2 %all-to-all-start = ((bf16[32,8,256]{2,1,0:T(8,128)(2,1)}), bf16[32,8,256]{2,1,0:T(8,128)(2,1)S(1)}, u32[]{:S(2)}, u32[]{:S(2)}) async-start(bf16[32,8,256]{2,1,0:T(8,128)(2,1)} %fusion.63), calls=%async_computation | async-start | bytes 262144 | tf_op jit(solution)/shard_map/all_to_all | solution.py:30
  53.5 1.0 reshape.243
  54.5 13.9 %all-to-all-done = bf16[32,8,256]{2,1,0:T(8,128)(2,1)S(1)} async-done(((bf16[32,8,256]{2,1,0:T(8,128)(2,1)}), bf16[32,8,256]{2,1,0:T(8,128)(2,1)S(1)}, u32[]{:S(2)}, u32[]{:S(2)}) %all-to-all-start) | async-done | bytes 131104 | tf_op jit(solution)/shard_map/all_to_all | solution.py:30
  68.4 5.2 %all-to-all-start.4 = ((bf16[32,4,2048]{2,1,0:T(4,128)(2,1)}), bf16[32,4,2048]{2,1,0:T(4,128)(2,1)S(1)}, u32[]{:S(2)}, u32[]{:S(2)}) async-start(bf16[32,4,2048]{2,1,0:T(4,128)(2,1)} %reshape.243), calls=%async_computation.4 | async-start | bytes 1048576 | tf_op jit(solution)/shard_map/all_to_all | solution.py:30
  73.7 2.1 pad_maximum_fusion
  75.8 3.2 %collective-permute-start = (bf16[2048,256]{1,0:T(8,128)(2,1)}, bf16[2048,256]{1,0:T(8,128)(2,1)S(1)}, u32[]{:S(2)}, u32[]{:S(2)}) collective-permute-start(bf16[2048,256]{1,0:T(8,128)(2,1)} %pad_maximum_fusion), channel_id=1, source_target_pairs={{0,1},{1,0},{2,3},{3,2},{4,5},{5,4},{6,7},{7,6},{8,9},{9,8},{10,11... | collective-permute-start | bytes 3145736 | tf_op jit(solution)/shard_map/ppermute | solution.py:26
  79.1 2.2 collective-permute-start.5
  82.1 1.8 dynamic-slice_bitcast_fusion.3
  83.9 0.7 copy.182
  84.6 0.7 convert_reduce_fusion
  85.3 2.5 fusion.5
  87.9 19.2 %all-to-all-done.4 = bf16[32,4,2048]{2,1,0:T(4,128)(2,1)S(1)} async-done(((bf16[32,4,2048]{2,1,0:T(4,128)(2,1)}), bf16[32,4,2048]{2,1,0:T(4,128)(2,1)S(1)}, u32[]{:S(2)}, u32[]{:S(2)}) %all-to-all-start.4) | async-done | bytes 524320 | tf_op jit(solution)/shard_map/all_to_all | solution.py:30
  107.1 0.9 reshape.244
  108.0 6.2 %collective-permute-start.1 = (bf16[128,2048]{1,0:T(8,128)(2,1)}, bf16[128,2048]{1,0:T(8,128)(2,1)S(1)}, u32[]{:S(2)}, u32[]{:S(2)}) collective-permute-start(bf16[128,2048]{1,0:T(8,128)(2,1)} %reshape.244), channel_id=1, source_target_pairs={{0,6},{1,7},{2,0},{3,1},{4,2},{5,3},{6,4},{7,5},{8,14},{9,15},{10,... | collective-permute-start | bytes 1572872 | tf_op jit(solution)/shard_map/ppermute | solution.py:21
  114.2 2.0 collective-permute-start.2
  116.2 1.7 fusion.130
  118.3 18.3 %collective-permute-done.1 = bf16[128,2048]{1,0:T(8,128)(2,1)S(1)} collective-permute-done((bf16[128,2048]{1,0:T(8,128)(2,1)}, bf16[128,2048]{1,0:T(8,128)(2,1)S(1)}, u32[]{:S(2)}, u32[]{:S(2)}) %collective-permute-start.1) | collective-permute-done | bytes 524320 | tf_op jit(solution)/shard_map/ppermute | solution.py:21
  137.7 2.0 collective-permute-start.3
  139.7 6.3 %collective-permute-start.4 = (bf16[64,2048]{1,0:T(8,128)(2,1)S(1)}, bf16[64,2048]{1,0:T(8,128)(2,1)S(1)}, u32[]{:S(2)}, u32[]{:S(2)}) collective-permute-start(bf16[64,2048]{1,0:T(8,128)(2,1)S(1)} %slice.116), channel_id=1, source_target_pairs={{0,6},{1,7},{2,0},{3,1},{4,2},{5,3},{6,4},{7,5},{8,14},{9,15},{10,... | collective-permute-start | bytes 786440 | tf_op jit(solution)/shard_map/ppermute | solution.py:21
  146.0 3.5 %collective-permute-done.3 = bf16[64,2048]{1,0:T(8,128)(2,1)S(1)} collective-permute-done((bf16[64,2048]{1,0:T(8,128)(2,1)S(1)}, bf16[64,2048]{1,0:T(8,128)(2,1)S(1)}, u32[]{:S(2)}, u32[]{:S(2)}) %collective-permute-start.3) | collective-permute-done | bytes 262176 | tf_op jit(solution)/shard_map/ppermute | solution.py:21
  149.6 0.9 collective-permute-done.4
  151.4 6.4 %collective-permute-start.7 = (bf16[512,256]{1,0:T(8,128)(2,1)S(1)}, bf16[512,256]{1,0:T(8,128)(2,1)S(1)}, u32[]{:S(2)}, u32[]{:S(2)}) collective-permute-start(bf16[512,256]{1,0:T(8,128)(2,1)S(1)} %constant_dynamic-slice_fusion.9), channel_id=1, source_target_pairs={{0,6},{1,7},{2,0},{3,1},{4,2},{5,3},{6,4},{7,5},{8,14},{9,15},{10,... | collective-permute-start | bytes 786440 | tf_op jit(solution)/shard_map/ppermute | solution.py:21
  157.8 2.0 collective-permute-start.6
  160.7 21.9 %all-to-all-start.1 = ((bf16[32,8,128]{2,1,0:T(8,128)(2,1)}), bf16[32,8,128]{2,1,0:T(8,128)(2,1)S(1)}, u32[]{:S(2)}, u32[]{:S(2)}) async-start(bf16[32,8,128]{2,1,0:T(8,128)(2,1)} %copy.162), calls=%async_computation.1 | async-start | bytes 131072 | tf_op jit(solution)/shard_map/all_to_all | solution.py:30
  182.6 1.1 constant_dynamic-slice_fusion.4
  183.8 5.9 %collective-permute-start.9 = (bf16[256,256]{1,0:T(8,128)(2,1)S(1)}, bf16[256,256]{1,0:T(8,128)(2,1)S(1)}, u32[]{:S(2)}, u32[]{:S(2)}) collective-permute-start(bf16[256,256]{1,0:T(8,128)(2,1)S(1)} %slice.122), channel_id=1, source_target_pairs={{0,6},{1,7},{2,0},{3,1},{4,2},{5,3},{6,4},{7,5},{8,14},{9,15},{10,... | collective-permute-start | bytes 393224 | tf_op jit(solution)/shard_map/ppermute | solution.py:21
  189.7 2.0 collective-permute-start.8
  192.3 2.7 collective-permute-done.9
  195.0 2.9 %collective-permute-done.8 = bf16[256,256]{1,0:T(8,128)(2,1)S(1)} collective-permute-done((bf16[256,256]{1,0:T(8,128)(2,1)S(1)}, bf16[256,256]{1,0:T(8,128)(2,1)S(1)}, u32[]{:S(2)}, u32[]{:S(2)}) %collective-permute-start.8) | collective-permute-done | bytes 131104 | tf_op jit(solution)/shard_map/ppermute | solution.py:21
  199.0 0.9 reshape.246
  199.9 16.5 %all-to-all-start.5 = ((bf16[32,16,512]{2,1,0:T(8,128)(2,1)}), bf16[32,16,512]{2,1,0:T(8,128)(2,1)S(1)}, u32[]{:S(2)}, u32[]{:S(2)}) async-start(bf16[32,16,512]{2,1,0:T(8,128)(2,1)} %reshape.246), calls=%async_computation.5 | async-start | bytes 1048576 | tf_op jit(solution)/shard_map/all_to_all | solution.py:30
  217.2 1.5 multiply_reduce_fusion
  219.2 1.1 convolution_convert_fusion.1
  220.4 29.3 %all-to-all-done.5 = bf16[32,16,512]{2,1,0:T(8,128)(2,1)S(1)} async-done(((bf16[32,16,512]{2,1,0:T(8,128)(2,1)}), bf16[32,16,512]{2,1,0:T(8,128)(2,1)S(1)}, u32[]{:S(2)}, u32[]{:S(2)}) %all-to-all-start.5) | async-done | bytes 524320 | tf_op jit(solution)/shard_map/all_to_all | solution.py:30
  249.7 3.8 %all-to-all-start.2 = ((bf16[8,16,2048]{2,1,0:T(8,128)(2,1)}), bf16[8,16,2048]{2,1,0:T(8,128)(2,1)S(1)}, u32[]{:S(2)}, u32[]{:S(2)}) async-start(bf16[8,16,2048]{2,1,0:T(8,128)(2,1)} %bitcast.15), calls=%async_computation.2 | async-start | bytes 1048576 | tf_op jit(solution)/shard_map/all_to_all | solution.py:30
  254.0 1.4 fusion.7
  256.1 14.0 %all-to-all-done.2 = bf16[8,16,2048]{2,1,0:T(8,128)(2,1)S(1)} async-done(((bf16[8,16,2048]{2,1,0:T(8,128)(2,1)}), bf16[8,16,2048]{2,1,0:T(8,128)(2,1)S(1)}, u32[]{:S(2)}, u32[]{:S(2)}) %all-to-all-start.2) | async-done | bytes 524320 | tf_op jit(solution)/shard_map/all_to_all | solution.py:30
  270.0 0.7 broadcast_in_dim.101
  270.8 3.6 %all-to-all-start.3 = ((bf16[8,128,128]{1,2,0:T(8,128)(2,1)}), bf16[8,128,128]{1,2,0:T(8,128)(2,1)S(1)}, u32[]{:S(2)}, u32[]{:S(2)}) async-start(bf16[8,128,128]{1,2,0:T(8,128)(2,1)} %broadcast_in_dim.101), calls=%async_computation.3 | async-start | bytes 524288 | tf_op jit(solution)/shard_map/all_to_all | solution.py:30
  275.4 3.1 %collective-permute-start.10 = (bf16[128,256]{1,0:T(8,128)(2,1)S(1)}, bf16[128,256]{1,0:T(8,128)(2,1)S(1)}, u32[]{:S(2)}, u32[]{:S(2)}) collective-permute-start(bf16[128,256]{1,0:T(8,128)(2,1)S(1)} %slice.167), channel_id=1, source_target_pairs={{0,1},{1,0},{2,3},{3,2},{4,5},{5,4},{6,7},{7,6},{8,9},{9,8},{10,11... | collective-permute-start | bytes 196616 | tf_op jit(solution)/shard_map/ppermute | solution.py:26
  278.5 0.7 reduce_sum.69
  279.2 4.7 %all-to-all-done.3 = bf16[8,128,128]{1,2,0:T(8,128)(2,1)S(1)} async-done(((bf16[8,128,128]{1,2,0:T(8,128)(2,1)}), bf16[8,128,128]{1,2,0:T(8,128)(2,1)S(1)}, u32[]{:S(2)}, u32[]{:S(2)}) %all-to-all-start.3) | async-done | bytes 262176 | tf_op jit(solution)/shard_map/all_to_all | solution.py:30
  284.0 0.9 add_convert_fusion
  (163 shorter events, 12.9 us)
Async XLA Ops:
  0.6 218.5 %copy-start = (bf16[256,2048]{1,0:T(8,128)(2,1)S(1)}, bf16[256,2048]{1,0:T(8,128)(2,1)}, u32[]{:S(2)}) copy-start(bf16[256,2048]{1,0:T(8,128)(2,1)} %param.27) | copy-start | bytes 3145732
  0.6 3.0 %copy-start.19 = (bf16[128,256]{1,0:T(8,128)(2,1)S(1)}, bf16[128,256]{1,0:T(8,128)(2,1)}, u32[]{:S(2)}) copy-start(bf16[128,256]{1,0:T(8,128)(2,1)} %param.22) | copy-start | bytes 196612
  4.7 47.9 %copy-start.23 = (s32[128,4]{0,1:T(4,128)S(1)}, s32[128,4]{0,1:T(4,128)}, u32[]{:S(2)}) copy-start(s32[128,4]{0,1:T(4,128)} %param.29) | copy-start | bytes 6148
  6.3 46.3 %copy-start.1 = (bf16[128,2048]{1,0:T(8,128)(2,1)S(1)}, bf16[128,2048]{1,0:T(8,128)(2,1)}, u32[]{:S(2)}) copy-start(bf16[128,2048]{1,0:T(8,128)(2,1)} %param.28) | copy-start | bytes 1572868
  6.3 46.8 %copy-start.21 = (f32[2048]{0:T(1024)S(1)}, f32[2048]{0:T(1024)}, u32[]{:S(2)}) copy-start(f32[2048]{0:T(1024)} %param.31) | copy-start | bytes 24580
  7.4 61.1 %all-to-all-start = ((bf16[32,8,256]{2,1,0:T(8,128)(2,1)}), bf16[32,8,256]{2,1,0:T(8,128)(2,1)S(1)}, u32[]{:S(2)}, u32[]{:S(2)}) async-start(bf16[32,8,256]{2,1,0:T(8,128)(2,1)} %fusion.63), calls=%async_computation | async-start | bytes 262144 | tf_op jit(solution)/shard_map/all_to_all | solution.py:30
  54.5 19.2 %copy-start.5 = (bf16[1,2048,128]{2,1,0:T(8,128)(2,1)S(1)}, bf16[1,2048,128]{2,1,0:T(8,128)(2,1)}, u32[]{:S(2)}) copy-start(bf16[1,2048,128]{2,1,0:T(8,128)(2,1)} %param.33) | copy-start | bytes 1572868
  68.4 5.3 %copy-start.4 = (bf16[32,8,256]{2,1,0:T(8,128)(2,1)}, bf16[32,8,256]{2,1,0:T(8,128)(2,1)S(1)}, u32[]{:S(2)}) copy-start(bf16[32,8,256]{2,1,0:T(8,128)(2,1)S(1)} %all-to-all-done) | copy-start | bytes 393220
  68.4 38.7 %all-to-all-start.4 = ((bf16[32,4,2048]{2,1,0:T(4,128)(2,1)}), bf16[32,4,2048]{2,1,0:T(4,128)(2,1)S(1)}, u32[]{:S(2)}, u32[]{:S(2)}) async-start(bf16[32,4,2048]{2,1,0:T(4,128)(2,1)} %reshape.243), calls=%async_computation.4 | async-start | bytes 1048576 | tf_op jit(solution)/shard_map/all_to_all | solution.py:30
  75.8 8.1 %slice-start = ((bf16[32,8,256]{2,1,0:T(8,128)(2,1)}), bf16[32,8,3]{2,1,0:T(8,128)(2,1)S(1)}, s32[]{:S(2)}) async-start(bf16[32,8,256]{2,1,0:T(8,128)(2,1)} %copy-done.4), calls=%async_computation.6 | async-start | bytes 131072 | tf_op jit(solution)/shard_map/slice | solution.py:74
  75.8 42.0 %collective-permute-start = (bf16[2048,256]{1,0:T(8,128)(2,1)}, bf16[2048,256]{1,0:T(8,128)(2,1)S(1)}, u32[]{:S(2)}, u32[]{:S(2)}) collective-permute-start(bf16[2048,256]{1,0:T(8,128)(2,1)} %pad_maximum_fusion), channel_id=1, source_target_pairs={{0,1},{1,0},{2,3},{3,2},{4,5},{5,4},{6,7},{7,6},{8,9},{9,8},{10,11... | collective-permute-start | bytes 3145736 | tf_op jit(solution)/shard_map/ppermute | solution.py:26
  79.1 103.5 %collective-permute-start.5 = (bf16[1024,256]{1,0:T(8,128)(2,1)}, bf16[1024,256]{1,0:T(8,128)(2,1)}, u32[]{:S(2)}, u32[]{:S(2)}) collective-permute-start(bf16[1024,256]{1,0:T(8,128)(2,1)} %bitcast.23), channel_id=1, source_target_pairs={{0,1},{1,0},{2,3},{3,2},{4,5},{5,4},{6,7},{7,6},{8,9},{9,8},{10,11... | collective-permute-start | bytes 1572872 | tf_op jit(solution)/shard_map/ppermute | solution.py:26
  108.0 9.8 %copy-start.2 = (bf16[128,2048]{1,0:T(8,128)(2,1)S(1)}, bf16[128,2048]{1,0:T(8,128)(2,1)}, u32[]{:S(2)}) copy-start(bf16[128,2048]{1,0:T(8,128)(2,1)} %reshape.244) | copy-start | bytes 1572868
  108.0 28.6 %collective-permute-start.1 = (bf16[128,2048]{1,0:T(8,128)(2,1)}, bf16[128,2048]{1,0:T(8,128)(2,1)S(1)}, u32[]{:S(2)}, u32[]{:S(2)}) collective-permute-start(bf16[128,2048]{1,0:T(8,128)(2,1)} %reshape.244), channel_id=1, source_target_pairs={{0,6},{1,7},{2,0},{3,1},{4,2},{5,3},{6,4},{7,5},{8,14},{9,15},{10,... | collective-permute-start | bytes 1572872 | tf_op jit(solution)/shard_map/ppermute | solution.py:21
  114.2 22.4 %collective-permute-start.2 = (bf16[128,2048]{1,0:T(8,128)(2,1)}, bf16[128,2048]{1,0:T(8,128)(2,1)S(1)}, u32[]{:S(2)}, u32[]{:S(2)}) collective-permute-start(bf16[128,2048]{1,0:T(8,128)(2,1)} %reshape.244), channel_id=1, source_target_pairs={{0,2},{1,3},{2,4},{3,5},{4,6},{5,7},{6,0},{7,1},{8,10},{9,11},{10,... | collective-permute-start | bytes 1572872 | tf_op jit(solution)/shard_map/ppermute | solution.py:21
  118.3 18.4 %copy-start.6 = (bf16[1,2048,128]{2,1,0:T(8,128)(2,1)S(1)}, bf16[1,2048,128]{2,1,0:T(8,128)(2,1)}, u32[]{:S(2)}) copy-start(bf16[1,2048,128]{2,1,0:T(8,128)(2,1)} %param.33) | copy-start | bytes 1572868
  118.3 18.4 %copy-start.7 = (bf16[1,2048,128]{2,1,0:T(8,128)(2,1)S(1)}, bf16[1,2048,128]{2,1,0:T(8,128)(2,1)}, u32[]{:S(2)}) copy-start(bf16[1,2048,128]{2,1,0:T(8,128)(2,1)} %param.32) | copy-start | bytes 1572868
  137.7 11.9 %collective-permute-start.3 = (bf16[64,2048]{1,0:T(8,128)(2,1)S(1)}, bf16[64,2048]{1,0:T(8,128)(2,1)S(1)}, u32[]{:S(2)}, u32[]{:S(2)}) collective-permute-start(bf16[64,2048]{1,0:T(8,128)(2,1)S(1)} %slice.115), channel_id=1, source_target_pairs={{0,2},{1,3},{2,4},{3,5},{4,6},{5,7},{6,0},{7,1},{8,10},{9,11},{10,... | collective-permute-start | bytes 786440 | tf_op jit(solution)/shard_map/ppermute | solution.py:21
  139.7 10.8 %collective-permute-start.4 = (bf16[64,2048]{1,0:T(8,128)(2,1)S(1)}, bf16[64,2048]{1,0:T(8,128)(2,1)S(1)}, u32[]{:S(2)}, u32[]{:S(2)}) collective-permute-start(bf16[64,2048]{1,0:T(8,128)(2,1)S(1)} %slice.116), channel_id=1, source_target_pairs={{0,6},{1,7},{2,0},{3,1},{4,2},{5,3},{6,4},{7,5},{8,14},{9,15},{10,... | collective-permute-start | bytes 786440 | tf_op jit(solution)/shard_map/ppermute | solution.py:21
  151.2 8.6 %slice-start.1 = ((bf16[32,8,256]{2,1,0:T(8,128)(2,1)}), bf16[32,8,128]{2,1,0:T(8,128)(2,1)S(1)}, s32[]{:S(2)}) async-start(bf16[32,8,256]{2,1,0:T(8,128)(2,1)} %copy-done.4), calls=%async_computation.7 | async-start | bytes 131072 | tf_op jit(solution)/shard_map/slice | solution.py:73
  151.2 8.6 %copy-start.16 = (f32[32,32,8]{1,2,0:T(8,128)S(1)}, f32[32,32,8]{1,2,0:T(8,128)}, u32[]{:S(2)}) copy-start(f32[32,32,8]{1,2,0:T(8,128)} %fusion.5) | copy-start | bytes 98308
  151.4 40.3 %copy-start.14 = (bf16[128,256]{1,0:T(8,128)(2,1)S(1)}, bf16[128,256]{1,0:T(8,128)(2,1)}, u32[]{:S(2)}) copy-start(bf16[128,256]{1,0:T(8,128)(2,1)} %get-tuple-element.92) | copy-start | bytes 196612
  151.4 40.3 %copy-start.15 = (bf16[128,256]{1,0:T(8,128)(2,1)S(1)}, bf16[128,256]{1,0:T(8,128)(2,1)}, u32[]{:S(2)}) copy-start(bf16[128,256]{1,0:T(8,128)(2,1)} %get-tuple-element.93) | copy-start | bytes 196612
  151.4 32.3 %collective-permute-start.7 = (bf16[512,256]{1,0:T(8,128)(2,1)S(1)}, bf16[512,256]{1,0:T(8,128)(2,1)S(1)}, u32[]{:S(2)}, u32[]{:S(2)}) collective-permute-start(bf16[512,256]{1,0:T(8,128)(2,1)S(1)} %constant_dynamic-slice_fusion.9), channel_id=1, source_target_pairs={{0,6},{1,7},{2,0},{3,1},{4,2},{5,3},{6,4},{7,5},{8,14},{9,15},{10,... | collective-permute-start | bytes 786440 | tf_op jit(solution)/shard_map/ppermute | solution.py:21
  157.8 31.9 %collective-permute-start.6 = (bf16[512,256]{1,0:T(8,128)(2,1)S(1)}, bf16[512,256]{1,0:T(8,128)(2,1)S(1)}, u32[]{:S(2)}, u32[]{:S(2)}) collective-permute-start(bf16[512,256]{1,0:T(8,128)(2,1)S(1)} %constant_dynamic-slice_fusion.9), channel_id=1, source_target_pairs={{0,2},{1,3},{2,4},{3,5},{4,6},{5,7},{6,0},{7,1},{8,10},{9,11},{10,... | collective-permute-start | bytes 786440 | tf_op jit(solution)/shard_map/ppermute | solution.py:21
  160.7 39.2 %all-to-all-start.1 = ((bf16[32,8,128]{2,1,0:T(8,128)(2,1)}), bf16[32,8,128]{2,1,0:T(8,128)(2,1)S(1)}, u32[]{:S(2)}, u32[]{:S(2)}) async-start(bf16[32,8,128]{2,1,0:T(8,128)(2,1)} %copy.162), calls=%async_computation.1 | async-start | bytes 131072 | tf_op jit(solution)/shard_map/all_to_all | solution.py:30
  183.7 8.3 %copy-start.12 = (bf16[128,256]{1,0:T(8,128)(2,1)S(1)}, bf16[128,256]{1,0:T(8,128)(2,1)}, u32[]{:S(2)}) copy-start(bf16[128,256]{1,0:T(8,128)(2,1)} %get-tuple-element.94) | copy-start | bytes 196612
  183.7 8.3 %copy-start.13 = (bf16[128,256]{1,0:T(8,128)(2,1)S(1)}, bf16[128,256]{1,0:T(8,128)(2,1)}, u32[]{:S(2)}) copy-start(bf16[128,256]{1,0:T(8,128)(2,1)} %get-tuple-element.95) | copy-start | bytes 196612
  183.8 11.3 %collective-permute-start.9 = (bf16[256,256]{1,0:T(8,128)(2,1)S(1)}, bf16[256,256]{1,0:T(8,128)(2,1)S(1)}, u32[]{:S(2)}, u32[]{:S(2)}) collective-permute-start(bf16[256,256]{1,0:T(8,128)(2,1)S(1)} %slice.122), channel_id=1, source_target_pairs={{0,6},{1,7},{2,0},{3,1},{4,2},{5,3},{6,4},{7,5},{8,14},{9,15},{10,... | collective-permute-start | bytes 393224 | tf_op jit(solution)/shard_map/ppermute | solution.py:21
  189.7 8.2 %collective-permute-start.8 = (bf16[256,256]{1,0:T(8,128)(2,1)S(1)}, bf16[256,256]{1,0:T(8,128)(2,1)S(1)}, u32[]{:S(2)}, u32[]{:S(2)}) collective-permute-start(bf16[256,256]{1,0:T(8,128)(2,1)S(1)} %slice.121), channel_id=1, source_target_pairs={{0,2},{1,3},{2,4},{3,5},{4,6},{5,7},{6,0},{7,1},{8,10},{9,11},{10,... | collective-permute-start | bytes 393224 | tf_op jit(solution)/shard_map/ppermute | solution.py:21
  192.0 5.9 %copy-start.10 = (bf16[128,256]{1,0:T(8,128)(2,1)S(1)}, bf16[128,256]{1,0:T(8,128)(2,1)}, u32[]{:S(2)}) copy-start(bf16[128,256]{1,0:T(8,128)(2,1)} %get-tuple-element.96) | copy-start | bytes 196612
  192.0 5.9 %copy-start.11 = (bf16[128,256]{1,0:T(8,128)(2,1)S(1)}, bf16[128,256]{1,0:T(8,128)(2,1)}, u32[]{:S(2)}) copy-start(bf16[128,256]{1,0:T(8,128)(2,1)} %get-tuple-element.97) | copy-start | bytes 196612
  192.3 5.9 %copy-start.8 = (bf16[128,256]{1,0:T(8,128)(2,1)S(1)}, bf16[128,256]{1,0:T(8,128)(2,1)}, u32[]{:S(2)}) copy-start(bf16[128,256]{1,0:T(8,128)(2,1)} %get-tuple-element.90) | copy-start | bytes 196612
  192.3 5.9 %copy-start.9 = (bf16[128,256]{1,0:T(8,128)(2,1)S(1)}, bf16[128,256]{1,0:T(8,128)(2,1)}, u32[]{:S(2)}) copy-start(bf16[128,256]{1,0:T(8,128)(2,1)} %get-tuple-element.91) | copy-start | bytes 196612
  199.0 17.5 %copy-start.17 = (bf16[128,256]{1,0:T(8,128)(2,1)S(1)}, bf16[128,256]{1,0:T(8,128)(2,1)}, u32[]{:S(2)}) copy-start(bf16[128,256]{1,0:T(8,128)(2,1)} %param.20) | copy-start | bytes 196612
  199.0 17.6 %copy-start.26 = (f32[2,2,128]{2,0,1:T(2,128)S(1)}, f32[2,2,128]{2,0,1:T(2,128)}, u32[]{:S(2)}) copy-start(f32[2,2,128]{2,0,1:T(2,128)} %get-tuple-element.114) | copy-start | bytes 6148
  199.0 17.6 %copy-start.20 = (f32[2,2,1,128]{3,2,1,0:T(1,128)S(1)}, f32[2,2,1,128]{3,2,1,0:T(1,128)}, u32[]{:S(2)}) copy-start(f32[2,2,1,128]{3,2,1,0:T(1,128)} %get-tuple-element.108) | copy-start | bytes 6148
  199.9 49.8 %all-to-all-start.5 = ((bf16[32,16,512]{2,1,0:T(8,128)(2,1)}), bf16[32,16,512]{2,1,0:T(8,128)(2,1)S(1)}, u32[]{:S(2)}, u32[]{:S(2)}) async-start(bf16[32,16,512]{2,1,0:T(8,128)(2,1)} %reshape.246), calls=%async_computation.5 | async-start | bytes 1048576 | tf_op jit(solution)/shard_map/all_to_all | solution.py:30
  217.0 2.2 copy-start.18
  217.0 2.2 copy-start.27
  219.2 34.4 %copy-start.22 = (f32[2048]{0:T(1024)S(1)}, f32[2048]{0:T(1024)}, u32[]{:S(2)}) copy-start(f32[2048]{0:T(1024)} %param.31) | copy-start | bytes 24580
  219.2 34.4 %copy-start.29 = (f32[128]{0:T(128)S(1)}, f32[128]{0:T(128)}, u32[]{:S(2)}) copy-start(f32[128]{0:T(128)} %copy-done.28) | copy-start | bytes 1540
  219.2 34.4 %copy-start.30 = (bf16[2048,128]{1,0:T(8,128)(2,1)S(1)}, bf16[2048,128]{1,0:T(8,128)(2,1)}, u32[]{:S(2)}) copy-start(bf16[2048,128]{1,0:T(8,128)(2,1)} %param.35) | copy-start | bytes 1572868
  249.7 4.2 %copy-start.25 = (f32[128,4]{0,1:T(4,128)S(1)}, f32[128,4]{0,1:T(4,128)}, u32[]{:S(2)}) copy-start(f32[128,4]{0,1:T(4,128)} %param.30) | copy-start | bytes 6148
  249.7 20.3 %all-to-all-start.2 = ((bf16[8,16,2048]{2,1,0:T(8,128)(2,1)}), bf16[8,16,2048]{2,1,0:T(8,128)(2,1)S(1)}, u32[]{:S(2)}, u32[]{:S(2)}) async-start(bf16[8,16,2048]{2,1,0:T(8,128)(2,1)} %bitcast.15), calls=%async_computation.2 | async-start | bytes 1048576 | tf_op jit(solution)/shard_map/all_to_all | solution.py:30
  270.8 13.2 %all-to-all-start.3 = ((bf16[8,128,128]{1,2,0:T(8,128)(2,1)}), bf16[8,128,128]{1,2,0:T(8,128)(2,1)S(1)}, u32[]{:S(2)}, u32[]{:S(2)}) async-start(bf16[8,128,128]{1,2,0:T(8,128)(2,1)} %broadcast_in_dim.101), calls=%async_computation.3 | async-start | bytes 524288 | tf_op jit(solution)/shard_map/all_to_all | solution.py:30
  274.9 9.1 %copy-start.3 = (bf16[1024,256]{1,0:T(8,128)(2,1)S(1)}, bf16[1024,256]{1,0:T(8,128)(2,1)}, u32[]{:S(2)}) copy-start(bf16[1024,256]{1,0:T(8,128)(2,1)} %param.37) | copy-start | bytes 1572868
  275.4 8.5 %collective-permute-start.10 = (bf16[128,256]{1,0:T(8,128)(2,1)S(1)}, bf16[128,256]{1,0:T(8,128)(2,1)S(1)}, u32[]{:S(2)}, u32[]{:S(2)}) collective-permute-start(bf16[128,256]{1,0:T(8,128)(2,1)S(1)} %slice.167), channel_id=1, source_target_pairs={{0,1},{1,0},{2,3},{3,2},{4,5},{5,4},{6,7},{7,6},{8,9},{9,8},{10,11... | collective-permute-start | bytes 196616 | tf_op jit(solution)/shard_map/ppermute | solution.py:26
  (2 other events, 3.3 us)

commit v2 on v1

--- a/solution.py
+++ b/solution.py
@@ -4,6 +4,7 @@
 from jax.sharding import Mesh
 from jax.sharding import PartitionSpec as P
 
+
 HEAD_CHANNELS = 128
 BLK = 64
 EP = ("ep_0", "ep_1")
@@ -21,34 +22,49 @@
     return lax.ppermute(array, axis, [(i, (i + step) % count) for i in range(count)])
 
 
-def swapped(array, axis):
+def swapped(array, axis, bit):
     count = lax.axis_size(axis)
-    return lax.ppermute(array, axis, [(i, i ^ 1) for i in range(count)])
+    return lax.ppermute(array, axis, [(i, i ^ bit) for i in range(count)])
 
 
 def exchanged(array, axis):
     return lax.all_to_all(array, axis, split_axis=0, concat_axis=0, tiled=True)
 
 
-def in_blocks(array, dim, count):
-    before, after = (array.shape[:dim], array.shape[dim + 1 :])
-    return jnp.moveaxis(array.reshape(*before, count, -1, *after), dim, 0)
-
-
-def sent_and_summed(array, axis, dim):
-    pieces = in_blocks(array, dim, lax.axis_size(axis))
-    return exchanged(pieces, axis).astype(jnp.float32).sum(axis=0)
-
-
-def joined_along(pieces, dim):
-    shape = list(pieces.shape[1:])
-    shape[dim] *= pieces.shape[0]
-    return jnp.moveaxis(pieces, 0, dim).reshape(shape)
-
-
-def copy_for_each(array, axis):
+def half_of(array, dim, place):
+    return lax.dynamic_index_in_dim(array, place, dim, keepdims=False)
+
+
+def summed_to_owners(array, axis):
     count = lax.axis_size(axis)
-    return exchanged(jnp.broadcast_to(array[None], (count, *array.shape)), axis)
+    bits = count.bit_length() - 1
+    member = lax.axis_index(axis)
+    kept = array.reshape(*[2] * bits, -1, array.shape[1])
+    for bit in range(bits):
+        mine = (member >> bit) & 1
+        dim = bits - 1 - bit
+        arrived = swapped(half_of(kept, dim, 1 - mine).astype(jnp.bfloat16), axis, 1 << bit)
+        kept = half_of(kept, dim, mine) + arrived.astype(jnp.float32)
+    return kept
+
+
+def gathered_columns(array, axis):
+    count = lax.axis_size(axis)
+    member = lax.axis_index(axis)
+    for bit in reversed(range(count.bit_length() - 1)):
+        arrived = swapped(array, axis, 1 << bit)
+        first = ((member >> bit) & 1) == 0
+        array = jnp.concatenate(
+            [jnp.where(first, array, arrived), jnp.where(first, arrived, array)], axis=1
+        )
+    return array
+
+
+def rows_by_reversed_bits(matrix, count):
+    bits = count.bit_length() - 1
+    split = matrix.reshape(*[2] * bits, -1, matrix.shape[1])
+    order = (*reversed(range(bits)), bits, bits + 1)
+    return split.transpose(order).reshape(matrix.shape)
 
 
 def in_parts(array, count):
@@ -69,7 +85,8 @@
     packed = jnp.concatenate(
         [state.astype(jnp.bfloat16).reshape(devices, part, width), logs], axis=2
     )
-    arrived = exchanged(packed, EP).astype(jnp.float32)
+    arrived = exchanged(packed, EP)
+    arrived = arrived.astype(jnp.float32)
     updates = arrived[:, :, :width]
     logs = jnp.sum(arrived[:, :, width : width + 3], axis=2)
     at = jnp.arange(devices)
@@ -155,14 +172,8 @@
         None, :
     ]
     gated_rows = (normed * jax.nn.silu(output_gate_input.astype(jnp.float32))).astype(jnp.bfloat16)
-    mixed = sent_and_summed(
-        jnp.dot(gated_rows, recurrence_out_weight, preferred_element_type=jnp.float32).astype(
-            jnp.bfloat16
-        ),
-        "tp",
-        0,
-    )
-    return mixed.astype(jnp.bfloat16)
+    partial = jnp.dot(gated_rows, recurrence_out_weight, preferred_element_type=jnp.float32)
+    return summed_to_owners(partial, "tp").astype(jnp.bfloat16)
 
 
 def expert_half(
@@ -183,19 +194,18 @@
     experts = local_experts * devices
     capacity = min(tokens, 2 * tokens * top // experts)
     width_out = routed_down_weight.shape[2]
-    width_members = lax.axis_size("tp")
-    quads = width_members // 2
+    members = lax.axis_size("tp")
+    quads = members // 2
     member = lax.axis_index("tp")
-    parity, quad = (member % 2, member // 2)
-    share = capacity // width_members
+    parity, quad = (member & 1, member >> 1)
     half = capacity // 2
-    width_in = routed_gate_weight.shape[1]
+    width_in = routed_gate_weight.shape[1] // quads
     units = routed_gate_weight.shape[2]
 
     own_in = jnp.concatenate([routed_gate_weight[0], routed_up_weight[0]], axis=1)
-    partner_in = swapped(own_in, "tp")
     own_down = routed_down_weight[0]
-    partner_down = swapped(own_down, "tp")
+    partner_in = swapped(own_in, "tp", 1)
+    partner_down = swapped(own_down, "tp", 1)
 
     features = expert_hidden_state.astype(jnp.float32)
     normed = (
@@ -214,80 +224,70 @@
         preferred_element_type=jnp.float32,
     )
     places = jnp.where(chosen, places.astype(jnp.int32), -1)
-    first = parity * half + quad * share
-    picks = places.T[:, None, :] == first + jnp.arange(share)[None, :, None]
-    outgoing = jnp.dot(
-        picks.reshape(experts * share, tokens).astype(jnp.bfloat16),
-        normed,
+    filled = places[:, :, None] == parity * half + jnp.arange(half)[None, None, :]
+    filled = filled.reshape(tokens, experts * half)
+    outgoing = lax.dot_general(
+        filled.astype(jnp.bfloat16),
+        lax.dynamic_slice_in_dim(normed, quad * width_in, width_in, 1),
+        (((0,), (0,)), ((), ())),
         preferred_element_type=jnp.float32,
     ).astype(jnp.bfloat16)
-    arrived = exchanged(outgoing.reshape(devices, share, width_in), EP)
-    chunk = arrived.reshape(devices * share, width_in)
-    rows = chunk.shape[0]
+    arrived = exchanged(outgoing.reshape(devices, half, width_in), EP)
+    chunk = arrived.reshape(devices * half, width_in)
+    middle = chunk.shape[0] // 2
 
     shared_hidden = (
         jax.nn.silu(jnp.dot(normed, shared_gate_weight, preferred_element_type=jnp.float32))
         * jnp.dot(normed, shared_up_weight, preferred_element_type=jnp.float32)
     ).astype(jnp.bfloat16)
-    shared_piece = joined_along(copy_for_each(shared_hidden, "tp"), 1)
-    shared = jnp.dot(shared_piece, shared_down_weight, preferred_element_type=jnp.float32)
-
-    def hidden_of(piece):
-        sides = []
-        for matrix in (own_in, partner_in):
-            both = jnp.dot(piece, matrix, preferred_element_type=jnp.float32)
-            sides.append((jax.nn.silu(both[:, :units]) * both[:, units:]).astype(jnp.bfloat16))
-        return jnp.concatenate(sides, axis=1)
-
-    from_before = shifted(chunk, "tp", 2)
-    from_after = shifted(chunk, "tp", -2)
-    across_first = shifted(from_before[: rows // 2], "tp", 2)
-    across_second = shifted(from_after[rows // 2 :], "tp", -2)
-    hidden_own = hidden_of(chunk)
-    hidden_sides = hidden_of(jnp.concatenate([from_after, from_before], axis=0))
-    hidden_across = hidden_of(jnp.concatenate([across_first, across_second], axis=0))
-    around = [hidden_own, hidden_sides[:rows], hidden_across, hidden_sides[rows:]]
-    hidden = lax.dynamic_slice_in_dim(
-        jnp.concatenate(around + around, axis=0), (quads - quad) % quads * rows, quads * rows, 0
-    )
-
-    middle = quads * rows // 2
-    hidden_before = shifted(hidden, "tp", 2)
-    hidden_after = shifted(hidden, "tp", -2)
-    hidden_far = jnp.concatenate(
-        [shifted(hidden_before[:middle], "tp", 2), shifted(hidden_after[middle:], "tp", -2)], axis=0
-    )
-
-    def down_of(step):
-        at = (quad + step) % quads * 2
-        blocks = []
-        for side in (parity, 1 - parity):
-            place = (at + side) * units
-            blocks.append(
-                jnp.concatenate(
-                    [
-                        lax.dynamic_slice_in_dim(matrix, place, units, 0)
-                        for matrix in (own_down, partner_down)
-                    ],
-                    axis=1,
-                )
+    shared_piece = gathered_columns(shared_hidden, "tp")
+    shared = jnp.dot(
+        shared_piece,
+        rows_by_reversed_bits(shared_down_weight, members),
+        preferred_element_type=jnp.float32,
+    )
+
+    def all_around(piece):
+        before = shifted(piece, "tp", 2)
+        after = shifted(piece, "tp", -2)
+        far = [shifted(before[:middle], "tp", 2), shifted(after[middle:], "tp", -2)]
+        return ((piece, 0), (before, -1), (after, 1), (jnp.concatenate(far, axis=0), 2))
+
+    def product(pieces, matrix):
+        total = None
+        for piece, step in pieces:
+            depth = piece.shape[1]
+            block = lax.dynamic_slice_in_dim(
+                matrix, ((quad + step) & (quads - 1)) * depth, depth, 0
             )
-        return jnp.concatenate(blocks, axis=0)
-
-    def product(piece, step):
-        return jnp.dot(piece, down_of(step), preferred_element_type=jnp.float32)
-
-    routed = product(hidden, 0) + product(hidden_before, -1) + product(hidden_after, 1)
-    routed = routed + product(hidden_far, 2)
-    answers = routed.astype(jnp.bfloat16).reshape(quads, devices, share, 2 * width_out)
-    answers = answers.transpose(1, 0, 2, 3).reshape(devices, half, 2 * width_out)
-    returned = exchanged(answers, EP).reshape(experts * half, 2 * width_out)
-    filled = places[:, :, None] == parity * half + jnp.arange(half)[None, None, :]
-    mixing = jnp.where(filled, gate_of[:, :, None], 0.0).reshape(tokens, experts * half)
+            part = jnp.dot(piece, block, preferred_element_type=jnp.float32)
+            total = part if total is None else total + part
+        return total
+
+    row_pieces = all_around(chunk)
+    sides = []
+    for matrix in (own_in, partner_in):
+        both = product(row_pieces, matrix)
+        sides.append((jax.nn.silu(both[:, :units]) * both[:, units:]).astype(jnp.bfloat16))
+    own, other = sides
+    even = parity == 0
+    hidden = jnp.concatenate([jnp.where(even, own, other), jnp.where(even, other, own)], axis=1)
+    hidden_pieces = all_around(hidden)
+    answers = jnp.concatenate(
+        [
+            product(hidden_pieces, matrix).astype(jnp.bfloat16)
+            for matrix in (own_down, partner_down)
+        ],
+        axis=1,
+    )
+    returned = exchanged(answers.reshape(devices, half, 2 * width_out), EP)
+    returned = returned.reshape(experts * half, 2 * width_out)
+    mixing = jnp.where(filled.reshape(tokens, experts, half), gate_of[:, :, None], 0.0)
+    mixing = mixing.reshape(tokens, experts * half)
     combined = sum(
         jnp.dot(part, returned, preferred_element_type=jnp.float32) for part in in_parts(mixing, 3)
     )
-    other = swapped(combined[:, width_out:].astype(jnp.bfloat16), "tp")
+    other = swapped(combined[:, width_out:].astype(jnp.bfloat16), "tp", 1)
     combined = shared + combined[:, :width_out] + other.astype(jnp.float32)
     return combined.astype(jnp.bfloat16)
 
@@ -363,6 +363,7 @@
         P(None, "tp"),
     )
     out_specs = (P(GRP_EP_TP, None), P(GRP_EP, "tp"))
+
     return jax.shard_map(
         per_device, mesh=split, in_specs=in_specs, out_specs=out_specs, check_vma=False
     )

time: 289 us -> 271 us (0.938)
  waiting for transfers between devices: 109 us -> 92 us
  matrix products: 15.7 us -> 25.9 us
  starting transfers between devices: 137 us -> 132 us
    all_to_all x6 -> x4, starting transfers between devices: 96.3 us -> 65.9 us  [exchanged(): return lax.all_to_all(array, axis, split_axis=0, concat_axis=0, tiled=True)]
    all_to_all x6 -> x4, waiting for transfers between devices: 81.2 us -> 53.8 us  [exchanged(): return lax.all_to_all(array, axis, split_axis=0, concat_axis=0, tiled=True)]
    ppermute x3 -> x9, starting transfers between devices: 8.57 us -> 35.5 us  [swapped(): return lax.ppermute(array, axis, [(i, i ^ bit) for i in range(count)])]
    dot_general x12 -> x18, matrix products: 5.97 us -> 19.3 us  [the longest x16 17.3 us: product(): part = jnp.dot(piece, block, preferred_element_type=jnp.float32)]
    ppermute x3 -> x9, waiting for transfers between devices: 0.01 us -> 8.86 us  [swapped(): return lax.ppermute(array, axis, [(i, i ^ bit) for i in range(count)])]
    dynamic_slice x3 -> x0, local copies, waits for them, and re-layouts: 2.97 us -> none  [the longest x2 2.95 us: down_of(): lax.dynamic_slice_in_dim(matrix, place, units, 0)]
    reshape x4 -> x0, local copies, waits for them, and re-layouts: 2.94 us -> none  [the longest x1 0.99 us: expert_half(): arrived = exchanged(outgoing.reshape(devices, share, width_in), EP)]
  transfers between devices with their start and end apart: 17 -> 21, of which waited for: 10 -> 11; matrix products, arithmetic and copies ran while one was open for 10% -> 14% of each run, Pallas kernels for 0% -> 0%
where the time goes in v2:
time: 271 us; the launch traced here: 269 us
  starting transfers between devices  132 us (49%)
  waiting for transfers between devices  92 us (34%)
  matrix products  25.9 us (10%)
  other arithmetic  8.92 us (3%)
  local copies, waits for them, and re-layouts  8.37 us (3%)
    all_to_all x4, starting transfers between devices, exchanged(): return lax.all_to_all(array, axis, split_axis=0, concat_axis=0, tiled=True)  65.9 us
    all_to_all x4, waiting for transfers between devices, exchanged(): return lax.all_to_all(array, axis, split_axis=0, concat_axis=0, tiled=True)  53.8 us
    ppermute x9, starting transfers between devices, swapped(): return lax.ppermute(array, axis, [(i, i ^ bit) for i in range(count)])  35.5 us
    ppermute x8, starting transfers between devices, shifted(): lax.ppermute(array, axis, [(i, (i + step) % count) for i in range(count)])  30.7 us
    ppermute x8, waiting for transfers between devices, shifted(): lax.ppermute(array, axis, [(i, (i + step) % count) for i in range(count)])  29.3 us
    dot_general x16, matrix products, product(): part = jnp.dot(piece, block, preferred_element_type=jnp.float32)  17.3 us
    ppermute x9, waiting for transfers between devices, swapped(): return lax.ppermute(array, axis, [(i, i ^ bit) for i in range(count)])  8.86 us
  transfers between devices with their start and end apart: 21, of which 11 were waited for; matrix products, arithmetic and copies ran while one was open for 14% of the time, Pallas kernels for 0%

profile of v2, /device:TPU:65, one launch (start us, length us, event | category | flops | bytes accessed | tf_op | source)
XLA Modules:
  0.0 269.0 jit_solution(2818172002940989756)
XLA Ops:
  0.7 2.4 pad_maximum_fusion
  3.0 4.2 %collective-permute-start.10 = (bf16[2048,256]{1,0:T(8,128)(2,1)}, bf16[2048,256]{1,0:T(8,128)(2,1)}, u32[]{:S(2)}, u32[]{:S(2)}) collective-permute-start(bf16[2048,256]{1,0:T(8,128)(2,1)} %pad_maximum_fusion), channel_id=1, source_target_pairs={{0,1},{1,0},{2,3},{3,2},{4,5},{5,4},{6,7},{7,6},{8,9},{9,8},{10,11... | collective-permute-start | bytes 3145736 | tf_op jit(solution)/shard_map/ppermute | solution.py:27
  7.3 2.0 collective-permute-start.15
  10.5 1.6 while.13
  13.2 45.0 %all-to-all-start = ((bf16[32,8,256]{2,1,0:T(8,128)(2,1)}), bf16[32,8,256]{2,1,0:T(8,128)(2,1)S(1)}, u32[]{:S(2)}, u32[]{:S(2)}) async-start(bf16[32,8,256]{2,1,0:T(8,128)(2,1)} %fusion.58), calls=%async_computation | async-start | bytes 262144 | tf_op jit(solution)/shard_map/all_to_all | solution.py:31
  59.3 14.9 %all-to-all-done = bf16[32,8,256]{2,1,0:T(8,128)(2,1)S(1)} async-done(((bf16[32,8,256]{2,1,0:T(8,128)(2,1)}), bf16[32,8,256]{2,1,0:T(8,128)(2,1)S(1)}, u32[]{:S(2)}, u32[]{:S(2)}) %all-to-all-start) | async-done | bytes 131104 | tf_op jit(solution)/shard_map/all_to_all | solution.py:31
  76.3 5.2 %all-to-all-start.1 = ((bf16[32,8,128]{2,1,0:T(8,128)(2,1)}), bf16[32,8,128]{2,1,0:T(8,128)(2,1)S(1)}, u32[]{:S(2)}, u32[]{:S(2)}) async-start(bf16[32,8,128]{2,1,0:T(8,128)(2,1)} %copy.191), calls=%async_computation.1 | async-start | bytes 131072 | tf_op jit(solution)/shard_map/all_to_all | solution.py:31
  83.5 11.4 %all-to-all-done.1 = bf16[32,8,128]{2,1,0:T(8,128)(2,1)S(1)} async-done(((bf16[32,8,128]{2,1,0:T(8,128)(2,1)}), bf16[32,8,128]{2,1,0:T(8,128)(2,1)S(1)}, u32[]{:S(2)}, u32[]{:S(2)}) %all-to-all-start.1) | async-done | bytes 65568 | tf_op jit(solution)/shard_map/all_to_all | solution.py:31
  95.0 5.0 %all-to-all-start.2 = ((bf16[32,16,512]{2,1,0:T(8,128)(2,1)}), bf16[32,16,512]{2,1,0:T(8,128)(2,1)S(1)}, u32[]{:S(2)}, u32[]{:S(2)}) async-start(bf16[32,16,512]{2,1,0:T(8,128)(2,1)} %bitcast.26), calls=%async_computation.2 | async-start | bytes 1048576 | tf_op jit(solution)/shard_map/all_to_all | solution.py:31
  101.4 7.6 %collective-permute-start.3 = (bf16[128,128]{0,1:T(8,128)(2,1)S(1)}, bf16[128,128]{0,1:T(8,128)(2,1)S(1)}, u32[]{:S(2)}, u32[]{:S(2)}) collective-permute-start(bf16[128,128]{0,1:T(8,128)(2,1)S(1)} %fusion.15), channel_id=1, source_target_pairs={{0,4},{1,5},{2,6},{3,7},{4,0},{5,1},{6,2},{7,3},{8,12},{9,13},{10,... | collective-permute-start | bytes 98312 | tf_op jit(solution)/shard_map/ppermute | solution.py:27
  111.9 3.6 %collective-permute-start.4 = (bf16[128,256]{0,1:T(8,128)(2,1)}, bf16[128,256]{0,1:T(8,128)(2,1)}, u32[]{:S(2)}, u32[]{:S(2)}) collective-permute-start(bf16[128,256]{0,1:T(8,128)(2,1)} %pad_maximum_fusion.4), channel_id=1, source_target_pairs={{0,2},{1,3},{2,0},{3,1},{4,6},{5,7},{6,4},{7,5},{8,10},{9,11},{10,... | collective-permute-start | bytes 196616 | tf_op jit(solution)/shard_map/ppermute | solution.py:27
  116.3 17.1 %all-to-all-done.2 = bf16[32,16,512]{2,1,0:T(8,128)(2,1)S(1)} async-done(((bf16[32,16,512]{2,1,0:T(8,128)(2,1)}), bf16[32,16,512]{2,1,0:T(8,128)(2,1)S(1)}, u32[]{:S(2)}, u32[]{:S(2)}) %all-to-all-start.2) | async-done | bytes 524320 | tf_op jit(solution)/shard_map/all_to_all | solution.py:31
  133.4 4.1 %collective-permute-start.6 = (bf16[512,512]{1,0:T(8,128)(2,1)S(1)}, bf16[512,512]{1,0:T(8,128)(2,1)}, u32[]{:S(2)}, u32[]{:S(2)}) collective-permute-start(bf16[512,512]{1,0:T(8,128)(2,1)S(1)} %bitcast.159), channel_id=1, source_target_pairs={{0,2},{1,3},{2,4},{3,5},{4,6},{5,7},{6,0},{7,1},{8,10},{9,11},{10,... | collective-permute-start | bytes 1572872 | tf_op jit(solution)/shard_map/ppermute | solution.py:22
  137.5 3.8 %collective-permute-start.7 = (bf16[512,512]{1,0:T(8,128)(2,1)S(1)}, bf16[512,512]{1,0:T(8,128)(2,1)S(1)}, u32[]{:S(2)}, u32[]{:S(2)}) collective-permute-start(bf16[512,512]{1,0:T(8,128)(2,1)S(1)} %bitcast.160), channel_id=1, source_target_pairs={{0,6},{1,7},{2,0},{3,1},{4,2},{5,3},{6,4},{7,5},{8,14},{9,15},{10,... | collective-permute-start | bytes 1572872 | tf_op jit(solution)/shard_map/ppermute | solution.py:22
  141.4 2.1 multiply_reduce_fusion
  145.0 12.3 %collective-permute-done.6 = bf16[512,512]{1,0:T(8,128)(2,1)} collective-permute-done((bf16[512,512]{1,0:T(8,128)(2,1)S(1)}, bf16[512,512]{1,0:T(8,128)(2,1)}, u32[]{:S(2)}, u32[]{:S(2)}) %collective-permute-start.6) | collective-permute-done | bytes 524320 | tf_op jit(solution)/shard_map/ppermute | solution.py:22
  158.3 3.3 %collective-permute-start.8 = (bf16[256,512]{1,0:T(8,128)(2,1)S(1)}, bf16[256,512]{1,0:T(8,128)(2,1)S(1)}, u32[]{:S(2)}, u32[]{:S(2)}) collective-permute-start(bf16[256,512]{1,0:T(8,128)(2,1)S(1)} %slice.65), channel_id=1, source_target_pairs={{0,2},{1,3},{2,4},{3,5},{4,6},{5,7},{6,0},{7,1},{8,10},{9,11},{10,... | collective-permute-start | bytes 786440 | tf_op jit(solution)/shard_map/ppermute | solution.py:22
  161.6 5.0 %collective-permute-done.7 = bf16[512,512]{1,0:T(8,128)(2,1)S(1)} collective-permute-done((bf16[512,512]{1,0:T(8,128)(2,1)S(1)}, bf16[512,512]{1,0:T(8,128)(2,1)S(1)}, u32[]{:S(2)}, u32[]{:S(2)}) %collective-permute-start.7) | collective-permute-done | bytes 524320 | tf_op jit(solution)/shard_map/ppermute | solution.py:22
  166.6 3.6 %collective-permute-start.9 = (bf16[256,512]{1,0:T(8,128)(2,1)S(1)}, bf16[256,512]{1,0:T(8,128)(2,1)S(1)}, u32[]{:S(2)}, u32[]{:S(2)}) collective-permute-start(bf16[256,512]{1,0:T(8,128)(2,1)S(1)} %slice.66), channel_id=1, source_target_pairs={{0,6},{1,7},{2,0},{3,1},{4,2},{5,3},{6,4},{7,5},{8,14},{9,15},{10,... | collective-permute-start | bytes 786440 | tf_op jit(solution)/shard_map/ppermute | solution.py:22
  170.1 1.4 convolution_add_fusion.5
  171.6 1.5 fusion.44
  173.0 1.3 fusion.42
  174.4 9.8 %collective-permute-done.9 = bf16[256,512]{1,0:T(8,128)(2,1)S(1)} collective-permute-done((bf16[256,512]{1,0:T(8,128)(2,1)S(1)}, bf16[256,512]{1,0:T(8,128)(2,1)S(1)}, u32[]{:S(2)}, u32[]{:S(2)}) %collective-permute-start.9) | collective-permute-done | bytes 262176 | tf_op jit(solution)/shard_map/ppermute | solution.py:22
  184.6 1.3 fusion.40
  186.3 1.3 fusion.4
  187.8 3.4 %collective-permute-start.11 = (bf16[512,256]{0,1:T(8,128)(2,1)S(1)}, bf16[512,256]{0,1:T(8,128)(2,1)S(1)}, u32[]{:S(2)}, u32[]{:S(2)}) collective-permute-start(bf16[512,256]{0,1:T(8,128)(2,1)S(1)} %pad_maximum_fusion.2), channel_id=1, source_target_pairs={{0,2},{1,3},{2,4},{3,5},{4,6},{5,7},{6,0},{7,1},{8,10},{9,11},{10,... | collective-permute-start | bytes 786440 | tf_op jit(solution)/shard_map/ppermute | solution.py:22
  191.2 4.0 %collective-permute-start.12 = (bf16[512,256]{0,1:T(8,128)(2,1)S(1)}, bf16[512,256]{0,1:T(8,128)(2,1)S(1)}, u32[]{:S(2)}, u32[]{:S(2)}) collective-permute-start(bf16[512,256]{0,1:T(8,128)(2,1)S(1)} %pad_maximum_fusion.2), channel_id=1, source_target_pairs={{0,6},{1,7},{2,0},{3,1},{4,2},{5,3},{6,4},{7,5},{8,14},{9,15},{10,... | collective-permute-start | bytes 786440 | tf_op jit(solution)/shard_map/ppermute | solution.py:22
  195.9 1.2 fusion.65
  197.0 2.2 collective-permute-done.11
  199.3 2.0 collective-permute-start.13
  201.3 6.4 %collective-permute-start.14 = (bf16[256,256]{0,1:T(8,128)(2,1)S(1)}, bf16[256,256]{0,1:T(8,128)(2,1)S(1)}, u32[]{:S(2)}, u32[]{:S(2)}) collective-permute-start(bf16[256,256]{0,1:T(8,128)(2,1)S(1)} %slice.72), channel_id=1, source_target_pairs={{0,6},{1,7},{2,0},{3,1},{4,2},{5,3},{6,4},{7,5},{8,14},{9,15},{10,... | collective-permute-start | bytes 393224 | tf_op jit(solution)/shard_map/ppermute | solution.py:22
  207.7 1.2 convolution_add_fusion.2
  208.9 1.2 fusion.75
  210.1 1.2 fusion.73
  211.4 1.2 fusion.61
  212.6 1.2 fusion.71
  213.7 1.2 fusion.7
  214.9 1.2 fusion.6
  217.2 10.6 %all-to-all-start.3 = ((bf16[32,16,512]{2,1,0:T(8,128)(2,1)}), bf16[32,16,512]{2,1,0:T(8,128)(2,1)S(1)}, u32[]{:S(2)}, u32[]{:S(2)}) async-start(bf16[32,16,512]{2,1,0:T(8,128)(2,1)} %bitcast.35), calls=%async_computation.3 | async-start | bytes 1048576 | tf_op jit(solution)/shard_map/all_to_all | solution.py:31
  227.8 4.0 %collective-permute-start = (bf16[2,2,16,2048]{3,2,0,1:T(8,128)(2,1)S(1)}, bf16[2,2,16,2048]{3,2,0,1:T(8,128)(2,1)S(1)}, u32[]{:S(2)}, u32[]{:S(2)}) collective-permute-start(bf16[2,2,16,2048]{3,2,0,1:T(8,128)(2,1)S(1)} %fusion.23), channel_id=1, source_target_pairs={{0,1},{1,0},{2,3},{3,2},{4,5},{5,4},{6,7},{7,6},{8,9},{9,8},{10,11... | collective-permute-start | bytes 786440 | tf_op jit(solution)/shard_map/ppermute | solution.py:27
  232.8 2.0 collective-permute-start.5
  234.8 3.1 %collective-permute-done = bf16[2,2,16,2048]{3,2,0,1:T(8,128)(2,1)S(1)} collective-permute-done((bf16[2,2,16,2048]{3,2,0,1:T(8,128)(2,1)S(1)}, bf16[2,2,16,2048]{3,2,0,1:T(8,128)(2,1)S(1)}, u32[]{:S(2)}, u32[]{:S(2)}) %collective-permute-start) | collective-permute-done | bytes 262176 | tf_op jit(solution)/shard_map/ppermute | solution.py:27
  238.0 4.0 %collective-permute-start.1 = (bf16[2,16,2048]{2,1,0:T(8,128)(2,1)S(1)}, bf16[2,16,2048]{2,1,0:T(8,128)(2,1)S(1)}, u32[]{:S(2)}, u32[]{:S(2)}) collective-permute-start(bf16[2,16,2048]{2,1,0:T(8,128)(2,1)S(1)} %fusion.59), channel_id=1, source_target_pairs={{0,2},{1,3},{2,0},{3,1},{4,6},{5,7},{6,4},{7,5},{8,10},{9,11},{10,... | collective-permute-start | bytes 393224 | tf_op jit(solution)/shard_map/ppermute | solution.py:27
  242.0 4.5 %collective-permute-done.1 = bf16[2,16,2048]{2,1,0:T(8,128)(2,1)S(1)} collective-permute-done((bf16[2,16,2048]{2,1,0:T(8,128)(2,1)S(1)}, bf16[2,16,2048]{2,1,0:T(8,128)(2,1)S(1)}, u32[]{:S(2)}, u32[]{:S(2)}) %collective-permute-start.1) | collective-permute-done | bytes 131104 | tf_op jit(solution)/shard_map/ppermute | solution.py:27
  246.6 4.1 %collective-permute-start.2 = (bf16[16,2048]{1,0:T(8,128)(2,1)S(1)}, bf16[16,2048]{1,0:T(8,128)(2,1)S(1)}, u32[]{:S(2)}, u32[]{:S(2)}) collective-permute-start(bf16[16,2048]{1,0:T(8,128)(2,1)S(1)} %fusion.106), channel_id=1, source_target_pairs={{0,4},{1,5},{2,6},{3,7},{4,0},{5,1},{6,2},{7,3},{8,12},{9,13},{10,... | collective-permute-start | bytes 196616 | tf_op jit(solution)/shard_map/ppermute | solution.py:27
  250.7 10.4 %all-to-all-done.3 = bf16[32,16,512]{2,1,0:T(8,128)(2,1)S(1)} async-done(((bf16[32,16,512]{2,1,0:T(8,128)(2,1)}), bf16[32,16,512]{2,1,0:T(8,128)(2,1)S(1)}, u32[]{:S(2)}, u32[]{:S(2)}) %all-to-all-start.3) | async-done | bytes 524320 | tf_op jit(solution)/shard_map/all_to_all | solution.py:31
  262.1 4.0 %collective-permute-start.16 = (bf16[128,256]{1,0:T(8,128)(2,1)S(1)}, bf16[128,256]{1,0:T(8,128)(2,1)S(1)}, u32[]{:S(2)}, u32[]{:S(2)}) collective-permute-start(bf16[128,256]{1,0:T(8,128)(2,1)S(1)} %slice.88), channel_id=1, source_target_pairs={{0,1},{1,0},{2,3},{3,2},{4,5},{5,4},{6,7},{7,6},{8,9},{9,8},{10,11... | collective-permute-start | bytes 196616 | tf_op jit(solution)/shard_map/ppermute | solution.py:27
  266.8 1.3 collective-permute-done.16
  (155 shorter events, 22.5 us)
Async XLA Ops:
  0.6 194.9 %copy-start = (bf16[256,2048]{1,0:T(8,128)(2,1)S(1)}, bf16[256,2048]{1,0:T(8,128)(2,1)}, u32[]{:S(2)}) copy-start(bf16[256,2048]{1,0:T(8,128)(2,1)} %param.27) | copy-start | bytes 3145732
  0.6 8.6 %copy-start.23 = (f32[128,2]{0,1:T(2,128)S(1)}, f32[128,2]{0,1:T(2,128)}, u32[]{:S(2)}) copy-start(f32[128,2]{0,1:T(2,128)} %param.25) | copy-start | bytes 3076
  0.7 8.9 %copy-start.14 = (bf16[128,256]{1,0:T(8,128)(2,1)S(1)}, bf16[128,256]{1,0:T(8,128)(2,1)}, u32[]{:S(2)}) copy-start(bf16[128,256]{1,0:T(8,128)(2,1)} %param.21) | copy-start | bytes 196612
  0.7 8.9 %copy-start.24 = (f32[256]{0:T(256)S(1)}, f32[256]{0:T(256)}, u32[]{:S(2)}) copy-start(f32[256]{0:T(256)} %param.24) | copy-start | bytes 3076
  3.0 7.0 %copy-start.17 = (bf16[128,256]{1,0:T(8,128)(2,1)S(1)}, bf16[128,256]{1,0:T(8,128)(2,1)}, u32[]{:S(2)}) copy-start(bf16[128,256]{1,0:T(8,128)(2,1)} %param.22) | copy-start | bytes 196612
  3.0 168.5 %collective-permute-start.10 = (bf16[2048,256]{1,0:T(8,128)(2,1)}, bf16[2048,256]{1,0:T(8,128)(2,1)}, u32[]{:S(2)}, u32[]{:S(2)}) collective-permute-start(bf16[2048,256]{1,0:T(8,128)(2,1)} %pad_maximum_fusion), channel_id=1, source_target_pairs={{0,1},{1,0},{2,3},{3,2},{4,5},{5,4},{6,7},{7,6},{8,9},{9,8},{10,11... | collective-permute-start | bytes 3145736 | tf_op jit(solution)/shard_map/ppermute | solution.py:27
  7.3 201.6 %collective-permute-start.15 = (bf16[1024,256]{1,0:T(8,128)(2,1)}, bf16[1024,256]{1,0:T(8,128)(2,1)}, u32[]{:S(2)}, u32[]{:S(2)}) collective-permute-start(bf16[1024,256]{1,0:T(8,128)(2,1)} %bitcast.34), channel_id=1, source_target_pairs={{0,1},{1,0},{2,3},{3,2},{4,5},{5,4},{6,7},{7,6},{8,9},{9,8},{10,11... | collective-permute-start | bytes 1572872 | tf_op jit(solution)/shard_map/ppermute | solution.py:27
  10.5 47.8 %copy-start.19 = (s32[128,4]{0,1:T(4,128)S(1)}, s32[128,4]{0,1:T(4,128)}, u32[]{:S(2)}) copy-start(s32[128,4]{0,1:T(4,128)} %param.29) | copy-start | bytes 6148
  12.2 46.1 %copy-start.3 = (bf16[128,2048]{1,0:T(8,128)(2,1)S(1)}, bf16[128,2048]{1,0:T(8,128)(2,1)}, u32[]{:S(2)}) copy-start(bf16[128,2048]{1,0:T(8,128)(2,1)} %param.28) | copy-start | bytes 1572868
  12.2 46.9 %copy-start.18 = (f32[2048]{0:T(1024)S(1)}, f32[2048]{0:T(1024)}, u32[]{:S(2)}) copy-start(f32[2048]{0:T(1024)} %param.31) | copy-start | bytes 24580
  13.2 60.9 %all-to-all-start = ((bf16[32,8,256]{2,1,0:T(8,128)(2,1)}), bf16[32,8,256]{2,1,0:T(8,128)(2,1)S(1)}, u32[]{:S(2)}, u32[]{:S(2)}) async-start(bf16[32,8,256]{2,1,0:T(8,128)(2,1)} %fusion.58), calls=%async_computation | async-start | bytes 262144 | tf_op jit(solution)/shard_map/all_to_all | solution.py:31
  58.5 0.5 copy-start.21
  75.7 24.3 %copy-start.5 = (bf16[2048,128]{1,0:T(8,128)(2,1)S(1)}, bf16[2048,128]{1,0:T(8,128)(2,1)}, u32[]{:S(2)}) copy-start(bf16[2048,128]{1,0:T(8,128)(2,1)} %param.35) | copy-start | bytes 1572868
  76.3 18.6 %all-to-all-start.1 = ((bf16[32,8,128]{2,1,0:T(8,128)(2,1)}), bf16[32,8,128]{2,1,0:T(8,128)(2,1)S(1)}, u32[]{:S(2)}, u32[]{:S(2)}) async-start(bf16[32,8,128]{2,1,0:T(8,128)(2,1)} %copy.191), calls=%async_computation.1 | async-start | bytes 131072 | tf_op jit(solution)/shard_map/all_to_all | solution.py:31
  81.7 0.6 copy-start.12
  95.0 38.4 %all-to-all-start.2 = ((bf16[32,16,512]{2,1,0:T(8,128)(2,1)}), bf16[32,16,512]{2,1,0:T(8,128)(2,1)S(1)}, u32[]{:S(2)}, u32[]{:S(2)}) async-start(bf16[32,16,512]{2,1,0:T(8,128)(2,1)} %bitcast.26), calls=%async_computation.2 | async-start | bytes 1048576 | tf_op jit(solution)/shard_map/all_to_all | solution.py:31
  100.0 1.0 copy-start.6
  100.0 9.0 %copy-start.20 = (f32[128,4]{0,1:T(4,128)S(1)}, f32[128,4]{0,1:T(4,128)}, u32[]{:S(2)}) copy-start(f32[128,4]{0,1:T(4,128)} %param.30) | copy-start | bytes 6148
  100.0 9.1 %copy-start.15 = (bf16[128,256]{1,0:T(8,128)(2,1)S(1)}, bf16[128,256]{1,0:T(8,128)(2,1)}, u32[]{:S(2)}) copy-start(bf16[128,256]{1,0:T(8,128)(2,1)} %param.20) | copy-start | bytes 196612
  101.4 8.5 %copy-start.7 = (bf16[1024,256]{1,0:T(8,128)(2,1)S(1)}, bf16[1024,256]{1,0:T(8,128)(2,1)}, u32[]{:S(2)}) copy-start(bf16[1024,256]{1,0:T(8,128)(2,1)} %param.37) | copy-start | bytes 1572868
  101.4 9.9 %collective-permute-start.3 = (bf16[128,128]{0,1:T(8,128)(2,1)S(1)}, bf16[128,128]{0,1:T(8,128)(2,1)S(1)}, u32[]{:S(2)}, u32[]{:S(2)}) collective-permute-start(bf16[128,128]{0,1:T(8,128)(2,1)S(1)} %fusion.15), channel_id=1, source_target_pairs={{0,4},{1,5},{2,6},{3,7},{4,0},{5,1},{6,2},{7,3},{8,12},{9,13},{10,... | collective-permute-start | bytes 98312 | tf_op jit(solution)/shard_map/ppermute | solution.py:27
  110.7 34.0 %copy-start.1 = (bf16[1,2048,128]{2,1,0:T(8,128)(2,1)S(1)}, bf16[1,2048,128]{2,1,0:T(8,128)(2,1)}, u32[]{:S(2)}) copy-start(bf16[1,2048,128]{2,1,0:T(8,128)(2,1)} %param.32) | copy-start | bytes 1572868
  110.7 34.0 %copy-start.2 = (bf16[1,2048,128]{2,1,0:T(8,128)(2,1)S(1)}, bf16[1,2048,128]{2,1,0:T(8,128)(2,1)}, u32[]{:S(2)}) copy-start(bf16[1,2048,128]{2,1,0:T(8,128)(2,1)} %param.33) | copy-start | bytes 1572868
  111.3 4.3 %copy-start.8 = (bf16[128,128]{0,1:T(8,128)(2,1)}, bf16[128,128]{0,1:T(8,128)(2,1)S(1)}, u32[]{:S(2)}) copy-start(bf16[128,128]{0,1:T(8,128)(2,1)S(1)} %get-tuple-element.112) | copy-start | bytes 98308
  111.3 4.3 %copy-start.10 = (bf16[128,128]{0,1:T(8,128)(2,1)}, bf16[128,128]{0,1:T(8,128)(2,1)S(1)}, u32[]{:S(2)}) copy-start(bf16[128,128]{0,1:T(8,128)(2,1)S(1)} %get-tuple-element.113) | copy-start | bytes 98308
  111.9 119.9 %collective-permute-start.4 = (bf16[128,256]{0,1:T(8,128)(2,1)}, bf16[128,256]{0,1:T(8,128)(2,1)}, u32[]{:S(2)}, u32[]{:S(2)}) collective-permute-start(bf16[128,256]{0,1:T(8,128)(2,1)} %pad_maximum_fusion.4), channel_id=1, source_target_pairs={{0,2},{1,3},{2,0},{3,1},{4,6},{5,7},{6,4},{7,5},{8,10},{9,11},{10,... | collective-permute-start | bytes 196616 | tf_op jit(solution)/shard_map/ppermute | solution.py:27
  133.4 23.9 %collective-permute-start.6 = (bf16[512,512]{1,0:T(8,128)(2,1)S(1)}, bf16[512,512]{1,0:T(8,128)(2,1)}, u32[]{:S(2)}, u32[]{:S(2)}) collective-permute-start(bf16[512,512]{1,0:T(8,128)(2,1)S(1)} %bitcast.159), channel_id=1, source_target_pairs={{0,2},{1,3},{2,4},{3,5},{4,6},{5,7},{6,0},{7,1},{8,10},{9,11},{10,... | collective-permute-start | bytes 1572872 | tf_op jit(solution)/shard_map/ppermute | solution.py:22
  137.5 29.0 %collective-permute-start.7 = (bf16[512,512]{1,0:T(8,128)(2,1)S(1)}, bf16[512,512]{1,0:T(8,128)(2,1)S(1)}, u32[]{:S(2)}, u32[]{:S(2)}) collective-permute-start(bf16[512,512]{1,0:T(8,128)(2,1)S(1)} %bitcast.160), channel_id=1, source_target_pairs={{0,6},{1,7},{2,0},{3,1},{4,2},{5,3},{6,4},{7,5},{8,14},{9,15},{10,... | collective-permute-start | bytes 1572872 | tf_op jit(solution)/shard_map/ppermute | solution.py:22
  158.3 16.1 %collective-permute-start.8 = (bf16[256,512]{1,0:T(8,128)(2,1)S(1)}, bf16[256,512]{1,0:T(8,128)(2,1)S(1)}, u32[]{:S(2)}, u32[]{:S(2)}) collective-permute-start(bf16[256,512]{1,0:T(8,128)(2,1)S(1)} %slice.65), channel_id=1, source_target_pairs={{0,2},{1,3},{2,4},{3,5},{4,6},{5,7},{6,0},{7,1},{8,10},{9,11},{10,... | collective-permute-start | bytes 786440 | tf_op jit(solution)/shard_map/ppermute | solution.py:22
  166.6 17.6 %collective-permute-start.9 = (bf16[256,512]{1,0:T(8,128)(2,1)S(1)}, bf16[256,512]{1,0:T(8,128)(2,1)S(1)}, u32[]{:S(2)}, u32[]{:S(2)}) collective-permute-start(bf16[256,512]{1,0:T(8,128)(2,1)S(1)} %slice.66), channel_id=1, source_target_pairs={{0,6},{1,7},{2,0},{3,1},{4,2},{5,3},{6,4},{7,5},{8,14},{9,15},{10,... | collective-permute-start | bytes 786440 | tf_op jit(solution)/shard_map/ppermute | solution.py:22
  187.6 7.9 %copy-start.16 = (bf16[128,256]{1,0:T(8,128)(2,1)S(1)}, bf16[128,256]{1,0:T(8,128)(2,1)}, u32[]{:S(2)}) copy-start(bf16[128,256]{1,0:T(8,128)(2,1)} %param.23) | copy-start | bytes 196612
  187.6 7.9 %copy-start.25 = (f32[256]{0:T(256)S(1)}, f32[256]{0:T(256)}, u32[]{:S(2)}) copy-start(f32[256]{0:T(256)} %param.26) | copy-start | bytes 3076
  187.8 11.5 %collective-permute-start.11 = (bf16[512,256]{0,1:T(8,128)(2,1)S(1)}, bf16[512,256]{0,1:T(8,128)(2,1)S(1)}, u32[]{:S(2)}, u32[]{:S(2)}) collective-permute-start(bf16[512,256]{0,1:T(8,128)(2,1)S(1)} %pad_maximum_fusion.2), channel_id=1, source_target_pairs={{0,2},{1,3},{2,4},{3,5},{4,6},{5,7},{6,0},{7,1},{8,10},{9,11},{10,... | collective-permute-start | bytes 786440 | tf_op jit(solution)/shard_map/ppermute | solution.py:22
  191.2 10.0 %collective-permute-start.12 = (bf16[512,256]{0,1:T(8,128)(2,1)S(1)}, bf16[512,256]{0,1:T(8,128)(2,1)S(1)}, u32[]{:S(2)}, u32[]{:S(2)}) collective-permute-start(bf16[512,256]{0,1:T(8,128)(2,1)S(1)} %pad_maximum_fusion.2), channel_id=1, source_target_pairs={{0,6},{1,7},{2,0},{3,1},{4,2},{5,3},{6,4},{7,5},{8,14},{9,15},{10,... | collective-permute-start | bytes 786440 | tf_op jit(solution)/shard_map/ppermute | solution.py:22
  199.3 12.0 %collective-permute-start.13 = (bf16[256,256]{0,1:T(8,128)(2,1)S(1)}, bf16[256,256]{0,1:T(8,128)(2,1)S(1)}, u32[]{:S(2)}, u32[]{:S(2)}) collective-permute-start(bf16[256,256]{0,1:T(8,128)(2,1)S(1)} %slice.71), channel_id=1, source_target_pairs={{0,2},{1,3},{2,4},{3,5},{4,6},{5,7},{6,0},{7,1},{8,10},{9,11},{10,... | collective-permute-start | bytes 393224 | tf_op jit(solution)/shard_map/ppermute | solution.py:22
  201.3 10.1 %collective-permute-start.14 = (bf16[256,256]{0,1:T(8,128)(2,1)S(1)}, bf16[256,256]{0,1:T(8,128)(2,1)S(1)}, u32[]{:S(2)}, u32[]{:S(2)}) collective-permute-start(bf16[256,256]{0,1:T(8,128)(2,1)S(1)} %slice.72), channel_id=1, source_target_pairs={{0,6},{1,7},{2,0},{3,1},{4,2},{5,3},{6,4},{7,5},{8,14},{9,15},{10,... | collective-permute-start | bytes 393224 | tf_op jit(solution)/shard_map/ppermute | solution.py:22
  217.2 14.7 %copy-start.9 = (bf16[128,128]{0,1:T(8,128)(2,1)S(1)}, bf16[128,128]{0,1:T(8,128)(2,1)}, u32[]{:S(2)}) copy-start(bf16[128,128]{0,1:T(8,128)(2,1)} %copy-done.8) | copy-start | bytes 98308
  217.2 14.7 %copy-start.11 = (bf16[128,128]{0,1:T(8,128)(2,1)S(1)}, bf16[128,128]{0,1:T(8,128)(2,1)}, u32[]{:S(2)}) copy-start(bf16[128,128]{0,1:T(8,128)(2,1)} %copy-done.10) | copy-start | bytes 98308
  217.2 43.9 %all-to-all-start.3 = ((bf16[32,16,512]{2,1,0:T(8,128)(2,1)}), bf16[32,16,512]{2,1,0:T(8,128)(2,1)S(1)}, u32[]{:S(2)}, u32[]{:S(2)}) async-start(bf16[32,16,512]{2,1,0:T(8,128)(2,1)} %bitcast.35), calls=%async_computation.3 | async-start | bytes 1048576 | tf_op jit(solution)/shard_map/all_to_all | solution.py:31
  227.8 10.0 %collective-permute-start = (bf16[2,2,16,2048]{3,2,0,1:T(8,128)(2,1)S(1)}, bf16[2,2,16,2048]{3,2,0,1:T(8,128)(2,1)S(1)}, u32[]{:S(2)}, u32[]{:S(2)}) collective-permute-start(bf16[2,2,16,2048]{3,2,0,1:T(8,128)(2,1)S(1)} %fusion.23), channel_id=1, source_target_pairs={{0,1},{1,0},{2,3},{3,2},{4,5},{5,4},{6,7},{7,6},{8,9},{9,8},{10,11... | collective-permute-start | bytes 786440 | tf_op jit(solution)/shard_map/ppermute | solution.py:27
  232.8 9.2 %collective-permute-start.5 = (bf16[128,512]{0,1:T(8,128)(2,1)S(1)}, bf16[128,512]{0,1:T(8,128)(2,1)S(1)}, u32[]{:S(2)}, u32[]{:S(2)}) collective-permute-start(bf16[128,512]{0,1:T(8,128)(2,1)S(1)} %pad_maximum_fusion.3), channel_id=1, source_target_pairs={{0,1},{1,0},{2,3},{3,2},{4,5},{5,4},{6,7},{7,6},{8,9},{9,8},{10,11... | collective-permute-start | bytes 393224 | tf_op jit(solution)/shard_map/ppermute | solution.py:27
  237.9 23.2 %copy-start.13 = (s32[128,32]{0,1:T(8,128)S(1)}, s32[128,32]{0,1:T(8,128)}, u32[]{:S(2)}) copy-start(s32[128,32]{0,1:T(8,128)} %copy-done.12) | copy-start | bytes 49156
  237.9 23.2 %copy-start.22 = (s32[16]{0:T(128)S(1)}, s32[16]{0:T(128)}, u32[]{:S(2)}) copy-start(s32[16]{0:T(128)} %copy-done.21) | copy-start | bytes 196
  238.0 8.5 %collective-permute-start.1 = (bf16[2,16,2048]{2,1,0:T(8,128)(2,1)S(1)}, bf16[2,16,2048]{2,1,0:T(8,128)(2,1)S(1)}, u32[]{:S(2)}, u32[]{:S(2)}) collective-permute-start(bf16[2,16,2048]{2,1,0:T(8,128)(2,1)S(1)} %fusion.59), channel_id=1, source_target_pairs={{0,2},{1,3},{2,0},{3,1},{4,6},{5,7},{6,4},{7,5},{8,10},{9,11},{10,... | collective-permute-start | bytes 393224 | tf_op jit(solution)/shard_map/ppermute | solution.py:27
  246.6 19.6 %collective-permute-start.2 = (bf16[16,2048]{1,0:T(8,128)(2,1)S(1)}, bf16[16,2048]{1,0:T(8,128)(2,1)S(1)}, u32[]{:S(2)}, u32[]{:S(2)}) collective-permute-start(bf16[16,2048]{1,0:T(8,128)(2,1)S(1)} %fusion.106), channel_id=1, source_target_pairs={{0,4},{1,5},{2,6},{3,7},{4,0},{5,1},{6,2},{7,3},{8,12},{9,13},{10,... | collective-permute-start | bytes 196616 | tf_op jit(solution)/shard_map/ppermute | solution.py:27
  261.8 6.3 %copy-start.4 = (bf16[2,2,2,128,256]{4,3,2,1,0:T(8,128)(2,1)S(1)}, bf16[2,2,2,128,256]{4,3,2,1,0:T(8,128)(2,1)}, u32[]{:S(2)}) copy-start(bf16[2,2,2,128,256]{4,3,2,1,0:T(8,128)(2,1)} %copy.197) | copy-start | bytes 1572868
  262.1 6.0 %collective-permute-start.16 = (bf16[128,256]{1,0:T(8,128)(2,1)S(1)}, bf16[128,256]{1,0:T(8,128)(2,1)S(1)}, u32[]{:S(2)}, u32[]{:S(2)}) collective-permute-start(bf16[128,256]{1,0:T(8,128)(2,1)S(1)} %slice.88), channel_id=1, source_target_pairs={{0,1},{1,0},{2,3},{3,2},{4,5},{5,4},{6,7},{7,6},{8,9},{9,8},{10,11... | collective-permute-start | bytes 196616 | tf_op jit(solution)/shard_map/ppermute | solution.py:27

commit v3 on v2

--- a/solution.py
+++ b/solution.py
@@ -1,6 +1,10 @@
+import functools
+
 import jax
 import jax.numpy as jnp
 from jax import lax
+from jax.experimental import pallas as pl
+from jax.experimental.pallas import tpu as pltpu
 from jax.sharding import Mesh
 from jax.sharding import PartitionSpec as P
 
@@ -174,6 +178,107 @@
     gated_rows = (normed * jax.nn.silu(output_gate_input.astype(jnp.float32))).astype(jnp.bfloat16)
     partial = jnp.dot(gated_rows, recurrence_out_weight, preferred_element_type=jnp.float32)
     return summed_to_owners(partial, "tp").astype(jnp.bfloat16)
+
+
+VMEM = pl.BlockSpec(memory_space=pltpu.VMEM)
+SMEM = pl.BlockSpec(memory_space=pltpu.SMEM)
+
+
+def in_vmem(kernel, shapes, *operands):
+    member = lax.axis_index("tp")
+    place = jnp.stack([member >> 1, member & 1])
+    return pl.pallas_call(
+        kernel,
+        out_shape=shapes,
+        in_specs=[SMEM] + [VMEM] * len(operands),
+        out_specs=jax.tree.map(lambda _: VMEM, shapes),
+    )(place, *operands)
+
+
+def select_kernel(experts, place, hidden_state, gain, index, normed, outgoing):
+    tokens, top = index.shape
+    slots, width = outgoing.shape
+    half = slots // experts
+    features = hidden_state[...].astype(jnp.float32)
+    factor = lax.rsqrt(jnp.mean(features * features, axis=1, keepdims=True) + EPSILON)
+    normed[...] = (features * factor * gain[...]).astype(jnp.bfloat16)
+    expert = lax.broadcasted_iota(jnp.int32, (tokens, experts), 1)
+    named = [index[:, j : j + 1] == expert for j in range(top)]
+    chosen = named[0]
+    for other in named[1:]:
+        chosen = chosen | other
+    earlier = lax.broadcasted_iota(jnp.int32, (tokens, tokens), 1) < lax.broadcasted_iota(
+        jnp.int32, (tokens, tokens), 0
+    )
+    one = jnp.float32(1)
+    zero = jnp.float32(0)
+    places = jnp.dot(
+        jnp.where(earlier, one, zero).astype(jnp.bfloat16),
+        jnp.where(chosen, one, zero).astype(jnp.bfloat16),
+        preferred_element_type=jnp.float32,
+    )
+    places = jnp.where(chosen, places, -one).astype(jnp.bfloat16)
+    slot = lax.broadcasted_iota(jnp.int32, (experts, slots), 1)
+    spread = jnp.where(
+        slot // half == lax.broadcasted_iota(jnp.int32, (experts, slots), 0), one, zero
+    ).astype(jnp.bfloat16)
+    wanted = jnp.dot(places, spread, preferred_element_type=jnp.float32).astype(jnp.int32)
+    own = lax.broadcasted_iota(jnp.int32, (tokens, slots), 1) % half + place[1] * half
+    filled = jnp.where(wanted == own, one, zero).astype(jnp.bfloat16)
+    start = pl.multiple_of(place[0] * width, width)
+    outgoing[...] = lax.dot_general(
+        filled,
+        normed[:, pl.ds(start, width)],
+        (((0,), (0,)), ((), ())),
+        preferred_element_type=jnp.float32,
+    ).astype(jnp.bfloat16)
+
+
+def around_product(place, pieces, matrix):
+    own, before, after, far_first, far_second = pieces
+    depth = own.shape[1]
+    count = matrix.shape[0] // depth
+
+    def block(step):
+        start = pl.multiple_of(((place[0] + step) & (count - 1)) * depth, depth)
+        return matrix[pl.ds(start, depth), :]
+
+    def dot(piece, step):
+        return jnp.dot(piece, block(step), preferred_element_type=jnp.float32)
+
+    near = dot(own[...], 0) + dot(before[...], -1) + dot(after[...], 1)
+    middle = far_first.shape[0]
+    return (near[:middle] + dot(far_first[...], 2), near[middle:] + dot(far_second[...], 2))
+
+
+def hidden_kernel(place, own, before, after, far_first, far_second, own_in, partner_in, hidden):
+    pieces = (own, before, after, far_first, far_second)
+    units = own_in.shape[1] // 2
+    middle = far_first.shape[0]
+    sides = []
+    for matrix in (own_in, partner_in):
+        sides.append(
+            [
+                (jax.nn.silu(both[:, :units]) * both[:, units:]).astype(jnp.bfloat16)
+                for both in around_product(place, pieces, matrix)
+            ]
+        )
+    even = place[1] == 0
+    for k in range(2):
+        rows = pl.ds(k * middle, middle)
+        hidden[rows, :units] = jnp.where(even, sides[0][k], sides[1][k])
+        hidden[rows, units:] = jnp.where(even, sides[1][k], sides[0][k])
+
+
+def down_kernel(place, own, before, after, far_first, far_second, own_down, partner_down, answers):
+    pieces = (own, before, after, far_first, far_second)
+    middle = far_first.shape[0]
+    width = own_down.shape[1]
+    for side, matrix in enumerate((own_down, partner_down)):
+        for k, part in enumerate(around_product(place, pieces, matrix)):
+            answers[pl.ds(k * middle, middle), pl.ds(side * width, width)] = part.astype(
+                jnp.bfloat16
+            )
 
 
 def expert_half(
@@ -197,7 +302,7 @@
     members = lax.axis_size("tp")
     quads = members // 2
     member = lax.axis_index("tp")
-    parity, quad = (member & 1, member >> 1)
+    parity = member & 1
     half = capacity // 2
     width_in = routed_gate_weight.shape[1] // quads
     units = routed_gate_weight.shape[2]
@@ -207,12 +312,20 @@
     partner_in = swapped(own_in, "tp", 1)
     partner_down = swapped(own_down, "tp", 1)
 
-    features = expert_hidden_state.astype(jnp.float32)
-    normed = (
-        features
-        * lax.rsqrt(jnp.mean(features * features, axis=1, keepdims=True) + EPSILON)
-        * expert_norm_gain[None, :]
-    ).astype(jnp.bfloat16)
+    normed, outgoing = in_vmem(
+        functools.partial(select_kernel, experts),
+        (
+            jax.ShapeDtypeStruct(expert_hidden_state.shape, jnp.bfloat16),
+            jax.ShapeDtypeStruct((experts * half, width_in), jnp.bfloat16),
+        ),
+        expert_hidden_state,
+        expert_norm_gain[None, :],
+        chosen_expert_index,
+    )
+    arrived = exchanged(outgoing.reshape(devices, half, width_in), EP)
+    chunk = arrived.reshape(devices * half, width_in)
+    middle = chunk.shape[0] // 2
+
     gates = ROUTED_SCALE * chosen_expert_score / jnp.sum(chosen_expert_score, axis=1, keepdims=True)
     named = chosen_expert_index[:, :, None] == jnp.arange(experts, dtype=jnp.int32)[None, None, :]
     chosen = jnp.any(named, axis=1)
@@ -226,16 +339,6 @@
     places = jnp.where(chosen, places.astype(jnp.int32), -1)
     filled = places[:, :, None] == parity * half + jnp.arange(half)[None, None, :]
     filled = filled.reshape(tokens, experts * half)
-    outgoing = lax.dot_general(
-        filled.astype(jnp.bfloat16),
-        lax.dynamic_slice_in_dim(normed, quad * width_in, width_in, 1),
-        (((0,), (0,)), ((), ())),
-        preferred_element_type=jnp.float32,
-    ).astype(jnp.bfloat16)
-    arrived = exchanged(outgoing.reshape(devices, half, width_in), EP)
-    chunk = arrived.reshape(devices * half, width_in)
-    middle = chunk.shape[0] // 2
-
     shared_hidden = (
         jax.nn.silu(jnp.dot(normed, shared_gate_weight, preferred_element_type=jnp.float32))
         * jnp.dot(normed, shared_up_weight, preferred_element_type=jnp.float32)
@@ -251,34 +354,21 @@
         before = shifted(piece, "tp", 2)
         after = shifted(piece, "tp", -2)
         far = [shifted(before[:middle], "tp", 2), shifted(after[middle:], "tp", -2)]
-        return ((piece, 0), (before, -1), (after, 1), (jnp.concatenate(far, axis=0), 2))
-
-    def product(pieces, matrix):
-        total = None
-        for piece, step in pieces:
-            depth = piece.shape[1]
-            block = lax.dynamic_slice_in_dim(
-                matrix, ((quad + step) & (quads - 1)) * depth, depth, 0
-            )
-            part = jnp.dot(piece, block, preferred_element_type=jnp.float32)
-            total = part if total is None else total + part
-        return total
-
-    row_pieces = all_around(chunk)
-    sides = []
-    for matrix in (own_in, partner_in):
-        both = product(row_pieces, matrix)
-        sides.append((jax.nn.silu(both[:, :units]) * both[:, units:]).astype(jnp.bfloat16))
-    own, other = sides
-    even = parity == 0
-    hidden = jnp.concatenate([jnp.where(even, own, other), jnp.where(even, other, own)], axis=1)
-    hidden_pieces = all_around(hidden)
-    answers = jnp.concatenate(
-        [
-            product(hidden_pieces, matrix).astype(jnp.bfloat16)
-            for matrix in (own_down, partner_down)
-        ],
-        axis=1,
+        return (piece, before, after, *far)
+
+    hidden = in_vmem(
+        hidden_kernel,
+        jax.ShapeDtypeStruct((chunk.shape[0], 2 * units), jnp.bfloat16),
+        *all_around(chunk),
+        own_in,
+        partner_in,
+    )
+    answers = in_vmem(
+        down_kernel,
+        jax.ShapeDtypeStruct((chunk.shape[0], 2 * width_out), jnp.bfloat16),
+        *all_around(hidden),
+        own_down,
+        partner_down,
     )
     returned = exchanged(answers.reshape(devices, half, 2 * width_out), EP)
     returned = returned.reshape(experts * half, 2 * width_out)

time: 271 us -> 249 us (0.919)
  waiting for transfers between devices: 92 us -> 59 us
  matrix products: 25.9 us -> 14.3 us
  Pallas kernels: 0 us -> 9.96 us
  starting transfers between devices: 132 us -> 140 us
  local copies, waits for them, and re-layouts: 8.37 us -> 11.5 us
    all_to_all x4, waiting for transfers between devices: 53.8 us -> 27.4 us  [exchanged(): return lax.all_to_all(array, axis, split_axis=0, concat_axis=0, tiled=True)]
    dot_general x17 -> x0, matrix products: 18.4 us -> none  [the longest x16 17.3 us: product(): part = jnp.dot(piece, block, preferred_element_type=jnp.float32)]
    pallas_call x0 -> x3, Pallas kernels: none -> 9.96 us  [in_vmem(): pl.pallas_call(kernel, out_shape=shapes, in_specs=[SMEM] + [VMEM] * len(o...]
    ppermute x8, waiting for transfers between devices: 29.3 us -> 23.4 us  [shifted(): lax.ppermute(array, axis, [(i, (i + step) % count) for i in range(count)])]
    ppermute x8, starting transfers between devices: 30.7 us -> 34.2 us  [shifted(): lax.ppermute(array, axis, [(i, (i + step) % count) for i in range(count)])]
    ppermute x9, starting transfers between devices: 35.5 us -> 38.4 us  [swapped(): return lax.ppermute(array, axis, [(i, i ^ bit) for i in range(count)])]
  transfers between devices with their start and end apart: 21 -> 21, of which waited for: 11 -> 10; matrix products, arithmetic and copies ran while one was open for 14% -> 12% of each run, Pallas kernels for 0% -> 4%
where the time goes in v3:
time: 249 us; the launch traced here: 246 us
  starting transfers between devices  140 us (56%)
  waiting for transfers between devices  59 us (24%)
  matrix products  14.3 us (6%)
  local copies, waits for them, and re-layouts  11.5 us (5%)
  other arithmetic  10.5 us (4%)
  Pallas kernels  9.96 us (4%)
    all_to_all x4, starting transfers between devices, exchanged(): return lax.all_to_all(array, axis, split_axis=0, concat_axis=0, tiled=True)  67.2 us
    ppermute x9, starting transfers between devices, swapped(): return lax.ppermute(array, axis, [(i, i ^ bit) for i in range(count)])  38.4 us
    ppermute x8, starting transfers between devices, shifted(): lax.ppermute(array, axis, [(i, (i + step) % count) for i in range(count)])  34.2 us
    all_to_all x4, waiting for transfers between devices, exchanged(): return lax.all_to_all(array, axis, split_axis=0, concat_axis=0, tiled=True)  27.4 us
    ppermute x8, waiting for transfers between devices, shifted(): lax.ppermute(array, axis, [(i, (i + step) % count) for i in range(count)])  23.4 us
    pallas_call x3, Pallas kernels, in_vmem(): pl.pallas_call(kernel, out_shape=shapes, in_specs=[SMEM] + [VMEM] * len(o...  9.96 us
    ppermute x9, waiting for transfers between devices, swapped(): return lax.ppermute(array, axis, [(i, i ^ bit) for i in range(count)])  8.21 us
  transfers between devices with their start and end apart: 21, of which 10 were waited for; matrix products, arithmetic and copies ran while one was open for 12% of the time, Pallas kernels for 4%

profile of v3, /device:TPU:65, one launch (start us, length us, event | category | flops | bytes accessed | tf_op | source)
XLA Modules:
  0.0 246.4 jit_solution(11366562359519688382)
XLA Ops:
  0.7 0.9 copy.188
  1.7 0.9 divide_multiply_fusion
  5.7 45.2 %all-to-all-start = ((bf16[32,8,256]{2,1,0:T(8,128)(2,1)}), bf16[32,8,256]{2,1,0:T(8,128)(2,1)S(1)}, u32[]{:S(2)}, u32[]{:S(2)}) async-start(bf16[32,8,256]{2,1,0:T(8,128)(2,1)} %fusion.31), calls=%async_computation | async-start | bytes 262144 | tf_op jit(solution)/shard_map/all_to_all | solution.py:35
  50.9 1.4 pad_maximum_fusion.own_in
  52.3 3.3 %collective-permute-start.10 = (bf16[2048,256]{1,0:T(8,128)(2,1)S(1)}, bf16[2048,256]{1,0:T(8,128)(2,1)}, u32[]{:S(2)}, u32[]{:S(2)}) collective-permute-start(bf16[2048,256]{1,0:T(8,128)(2,1)S(1)} %pad_maximum_fusion.own_in), channel_id=1, source_target_pairs={{0,1},{1,0},{2,3},{3,2},{4,5},{5,4},{6,7},{7,6},{8,9},{9,8},{10,11... | collective-permute-start | bytes 3145736 | tf_op jit(solution)/shard_map/ppermute | solution.py:31
  55.6 2.1 collective-permute-start.15
  59.0 2.7 %shard_map.185 = (bf16[128,2048]{1,0:T(8,128)(2,1)}, bf16[512,512]{1,0:T(8,128)(2,1)}) custom-call(s32[2]{0:T(128)} %pad_add_fusion.place, bf16[128,2048]{1,0:T(8,128)(2,1)} %hidden_state.1, f32[1,2048]{1,0:T(1,128)} %bitcast.143, s32[128,4]{1,0:T(8,128)} %copy.208.index), custom_call_target="tpu_custom_call" | custom-call | tf_op jit(solution)/shard_map/pallas_call | solution.py:190
  61.8 2.1 fusion.80
  63.9 3.0 %all-to-all-done = bf16[32,8,256]{2,1,0:T(8,128)(2,1)S(1)} async-done(((bf16[32,8,256]{2,1,0:T(8,128)(2,1)}), bf16[32,8,256]{2,1,0:T(8,128)(2,1)S(1)}, u32[]{:S(2)}, u32[]{:S(2)}) %all-to-all-start) | async-done | bytes 131104 | tf_op jit(solution)/shard_map/all_to_all | solution.py:35
  66.8 10.3 %all-to-all-start.2 = ((bf16[32,16,512]{2,1,0:T(8,128)(2,1)}), bf16[32,16,512]{2,1,0:T(8,128)(2,1)S(1)}, u32[]{:S(2)}, u32[]{:S(2)}) async-start(bf16[32,16,512]{2,1,0:T(8,128)(2,1)} %bitcast.131), calls=%async_computation.2 | async-start | bytes 1048576 | tf_op jit(solution)/shard_map/all_to_all | solution.py:35
  77.1 2.0 fusion.7
  79.2 7.4 %collective-permute-start.3 = (bf16[128,128]{0,1:T(8,128)(2,1)}, bf16[128,128]{0,1:T(8,128)(2,1)}, u32[]{:S(2)}, u32[]{:S(2)}) collective-permute-start(bf16[128,128]{0,1:T(8,128)(2,1)} %fusion.7), channel_id=1, source_target_pairs={{0,4},{1,5},{2,6},{3,7},{4,0},{5,1},{6,2},{7,3},{8,12},{9,13},{10,... | collective-permute-start | bytes 98312 | tf_op jit(solution)/shard_map/ppermute | solution.py:31
  86.6 1.1 copy.209
  89.0 1.0 reshape.210
  92.6 1.1 convolution_select_fusion
  93.7 1.7 fusion.63
  95.5 14.9 %all-to-all-done.2 = bf16[32,16,512]{2,1,0:T(8,128)(2,1)S(1)} async-done(((bf16[32,16,512]{2,1,0:T(8,128)(2,1)}), bf16[32,16,512]{2,1,0:T(8,128)(2,1)S(1)}, u32[]{:S(2)}, u32[]{:S(2)}) %all-to-all-start.2) | async-done | bytes 524320 | tf_op jit(solution)/shard_map/all_to_all | solution.py:35
  110.4 4.1 %collective-permute-start.6 = (bf16[512,512]{1,0:T(8,128)(2,1)S(1)}, bf16[512,512]{1,0:T(8,128)(2,1)}, u32[]{:S(2)}, u32[]{:S(2)}) collective-permute-start(bf16[512,512]{1,0:T(8,128)(2,1)S(1)} %bitcast.122), channel_id=1, source_target_pairs={{0,2},{1,3},{2,4},{3,5},{4,6},{5,7},{6,0},{7,1},{8,10},{9,11},{10,... | collective-permute-start | bytes 1572872 | tf_op jit(solution)/shard_map/ppermute | solution.py:26
  114.5 3.8 %collective-permute-start.7 = (bf16[512,512]{1,0:T(8,128)(2,1)S(1)}, bf16[512,512]{1,0:T(8,128)(2,1)}, u32[]{:S(2)}, u32[]{:S(2)}) collective-permute-start(bf16[512,512]{1,0:T(8,128)(2,1)S(1)} %bitcast.123), channel_id=1, source_target_pairs={{0,6},{1,7},{2,0},{3,1},{4,2},{5,3},{6,4},{7,5},{8,14},{9,15},{10,... | collective-permute-start | bytes 1572872 | tf_op jit(solution)/shard_map/ppermute | solution.py:26
  118.3 1.9 fusion.4
  122.0 4.5 %all-to-all-start.1 = ((bf16[32,8,128]{2,1,0:T(8,128)(2,1)}), bf16[32,8,128]{2,1,0:T(8,128)(2,1)S(1)}, u32[]{:S(2)}, u32[]{:S(2)}) async-start(bf16[32,8,128]{2,1,0:T(8,128)(2,1)} %copy.202), calls=%async_computation.1 | async-start | bytes 131072 | tf_op jit(solution)/shard_map/all_to_all | solution.py:35
  127.3 7.2 %collective-permute-done.6.before = bf16[512,512]{1,0:T(8,128)(2,1)} collective-permute-done((bf16[512,512]{1,0:T(8,128)(2,1)S(1)}, bf16[512,512]{1,0:T(8,128)(2,1)}, u32[]{:S(2)}, u32[]{:S(2)}) %collective-permute-start.6) | collective-permute-done | bytes 524320 | tf_op jit(solution)/shard_map/ppermute | solution.py:26
  134.5 1.7 slice.49
  136.2 7.4 %collective-permute-start.8 = (bf16[256,512]{1,0:T(8,128)(2,1)}, bf16[256,512]{1,0:T(8,128)(2,1)}, u32[]{:S(2)}, u32[]{:S(2)}) collective-permute-start(bf16[256,512]{1,0:T(8,128)(2,1)} %slice.49), channel_id=1, source_target_pairs={{0,2},{1,3},{2,4},{3,5},{4,6},{5,7},{6,0},{7,1},{8,10},{9,11},{10,... | collective-permute-start | bytes 786440 | tf_op jit(solution)/shard_map/ppermute | solution.py:26
  143.7 1.7 slice.50
  145.4 3.5 %collective-permute-start.9 = (bf16[256,512]{1,0:T(8,128)(2,1)}, bf16[256,512]{1,0:T(8,128)(2,1)}, u32[]{:S(2)}, u32[]{:S(2)}) collective-permute-start(bf16[256,512]{1,0:T(8,128)(2,1)} %slice.50), channel_id=1, source_target_pairs={{0,6},{1,7},{2,0},{3,1},{4,2},{5,3},{6,4},{7,5},{8,14},{9,15},{10,... | collective-permute-start | bytes 786440 | tf_op jit(solution)/shard_map/ppermute | solution.py:26
  149.5 5.0 %collective-permute-start.4 = (bf16[128,256]{0,1:T(8,128)(2,1)}, bf16[128,256]{0,1:T(8,128)(2,1)}, u32[]{:S(2)}, u32[]{:S(2)}) collective-permute-start(bf16[128,256]{0,1:T(8,128)(2,1)} %pad_maximum_fusion.2), channel_id=1, source_target_pairs={{0,2},{1,3},{2,0},{3,1},{4,6},{5,7},{6,4},{7,5},{8,10},{9,11},{10,... | collective-permute-start | bytes 196616 | tf_op jit(solution)/shard_map/ppermute | solution.py:31
  154.5 10.8 %collective-permute-done.9.far_second = bf16[256,512]{1,0:T(8,128)(2,1)} collective-permute-done((bf16[256,512]{1,0:T(8,128)(2,1)}, bf16[256,512]{1,0:T(8,128)(2,1)}, u32[]{:S(2)}, u32[]{:S(2)}) %collective-permute-start.9) | collective-permute-done | bytes 262176 | tf_op jit(solution)/shard_map/ppermute | solution.py:26
  165.4 4.2 %shard_map.186.own = bf16[512,256]{1,0:T(8,128)(2,1)} custom-call(s32[2]{0:T(128)} %pad_add_fusion.place, bf16[512,512]{1,0:T(8,128)(2,1)} %bitcast.124, bf16[512,512]{1,0:T(8,128)(2,1)} %collective-permute-done.6.before, bf16[512,512]{1,0:T(8,128)(2,1)} %collective-permute-done.7.after, bf16[256,512]{1,0:T(8,128)(2,1)} %collective-permute-done.8.far_first, ...), custom_call_target="tpu_custom_call" | custom-call | tf_op jit(solution)/shard_map/pallas_call | solution.py:190
  169.5 3.5 %collective-permute-start.11 = (bf16[512,256]{1,0:T(8,128)(2,1)}, bf16[512,256]{1,0:T(8,128)(2,1)S(1)}, u32[]{:S(2)}, u32[]{:S(2)}) collective-permute-start(bf16[512,256]{1,0:T(8,128)(2,1)} %shard_map.186.own), channel_id=1, source_target_pairs={{0,2},{1,3},{2,4},{3,5},{4,6},{5,7},{6,0},{7,1},{8,10},{9,11},{10,... | collective-permute-start | bytes 786440 | tf_op jit(solution)/shard_map/ppermute | solution.py:26
  173.1 3.9 %collective-permute-start.12 = (bf16[512,256]{1,0:T(8,128)(2,1)}, bf16[512,256]{1,0:T(8,128)(2,1)S(1)}, u32[]{:S(2)}, u32[]{:S(2)}) collective-permute-start(bf16[512,256]{1,0:T(8,128)(2,1)} %shard_map.186.own), channel_id=1, source_target_pairs={{0,6},{1,7},{2,0},{3,1},{4,2},{5,3},{6,4},{7,5},{8,14},{9,15},{10,... | collective-permute-start | bytes 786440 | tf_op jit(solution)/shard_map/ppermute | solution.py:26
  177.8 4.8 %collective-permute-done.11.before = bf16[512,256]{1,0:T(8,128)(2,1)S(1)} collective-permute-done((bf16[512,256]{1,0:T(8,128)(2,1)}, bf16[512,256]{1,0:T(8,128)(2,1)S(1)}, u32[]{:S(2)}, u32[]{:S(2)}) %collective-permute-start.11) | collective-permute-done | bytes 262176 | tf_op jit(solution)/shard_map/ppermute | solution.py:26
  182.6 2.0 collective-permute-start.13
  184.6 6.0 %collective-permute-start.14 = (bf16[256,256]{1,0:T(8,128)(2,1)S(1)}, bf16[256,256]{1,0:T(8,128)(2,1)S(1)}, u32[]{:S(2)}, u32[]{:S(2)}) collective-permute-start(bf16[256,256]{1,0:T(8,128)(2,1)S(1)} %slice.52), channel_id=1, source_target_pairs={{0,6},{1,7},{2,0},{3,1},{4,2},{5,3},{6,4},{7,5},{8,14},{9,15},{10,... | collective-permute-start | bytes 393224 | tf_op jit(solution)/shard_map/ppermute | solution.py:26
  190.9 1.2 fusion.59
  193.4 3.1 %shard_map.187 = bf16[512,512]{1,0:T(8,128)(2,1)} custom-call(s32[2]{0:T(128)} %pad_add_fusion.place, bf16[512,256]{1,0:T(8,128)(2,1)} %shard_map.186.own, bf16[512,256]{1,0:T(8,128)(2,1)} %copy-done.5, bf16[512,256]{1,0:T(8,128)(2,1)} %copy-done.6, bf16[256,256]{1,0:T(8,128)(2,1)} %copy-done.17, bf16[256,256]{1,0:T(8,128)(2,1)} %copy-done.18, ...), custom_call_target="tpu_custom_call" | custom-call | tf_op jit(solution)/shard_map/pallas_call | solution.py:190
  196.5 7.2 %all-to-all-start.3 = ((bf16[32,16,512]{2,1,0:T(8,128)(2,1)}), bf16[32,16,512]{2,1,0:T(8,128)(2,1)S(1)}, u32[]{:S(2)}, u32[]{:S(2)}) async-start(bf16[32,16,512]{2,1,0:T(8,128)(2,1)} %bitcast.126), calls=%async_computation.3 | async-start | bytes 1048576 | tf_op jit(solution)/shard_map/all_to_all | solution.py:35
  203.7 5.3 %collective-permute-start = (bf16[2,2,16,2048]{3,2,0,1:T(8,128)(2,1)S(1)}, bf16[2,2,16,2048]{3,2,0,1:T(8,128)(2,1)S(1)}, u32[]{:S(2)}, u32[]{:S(2)}) collective-permute-start(bf16[2,2,16,2048]{3,2,0,1:T(8,128)(2,1)S(1)} %fusion.15), channel_id=1, source_target_pairs={{0,1},{1,0},{2,3},{3,2},{4,5},{5,4},{6,7},{7,6},{8,9},{9,8},{10,11... | collective-permute-start | bytes 786440 | tf_op jit(solution)/shard_map/ppermute | solution.py:31
  209.0 0.9 broadcast_select_fusion.3
  209.9 2.0 collective-permute-start.5
  211.9 2.8 %collective-permute-done = bf16[2,2,16,2048]{3,2,0,1:T(8,128)(2,1)S(1)} collective-permute-done((bf16[2,2,16,2048]{3,2,0,1:T(8,128)(2,1)S(1)}, bf16[2,2,16,2048]{3,2,0,1:T(8,128)(2,1)S(1)}, u32[]{:S(2)}, u32[]{:S(2)}) %collective-permute-start) | collective-permute-done | bytes 262176 | tf_op jit(solution)/shard_map/ppermute | solution.py:31
  214.7 3.8 %collective-permute-start.1 = (bf16[2,16,2048]{2,1,0:T(8,128)(2,1)S(1)}, bf16[2,16,2048]{2,1,0:T(8,128)(2,1)S(1)}, u32[]{:S(2)}, u32[]{:S(2)}) collective-permute-start(bf16[2,16,2048]{2,1,0:T(8,128)(2,1)S(1)} %fusion.32), channel_id=1, source_target_pairs={{0,2},{1,3},{2,0},{3,1},{4,6},{5,7},{6,4},{7,5},{8,10},{9,11},{10,... | collective-permute-start | bytes 393224 | tf_op jit(solution)/shard_map/ppermute | solution.py:31
  218.6 4.4 %collective-permute-done.1 = bf16[2,16,2048]{2,1,0:T(8,128)(2,1)S(1)} collective-permute-done((bf16[2,16,2048]{2,1,0:T(8,128)(2,1)S(1)}, bf16[2,16,2048]{2,1,0:T(8,128)(2,1)S(1)}, u32[]{:S(2)}, u32[]{:S(2)}) %collective-permute-start.1) | collective-permute-done | bytes 131104 | tf_op jit(solution)/shard_map/ppermute | solution.py:31
  223.1 4.4 %collective-permute-start.2 = (bf16[16,2048]{1,0:T(8,128)(2,1)S(1)}, bf16[16,2048]{1,0:T(8,128)(2,1)S(1)}, u32[]{:S(2)}, u32[]{:S(2)}) collective-permute-start(bf16[16,2048]{1,0:T(8,128)(2,1)S(1)} %fusion.61), channel_id=1, source_target_pairs={{0,4},{1,5},{2,6},{3,7},{4,0},{5,1},{6,2},{7,3},{8,12},{9,13},{10,... | collective-permute-start | bytes 196616 | tf_op jit(solution)/shard_map/ppermute | solution.py:31
  227.5 9.5 %all-to-all-done.3 = bf16[32,16,512]{2,1,0:T(8,128)(2,1)S(1)} async-done(((bf16[32,16,512]{2,1,0:T(8,128)(2,1)}), bf16[32,16,512]{2,1,0:T(8,128)(2,1)S(1)}, u32[]{:S(2)}, u32[]{:S(2)}) %all-to-all-start.3) | async-done | bytes 524320 | tf_op jit(solution)/shard_map/all_to_all | solution.py:35
  238.6 5.3 %collective-permute-start.16 = (bf16[128,256]{1,0:T(8,128)(2,1)S(1)}, bf16[128,256]{1,0:T(8,128)(2,1)S(1)}, u32[]{:S(2)}, u32[]{:S(2)}) collective-permute-start(bf16[128,256]{1,0:T(8,128)(2,1)S(1)} %slice.60), channel_id=1, source_target_pairs={{0,1},{1,0},{2,3},{3,2},{4,5},{5,4},{6,7},{7,6},{8,9},{9,8},{10,11... | collective-permute-start | bytes 196616 | tf_op jit(solution)/shard_map/ppermute | solution.py:31
  244.6 1.0 collective-permute-done.16
  245.5 0.9 fusion.5
  (128 shorter events, 16.7 us)
Async XLA Ops:
  0.6 190.2 %copy-start = (bf16[256,2048]{1,0:T(8,128)(2,1)S(1)}, bf16[256,2048]{1,0:T(8,128)(2,1)}, u32[]{:S(2)}) copy-start(bf16[256,2048]{1,0:T(8,128)(2,1)} %param.27) | copy-start | bytes 3145732
  0.6 3.0 %copy-start.20 = (bf16[128,256]{1,0:T(8,128)(2,1)S(1)}, bf16[128,256]{1,0:T(8,128)(2,1)}, u32[]{:S(2)}) copy-start(bf16[128,256]{1,0:T(8,128)(2,1)} %param.22) | copy-start | bytes 196612
  3.7 0.6 copy-start.4
  4.7 46.2 %copy-start.15 = (f32[2,2,128,128]{3,2,1,0:T(8,128)}, f32[2,2,128,128]{3,2,1,0:T(8,128)S(1)}, u32[]{:S(2)}) copy-start(f32[2,2,128,128]{3,2,1,0:T(8,128)S(1)} %get-tuple-element.32) | copy-start | bytes 786436
  5.7 61.1 %all-to-all-start = ((bf16[32,8,256]{2,1,0:T(8,128)(2,1)}), bf16[32,8,256]{2,1,0:T(8,128)(2,1)S(1)}, u32[]{:S(2)}, u32[]{:S(2)}) async-start(bf16[32,8,256]{2,1,0:T(8,128)(2,1)} %fusion.31), calls=%async_computation | async-start | bytes 262144 | tf_op jit(solution)/shard_map/all_to_all | solution.py:35
  50.9 6.8 %copy-start.21 = (s32[128,4]{0,1:T(4,128)S(1)}, s32[128,4]{0,1:T(4,128)}, u32[]{:S(2)}) copy-start(s32[128,4]{0,1:T(4,128)} %param.29) | copy-start | bytes 6148
  50.9 10.8 %copy-start.8 = (bf16[2048,128]{1,0:T(8,128)(2,1)S(1)}, bf16[2048,128]{1,0:T(8,128)(2,1)}, u32[]{:S(2)}) copy-start(bf16[2048,128]{1,0:T(8,128)(2,1)} %param.35) | copy-start | bytes 1572868
  52.3 14.5 %copy-start.1 = (bf16[2048,256]{1,0:T(8,128)(2,1)}, bf16[2048,256]{1,0:T(8,128)(2,1)S(1)}, u32[]{:S(2)}) copy-start(bf16[2048,256]{1,0:T(8,128)(2,1)S(1)} %pad_maximum_fusion.own_in) | copy-start | bytes 3145732
  52.3 102.2 %collective-permute-start.10 = (bf16[2048,256]{1,0:T(8,128)(2,1)S(1)}, bf16[2048,256]{1,0:T(8,128)(2,1)}, u32[]{:S(2)}, u32[]{:S(2)}) collective-permute-start(bf16[2048,256]{1,0:T(8,128)(2,1)S(1)} %pad_maximum_fusion.own_in), channel_id=1, source_target_pairs={{0,1},{1,0},{2,3},{3,2},{4,5},{5,4},{6,7},{7,6},{8,9},{9,8},{10,11... | collective-permute-start | bytes 3145736 | tf_op jit(solution)/shard_map/ppermute | solution.py:31
  55.6 136.5 %collective-permute-start.15 = (bf16[1024,256]{1,0:T(8,128)(2,1)}, bf16[1024,256]{1,0:T(8,128)(2,1)}, u32[]{:S(2)}, u32[]{:S(2)}) collective-permute-start(bf16[1024,256]{1,0:T(8,128)(2,1)} %bitcast.32.own_down), channel_id=1, source_target_pairs={{0,1},{1,0},{2,3},{3,2},{4,5},{5,4},{6,7},{7,6},{8,9},{9,8},{10,11... | collective-permute-start | bytes 1572872 | tf_op jit(solution)/shard_map/ppermute | solution.py:31
  61.8 15.4 %copy-start.3 = (bf16[128,2048]{1,0:T(8,128)(2,1)S(1)}, bf16[128,2048]{1,0:T(8,128)(2,1)}, u32[]{:S(2)}) copy-start(bf16[128,2048]{1,0:T(8,128)(2,1)} %get-tuple-element.34) | copy-start | bytes 1572868
  66.8 12.3 %copy-start.9 = (bf16[32,8,256]{2,1,0:T(8,128)(2,1)}, bf16[32,8,256]{2,1,0:T(8,128)(2,1)S(1)}, u32[]{:S(2)}) copy-start(bf16[32,8,256]{2,1,0:T(8,128)(2,1)S(1)} %all-to-all-done) | copy-start | bytes 393220
  66.8 19.8 %copy-start.24 = (f32[128,4]{0,1:T(4,128)S(1)}, f32[128,4]{0,1:T(4,128)}, u32[]{:S(2)}) copy-start(f32[128,4]{0,1:T(4,128)} %param.30) | copy-start | bytes 6148
  66.8 43.6 %all-to-all-start.2 = ((bf16[32,16,512]{2,1,0:T(8,128)(2,1)}), bf16[32,16,512]{2,1,0:T(8,128)(2,1)S(1)}, u32[]{:S(2)}, u32[]{:S(2)}) async-start(bf16[32,16,512]{2,1,0:T(8,128)(2,1)} %bitcast.131), calls=%async_computation.2 | async-start | bytes 1048576 | tf_op jit(solution)/shard_map/all_to_all | solution.py:35
  79.2 47.3 %collective-permute-start.3 = (bf16[128,128]{0,1:T(8,128)(2,1)}, bf16[128,128]{0,1:T(8,128)(2,1)}, u32[]{:S(2)}, u32[]{:S(2)}) collective-permute-start(bf16[128,128]{0,1:T(8,128)(2,1)} %fusion.7), channel_id=1, source_target_pairs={{0,4},{1,5},{2,6},{3,7},{4,0},{5,1},{6,2},{7,3},{8,12},{9,13},{10,... | collective-permute-start | bytes 98312 | tf_op jit(solution)/shard_map/ppermute | solution.py:31
  86.6 1.7 copy-start.19
  90.0 5.5 %copy-start.10 = (bf16[32,8,256]{2,1,0:T(8,128)(2,1)S(1)}, bf16[32,8,256]{2,1,0:T(8,128)(2,1)}, u32[]{:S(2)}) copy-start(bf16[32,8,256]{2,1,0:T(8,128)(2,1)} %copy-done.9) | copy-start | bytes 393220
  110.4 39.0 %copy-start.2 = (bf16[32,16,512]{2,1,0:T(8,128)(2,1)}, bf16[32,16,512]{2,1,0:T(8,128)(2,1)S(1)}, u32[]{:S(2)}) copy-start(bf16[32,16,512]{2,1,0:T(8,128)(2,1)S(1)} %all-to-all-done.2) | copy-start | bytes 1572868
  110.4 24.1 %collective-permute-start.6 = (bf16[512,512]{1,0:T(8,128)(2,1)S(1)}, bf16[512,512]{1,0:T(8,128)(2,1)}, u32[]{:S(2)}, u32[]{:S(2)}) collective-permute-start(bf16[512,512]{1,0:T(8,128)(2,1)S(1)} %bitcast.122), channel_id=1, source_target_pairs={{0,2},{1,3},{2,4},{3,5},{4,6},{5,7},{6,0},{7,1},{8,10},{9,11},{10,... | collective-permute-start | bytes 1572872 | tf_op jit(solution)/shard_map/ppermute | solution.py:26
  114.5 29.2 %collective-permute-start.7 = (bf16[512,512]{1,0:T(8,128)(2,1)S(1)}, bf16[512,512]{1,0:T(8,128)(2,1)}, u32[]{:S(2)}, u32[]{:S(2)}) collective-permute-start(bf16[512,512]{1,0:T(8,128)(2,1)S(1)} %bitcast.123), channel_id=1, source_target_pairs={{0,6},{1,7},{2,0},{3,1},{4,2},{5,3},{6,4},{7,5},{8,14},{9,15},{10,... | collective-permute-start | bytes 1572872 | tf_op jit(solution)/shard_map/ppermute | solution.py:26
  122.0 32.5 %all-to-all-start.1 = ((bf16[32,8,128]{2,1,0:T(8,128)(2,1)}), bf16[32,8,128]{2,1,0:T(8,128)(2,1)S(1)}, u32[]{:S(2)}, u32[]{:S(2)}) async-start(bf16[32,8,128]{2,1,0:T(8,128)(2,1)} %copy.202), calls=%async_computation.1 | async-start | bytes 131072 | tf_op jit(solution)/shard_map/all_to_all | solution.py:35
  127.3 38.1 %copy-start.11 = (bf16[128,128]{0,1:T(8,128)(2,1)}, bf16[128,128]{0,1:T(8,128)(2,1)S(1)}, u32[]{:S(2)}) copy-start(bf16[128,128]{0,1:T(8,128)(2,1)S(1)} %get-tuple-element.113) | copy-start | bytes 98308
  127.3 38.1 %copy-start.13 = (bf16[128,128]{0,1:T(8,128)(2,1)}, bf16[128,128]{0,1:T(8,128)(2,1)S(1)}, u32[]{:S(2)}) copy-start(bf16[128,128]{0,1:T(8,128)(2,1)S(1)} %get-tuple-element.114) | copy-start | bytes 98308
  136.2 18.3 %collective-permute-start.8 = (bf16[256,512]{1,0:T(8,128)(2,1)}, bf16[256,512]{1,0:T(8,128)(2,1)}, u32[]{:S(2)}, u32[]{:S(2)}) collective-permute-start(bf16[256,512]{1,0:T(8,128)(2,1)} %slice.49), channel_id=1, source_target_pairs={{0,2},{1,3},{2,4},{3,5},{4,6},{5,7},{6,0},{7,1},{8,10},{9,11},{10,... | collective-permute-start | bytes 786440 | tf_op jit(solution)/shard_map/ppermute | solution.py:26
  145.4 20.0 %collective-permute-start.9 = (bf16[256,512]{1,0:T(8,128)(2,1)}, bf16[256,512]{1,0:T(8,128)(2,1)}, u32[]{:S(2)}, u32[]{:S(2)}) collective-permute-start(bf16[256,512]{1,0:T(8,128)(2,1)} %slice.50), channel_id=1, source_target_pairs={{0,6},{1,7},{2,0},{3,1},{4,2},{5,3},{6,4},{7,5},{8,14},{9,15},{10,... | collective-permute-start | bytes 786440 | tf_op jit(solution)/shard_map/ppermute | solution.py:26
  149.5 59.5 %collective-permute-start.4 = (bf16[128,256]{0,1:T(8,128)(2,1)}, bf16[128,256]{0,1:T(8,128)(2,1)}, u32[]{:S(2)}, u32[]{:S(2)}) collective-permute-start(bf16[128,256]{0,1:T(8,128)(2,1)} %pad_maximum_fusion.2), channel_id=1, source_target_pairs={{0,2},{1,3},{2,0},{3,1},{4,6},{5,7},{6,4},{7,5},{8,10},{9,11},{10,... | collective-permute-start | bytes 196616 | tf_op jit(solution)/shard_map/ppermute | solution.py:31
  154.5 22.5 %copy-start.7 = (f32[2,2,64,128]{3,2,1,0:T(8,128)S(1)}, f32[2,2,64,128]{3,2,1,0:T(8,128)}, u32[]{:S(2)}) copy-start(f32[2,2,64,128]{3,2,1,0:T(8,128)} %fusion.63) | copy-start | bytes 393220
  154.5 22.5 %copy-start.23 = (f32[2,2,128]{2,1,0:T(2,128)S(1)}, f32[2,2,128]{2,1,0:T(2,128)}, u32[]{:S(2)}) copy-start(f32[2,2,128]{2,1,0:T(2,128)} %copy.195) | copy-start | bytes 6148
  154.5 22.5 %copy-start.16 = (f32[2,2,128,128]{3,2,1,0:T(8,128)S(1)}, f32[2,2,128,128]{3,2,1,0:T(8,128)}, u32[]{:S(2)}) copy-start(f32[2,2,128,128]{3,2,1,0:T(8,128)} %copy-done.15) | copy-start | bytes 786436
  169.5 13.1 %collective-permute-start.11 = (bf16[512,256]{1,0:T(8,128)(2,1)}, bf16[512,256]{1,0:T(8,128)(2,1)S(1)}, u32[]{:S(2)}, u32[]{:S(2)}) collective-permute-start(bf16[512,256]{1,0:T(8,128)(2,1)} %shard_map.186.own), channel_id=1, source_target_pairs={{0,2},{1,3},{2,4},{3,5},{4,6},{5,7},{6,0},{7,1},{8,10},{9,11},{10,... | collective-permute-start | bytes 786440 | tf_op jit(solution)/shard_map/ppermute | solution.py:26
  173.1 11.5 %collective-permute-start.12 = (bf16[512,256]{1,0:T(8,128)(2,1)}, bf16[512,256]{1,0:T(8,128)(2,1)S(1)}, u32[]{:S(2)}, u32[]{:S(2)}) collective-permute-start(bf16[512,256]{1,0:T(8,128)(2,1)} %shard_map.186.own), channel_id=1, source_target_pairs={{0,6},{1,7},{2,0},{3,1},{4,2},{5,3},{6,4},{7,5},{8,14},{9,15},{10,... | collective-permute-start | bytes 786440 | tf_op jit(solution)/shard_map/ppermute | solution.py:26
  182.6 9.4 %copy-start.5 = (bf16[512,256]{1,0:T(8,128)(2,1)}, bf16[512,256]{1,0:T(8,128)(2,1)S(1)}, u32[]{:S(2)}) copy-start(bf16[512,256]{1,0:T(8,128)(2,1)S(1)} %collective-permute-done.11.before) | copy-start | bytes 786436
  182.6 9.4 %collective-permute-start.13 = (bf16[256,256]{1,0:T(8,128)(2,1)S(1)}, bf16[256,256]{1,0:T(8,128)(2,1)S(1)}, u32[]{:S(2)}, u32[]{:S(2)}) collective-permute-start(bf16[256,256]{1,0:T(8,128)(2,1)S(1)} %slice.51), channel_id=1, source_target_pairs={{0,2},{1,3},{2,4},{3,5},{4,6},{5,7},{6,0},{7,1},{8,10},{9,11},{10,... | collective-permute-start | bytes 393224 | tf_op jit(solution)/shard_map/ppermute | solution.py:26
  184.6 7.4 %copy-start.6 = (bf16[512,256]{1,0:T(8,128)(2,1)}, bf16[512,256]{1,0:T(8,128)(2,1)S(1)}, u32[]{:S(2)}) copy-start(bf16[512,256]{1,0:T(8,128)(2,1)S(1)} %collective-permute-done.12.after) | copy-start | bytes 786436
  184.6 7.9 %collective-permute-start.14 = (bf16[256,256]{1,0:T(8,128)(2,1)S(1)}, bf16[256,256]{1,0:T(8,128)(2,1)S(1)}, u32[]{:S(2)}, u32[]{:S(2)}) collective-permute-start(bf16[256,256]{1,0:T(8,128)(2,1)S(1)} %slice.52), channel_id=1, source_target_pairs={{0,6},{1,7},{2,0},{3,1},{4,2},{5,3},{6,4},{7,5},{8,14},{9,15},{10,... | collective-permute-start | bytes 393224 | tf_op jit(solution)/shard_map/ppermute | solution.py:26
  192.1 0.7 copy-start.17
  192.7 0.6 copy-start.18
  196.5 12.5 %copy-start.12 = (bf16[128,128]{0,1:T(8,128)(2,1)S(1)}, bf16[128,128]{0,1:T(8,128)(2,1)}, u32[]{:S(2)}) copy-start(bf16[128,128]{0,1:T(8,128)(2,1)} %copy-done.11) | copy-start | bytes 98308
  196.5 12.6 %copy-start.14 = (bf16[128,128]{0,1:T(8,128)(2,1)S(1)}, bf16[128,128]{0,1:T(8,128)(2,1)}, u32[]{:S(2)}) copy-start(bf16[128,128]{0,1:T(8,128)(2,1)} %copy-done.13) | copy-start | bytes 98308
  196.5 40.6 %all-to-all-start.3 = ((bf16[32,16,512]{2,1,0:T(8,128)(2,1)}), bf16[32,16,512]{2,1,0:T(8,128)(2,1)S(1)}, u32[]{:S(2)}, u32[]{:S(2)}) async-start(bf16[32,16,512]{2,1,0:T(8,128)(2,1)} %bitcast.126), calls=%async_computation.3 | async-start | bytes 1048576 | tf_op jit(solution)/shard_map/all_to_all | solution.py:35
  203.7 10.9 %collective-permute-start = (bf16[2,2,16,2048]{3,2,0,1:T(8,128)(2,1)S(1)}, bf16[2,2,16,2048]{3,2,0,1:T(8,128)(2,1)S(1)}, u32[]{:S(2)}, u32[]{:S(2)}) collective-permute-start(bf16[2,2,16,2048]{3,2,0,1:T(8,128)(2,1)S(1)} %fusion.15), channel_id=1, source_target_pairs={{0,1},{1,0},{2,3},{3,2},{4,5},{5,4},{6,7},{7,6},{8,9},{9,8},{10,11... | collective-permute-start | bytes 786440 | tf_op jit(solution)/shard_map/ppermute | solution.py:31
  209.9 8.7 %collective-permute-start.5 = (bf16[128,512]{0,1:T(8,128)(2,1)S(1)}, bf16[128,512]{0,1:T(8,128)(2,1)S(1)}, u32[]{:S(2)}, u32[]{:S(2)}) collective-permute-start(bf16[128,512]{0,1:T(8,128)(2,1)S(1)} %pad_maximum_fusion.1), channel_id=1, source_target_pairs={{0,1},{1,0},{2,3},{3,2},{4,5},{5,4},{6,7},{7,6},{8,9},{9,8},{10,11... | collective-permute-start | bytes 393224 | tf_op jit(solution)/shard_map/ppermute | solution.py:31
  214.7 22.4 %copy-start.22 = (s32[128,32]{0,1:T(8,128)S(1)}, s32[128,32]{0,1:T(8,128)}, u32[]{:S(2)}) copy-start(s32[128,32]{0,1:T(8,128)} %fusion.8) | copy-start | bytes 49156
  214.7 22.4 %copy-start.25 = (s32[16]{0:T(128)S(1)}, s32[16]{0:T(128)}, u32[]{:S(2)}) copy-start(s32[16]{0:T(128)} %iota_add_fusion) | copy-start | bytes 196
  214.7 8.3 %collective-permute-start.1 = (bf16[2,16,2048]{2,1,0:T(8,128)(2,1)S(1)}, bf16[2,16,2048]{2,1,0:T(8,128)(2,1)S(1)}, u32[]{:S(2)}, u32[]{:S(2)}) collective-permute-start(bf16[2,16,2048]{2,1,0:T(8,128)(2,1)S(1)} %fusion.32), channel_id=1, source_target_pairs={{0,2},{1,3},{2,0},{3,1},{4,6},{5,7},{6,4},{7,5},{8,10},{9,11},{10,... | collective-permute-start | bytes 393224 | tf_op jit(solution)/shard_map/ppermute | solution.py:31
  223.1 20.8 %collective-permute-start.2 = (bf16[16,2048]{1,0:T(8,128)(2,1)S(1)}, bf16[16,2048]{1,0:T(8,128)(2,1)S(1)}, u32[]{:S(2)}, u32[]{:S(2)}) collective-permute-start(bf16[16,2048]{1,0:T(8,128)(2,1)S(1)} %fusion.61), channel_id=1, source_target_pairs={{0,4},{1,5},{2,6},{3,7},{4,0},{5,1},{6,2},{7,3},{8,12},{9,13},{10,... | collective-permute-start | bytes 196616 | tf_op jit(solution)/shard_map/ppermute | solution.py:31
  238.6 6.9 %collective-permute-start.16 = (bf16[128,256]{1,0:T(8,128)(2,1)S(1)}, bf16[128,256]{1,0:T(8,128)(2,1)S(1)}, u32[]{:S(2)}, u32[]{:S(2)}) collective-permute-start(bf16[128,256]{1,0:T(8,128)(2,1)S(1)} %slice.60), channel_id=1, source_target_pairs={{0,1},{1,0},{2,3},{3,2},{4,5},{5,4},{6,7},{7,6},{8,9},{9,8},{10,11... | collective-permute-start | bytes 196616 | tf_op jit(solution)/shard_map/ppermute | solution.py:31

commit v4 on v3

--- a/solution.py
+++ b/solution.py
@@ -181,66 +181,61 @@
 
 
 VMEM = pl.BlockSpec(memory_space=pltpu.VMEM)
-SMEM = pl.BlockSpec(memory_space=pltpu.SMEM)
 
 
 def in_vmem(kernel, shapes, *operands):
-    member = lax.axis_index("tp")
-    place = jnp.stack([member >> 1, member & 1])
     return pl.pallas_call(
         kernel,
         out_shape=shapes,
-        in_specs=[SMEM] + [VMEM] * len(operands),
+        in_specs=[VMEM] * len(operands),
         out_specs=jax.tree.map(lambda _: VMEM, shapes),
-    )(place, *operands)
-
-
-def select_kernel(experts, place, hidden_state, gain, index, normed, outgoing):
-    tokens, top = index.shape
+    )(*operands)
+
+
+def select_kernel(experts, hidden_state, gain, index, normed, outgoing):
+    top, tokens = index.shape
     slots, width = outgoing.shape
     half = slots // experts
+    member = lax.axis_index("tp")
     features = hidden_state[...].astype(jnp.float32)
     factor = lax.rsqrt(jnp.mean(features * features, axis=1, keepdims=True) + EPSILON)
     normed[...] = (features * factor * gain[...]).astype(jnp.bfloat16)
-    expert = lax.broadcasted_iota(jnp.int32, (tokens, experts), 1)
-    named = [index[:, j : j + 1] == expert for j in range(top)]
-    chosen = named[0]
-    for other in named[1:]:
-        chosen = chosen | other
-    earlier = lax.broadcasted_iota(jnp.int32, (tokens, tokens), 1) < lax.broadcasted_iota(
-        jnp.int32, (tokens, tokens), 0
+    expert = lax.broadcasted_iota(jnp.int32, (experts, tokens), 0)
+    chosen = index[0:1, :] == expert
+    for j in range(1, top):
+        chosen = chosen | (index[j : j + 1, :] == expert)
+    earlier = lax.broadcasted_iota(jnp.int32, (tokens, tokens), 0) < lax.broadcasted_iota(
+        jnp.int32, (tokens, tokens), 1
     )
     one = jnp.float32(1)
     zero = jnp.float32(0)
     places = jnp.dot(
+        jnp.where(chosen, one, zero).astype(jnp.bfloat16),
         jnp.where(earlier, one, zero).astype(jnp.bfloat16),
-        jnp.where(chosen, one, zero).astype(jnp.bfloat16),
         preferred_element_type=jnp.float32,
     )
     places = jnp.where(chosen, places, -one).astype(jnp.bfloat16)
-    slot = lax.broadcasted_iota(jnp.int32, (experts, slots), 1)
+    slot = lax.broadcasted_iota(jnp.int32, (slots, experts), 0)
     spread = jnp.where(
-        slot // half == lax.broadcasted_iota(jnp.int32, (experts, slots), 0), one, zero
+        slot // half == lax.broadcasted_iota(jnp.int32, (slots, experts), 1), one, zero
     ).astype(jnp.bfloat16)
-    wanted = jnp.dot(places, spread, preferred_element_type=jnp.float32).astype(jnp.int32)
-    own = lax.broadcasted_iota(jnp.int32, (tokens, slots), 1) % half + place[1] * half
+    wanted = jnp.dot(spread, places, preferred_element_type=jnp.float32).astype(jnp.int32)
+    own = lax.broadcasted_iota(jnp.int32, (slots, tokens), 0) % half + (member & 1) * half
     filled = jnp.where(wanted == own, one, zero).astype(jnp.bfloat16)
-    start = pl.multiple_of(place[0] * width, width)
-    outgoing[...] = lax.dot_general(
-        filled,
-        normed[:, pl.ds(start, width)],
-        (((0,), (0,)), ((), ())),
-        preferred_element_type=jnp.float32,
+    start = pl.multiple_of((member >> 1) * width, width)
+    outgoing[...] = jnp.dot(
+        filled, normed[:, pl.ds(start, width)], preferred_element_type=jnp.float32
     ).astype(jnp.bfloat16)
 
 
-def around_product(place, pieces, matrix):
+def around_product(pieces, matrix):
     own, before, after, far_first, far_second = pieces
     depth = own.shape[1]
     count = matrix.shape[0] // depth
+    quad = lax.axis_index("tp") >> 1
 
     def block(step):
-        start = pl.multiple_of(((place[0] + step) & (count - 1)) * depth, depth)
+        start = pl.multiple_of(((quad + step) & (count - 1)) * depth, depth)
         return matrix[pl.ds(start, depth), :]
 
     def dot(piece, step):
@@ -251,7 +246,9 @@
     return (near[:middle] + dot(far_first[...], 2), near[middle:] + dot(far_second[...], 2))
 
 
-def hidden_kernel(place, own, before, after, far_first, far_second, own_in, partner_in, hidden):
+def hidden_kernel(
+    own, before, after, far_first, far_second, own_in, partner_in, hidden, hidden_first, hidden_second
+):
     pieces = (own, before, after, far_first, far_second)
     units = own_in.shape[1] // 2
     middle = far_first.shape[0]
@@ -260,22 +257,22 @@
         sides.append(
             [
                 (jax.nn.silu(both[:, :units]) * both[:, units:]).astype(jnp.bfloat16)
-                for both in around_product(place, pieces, matrix)
+                for both in around_product(pieces, matrix)
             ]
         )
-    even = place[1] == 0
-    for k in range(2):
-        rows = pl.ds(k * middle, middle)
-        hidden[rows, :units] = jnp.where(even, sides[0][k], sides[1][k])
-        hidden[rows, units:] = jnp.where(even, sides[1][k], sides[0][k])
-
-
-def down_kernel(place, own, before, after, far_first, far_second, own_down, partner_down, answers):
+    even = (lax.axis_index("tp") & 1) == 0
+    for k, part in enumerate((hidden_first, hidden_second)):
+        part[:, :units] = jnp.where(even, sides[0][k], sides[1][k])
+        part[:, units:] = jnp.where(even, sides[1][k], sides[0][k])
+        hidden[pl.ds(k * middle, middle), :] = part[...]
+
+
+def down_kernel(own, before, after, far_first, far_second, own_down, partner_down, answers):
     pieces = (own, before, after, far_first, far_second)
     middle = far_first.shape[0]
     width = own_down.shape[1]
     for side, matrix in enumerate((own_down, partner_down)):
-        for k, part in enumerate(around_product(place, pieces, matrix)):
+        for k, part in enumerate(around_product(pieces, matrix)):
             answers[pl.ds(k * middle, middle), pl.ds(side * width, width)] = part.astype(
                 jnp.bfloat16
             )
@@ -320,7 +317,7 @@
         ),
         expert_hidden_state,
         expert_norm_gain[None, :],
-        chosen_expert_index,
+        chosen_expert_index.T,
     )
     arrived = exchanged(outgoing.reshape(devices, half, width_in), EP)
     chunk = arrived.reshape(devices * half, width_in)
@@ -350,23 +347,30 @@
         preferred_element_type=jnp.float32,
     )
 
-    def all_around(piece):
-        before = shifted(piece, "tp", 2)
-        after = shifted(piece, "tp", -2)
-        far = [shifted(before[:middle], "tp", 2), shifted(after[middle:], "tp", -2)]
-        return (piece, before, after, *far)
-
-    hidden = in_vmem(
+    before = shifted(chunk, "tp", 2)
+    after = shifted(chunk, "tp", -2)
+    far = [shifted(before[:middle], "tp", 2), shifted(after[middle:], "tp", -2)]
+    part_shape = jax.ShapeDtypeStruct((middle, 2 * units), jnp.bfloat16)
+    hidden, hidden_first, hidden_second = in_vmem(
         hidden_kernel,
-        jax.ShapeDtypeStruct((chunk.shape[0], 2 * units), jnp.bfloat16),
-        *all_around(chunk),
+        (jax.ShapeDtypeStruct((chunk.shape[0], 2 * units), jnp.bfloat16), part_shape, part_shape),
+        chunk,
+        before,
+        after,
+        *far,
         own_in,
         partner_in,
     )
+    far = [shifted(hidden_first, "tp", 4), shifted(hidden_second, "tp", -4)]
+    before = shifted(hidden, "tp", 2)
+    after = shifted(hidden, "tp", -2)
     answers = in_vmem(
         down_kernel,
         jax.ShapeDtypeStruct((chunk.shape[0], 2 * width_out), jnp.bfloat16),
-        *all_around(hidden),
+        hidden,
+        before,
+        after,
+        *far,
         own_down,
         partner_down,
     )

time: 249 us -> 267 us (1.072)
  waiting for transfers between devices: 59 us -> 79.2 us
  starting transfers between devices: 140 us -> 148 us
  matrix products: 14.3 us -> 11.4 us
  local copies, waits for them, and re-layouts: 11.5 us -> 8.73 us
  other arithmetic: 10.5 us -> 7.83 us
    all_to_all x4, waiting for transfers between devices: 27.4 us -> 39.8 us  [exchanged(): return lax.all_to_all(array, axis, split_axis=0, concat_axis=0, tiled=True)]
    all_to_all x4, starting transfers between devices: 67.2 us -> 76 us  [exchanged(): return lax.all_to_all(array, axis, split_axis=0, concat_axis=0, tiled=True)]
    ppermute x8, waiting for transfers between devices: 23.4 us -> 27.6 us  [shifted(): lax.ppermute(array, axis, [(i, (i + step) % count) for i in range(count)])]
    ppermute x9, waiting for transfers between devices: 8.21 us -> 11.7 us  [swapped(): return lax.ppermute(array, axis, [(i, i ^ bit) for i in range(count)])]
  transfers between devices with their start and end apart: 21 -> 21, of which waited for: 10 -> 13; matrix products, arithmetic and copies ran while one was open for 12% -> 9% of each run, Pallas kernels for 4% -> 4%
where the time goes in v4:
time: 267 us; the launch traced here: 266 us
  starting transfers between devices  148 us (55%)
  waiting for transfers between devices  79.2 us (30%)
  matrix products  11.4 us (4%)
  Pallas kernels  9.67 us (4%)
  local copies, waits for them, and re-layouts  8.73 us (3%)
  other arithmetic  7.83 us (3%)
    all_to_all x4, starting transfers between devices, exchanged(): return lax.all_to_all(array, axis, split_axis=0, concat_axis=0, tiled=True)  76 us
    all_to_all x4, waiting for transfers between devices, exchanged(): return lax.all_to_all(array, axis, split_axis=0, concat_axis=0, tiled=True)  39.8 us
    ppermute x9, starting transfers between devices, swapped(): return lax.ppermute(array, axis, [(i, i ^ bit) for i in range(count)])  39.8 us
    ppermute x8, starting transfers between devices, shifted(): lax.ppermute(array, axis, [(i, (i + step) % count) for i in range(count)])  31.9 us
    ppermute x8, waiting for transfers between devices, shifted(): lax.ppermute(array, axis, [(i, (i + step) % count) for i in range(count)])  27.6 us
    ppermute x9, waiting for transfers between devices, swapped(): return lax.ppermute(array, axis, [(i, i ^ bit) for i in range(count)])  11.7 us
    pallas_call x3, Pallas kernels, in_vmem(): pl.pallas_call(kernel, out_shape=shapes, in_specs=[VMEM] * len(operands),...  9.67 us
  transfers between devices with their start and end apart: 21, of which 13 were waited for; matrix products, arithmetic and copies ran while one was open for 9% of the time, Pallas kernels for 4%

profile of v4, /device:TPU:65, one launch (start us, length us, event | category | flops | bytes accessed | tf_op | source)
XLA Modules:
  0.0 266.1 jit_solution(17865801660400742883)
XLA Ops:
  0.7 1.4 pad_maximum_fusion.own_in
  2.1 4.2 %collective-permute-start.10 = (bf16[2048,256]{1,0:T(8,128)(2,1)S(1)}, bf16[2048,256]{1,0:T(8,128)(2,1)}, u32[]{:S(2)}, u32[]{:S(2)}) collective-permute-start(bf16[2048,256]{1,0:T(8,128)(2,1)S(1)} %pad_maximum_fusion.own_in), channel_id=1, source_target_pairs={{0,1},{1,0},{2,3},{3,2},{4,5},{5,4},{6,7},{7,6},{8,9},{9,8},{10,11... | collective-permute-start | bytes 3145736 | tf_op jit(solution)/shard_map/ppermute | solution.py:31
  6.3 2.0 collective-permute-start.15
  9.6 1.6 while.13
  12.3 45.0 %all-to-all-start = ((bf16[32,8,256]{2,1,0:T(8,128)(2,1)}), bf16[32,8,256]{2,1,0:T(8,128)(2,1)S(1)}, u32[]{:S(2)}, u32[]{:S(2)}) async-start(bf16[32,8,256]{2,1,0:T(8,128)(2,1)} %fusion.31), calls=%async_computation | async-start | bytes 262144 | tf_op jit(solution)/shard_map/all_to_all | solution.py:35
  57.3 2.4 shard_map.185
  59.7 1.4 fusion.80
  61.2 2.1 fusion.7
  63.3 7.7 %collective-permute-start.3 = (bf16[128,128]{0,1:T(8,128)(2,1)}, bf16[128,128]{0,1:T(8,128)(2,1)}, u32[]{:S(2)}, u32[]{:S(2)}) collective-permute-start(bf16[128,128]{0,1:T(8,128)(2,1)} %fusion.7), channel_id=1, source_target_pairs={{0,4},{1,5},{2,6},{3,7},{4,0},{5,1},{6,2},{7,3},{8,12},{9,13},{10,... | collective-permute-start | bytes 98312 | tf_op jit(solution)/shard_map/ppermute | solution.py:31
  71.0 0.8 copy.201
  73.2 12.1 %all-to-all-start.2 = ((bf16[32,16,512]{2,1,0:T(8,128)(2,1)}), bf16[32,16,512]{2,1,0:T(8,128)(2,1)S(1)}, u32[]{:S(2)}, u32[]{:S(2)}) async-start(bf16[32,16,512]{2,1,0:T(8,128)(2,1)} %bitcast.130), calls=%async_computation.2 | async-start | bytes 1048576 | tf_op jit(solution)/shard_map/all_to_all | solution.py:35
  87.4 1.2 fusion.4
  89.4 29.2 %all-to-all-done.2 = bf16[32,16,512]{2,1,0:T(8,128)(2,1)S(1)} async-done(((bf16[32,16,512]{2,1,0:T(8,128)(2,1)}), bf16[32,16,512]{2,1,0:T(8,128)(2,1)S(1)}, u32[]{:S(2)}, u32[]{:S(2)}) %all-to-all-start.2) | async-done | bytes 524320 | tf_op jit(solution)/shard_map/all_to_all | solution.py:35
  118.6 4.8 %all-to-all-start.1 = ((bf16[32,8,128]{2,1,0:T(8,128)(2,1)}), bf16[32,8,128]{2,1,0:T(8,128)(2,1)}, u32[]{:S(2)}, u32[]{:S(2)}) async-start(bf16[32,8,128]{2,1,0:T(8,128)(2,1)} %copy.195), calls=%async_computation.1 | async-start | bytes 131072 | tf_op jit(solution)/shard_map/all_to_all | solution.py:35
  123.5 2.6 collective-permute-start.6
  126.0 4.9 %collective-permute-start.7 = (bf16[512,512]{1,0:T(8,128)(2,1)S(1)}, bf16[512,512]{1,0:T(8,128)(2,1)}, u32[]{:S(2)}, u32[]{:S(2)}) collective-permute-start(bf16[512,512]{1,0:T(8,128)(2,1)S(1)} %bitcast.124), channel_id=1, source_target_pairs={{0,6},{1,7},{2,0},{3,1},{4,2},{5,3},{6,4},{7,5},{8,14},{9,15},{10,... | collective-permute-start | bytes 1572872 | tf_op jit(solution)/shard_map/ppermute | solution.py:26
  131.0 0.8 broadcast_select_fusion.5
  133.0 4.0 %all-to-all-done.1 = bf16[32,8,128]{2,1,0:T(8,128)(2,1)} async-done(((bf16[32,8,128]{2,1,0:T(8,128)(2,1)}), bf16[32,8,128]{2,1,0:T(8,128)(2,1)}, u32[]{:S(2)}, u32[]{:S(2)}) %all-to-all-start.1) | async-done | bytes 65568 | tf_op jit(solution)/shard_map/all_to_all | solution.py:35
  137.0 0.9 bitcast_convert_fusion
  137.8 9.2 %collective-permute-done.6.before = bf16[512,512]{1,0:T(8,128)(2,1)S(1)} collective-permute-done((bf16[512,512]{1,0:T(8,128)(2,1)S(1)}, bf16[512,512]{1,0:T(8,128)(2,1)S(1)}, u32[]{:S(2)}, u32[]{:S(2)}) %collective-permute-start.6) | collective-permute-done | bytes 524320 | tf_op jit(solution)/shard_map/ppermute | solution.py:26
  147.1 0.8 slice.41
  147.9 1.9 collective-permute-start.8
  149.8 3.8 %collective-permute-done.7.after = bf16[512,512]{1,0:T(8,128)(2,1)} collective-permute-done((bf16[512,512]{1,0:T(8,128)(2,1)S(1)}, bf16[512,512]{1,0:T(8,128)(2,1)}, u32[]{:S(2)}, u32[]{:S(2)}) %collective-permute-start.7) | collective-permute-done | bytes 524320 | tf_op jit(solution)/shard_map/ppermute | solution.py:26
  153.6 1.7 slice.42
  155.2 5.5 %collective-permute-start.9 = (bf16[256,512]{1,0:T(8,128)(2,1)}, bf16[256,512]{1,0:T(8,128)(2,1)}, u32[]{:S(2)}, u32[]{:S(2)}) collective-permute-start(bf16[256,512]{1,0:T(8,128)(2,1)} %slice.42), channel_id=1, source_target_pairs={{0,6},{1,7},{2,0},{3,1},{4,2},{5,3},{6,4},{7,5},{8,14},{9,15},{10,... | collective-permute-start | bytes 786440 | tf_op jit(solution)/shard_map/ppermute | solution.py:26
  160.7 2.1 multiply_reduce_fusion
  162.9 1.0 copy.197
  164.0 7.6 %collective-permute-done.9.far_second = bf16[256,512]{1,0:T(8,128)(2,1)} collective-permute-done((bf16[256,512]{1,0:T(8,128)(2,1)}, bf16[256,512]{1,0:T(8,128)(2,1)}, u32[]{:S(2)}, u32[]{:S(2)}) %collective-permute-start.9) | collective-permute-done | bytes 262176 | tf_op jit(solution)/shard_map/ppermute | solution.py:26
  171.5 4.2 %shard_map.186 = (bf16[512,256]{1,0:T(8,128)(2,1)}, bf16[256,256]{1,0:T(8,128)(2,1)}, bf16[256,256]{1,0:T(8,128)(2,1)}) custom-call(bf16[512,512]{1,0:T(8,128)(2,1)} %bitcast.125, bf16[512,512]{1,0:T(8,128)(2,1)} %copy-done.5, bf16[512,512]{1,0:T(8,128)(2,1)} %collective-permute-done.7.after, bf16[256,512]{1,0:T(8,128)(2,1)} %collective-permute-done.8.far_first, ...), custom_call_target="tpu_custom_call" | custom-call | tf_op jit(solution)/shard_map/pallas_call | solution.py:187
  175.8 4.3 %collective-permute-start.11 = (bf16[512,256]{1,0:T(8,128)(2,1)}, bf16[512,256]{1,0:T(8,128)(2,1)S(1)}, u32[]{:S(2)}, u32[]{:S(2)}) collective-permute-start(bf16[512,256]{1,0:T(8,128)(2,1)} %get-tuple-element.39.own), channel_id=1, source_target_pairs={{0,2},{1,3},{2,4},{3,5},{4,6},{5,7},{6,0},{7,1},{8,10},{9,11},{10,... | collective-permute-start | bytes 786440 | tf_op jit(solution)/shard_map/ppermute | solution.py:26
  180.1 3.6 %collective-permute-start.12 = (bf16[512,256]{1,0:T(8,128)(2,1)}, bf16[512,256]{1,0:T(8,128)(2,1)S(1)}, u32[]{:S(2)}, u32[]{:S(2)}) collective-permute-start(bf16[512,256]{1,0:T(8,128)(2,1)} %get-tuple-element.39.own), channel_id=1, source_target_pairs={{0,6},{1,7},{2,0},{3,1},{4,2},{5,3},{6,4},{7,5},{8,14},{9,15},{10,... | collective-permute-start | bytes 786440 | tf_op jit(solution)/shard_map/ppermute | solution.py:26
  183.6 5.4 %collective-permute-start.13 = (bf16[256,256]{1,0:T(8,128)(2,1)}, bf16[256,256]{1,0:T(8,128)(2,1)S(1)}, u32[]{:S(2)}, u32[]{:S(2)}) collective-permute-start(bf16[256,256]{1,0:T(8,128)(2,1)} %get-tuple-element.40), channel_id=1, source_target_pairs={{0,4},{1,5},{2,6},{3,7},{4,0},{5,1},{6,2},{7,3},{8,12},{9,13},{10,... | collective-permute-start | bytes 393224 | tf_op jit(solution)/shard_map/ppermute | solution.py:26
  189.0 3.8 %collective-permute-start.14 = (bf16[256,256]{1,0:T(8,128)(2,1)}, bf16[256,256]{1,0:T(8,128)(2,1)S(1)}, u32[]{:S(2)}, u32[]{:S(2)}) collective-permute-start(bf16[256,256]{1,0:T(8,128)(2,1)} %get-tuple-element.41), channel_id=1, source_target_pairs={{0,4},{1,5},{2,6},{3,7},{4,0},{5,1},{6,2},{7,3},{8,12},{9,13},{10,... | collective-permute-start | bytes 393224 | tf_op jit(solution)/shard_map/ppermute | solution.py:26
  194.0 2.7 %collective-permute-start.4 = (bf16[128,256]{0,1:T(8,128)(2,1)S(1)}, bf16[128,256]{0,1:T(8,128)(2,1)S(1)}, u32[]{:S(2)}, u32[]{:S(2)}) collective-permute-start(bf16[128,256]{0,1:T(8,128)(2,1)S(1)} %copy-done.20), channel_id=1, source_target_pairs={{0,2},{1,3},{2,0},{3,1},{4,6},{5,7},{6,4},{7,5},{8,10},{9,11},{10,... | collective-permute-start | bytes 196616 | tf_op jit(solution)/shard_map/ppermute | solution.py:31
  196.7 2.3 collective-permute-done.14.far_second
  198.9 4.8 %collective-permute-done.12.after = bf16[512,256]{1,0:T(8,128)(2,1)S(1)} collective-permute-done((bf16[512,256]{1,0:T(8,128)(2,1)}, bf16[512,256]{1,0:T(8,128)(2,1)S(1)}, u32[]{:S(2)}, u32[]{:S(2)}) %collective-permute-start.12) | collective-permute-done | bytes 262176 | tf_op jit(solution)/shard_map/ppermute | solution.py:26
  204.5 3.0 %shard_map.187 = bf16[512,512]{1,0:T(8,128)(2,1)} custom-call(bf16[512,256]{1,0:T(8,128)(2,1)} %get-tuple-element.39.own, bf16[512,256]{1,0:T(8,128)(2,1)} %copy-done.12, bf16[512,256]{1,0:T(8,128)(2,1)} %copy-done.13, bf16[256,256]{1,0:T(8,128)(2,1)} %copy-done.14, bf16[256,256]{1,0:T(8,128)(2,1)} %copy-done.15, bf16[1024,256]{1,0:T(8,128)(2,1)} %bitcast.31.own_down, ...), custom_call_target="tpu_custom_call" | custom-call | tf_op jit(solution)/shard_map/pallas_call | solution.py:187
  207.5 14.0 %all-to-all-start.3 = ((bf16[32,16,512]{2,1,0:T(8,128)(2,1)}), bf16[32,16,512]{2,1,0:T(8,128)(2,1)S(1)}, u32[]{:S(2)}, u32[]{:S(2)}) async-start(bf16[32,16,512]{2,1,0:T(8,128)(2,1)} %bitcast.121), calls=%async_computation.3 | async-start | bytes 1048576 | tf_op jit(solution)/shard_map/all_to_all | solution.py:35
  221.6 6.8 %collective-permute-start = (bf16[2,2,16,2048]{3,2,0,1:T(8,128)(2,1)S(1)}, bf16[2,2,16,2048]{3,2,0,1:T(8,128)(2,1)S(1)}, u32[]{:S(2)}, u32[]{:S(2)}) collective-permute-start(bf16[2,2,16,2048]{3,2,0,1:T(8,128)(2,1)S(1)} %fusion.15), channel_id=1, source_target_pairs={{0,1},{1,0},{2,3},{3,2},{4,5},{5,4},{6,7},{7,6},{8,9},{9,8},{10,11... | collective-permute-start | bytes 786440 | tf_op jit(solution)/shard_map/ppermute | solution.py:31
  228.5 2.0 collective-permute-start.5
  230.4 3.9 %collective-permute-done = bf16[2,2,16,2048]{3,2,0,1:T(8,128)(2,1)S(1)} collective-permute-done((bf16[2,2,16,2048]{3,2,0,1:T(8,128)(2,1)S(1)}, bf16[2,2,16,2048]{3,2,0,1:T(8,128)(2,1)S(1)}, u32[]{:S(2)}, u32[]{:S(2)}) %collective-permute-start) | collective-permute-done | bytes 262176 | tf_op jit(solution)/shard_map/ppermute | solution.py:31
  234.5 2.0 collective-permute-start.1
  237.2 5.8 %collective-permute-done.1 = bf16[2,16,2048]{2,1,0:T(8,128)(2,1)S(1)} collective-permute-done((bf16[2,16,2048]{2,1,0:T(8,128)(2,1)S(1)}, bf16[2,16,2048]{2,1,0:T(8,128)(2,1)S(1)}, u32[]{:S(2)}, u32[]{:S(2)}) %collective-permute-start.1) | collective-permute-done | bytes 131104 | tf_op jit(solution)/shard_map/ppermute | solution.py:31
  243.1 5.6 %collective-permute-start.2 = (bf16[16,2048]{1,0:T(8,128)(2,1)S(1)}, bf16[16,2048]{1,0:T(8,128)(2,1)S(1)}, u32[]{:S(2)}, u32[]{:S(2)}) collective-permute-start(bf16[16,2048]{1,0:T(8,128)(2,1)S(1)} %fusion.61), channel_id=1, source_target_pairs={{0,4},{1,5},{2,6},{3,7},{4,0},{5,1},{6,2},{7,3},{8,12},{9,13},{10,... | collective-permute-start | bytes 196616 | tf_op jit(solution)/shard_map/ppermute | solution.py:31
  248.7 6.1 %all-to-all-done.3 = bf16[32,16,512]{2,1,0:T(8,128)(2,1)S(1)} async-done(((bf16[32,16,512]{2,1,0:T(8,128)(2,1)}), bf16[32,16,512]{2,1,0:T(8,128)(2,1)S(1)}, u32[]{:S(2)}, u32[]{:S(2)}) %all-to-all-start.3) | async-done | bytes 524320 | tf_op jit(solution)/shard_map/all_to_all | solution.py:35
  256.4 6.8 %collective-permute-start.16 = (bf16[128,256]{1,0:T(8,128)(2,1)S(1)}, bf16[128,256]{1,0:T(8,128)(2,1)S(1)}, u32[]{:S(2)}, u32[]{:S(2)}) collective-permute-start(bf16[128,256]{1,0:T(8,128)(2,1)S(1)} %slice.50), channel_id=1, source_target_pairs={{0,1},{1,0},{2,3},{3,2},{4,5},{5,4},{6,7},{7,6},{8,9},{9,8},{10,11... | collective-permute-start | bytes 196616 | tf_op jit(solution)/shard_map/ppermute | solution.py:31
  263.9 1.3 collective-permute-done.16
  265.2 0.9 fusion.5
  (130 shorter events, 14.3 us)
Async XLA Ops:
  0.6 192.5 %copy-start = (bf16[256,2048]{1,0:T(8,128)(2,1)S(1)}, bf16[256,2048]{1,0:T(8,128)(2,1)}, u32[]{:S(2)}) copy-start(bf16[256,2048]{1,0:T(8,128)(2,1)} %param.27) | copy-start | bytes 3145732
  0.6 7.7 %copy-start.25 = (f32[128,2]{0,1:T(2,128)S(1)}, f32[128,2]{0,1:T(2,128)}, u32[]{:S(2)}) copy-start(f32[128,2]{0,1:T(2,128)} %param.25) | copy-start | bytes 3076
  0.7 8.0 %copy-start.16 = (bf16[128,256]{1,0:T(8,128)(2,1)S(1)}, bf16[128,256]{1,0:T(8,128)(2,1)}, u32[]{:S(2)}) copy-start(bf16[128,256]{1,0:T(8,128)(2,1)} %param.21) | copy-start | bytes 196612
  0.7 8.0 %copy-start.26 = (f32[256]{0:T(256)S(1)}, f32[256]{0:T(256)}, u32[]{:S(2)}) copy-start(f32[256]{0:T(256)} %param.24) | copy-start | bytes 3076
  2.1 7.5 %copy-start.1 = (bf16[2048,256]{1,0:T(8,128)(2,1)}, bf16[2048,256]{1,0:T(8,128)(2,1)S(1)}, u32[]{:S(2)}) copy-start(bf16[2048,256]{1,0:T(8,128)(2,1)S(1)} %pad_maximum_fusion.own_in) | copy-start | bytes 3145732
  2.1 7.1 %copy-start.19 = (bf16[128,256]{1,0:T(8,128)(2,1)S(1)}, bf16[128,256]{1,0:T(8,128)(2,1)}, u32[]{:S(2)}) copy-start(bf16[128,256]{1,0:T(8,128)(2,1)} %param.22) | copy-start | bytes 196612
  2.1 161.8 %collective-permute-start.10 = (bf16[2048,256]{1,0:T(8,128)(2,1)S(1)}, bf16[2048,256]{1,0:T(8,128)(2,1)}, u32[]{:S(2)}, u32[]{:S(2)}) collective-permute-start(bf16[2048,256]{1,0:T(8,128)(2,1)S(1)} %pad_maximum_fusion.own_in), channel_id=1, source_target_pairs={{0,1},{1,0},{2,3},{3,2},{4,5},{5,4},{6,7},{7,6},{8,9},{9,8},{10,11... | collective-permute-start | bytes 3145736 | tf_op jit(solution)/shard_map/ppermute | solution.py:31
  6.3 187.1 %collective-permute-start.15 = (bf16[1024,256]{1,0:T(8,128)(2,1)}, bf16[1024,256]{1,0:T(8,128)(2,1)}, u32[]{:S(2)}, u32[]{:S(2)}) collective-permute-start(bf16[1024,256]{1,0:T(8,128)(2,1)} %bitcast.31.own_down), channel_id=1, source_target_pairs={{0,1},{1,0},{2,3},{3,2},{4,5},{5,4},{6,7},{7,6},{8,9},{9,8},{10,11... | collective-permute-start | bytes 1572872 | tf_op jit(solution)/shard_map/ppermute | solution.py:31
  11.2 48.5 %copy-start.6 = (bf16[2048,128]{1,0:T(8,128)(2,1)S(1)}, bf16[2048,128]{1,0:T(8,128)(2,1)}, u32[]{:S(2)}) copy-start(bf16[2048,128]{1,0:T(8,128)(2,1)} %param.35) | copy-start | bytes 1572868
  12.3 60.9 %all-to-all-start = ((bf16[32,8,256]{2,1,0:T(8,128)(2,1)}), bf16[32,8,256]{2,1,0:T(8,128)(2,1)S(1)}, u32[]{:S(2)}, u32[]{:S(2)}) async-start(bf16[32,8,256]{2,1,0:T(8,128)(2,1)} %fusion.31), calls=%async_computation | async-start | bytes 262144 | tf_op jit(solution)/shard_map/all_to_all | solution.py:35
  59.7 1.5 copy-start.3
  59.7 11.3 %copy-start.24 = (f32[128,4]{0,1:T(4,128)S(1)}, f32[128,4]{0,1:T(4,128)}, u32[]{:S(2)}) copy-start(f32[128,4]{0,1:T(4,128)} %param.30) | copy-start | bytes 6148
  61.2 9.8 %copy-start.7 = (bf16[1024,256]{1,0:T(8,128)(2,1)S(1)}, bf16[1024,256]{1,0:T(8,128)(2,1)}, u32[]{:S(2)}) copy-start(bf16[1024,256]{1,0:T(8,128)(2,1)} %param.37) | copy-start | bytes 1572868
  61.2 11.3 %copy-start.17 = (bf16[128,256]{1,0:T(8,128)(2,1)S(1)}, bf16[128,256]{1,0:T(8,128)(2,1)}, u32[]{:S(2)}) copy-start(bf16[128,256]{1,0:T(8,128)(2,1)} %param.20) | copy-start | bytes 196612
  63.3 67.7 %collective-permute-start.3 = (bf16[128,128]{0,1:T(8,128)(2,1)}, bf16[128,128]{0,1:T(8,128)(2,1)}, u32[]{:S(2)}, u32[]{:S(2)}) collective-permute-start(bf16[128,128]{0,1:T(8,128)(2,1)} %fusion.7), channel_id=1, source_target_pairs={{0,4},{1,5},{2,6},{3,7},{4,0},{5,1},{6,2},{7,3},{8,12},{9,13},{10,... | collective-permute-start | bytes 98312 | tf_op jit(solution)/shard_map/ppermute | solution.py:31
  71.0 14.9 %copy-start.21 = (s32[128,4]{0,1:T(4,128)S(1)}, s32[128,4]{0,1:T(4,128)}, u32[]{:S(2)}) copy-start(s32[128,4]{0,1:T(4,128)} %param.29) | copy-start | bytes 6148
  73.2 45.4 %all-to-all-start.2 = ((bf16[32,16,512]{2,1,0:T(8,128)(2,1)}), bf16[32,16,512]{2,1,0:T(8,128)(2,1)S(1)}, u32[]{:S(2)}, u32[]{:S(2)}) async-start(bf16[32,16,512]{2,1,0:T(8,128)(2,1)} %bitcast.130), calls=%async_computation.2 | async-start | bytes 1048576 | tf_op jit(solution)/shard_map/all_to_all | solution.py:35
  118.6 44.1 %copy-start.4 = (bf16[32,16,512]{2,1,0:T(8,128)(2,1)}, bf16[32,16,512]{2,1,0:T(8,128)(2,1)S(1)}, u32[]{:S(2)}) copy-start(bf16[32,16,512]{2,1,0:T(8,128)(2,1)S(1)} %all-to-all-done.2) | copy-start | bytes 1572868
  118.6 18.3 %all-to-all-start.1 = ((bf16[32,8,128]{2,1,0:T(8,128)(2,1)}), bf16[32,8,128]{2,1,0:T(8,128)(2,1)}, u32[]{:S(2)}, u32[]{:S(2)}) async-start(bf16[32,8,128]{2,1,0:T(8,128)(2,1)} %copy.195), calls=%async_computation.1 | async-start | bytes 131072 | tf_op jit(solution)/shard_map/all_to_all | solution.py:35
  123.5 23.6 %collective-permute-start.6 = (bf16[512,512]{1,0:T(8,128)(2,1)S(1)}, bf16[512,512]{1,0:T(8,128)(2,1)S(1)}, u32[]{:S(2)}, u32[]{:S(2)}) collective-permute-start(bf16[512,512]{1,0:T(8,128)(2,1)S(1)} %bitcast.123), channel_id=1, source_target_pairs={{0,2},{1,3},{2,4},{3,5},{4,6},{5,7},{6,0},{7,1},{8,10},{9,11},{10,... | collective-permute-start | bytes 1572872 | tf_op jit(solution)/shard_map/ppermute | solution.py:26
  126.0 27.5 %collective-permute-start.7 = (bf16[512,512]{1,0:T(8,128)(2,1)S(1)}, bf16[512,512]{1,0:T(8,128)(2,1)}, u32[]{:S(2)}, u32[]{:S(2)}) collective-permute-start(bf16[512,512]{1,0:T(8,128)(2,1)S(1)} %bitcast.124), channel_id=1, source_target_pairs={{0,6},{1,7},{2,0},{3,1},{4,2},{5,3},{6,4},{7,5},{8,14},{9,15},{10,... | collective-permute-start | bytes 1572872 | tf_op jit(solution)/shard_map/ppermute | solution.py:26
  137.0 23.7 %copy-start.23 = (f32[2,2,128]{2,1,0:T(2,128)S(1)}, f32[2,2,128]{2,1,0:T(2,128)}, u32[]{:S(2)}) copy-start(f32[2,2,128]{2,1,0:T(2,128)} %copy.188) | copy-start | bytes 6148
  147.1 16.8 %copy-start.5 = (bf16[512,512]{1,0:T(8,128)(2,1)}, bf16[512,512]{1,0:T(8,128)(2,1)S(1)}, u32[]{:S(2)}) copy-start(bf16[512,512]{1,0:T(8,128)(2,1)S(1)} %collective-permute-done.6.before) | copy-start | bytes 1572868
  147.9 16.1 %collective-permute-start.8 = (bf16[256,512]{1,0:T(8,128)(2,1)}, bf16[256,512]{1,0:T(8,128)(2,1)}, u32[]{:S(2)}, u32[]{:S(2)}) collective-permute-start(bf16[256,512]{1,0:T(8,128)(2,1)} %slice.41), channel_id=1, source_target_pairs={{0,2},{1,3},{2,4},{3,5},{4,6},{5,7},{6,0},{7,1},{8,10},{9,11},{10,... | collective-permute-start | bytes 786440 | tf_op jit(solution)/shard_map/ppermute | solution.py:26
  155.2 16.3 %collective-permute-start.9 = (bf16[256,512]{1,0:T(8,128)(2,1)}, bf16[256,512]{1,0:T(8,128)(2,1)}, u32[]{:S(2)}, u32[]{:S(2)}) collective-permute-start(bf16[256,512]{1,0:T(8,128)(2,1)} %slice.42), channel_id=1, source_target_pairs={{0,6},{1,7},{2,0},{3,1},{4,2},{5,3},{6,4},{7,5},{8,14},{9,15},{10,... | collective-permute-start | bytes 786440 | tf_op jit(solution)/shard_map/ppermute | solution.py:26
  163.9 29.2 %copy-start.18 = (bf16[128,256]{1,0:T(8,128)(2,1)S(1)}, bf16[128,256]{1,0:T(8,128)(2,1)}, u32[]{:S(2)}) copy-start(bf16[128,256]{1,0:T(8,128)(2,1)} %param.23) | copy-start | bytes 196612
  164.0 29.2 %copy-start.27 = (f32[256]{0:T(256)S(1)}, f32[256]{0:T(256)}, u32[]{:S(2)}) copy-start(f32[256]{0:T(256)} %param.26) | copy-start | bytes 3076
  175.8 23.2 %collective-permute-start.11 = (bf16[512,256]{1,0:T(8,128)(2,1)}, bf16[512,256]{1,0:T(8,128)(2,1)S(1)}, u32[]{:S(2)}, u32[]{:S(2)}) collective-permute-start(bf16[512,256]{1,0:T(8,128)(2,1)} %get-tuple-element.39.own), channel_id=1, source_target_pairs={{0,2},{1,3},{2,4},{3,5},{4,6},{5,7},{6,0},{7,1},{8,10},{9,11},{10,... | collective-permute-start | bytes 786440 | tf_op jit(solution)/shard_map/ppermute | solution.py:26
  180.1 23.7 %collective-permute-start.12 = (bf16[512,256]{1,0:T(8,128)(2,1)}, bf16[512,256]{1,0:T(8,128)(2,1)S(1)}, u32[]{:S(2)}, u32[]{:S(2)}) collective-permute-start(bf16[512,256]{1,0:T(8,128)(2,1)} %get-tuple-element.39.own), channel_id=1, source_target_pairs={{0,6},{1,7},{2,0},{3,1},{4,2},{5,3},{6,4},{7,5},{8,14},{9,15},{10,... | collective-permute-start | bytes 786440 | tf_op jit(solution)/shard_map/ppermute | solution.py:26
  183.6 13.0 %collective-permute-start.13 = (bf16[256,256]{1,0:T(8,128)(2,1)}, bf16[256,256]{1,0:T(8,128)(2,1)S(1)}, u32[]{:S(2)}, u32[]{:S(2)}) collective-permute-start(bf16[256,256]{1,0:T(8,128)(2,1)} %get-tuple-element.40), channel_id=1, source_target_pairs={{0,4},{1,5},{2,6},{3,7},{4,0},{5,1},{6,2},{7,3},{8,12},{9,13},{10,... | collective-permute-start | bytes 393224 | tf_op jit(solution)/shard_map/ppermute | solution.py:26
  189.0 9.9 %collective-permute-start.14 = (bf16[256,256]{1,0:T(8,128)(2,1)}, bf16[256,256]{1,0:T(8,128)(2,1)S(1)}, u32[]{:S(2)}, u32[]{:S(2)}) collective-permute-start(bf16[256,256]{1,0:T(8,128)(2,1)} %get-tuple-element.41), channel_id=1, source_target_pairs={{0,4},{1,5},{2,6},{3,7},{4,0},{5,1},{6,2},{7,3},{8,12},{9,13},{10,... | collective-permute-start | bytes 393224 | tf_op jit(solution)/shard_map/ppermute | solution.py:26
  193.1 0.8 copy-start.20
  194.0 34.4 %collective-permute-start.4 = (bf16[128,256]{0,1:T(8,128)(2,1)S(1)}, bf16[128,256]{0,1:T(8,128)(2,1)S(1)}, u32[]{:S(2)}, u32[]{:S(2)}) collective-permute-start(bf16[128,256]{0,1:T(8,128)(2,1)S(1)} %copy-done.20), channel_id=1, source_target_pairs={{0,2},{1,3},{2,0},{3,1},{4,6},{5,7},{6,4},{7,5},{8,10},{9,11},{10,... | collective-permute-start | bytes 196616 | tf_op jit(solution)/shard_map/ppermute | solution.py:31
  196.7 7.1 %copy-start.14 = (bf16[256,256]{1,0:T(8,128)(2,1)}, bf16[256,256]{1,0:T(8,128)(2,1)S(1)}, u32[]{:S(2)}) copy-start(bf16[256,256]{1,0:T(8,128)(2,1)S(1)} %collective-permute-done.13.far_first) | copy-start | bytes 393220
  198.9 4.8 %copy-start.15 = (bf16[256,256]{1,0:T(8,128)(2,1)}, bf16[256,256]{1,0:T(8,128)(2,1)S(1)}, u32[]{:S(2)}) copy-start(bf16[256,256]{1,0:T(8,128)(2,1)S(1)} %collective-permute-done.14.far_second) | copy-start | bytes 393220
  198.9 4.8 %copy-start.12 = (bf16[512,256]{1,0:T(8,128)(2,1)}, bf16[512,256]{1,0:T(8,128)(2,1)S(1)}, u32[]{:S(2)}) copy-start(bf16[512,256]{1,0:T(8,128)(2,1)S(1)} %collective-permute-done.11.before) | copy-start | bytes 786436
  203.7 0.7 copy-start.13
  207.5 20.9 %copy-start.9 = (bf16[128,128]{0,1:T(8,128)(2,1)S(1)}, bf16[128,128]{0,1:T(8,128)(2,1)}, u32[]{:S(2)}) copy-start(bf16[128,128]{0,1:T(8,128)(2,1)} %copy-done.8) | copy-start | bytes 98308
  207.5 20.9 %copy-start.11 = (bf16[128,128]{0,1:T(8,128)(2,1)S(1)}, bf16[128,128]{0,1:T(8,128)(2,1)}, u32[]{:S(2)}) copy-start(bf16[128,128]{0,1:T(8,128)(2,1)} %copy-done.10) | copy-start | bytes 98308
  207.5 47.3 %all-to-all-start.3 = ((bf16[32,16,512]{2,1,0:T(8,128)(2,1)}), bf16[32,16,512]{2,1,0:T(8,128)(2,1)S(1)}, u32[]{:S(2)}, u32[]{:S(2)}) async-start(bf16[32,16,512]{2,1,0:T(8,128)(2,1)} %bitcast.121), calls=%async_computation.3 | async-start | bytes 1048576 | tf_op jit(solution)/shard_map/all_to_all | solution.py:35
  221.6 12.8 %collective-permute-start = (bf16[2,2,16,2048]{3,2,0,1:T(8,128)(2,1)S(1)}, bf16[2,2,16,2048]{3,2,0,1:T(8,128)(2,1)S(1)}, u32[]{:S(2)}, u32[]{:S(2)}) collective-permute-start(bf16[2,2,16,2048]{3,2,0,1:T(8,128)(2,1)S(1)} %fusion.15), channel_id=1, source_target_pairs={{0,1},{1,0},{2,3},{3,2},{4,5},{5,4},{6,7},{7,6},{8,9},{9,8},{10,11... | collective-permute-start | bytes 786440 | tf_op jit(solution)/shard_map/ppermute | solution.py:31
  228.5 8.7 %collective-permute-start.5 = (bf16[128,512]{0,1:T(8,128)(2,1)S(1)}, bf16[128,512]{0,1:T(8,128)(2,1)S(1)}, u32[]{:S(2)}, u32[]{:S(2)}) collective-permute-start(bf16[128,512]{0,1:T(8,128)(2,1)S(1)} %pad_maximum_fusion.1), channel_id=1, source_target_pairs={{0,1},{1,0},{2,3},{3,2},{4,5},{5,4},{6,7},{7,6},{8,9},{9,8},{10,11... | collective-permute-start | bytes 393224 | tf_op jit(solution)/shard_map/ppermute | solution.py:31
  234.4 20.4 %copy-start.22 = (s32[128,32]{0,1:T(8,128)S(1)}, s32[128,32]{0,1:T(8,128)}, u32[]{:S(2)}) copy-start(s32[128,32]{0,1:T(8,128)} %fusion.8) | copy-start | bytes 49156
  234.4 20.4 %copy-start.28 = (s32[16]{0:T(128)S(1)}, s32[16]{0:T(128)}, u32[]{:S(2)}) copy-start(s32[16]{0:T(128)} %iota_add_fusion) | copy-start | bytes 196
  234.5 8.5 %collective-permute-start.1 = (bf16[2,16,2048]{2,1,0:T(8,128)(2,1)S(1)}, bf16[2,16,2048]{2,1,0:T(8,128)(2,1)S(1)}, u32[]{:S(2)}, u32[]{:S(2)}) collective-permute-start(bf16[2,16,2048]{2,1,0:T(8,128)(2,1)S(1)} %fusion.32), channel_id=1, source_target_pairs={{0,2},{1,3},{2,0},{3,1},{4,6},{5,7},{6,4},{7,5},{8,10},{9,11},{10,... | collective-permute-start | bytes 393224 | tf_op jit(solution)/shard_map/ppermute | solution.py:31
  243.1 20.1 %collective-permute-start.2 = (bf16[16,2048]{1,0:T(8,128)(2,1)S(1)}, bf16[16,2048]{1,0:T(8,128)(2,1)S(1)}, u32[]{:S(2)}, u32[]{:S(2)}) collective-permute-start(bf16[16,2048]{1,0:T(8,128)(2,1)S(1)} %fusion.61), channel_id=1, source_target_pairs={{0,4},{1,5},{2,6},{3,7},{4,0},{5,1},{6,2},{7,3},{8,12},{9,13},{10,... | collective-permute-start | bytes 196616 | tf_op jit(solution)/shard_map/ppermute | solution.py:31
  255.8 9.3 %copy-start.2 = (bf16[2,2,2,128,256]{4,3,2,1,0:T(8,128)(2,1)S(1)}, bf16[2,2,2,128,256]{4,3,2,1,0:T(8,128)(2,1)}, u32[]{:S(2)}) copy-start(bf16[2,2,2,128,256]{4,3,2,1,0:T(8,128)(2,1)} %copy.201) | copy-start | bytes 1572868
  256.4 8.8 %collective-permute-start.16 = (bf16[128,256]{1,0:T(8,128)(2,1)S(1)}, bf16[128,256]{1,0:T(8,128)(2,1)S(1)}, u32[]{:S(2)}, u32[]{:S(2)}) collective-permute-start(bf16[128,256]{1,0:T(8,128)(2,1)S(1)} %slice.50), channel_id=1, source_target_pairs={{0,1},{1,0},{2,3},{3,2},{4,5},{5,4},{6,7},{7,6},{8,9},{9,8},{10,11... | collective-permute-start | bytes 196616 | tf_op jit(solution)/shard_map/ppermute | solution.py:31
  (2 other events, 1.2 us)

commit v5 on v4

--- a/solution.py
+++ b/solution.py
@@ -181,6 +181,7 @@
 
 
 VMEM = pl.BlockSpec(memory_space=pltpu.VMEM)
+ANY = pl.BlockSpec(memory_space=pl.ANY)
 
 
 def in_vmem(kernel, shapes, *operands):
@@ -190,6 +191,61 @@
         in_specs=[VMEM] * len(operands),
         out_specs=jax.tree.map(lambda _: VMEM, shapes),
     )(*operands)
+
+
+def fetching(kernel, shapes, *operands):
+    count = len(operands)
+
+    def body(*refs):
+        sources, rest = refs[:count], refs[count:]
+        outputs, held, arrived = rest[: -count - 1], rest[-count - 1 : -1], rest[-1]
+        copies = [
+            pltpu.make_async_copy(source, target, arrived.at[i])
+            for i, (source, target) in enumerate(zip(sources, held))
+        ]
+        for copy in copies:
+            copy.start()
+
+        def fetch(i):
+            def ready():
+                copies[i].wait()
+                return held[i]
+
+            return ready
+
+        kernel(*[fetch(i) for i in range(count)], *outputs)
+
+    return pl.pallas_call(
+        body,
+        out_shape=shapes,
+        in_specs=[ANY] * count,
+        out_specs=jax.tree.map(lambda _: VMEM, shapes),
+        scratch_shapes=[pltpu.VMEM(a.shape, a.dtype) for a in operands]
+        + [pltpu.SemaphoreType.DMA((count,))],
+    )(*operands)
+
+
+def halves_kernel(before, after, first, second, arrived):
+    middle = first.shape[0]
+    copies = [
+        pltpu.make_async_copy(before.at[pl.ds(0, middle), :], first, arrived.at[0]),
+        pltpu.make_async_copy(after.at[pl.ds(middle, middle), :], second, arrived.at[1]),
+    ]
+    for copy in copies:
+        copy.start()
+    for copy in copies:
+        copy.wait()
+
+
+def far_halves(before, after):
+    half = jax.ShapeDtypeStruct((before.shape[0] // 2, before.shape[1]), before.dtype)
+    return pl.pallas_call(
+        halves_kernel,
+        out_shape=(half, half),
+        in_specs=[ANY, ANY],
+        out_specs=(ANY, ANY),
+        scratch_shapes=[pltpu.SemaphoreType.DMA((2,))],
+    )(before, after)
 
 
 def select_kernel(experts, hidden_state, gain, index, normed, outgoing):
@@ -228,38 +284,46 @@
     ).astype(jnp.bfloat16)
 
 
-def around_product(pieces, matrix):
-    own, before, after, far_first, far_second = pieces
-    depth = own.shape[1]
-    count = matrix.shape[0] // depth
+def around_products(pieces, matrices):
     quad = lax.axis_index("tp") >> 1
-
-    def block(step):
+    held = []
+
+    def dot(piece, matrix, step):
+        depth = piece.shape[1]
+        count = matrix.shape[0] // depth
         start = pl.multiple_of(((quad + step) & (count - 1)) * depth, depth)
-        return matrix[pl.ds(start, depth), :]
-
-    def dot(piece, step):
-        return jnp.dot(piece, block(step), preferred_element_type=jnp.float32)
-
-    near = dot(own[...], 0) + dot(before[...], -1) + dot(after[...], 1)
-    middle = far_first.shape[0]
-    return (near[:middle] + dot(far_first[...], 2), near[middle:] + dot(far_second[...], 2))
+        return jnp.dot(
+            piece[...], matrix[pl.ds(start, depth), :], preferred_element_type=jnp.float32
+        )
+
+    near = [None] * len(matrices)
+    for fetch, step in zip(pieces[:3], (0, -1, 1)):
+        piece = fetch()
+        for k, fetch_matrix in enumerate(matrices):
+            if step == 0:
+                held.append(fetch_matrix())
+            part = dot(piece, held[k], step)
+            near[k] = part if near[k] is None else near[k] + part
+    first, second = (fetch() for fetch in pieces[3:])
+    middle = first.shape[0]
+    return [
+        (part[:middle] + dot(first, matrix, 2), part[middle:] + dot(second, matrix, 2))
+        for part, matrix in zip(near, held)
+    ]
 
 
 def hidden_kernel(
     own, before, after, far_first, far_second, own_in, partner_in, hidden, hidden_first, hidden_second
 ):
     pieces = (own, before, after, far_first, far_second)
-    units = own_in.shape[1] // 2
-    middle = far_first.shape[0]
-    sides = []
-    for matrix in (own_in, partner_in):
-        sides.append(
-            [
-                (jax.nn.silu(both[:, :units]) * both[:, units:]).astype(jnp.bfloat16)
-                for both in around_product(pieces, matrix)
-            ]
-        )
+    middle, units = (hidden_first.shape[0], hidden_first.shape[1] // 2)
+    sides = [
+        [
+            (jax.nn.silu(both[:, :units]) * both[:, units:]).astype(jnp.bfloat16)
+            for both in halves
+        ]
+        for halves in around_products(pieces, (own_in, partner_in))
+    ]
     even = (lax.axis_index("tp") & 1) == 0
     for k, part in enumerate((hidden_first, hidden_second)):
         part[:, :units] = jnp.where(even, sides[0][k], sides[1][k])
@@ -269,10 +333,9 @@
 
 def down_kernel(own, before, after, far_first, far_second, own_down, partner_down, answers):
     pieces = (own, before, after, far_first, far_second)
-    middle = far_first.shape[0]
-    width = own_down.shape[1]
-    for side, matrix in enumerate((own_down, partner_down)):
-        for k, part in enumerate(around_product(pieces, matrix)):
+    middle, width = (answers.shape[0] // 2, answers.shape[1] // 2)
+    for side, halves in enumerate(around_products(pieces, (own_down, partner_down))):
+        for k, part in enumerate(halves):
             answers[pl.ds(k * middle, middle), pl.ds(side * width, width)] = part.astype(
                 jnp.bfloat16
             )
@@ -349,9 +412,10 @@
 
     before = shifted(chunk, "tp", 2)
     after = shifted(chunk, "tp", -2)
-    far = [shifted(before[:middle], "tp", 2), shifted(after[middle:], "tp", -2)]
+    first, second = far_halves(before, after)
+    far = [shifted(first, "tp", 2), shifted(second, "tp", -2)]
     part_shape = jax.ShapeDtypeStruct((middle, 2 * units), jnp.bfloat16)
-    hidden, hidden_first, hidden_second = in_vmem(
+    hidden, hidden_first, hidden_second = fetching(
         hidden_kernel,
         (jax.ShapeDtypeStruct((chunk.shape[0], 2 * units), jnp.bfloat16), part_shape, part_shape),
         chunk,
@@ -364,7 +428,7 @@
     far = [shifted(hidden_first, "tp", 4), shifted(hidden_second, "tp", -4)]
     before = shifted(hidden, "tp", 2)
     after = shifted(hidden, "tp", -2)
-    answers = in_vmem(
+    answers = fetching(
         down_kernel,
         jax.ShapeDtypeStruct((chunk.shape[0], 2 * width_out), jnp.bfloat16),
         hidden,

time: 267 us -> 282 us (1.056)
  Pallas kernels: 9.67 us -> 27.1 us
  starting transfers between devices: 148 us -> 142 us
  other arithmetic: 7.83 us -> 10.8 us
    pallas_call x0 -> x3, Pallas kernels: none -> 24.7 us  [the longest x1 17 us: far_halves(): pl.pallas_call(halves_kernel, out_shape=(half, half), in_specs=[ANY, ANY]...]
    ppermute x9, starting transfers between devices: 39.8 us -> 31.9 us  [swapped(): return lax.ppermute(array, axis, [(i, i ^ bit) for i in range(count)])]
    pallas_call x3 -> x1, Pallas kernels: 9.67 us -> 2.41 us  [in_vmem(): pl.pallas_call(kernel, out_shape=shapes, in_specs=[VMEM] * len(operands),...]
    all_to_all x4, waiting for transfers between devices: 39.8 us -> 44 us  [exchanged(): return lax.all_to_all(array, axis, split_axis=0, concat_axis=0, tiled=True)]
    all_to_all x4, starting transfers between devices: 76 us -> 78.9 us  [exchanged(): return lax.all_to_all(array, axis, split_axis=0, concat_axis=0, tiled=True)]
  transfers between devices with their start and end apart: 21 -> 21, of which waited for: 13 -> 12; matrix products, arithmetic and copies ran while one was open for 9% -> 8% of each run, Pallas kernels for 4% -> 10%
where the time goes in v5:
time: 282 us; the launch traced here: 280 us
  starting transfers between devices  142 us (50%)
  waiting for transfers between devices  81.2 us (29%)
  Pallas kernels  27.1 us (10%)
  other arithmetic  10.8 us (4%)
  matrix products  9.78 us (3%)
  local copies, waits for them, and re-layouts  7.58 us (3%)
    all_to_all x4, starting transfers between devices, exchanged(): return lax.all_to_all(array, axis, split_axis=0, concat_axis=0, tiled=True)  78.9 us
    all_to_all x4, waiting for transfers between devices, exchanged(): return lax.all_to_all(array, axis, split_axis=0, concat_axis=0, tiled=True)  44 us
    ppermute x9, starting transfers between devices, swapped(): return lax.ppermute(array, axis, [(i, i ^ bit) for i in range(count)])  31.9 us
    ppermute x8, starting transfers between devices, shifted(): lax.ppermute(array, axis, [(i, (i + step) % count) for i in range(count)])  31.6 us
    ppermute x8, waiting for transfers between devices, shifted(): lax.ppermute(array, axis, [(i, (i + step) % count) for i in range(count)])  27.1 us
    pallas_call x1, Pallas kernels, far_halves(): pl.pallas_call(halves_kernel, out_shape=(half, half), in_specs=[ANY, ANY]...  17 us
    ppermute x9, waiting for transfers between devices, swapped(): return lax.ppermute(array, axis, [(i, i ^ bit) for i in range(count)])  10.1 us
    pallas_call x2, Pallas kernels, fetching(): pl.pallas_call(body, out_shape=shapes, in_specs=[ANY] * count, out_specs=...  7.67 us
  transfers between devices with their start and end apart: 21, of which 12 were waited for; matrix products, arithmetic and copies ran while one was open for 8% of the time, Pallas kernels for 10%

profile of v5, /device:TPU:65, one launch (start us, length us, event | category | flops | bytes accessed | tf_op | source)
XLA Modules:
  0.0 280.5 jit_solution(9159551019328581421)
XLA Ops:
  0.7 1.4 pad_maximum_fusion.refs_5_
  2.1 4.2 %collective-permute-start.10 = (bf16[2048,256]{1,0:T(8,128)(2,1)S(1)}, bf16[2048,256]{1,0:T(8,128)(2,1)}, u32[]{:S(2)}, u32[]{:S(2)}) collective-permute-start(bf16[2048,256]{1,0:T(8,128)(2,1)S(1)} %pad_maximum_fusion.refs_5_), channel_id=1, source_target_pairs={{0,1},{1,0},{2,3},{3,2},{4,5},{5,4},{6,7},{7,6},{8,9},{9,8},{10,11... | collective-permute-start | bytes 3145736 | tf_op jit(solution)/shard_map/ppermute | solution.py:31
  6.3 2.0 collective-permute-start.15
  10.2 1.6 while.13
  12.8 1.6 fusion.31
  14.4 45.6 %all-to-all-start = ((bf16[32,8,256]{2,1,0:T(8,128)(2,1)}), bf16[32,8,256]{2,1,0:T(8,128)(2,1)}, u32[]{:S(2)}, u32[]{:S(2)}) async-start(bf16[32,8,256]{2,1,0:T(8,128)(2,1)} %fusion.31), calls=%async_computation | async-start | bytes 262144 | tf_op jit(solution)/shard_map/all_to_all | solution.py:35
  60.0 2.4 shard_map.185
  62.4 1.4 fusion.80
  63.9 1.0 fusion.7
  64.9 7.1 %collective-permute-start.3 = (bf16[128,128]{0,1:T(8,128)(2,1)}, bf16[128,128]{0,1:T(8,128)(2,1)}, u32[]{:S(2)}, u32[]{:S(2)}) collective-permute-start(bf16[128,128]{0,1:T(8,128)(2,1)} %fusion.7), channel_id=1, source_target_pairs={{0,4},{1,5},{2,6},{3,7},{4,0},{5,1},{6,2},{7,3},{8,12},{9,13},{10,... | collective-permute-start | bytes 98312 | tf_op jit(solution)/shard_map/ppermute | solution.py:31
  73.6 2.1 all-to-all-done
  75.7 10.6 %all-to-all-start.2 = ((bf16[32,16,512]{2,1,0:T(8,128)(2,1)}), bf16[32,16,512]{2,1,0:T(8,128)(2,1)S(1)}, u32[]{:S(2)}, u32[]{:S(2)}) async-start(bf16[32,16,512]{2,1,0:T(8,128)(2,1)} %bitcast.130), calls=%async_computation.2 | async-start | bytes 1048576 | tf_op jit(solution)/shard_map/all_to_all | solution.py:35
  88.4 0.8 slice.31
  89.2 0.9 convert_reduce_fusion
  90.1 1.1 fusion.4
  92.2 27.5 %all-to-all-done.2 = bf16[32,16,512]{2,1,0:T(8,128)(2,1)S(1)} async-done(((bf16[32,16,512]{2,1,0:T(8,128)(2,1)}), bf16[32,16,512]{2,1,0:T(8,128)(2,1)S(1)}, u32[]{:S(2)}, u32[]{:S(2)}) %all-to-all-start.2) | async-done | bytes 524320 | tf_op jit(solution)/shard_map/all_to_all | solution.py:35
  119.6 4.8 %all-to-all-start.1 = ((bf16[32,8,128]{2,1,0:T(8,128)(2,1)}), bf16[32,8,128]{2,1,0:T(8,128)(2,1)}, u32[]{:S(2)}, u32[]{:S(2)}) async-start(bf16[32,8,128]{2,1,0:T(8,128)(2,1)} %copy.195), calls=%async_computation.1 | async-start | bytes 131072 | tf_op jit(solution)/shard_map/all_to_all | solution.py:35
  124.5 2.6 collective-permute-start.6
  127.1 4.9 %collective-permute-start.7 = (bf16[512,512]{1,0:T(8,128)(2,1)S(1)}, bf16[512,512]{1,0:T(8,128)(2,1)}, u32[]{:S(2)}, u32[]{:S(2)}) collective-permute-start(bf16[512,512]{1,0:T(8,128)(2,1)S(1)} %bitcast.124), channel_id=1, source_target_pairs={{0,6},{1,7},{2,0},{3,1},{4,2},{5,3},{6,4},{7,5},{8,14},{9,15},{10,... | collective-permute-start | bytes 1572872 | tf_op jit(solution)/shard_map/ppermute | solution.py:26
  134.0 4.0 %all-to-all-done.1 = bf16[32,8,128]{2,1,0:T(8,128)(2,1)} async-done(((bf16[32,8,128]{2,1,0:T(8,128)(2,1)}), bf16[32,8,128]{2,1,0:T(8,128)(2,1)}, u32[]{:S(2)}, u32[]{:S(2)}) %all-to-all-start.1) | async-done | bytes 65568 | tf_op jit(solution)/shard_map/all_to_all | solution.py:35
  138.0 1.5 bitcast_convert_fusion
  139.5 13.0 %collective-permute-done.6.before.refs_1_ = bf16[512,512]{1,0:T(8,128)(2,1)S(1)} collective-permute-done((bf16[512,512]{1,0:T(8,128)(2,1)S(1)}, bf16[512,512]{1,0:T(8,128)(2,1)S(1)}, u32[]{:S(2)}, u32[]{:S(2)}) %collective-permute-start.6) | collective-permute-done | bytes 524320 | tf_op jit(solution)/shard_map/ppermute | solution.py:26
  152.5 2.2 collective-permute-done.7.after.refs_2_
  154.7 17.0 %shard_map.186 = (bf16[256,512]{1,0:T(8,128)(2,1)}, bf16[256,512]{1,0:T(8,128)(2,1)}) custom-call(bf16[512,512]{1,0:T(8,128)(2,1)} %copy-done.5, bf16[512,512]{1,0:T(8,128)(2,1)} %collective-permute-done.7.after.refs_2_), custom_call_target="tpu_custom_call" | custom-call | tf_op jit(solution)/shard_map/pallas_call | solution.py:242
  171.8 3.2 %collective-permute-start.8 = (bf16[256,512]{1,0:T(8,128)(2,1)}, bf16[256,512]{1,0:T(8,128)(2,1)S(1)}, u32[]{:S(2)}, u32[]{:S(2)}) collective-permute-start(bf16[256,512]{1,0:T(8,128)(2,1)} %get-tuple-element.41), channel_id=1, source_target_pairs={{0,2},{1,3},{2,4},{3,5},{4,6},{5,7},{6,0},{7,1},{8,10},{9,11},{10,... | collective-permute-start | bytes 786440 | tf_op jit(solution)/shard_map/ppermute | solution.py:26
  175.0 4.3 %collective-permute-start.9 = (bf16[256,512]{1,0:T(8,128)(2,1)}, bf16[256,512]{1,0:T(8,128)(2,1)}, u32[]{:S(2)}, u32[]{:S(2)}) collective-permute-start(bf16[256,512]{1,0:T(8,128)(2,1)} %get-tuple-element.42), channel_id=1, source_target_pairs={{0,6},{1,7},{2,0},{3,1},{4,2},{5,3},{6,4},{7,5},{8,14},{9,15},{10,... | collective-permute-start | bytes 786440 | tf_op jit(solution)/shard_map/ppermute | solution.py:26
  179.2 1.6 multiply_reduce_fusion
  181.1 3.1 %collective-permute-done.8.refs_3_ = bf16[256,512]{1,0:T(8,128)(2,1)S(1)} collective-permute-done((bf16[256,512]{1,0:T(8,128)(2,1)}, bf16[256,512]{1,0:T(8,128)(2,1)S(1)}, u32[]{:S(2)}, u32[]{:S(2)}) %collective-permute-start.8) | collective-permute-done | bytes 262176 | tf_op jit(solution)/shard_map/ppermute | solution.py:26
  184.2 5.1 %collective-permute-done.9.refs_4_ = bf16[256,512]{1,0:T(8,128)(2,1)} collective-permute-done((bf16[256,512]{1,0:T(8,128)(2,1)}, bf16[256,512]{1,0:T(8,128)(2,1)}, u32[]{:S(2)}, u32[]{:S(2)}) %collective-permute-start.9) | collective-permute-done | bytes 262176 | tf_op jit(solution)/shard_map/ppermute | solution.py:26
  189.4 4.5 %shard_map.187 = (bf16[512,256]{1,0:T(8,128)(2,1)}, bf16[256,256]{1,0:T(8,128)(2,1)}, bf16[256,256]{1,0:T(8,128)(2,1)}) custom-call(bf16[512,512]{1,0:T(8,128)(2,1)} %bitcast.125, bf16[512,512]{1,0:T(8,128)(2,1)} %copy-done.5, bf16[512,512]{1,0:T(8,128)(2,1)} %collective-permute-done.7.after.refs_2_, bf16[256,512]{1,0:T(8,128)(2,1)} %copy-done.13, ...), custom_call_target="tpu_custom_call" | custom-call | tf_op jit(solution)/shard_map/pallas_call | solution.py:218
  193.8 2.2 collective-permute-start.11
  196.0 5.3 %collective-permute-start.12 = (bf16[512,256]{1,0:T(8,128)(2,1)}, bf16[512,256]{1,0:T(8,128)(2,1)S(1)}, u32[]{:S(2)}, u32[]{:S(2)}) collective-permute-start(bf16[512,256]{1,0:T(8,128)(2,1)} %get-tuple-element.43.refs_0_), channel_id=1, source_target_pairs={{0,6},{1,7},{2,0},{3,1},{4,2},{5,3},{6,4},{7,5},{8,14},{9,15},{10,... | collective-permute-start | bytes 786440 | tf_op jit(solution)/shard_map/ppermute | solution.py:26
  201.3 3.0 %collective-permute-start.13 = (bf16[256,256]{1,0:T(8,128)(2,1)}, bf16[256,256]{1,0:T(8,128)(2,1)S(1)}, u32[]{:S(2)}, u32[]{:S(2)}) collective-permute-start(bf16[256,256]{1,0:T(8,128)(2,1)} %get-tuple-element.44), channel_id=1, source_target_pairs={{0,4},{1,5},{2,6},{3,7},{4,0},{5,1},{6,2},{7,3},{8,12},{9,13},{10,... | collective-permute-start | bytes 393224 | tf_op jit(solution)/shard_map/ppermute | solution.py:26
  204.3 6.3 %collective-permute-start.14 = (bf16[256,256]{1,0:T(8,128)(2,1)}, bf16[256,256]{1,0:T(8,128)(2,1)S(1)}, u32[]{:S(2)}, u32[]{:S(2)}) collective-permute-start(bf16[256,256]{1,0:T(8,128)(2,1)} %get-tuple-element.45), channel_id=1, source_target_pairs={{0,4},{1,5},{2,6},{3,7},{4,0},{5,1},{6,2},{7,3},{8,12},{9,13},{10,... | collective-permute-start | bytes 393224 | tf_op jit(solution)/shard_map/ppermute | solution.py:26
  211.6 1.9 collective-permute-start.4
  213.6 3.5 %collective-permute-done.14.refs_4_ = bf16[256,256]{1,0:T(8,128)(2,1)S(1)} collective-permute-done((bf16[256,256]{1,0:T(8,128)(2,1)}, bf16[256,256]{1,0:T(8,128)(2,1)S(1)}, u32[]{:S(2)}, u32[]{:S(2)}) %collective-permute-start.14) | collective-permute-done | bytes 131104 | tf_op jit(solution)/shard_map/ppermute | solution.py:26
  218.6 3.2 %shard_map.188 = bf16[512,512]{1,0:T(8,128)(2,1)} custom-call(bf16[512,256]{1,0:T(8,128)(2,1)} %get-tuple-element.43.refs_0_, bf16[512,256]{1,0:T(8,128)(2,1)} %copy-done.14, bf16[512,256]{1,0:T(8,128)(2,1)} %copy-done.15, bf16[256,256]{1,0:T(8,128)(2,1)} %copy-done.16, bf16[256,256]{1,0:T(8,128)(2,1)} %copy-done.17, bf16[1024,256]{1,0:T(8,128)(2,1)} %bitcast.31.refs_5_, ...), custom_call_target="tpu_custom_call" | custom-call | tf_op jit(solution)/shard_map/pallas_call | solution.py:218
  221.8 17.8 %all-to-all-start.3 = ((bf16[32,16,512]{2,1,0:T(8,128)(2,1)}), bf16[32,16,512]{2,1,0:T(8,128)(2,1)S(1)}, u32[]{:S(2)}, u32[]{:S(2)}) async-start(bf16[32,16,512]{2,1,0:T(8,128)(2,1)} %bitcast.121), calls=%async_computation.3 | async-start | bytes 1048576 | tf_op jit(solution)/shard_map/all_to_all | solution.py:35
  239.7 2.0 collective-permute-start
  241.8 3.4 %collective-permute-start.5 = (bf16[128,512]{0,1:T(8,128)(2,1)S(1)}, bf16[128,512]{0,1:T(8,128)(2,1)S(1)}, u32[]{:S(2)}, u32[]{:S(2)}) collective-permute-start(bf16[128,512]{0,1:T(8,128)(2,1)S(1)} %pad_maximum_fusion.1), channel_id=1, source_target_pairs={{0,1},{1,0},{2,3},{3,2},{4,5},{5,4},{6,7},{7,6},{8,9},{9,8},{10,11... | collective-permute-start | bytes 393224 | tf_op jit(solution)/shard_map/ppermute | solution.py:31
  245.2 3.6 %collective-permute-done = bf16[2,2,16,2048]{3,2,0,1:T(8,128)(2,1)S(1)} collective-permute-done((bf16[2,2,16,2048]{3,2,0,1:T(8,128)(2,1)S(1)}, bf16[2,2,16,2048]{3,2,0,1:T(8,128)(2,1)S(1)}, u32[]{:S(2)}, u32[]{:S(2)}) %collective-permute-start) | collective-permute-done | bytes 262176 | tf_op jit(solution)/shard_map/ppermute | solution.py:31
  248.9 4.7 %collective-permute-start.1 = (bf16[2,16,2048]{2,1,0:T(8,128)(2,1)S(1)}, bf16[2,16,2048]{2,1,0:T(8,128)(2,1)S(1)}, u32[]{:S(2)}, u32[]{:S(2)}) collective-permute-start(bf16[2,16,2048]{2,1,0:T(8,128)(2,1)S(1)} %fusion.32), channel_id=1, source_target_pairs={{0,2},{1,3},{2,0},{3,1},{4,6},{5,7},{6,4},{7,5},{8,10},{9,11},{10,... | collective-permute-start | bytes 393224 | tf_op jit(solution)/shard_map/ppermute | solution.py:31
  253.7 4.0 %collective-permute-done.1 = bf16[2,16,2048]{2,1,0:T(8,128)(2,1)S(1)} collective-permute-done((bf16[2,16,2048]{2,1,0:T(8,128)(2,1)S(1)}, bf16[2,16,2048]{2,1,0:T(8,128)(2,1)S(1)}, u32[]{:S(2)}, u32[]{:S(2)}) %collective-permute-start.1) | collective-permute-done | bytes 131104 | tf_op jit(solution)/shard_map/ppermute | solution.py:31
  257.8 4.7 %collective-permute-start.2 = (bf16[16,2048]{1,0:T(8,128)(2,1)S(1)}, bf16[16,2048]{1,0:T(8,128)(2,1)S(1)}, u32[]{:S(2)}, u32[]{:S(2)}) collective-permute-start(bf16[16,2048]{1,0:T(8,128)(2,1)S(1)} %fusion.61), channel_id=1, source_target_pairs={{0,4},{1,5},{2,6},{3,7},{4,0},{5,1},{6,2},{7,3},{8,12},{9,13},{10,... | collective-permute-start | bytes 196616 | tf_op jit(solution)/shard_map/ppermute | solution.py:31
  262.5 10.5 %all-to-all-done.3 = bf16[32,16,512]{2,1,0:T(8,128)(2,1)S(1)} async-done(((bf16[32,16,512]{2,1,0:T(8,128)(2,1)}), bf16[32,16,512]{2,1,0:T(8,128)(2,1)S(1)}, u32[]{:S(2)}, u32[]{:S(2)}) %all-to-all-start.3) | async-done | bytes 524320 | tf_op jit(solution)/shard_map/all_to_all | solution.py:35
  274.5 2.0 collective-permute-start.16
  277.1 2.4 collective-permute-done.16
  279.6 0.9 fusion.5
  (135 shorter events, 15.9 us)
Async XLA Ops:
  0.6 210.1 %copy-start = (bf16[256,2048]{1,0:T(8,128)(2,1)S(1)}, bf16[256,2048]{1,0:T(8,128)(2,1)}, u32[]{:S(2)}) copy-start(bf16[256,2048]{1,0:T(8,128)(2,1)} %param.27) | copy-start | bytes 3145732
  0.6 7.7 %copy-start.28 = (f32[128,2]{0,1:T(2,128)S(1)}, f32[128,2]{0,1:T(2,128)}, u32[]{:S(2)}) copy-start(f32[128,2]{0,1:T(2,128)} %param.25) | copy-start | bytes 3076
  0.7 8.0 %copy-start.18 = (bf16[128,256]{1,0:T(8,128)(2,1)S(1)}, bf16[128,256]{1,0:T(8,128)(2,1)}, u32[]{:S(2)}) copy-start(bf16[128,256]{1,0:T(8,128)(2,1)} %param.21) | copy-start | bytes 196612
  0.7 8.0 %copy-start.29 = (f32[256]{0:T(256)S(1)}, f32[256]{0:T(256)}, u32[]{:S(2)}) copy-start(f32[256]{0:T(256)} %param.24) | copy-start | bytes 3076
  2.1 8.1 %copy-start.1 = (bf16[2048,256]{1,0:T(8,128)(2,1)}, bf16[2048,256]{1,0:T(8,128)(2,1)S(1)}, u32[]{:S(2)}) copy-start(bf16[2048,256]{1,0:T(8,128)(2,1)S(1)} %pad_maximum_fusion.refs_5_) | copy-start | bytes 3145732
  2.1 7.6 %copy-start.21 = (bf16[128,256]{1,0:T(8,128)(2,1)S(1)}, bf16[128,256]{1,0:T(8,128)(2,1)}, u32[]{:S(2)}) copy-start(bf16[128,256]{1,0:T(8,128)(2,1)} %param.22) | copy-start | bytes 196612
  2.1 179.0 %collective-permute-start.10 = (bf16[2048,256]{1,0:T(8,128)(2,1)S(1)}, bf16[2048,256]{1,0:T(8,128)(2,1)}, u32[]{:S(2)}, u32[]{:S(2)}) collective-permute-start(bf16[2048,256]{1,0:T(8,128)(2,1)S(1)} %pad_maximum_fusion.refs_5_), channel_id=1, source_target_pairs={{0,1},{1,0},{2,3},{3,2},{4,5},{5,4},{6,7},{7,6},{8,9},{9,8},{10,11... | collective-permute-start | bytes 3145736 | tf_op jit(solution)/shard_map/ppermute | solution.py:31
  6.3 204.8 %collective-permute-start.15 = (bf16[1024,256]{1,0:T(8,128)(2,1)}, bf16[1024,256]{1,0:T(8,128)(2,1)}, u32[]{:S(2)}, u32[]{:S(2)}) collective-permute-start(bf16[1024,256]{1,0:T(8,128)(2,1)} %bitcast.31.refs_5_), channel_id=1, source_target_pairs={{0,1},{1,0},{2,3},{3,2},{4,5},{5,4},{6,7},{7,6},{8,9},{9,8},{10,11... | collective-permute-start | bytes 1572872 | tf_op jit(solution)/shard_map/ppermute | solution.py:31
  11.8 50.6 %copy-start.6 = (bf16[2048,128]{1,0:T(8,128)(2,1)S(1)}, bf16[2048,128]{1,0:T(8,128)(2,1)}, u32[]{:S(2)}) copy-start(bf16[2048,128]{1,0:T(8,128)(2,1)} %param.35) | copy-start | bytes 1572868
  12.8 51.1 %copy-start.7 = (bf16[2048,128]{1,0:T(8,128)(2,1)S(1)}, bf16[2048,128]{1,0:T(8,128)(2,1)}, u32[]{:S(2)}) copy-start(bf16[2048,128]{1,0:T(8,128)(2,1)} %param.36) | copy-start | bytes 1572868
  14.4 61.3 %all-to-all-start = ((bf16[32,8,256]{2,1,0:T(8,128)(2,1)}), bf16[32,8,256]{2,1,0:T(8,128)(2,1)}, u32[]{:S(2)}, u32[]{:S(2)}) async-start(bf16[32,8,256]{2,1,0:T(8,128)(2,1)} %fusion.31), calls=%async_computation | async-start | bytes 262144 | tf_op jit(solution)/shard_map/all_to_all | solution.py:35
  62.4 1.5 copy-start.3
  62.4 9.6 %copy-start.27 = (f32[128,4]{0,1:T(4,128)S(1)}, f32[128,4]{0,1:T(4,128)}, u32[]{:S(2)}) copy-start(f32[128,4]{0,1:T(4,128)} %param.30) | copy-start | bytes 6148
  63.9 8.2 %copy-start.8 = (bf16[1024,256]{1,0:T(8,128)(2,1)S(1)}, bf16[1024,256]{1,0:T(8,128)(2,1)}, u32[]{:S(2)}) copy-start(bf16[1024,256]{1,0:T(8,128)(2,1)} %param.37) | copy-start | bytes 1572868
  63.9 9.6 %copy-start.19 = (bf16[128,256]{1,0:T(8,128)(2,1)S(1)}, bf16[128,256]{1,0:T(8,128)(2,1)}, u32[]{:S(2)}) copy-start(bf16[128,256]{1,0:T(8,128)(2,1)} %param.20) | copy-start | bytes 196612
  64.9 67.1 %collective-permute-start.3 = (bf16[128,128]{0,1:T(8,128)(2,1)}, bf16[128,128]{0,1:T(8,128)(2,1)}, u32[]{:S(2)}, u32[]{:S(2)}) collective-permute-start(bf16[128,128]{0,1:T(8,128)(2,1)} %fusion.7), channel_id=1, source_target_pairs={{0,4},{1,5},{2,6},{3,7},{4,0},{5,1},{6,2},{7,3},{8,12},{9,13},{10,... | collective-permute-start | bytes 98312 | tf_op jit(solution)/shard_map/ppermute | solution.py:31
  72.1 14.9 %copy-start.24 = (s32[128,4]{0,1:T(4,128)S(1)}, s32[128,4]{0,1:T(4,128)}, u32[]{:S(2)}) copy-start(s32[128,4]{0,1:T(4,128)} %param.29) | copy-start | bytes 6148
  72.9 14.1 %copy-start.25 = (s32[128,4]{0,1:T(4,128)S(1)}, s32[128,4]{0,1:T(4,128)}, u32[]{:S(2)}) copy-start(s32[128,4]{0,1:T(4,128)} %param.29) | copy-start | bytes 6148
  72.9 14.9 %copy-start.23 = (f32[2,2,1,128]{3,2,1,0:T(1,128)S(1)}, f32[2,2,1,128]{3,2,1,0:T(1,128)}, u32[]{:S(2)}) copy-start(f32[2,2,1,128]{3,2,1,0:T(1,128)} %get-tuple-element.120) | copy-start | bytes 6148
  75.7 43.9 %all-to-all-start.2 = ((bf16[32,16,512]{2,1,0:T(8,128)(2,1)}), bf16[32,16,512]{2,1,0:T(8,128)(2,1)S(1)}, u32[]{:S(2)}, u32[]{:S(2)}) async-start(bf16[32,16,512]{2,1,0:T(8,128)(2,1)} %bitcast.130), calls=%async_computation.2 | async-start | bytes 1048576 | tf_op jit(solution)/shard_map/all_to_all | solution.py:35
  119.6 61.1 %copy-start.4 = (bf16[32,16,512]{2,1,0:T(8,128)(2,1)}, bf16[32,16,512]{2,1,0:T(8,128)(2,1)S(1)}, u32[]{:S(2)}) copy-start(bf16[32,16,512]{2,1,0:T(8,128)(2,1)S(1)} %all-to-all-done.2) | copy-start | bytes 1572868
  119.6 18.3 %all-to-all-start.1 = ((bf16[32,8,128]{2,1,0:T(8,128)(2,1)}), bf16[32,8,128]{2,1,0:T(8,128)(2,1)}, u32[]{:S(2)}, u32[]{:S(2)}) async-start(bf16[32,8,128]{2,1,0:T(8,128)(2,1)} %copy.195), calls=%async_computation.1 | async-start | bytes 131072 | tf_op jit(solution)/shard_map/all_to_all | solution.py:35
  124.5 28.0 %collective-permute-start.6 = (bf16[512,512]{1,0:T(8,128)(2,1)S(1)}, bf16[512,512]{1,0:T(8,128)(2,1)S(1)}, u32[]{:S(2)}, u32[]{:S(2)}) collective-permute-start(bf16[512,512]{1,0:T(8,128)(2,1)S(1)} %bitcast.123), channel_id=1, source_target_pairs={{0,2},{1,3},{2,4},{3,5},{4,6},{5,7},{6,0},{7,1},{8,10},{9,11},{10,... | collective-permute-start | bytes 1572872 | tf_op jit(solution)/shard_map/ppermute | solution.py:26
  127.1 27.7 %collective-permute-start.7 = (bf16[512,512]{1,0:T(8,128)(2,1)S(1)}, bf16[512,512]{1,0:T(8,128)(2,1)}, u32[]{:S(2)}, u32[]{:S(2)}) collective-permute-start(bf16[512,512]{1,0:T(8,128)(2,1)S(1)} %bitcast.124), channel_id=1, source_target_pairs={{0,6},{1,7},{2,0},{3,1},{4,2},{5,3},{6,4},{7,5},{8,14},{9,15},{10,... | collective-permute-start | bytes 1572872 | tf_op jit(solution)/shard_map/ppermute | solution.py:26
  152.5 2.2 copy-start.5
  171.8 12.5 %collective-permute-start.8 = (bf16[256,512]{1,0:T(8,128)(2,1)}, bf16[256,512]{1,0:T(8,128)(2,1)S(1)}, u32[]{:S(2)}, u32[]{:S(2)}) collective-permute-start(bf16[256,512]{1,0:T(8,128)(2,1)} %get-tuple-element.41), channel_id=1, source_target_pairs={{0,2},{1,3},{2,4},{3,5},{4,6},{5,7},{6,0},{7,1},{8,10},{9,11},{10,... | collective-permute-start | bytes 786440 | tf_op jit(solution)/shard_map/ppermute | solution.py:26
  175.0 14.4 %collective-permute-start.9 = (bf16[256,512]{1,0:T(8,128)(2,1)}, bf16[256,512]{1,0:T(8,128)(2,1)}, u32[]{:S(2)}, u32[]{:S(2)}) collective-permute-start(bf16[256,512]{1,0:T(8,128)(2,1)} %get-tuple-element.42), channel_id=1, source_target_pairs={{0,6},{1,7},{2,0},{3,1},{4,2},{5,3},{6,4},{7,5},{8,14},{9,15},{10,... | collective-permute-start | bytes 786440 | tf_op jit(solution)/shard_map/ppermute | solution.py:26
  181.0 29.7 %copy-start.20 = (bf16[128,256]{1,0:T(8,128)(2,1)S(1)}, bf16[128,256]{1,0:T(8,128)(2,1)}, u32[]{:S(2)}) copy-start(bf16[128,256]{1,0:T(8,128)(2,1)} %param.23) | copy-start | bytes 196612
  181.0 29.7 %copy-start.30 = (f32[256]{0:T(256)S(1)}, f32[256]{0:T(256)}, u32[]{:S(2)}) copy-start(f32[256]{0:T(256)} %param.26) | copy-start | bytes 3076
  184.2 5.1 %copy-start.13 = (bf16[256,512]{1,0:T(8,128)(2,1)}, bf16[256,512]{1,0:T(8,128)(2,1)S(1)}, u32[]{:S(2)}) copy-start(bf16[256,512]{1,0:T(8,128)(2,1)S(1)} %collective-permute-done.8.refs_3_) | copy-start | bytes 786436
  193.8 23.3 %collective-permute-start.11 = (bf16[512,256]{1,0:T(8,128)(2,1)}, bf16[512,256]{1,0:T(8,128)(2,1)S(1)}, u32[]{:S(2)}, u32[]{:S(2)}) collective-permute-start(bf16[512,256]{1,0:T(8,128)(2,1)} %get-tuple-element.43.refs_0_), channel_id=1, source_target_pairs={{0,2},{1,3},{2,4},{3,5},{4,6},{5,7},{6,0},{7,1},{8,10},{9,11},{10,... | collective-permute-start | bytes 786440 | tf_op jit(solution)/shard_map/ppermute | solution.py:26
  196.0 21.1 %collective-permute-start.12 = (bf16[512,256]{1,0:T(8,128)(2,1)}, bf16[512,256]{1,0:T(8,128)(2,1)S(1)}, u32[]{:S(2)}, u32[]{:S(2)}) collective-permute-start(bf16[512,256]{1,0:T(8,128)(2,1)} %get-tuple-element.43.refs_0_), channel_id=1, source_target_pairs={{0,6},{1,7},{2,0},{3,1},{4,2},{5,3},{6,4},{7,5},{8,14},{9,15},{10,... | collective-permute-start | bytes 786440 | tf_op jit(solution)/shard_map/ppermute | solution.py:26
  201.3 12.3 %collective-permute-start.13 = (bf16[256,256]{1,0:T(8,128)(2,1)}, bf16[256,256]{1,0:T(8,128)(2,1)S(1)}, u32[]{:S(2)}, u32[]{:S(2)}) collective-permute-start(bf16[256,256]{1,0:T(8,128)(2,1)} %get-tuple-element.44), channel_id=1, source_target_pairs={{0,4},{1,5},{2,6},{3,7},{4,0},{5,1},{6,2},{7,3},{8,12},{9,13},{10,... | collective-permute-start | bytes 393224 | tf_op jit(solution)/shard_map/ppermute | solution.py:26
  204.3 12.8 %collective-permute-start.14 = (bf16[256,256]{1,0:T(8,128)(2,1)}, bf16[256,256]{1,0:T(8,128)(2,1)S(1)}, u32[]{:S(2)}, u32[]{:S(2)}) collective-permute-start(bf16[256,256]{1,0:T(8,128)(2,1)} %get-tuple-element.45), channel_id=1, source_target_pairs={{0,4},{1,5},{2,6},{3,7},{4,0},{5,1},{6,2},{7,3},{8,12},{9,13},{10,... | collective-permute-start | bytes 393224 | tf_op jit(solution)/shard_map/ppermute | solution.py:26
  210.8 0.8 copy-start.22
  211.6 30.1 %collective-permute-start.4 = (bf16[128,256]{0,1:T(8,128)(2,1)S(1)}, bf16[128,256]{0,1:T(8,128)(2,1)S(1)}, u32[]{:S(2)}, u32[]{:S(2)}) collective-permute-start(bf16[128,256]{0,1:T(8,128)(2,1)S(1)} %copy-done.22), channel_id=1, source_target_pairs={{0,2},{1,3},{2,0},{3,1},{4,6},{5,7},{6,4},{7,5},{8,10},{9,11},{10,... | collective-permute-start | bytes 196616 | tf_op jit(solution)/shard_map/ppermute | solution.py:31
  213.6 3.5 %copy-start.16 = (bf16[256,256]{1,0:T(8,128)(2,1)}, bf16[256,256]{1,0:T(8,128)(2,1)S(1)}, u32[]{:S(2)}) copy-start(bf16[256,256]{1,0:T(8,128)(2,1)S(1)} %collective-permute-done.13.refs_3_) | copy-start | bytes 393220
  221.8 19.9 %copy-start.10 = (bf16[128,128]{0,1:T(8,128)(2,1)S(1)}, bf16[128,128]{0,1:T(8,128)(2,1)}, u32[]{:S(2)}) copy-start(bf16[128,128]{0,1:T(8,128)(2,1)} %copy-done.9) | copy-start | bytes 98308
  221.8 19.9 %copy-start.12 = (bf16[128,128]{0,1:T(8,128)(2,1)S(1)}, bf16[128,128]{0,1:T(8,128)(2,1)}, u32[]{:S(2)}) copy-start(bf16[128,128]{0,1:T(8,128)(2,1)} %copy-done.11) | copy-start | bytes 98308
  221.8 51.2 %all-to-all-start.3 = ((bf16[32,16,512]{2,1,0:T(8,128)(2,1)}), bf16[32,16,512]{2,1,0:T(8,128)(2,1)S(1)}, u32[]{:S(2)}, u32[]{:S(2)}) async-start(bf16[32,16,512]{2,1,0:T(8,128)(2,1)} %bitcast.121), calls=%async_computation.3 | async-start | bytes 1048576 | tf_op jit(solution)/shard_map/all_to_all | solution.py:35
  239.7 9.1 %collective-permute-start = (bf16[2,2,16,2048]{3,2,0,1:T(8,128)(2,1)S(1)}, bf16[2,2,16,2048]{3,2,0,1:T(8,128)(2,1)S(1)}, u32[]{:S(2)}, u32[]{:S(2)}) collective-permute-start(bf16[2,2,16,2048]{3,2,0,1:T(8,128)(2,1)S(1)} %fusion.15), channel_id=1, source_target_pairs={{0,1},{1,0},{2,3},{3,2},{4,5},{5,4},{6,7},{7,6},{8,9},{9,8},{10,11... | collective-permute-start | bytes 786440 | tf_op jit(solution)/shard_map/ppermute | solution.py:31
  241.8 11.9 %collective-permute-start.5 = (bf16[128,512]{0,1:T(8,128)(2,1)S(1)}, bf16[128,512]{0,1:T(8,128)(2,1)S(1)}, u32[]{:S(2)}, u32[]{:S(2)}) collective-permute-start(bf16[128,512]{0,1:T(8,128)(2,1)S(1)} %pad_maximum_fusion.1), channel_id=1, source_target_pairs={{0,1},{1,0},{2,3},{3,2},{4,5},{5,4},{6,7},{7,6},{8,9},{9,8},{10,11... | collective-permute-start | bytes 393224 | tf_op jit(solution)/shard_map/ppermute | solution.py:31
  248.9 24.1 %copy-start.26 = (s32[128,32]{0,1:T(8,128)S(1)}, s32[128,32]{0,1:T(8,128)}, u32[]{:S(2)}) copy-start(s32[128,32]{0,1:T(8,128)} %fusion.8) | copy-start | bytes 49156
  248.9 24.1 %copy-start.31 = (s32[16]{0:T(128)S(1)}, s32[16]{0:T(128)}, u32[]{:S(2)}) copy-start(s32[16]{0:T(128)} %iota_add_fusion) | copy-start | bytes 196
  248.9 8.8 %collective-permute-start.1 = (bf16[2,16,2048]{2,1,0:T(8,128)(2,1)S(1)}, bf16[2,16,2048]{2,1,0:T(8,128)(2,1)S(1)}, u32[]{:S(2)}, u32[]{:S(2)}) collective-permute-start(bf16[2,16,2048]{2,1,0:T(8,128)(2,1)S(1)} %fusion.32), channel_id=1, source_target_pairs={{0,2},{1,3},{2,0},{3,1},{4,6},{5,7},{6,4},{7,5},{8,10},{9,11},{10,... | collective-permute-start | bytes 393224 | tf_op jit(solution)/shard_map/ppermute | solution.py:31
  257.8 18.7 %collective-permute-start.2 = (bf16[16,2048]{1,0:T(8,128)(2,1)S(1)}, bf16[16,2048]{1,0:T(8,128)(2,1)S(1)}, u32[]{:S(2)}, u32[]{:S(2)}) collective-permute-start(bf16[16,2048]{1,0:T(8,128)(2,1)S(1)} %fusion.61), channel_id=1, source_target_pairs={{0,4},{1,5},{2,6},{3,7},{4,0},{5,1},{6,2},{7,3},{8,12},{9,13},{10,... | collective-permute-start | bytes 196616 | tf_op jit(solution)/shard_map/ppermute | solution.py:31
  274.0 5.6 %copy-start.2 = (bf16[2,2,2,128,256]{4,3,2,1,0:T(8,128)(2,1)S(1)}, bf16[2,2,2,128,256]{4,3,2,1,0:T(8,128)(2,1)}, u32[]{:S(2)}) copy-start(bf16[2,2,2,128,256]{4,3,2,1,0:T(8,128)(2,1)} %copy.201) | copy-start | bytes 1572868
  274.5 5.0 %collective-permute-start.16 = (bf16[128,256]{1,0:T(8,128)(2,1)S(1)}, bf16[128,256]{1,0:T(8,128)(2,1)S(1)}, u32[]{:S(2)}, u32[]{:S(2)}) collective-permute-start(bf16[128,256]{1,0:T(8,128)(2,1)S(1)} %slice.40), channel_id=1, source_target_pairs={{0,1},{1,0},{2,3},{3,2},{4,5},{5,4},{6,7},{7,6},{8,9},{9,8},{10,11... | collective-permute-start | bytes 196616 | tf_op jit(solution)/shard_map/ppermute | solution.py:31
  (5 other events, 3.3 us)

commit v6 on v5

--- a/solution.py
+++ b/solution.py
@@ -103,7 +103,8 @@
     earlier = at[None, :, None] < at[:, None, None]
     factors = jnp.where(earlier, jnp.exp(spans), 0.0)
     prefix = jnp.einsum("rqc,qcv->rcv", factors, updates, precision=HIGHEST_PRECISION)
-    returned = exchanged(prefix.astype(jnp.bfloat16), EP)
+    prefix = prefix.astype(jnp.bfloat16)
+    returned = exchanged(prefix, EP)
     return returned.astype(jnp.float32).reshape(channels, width)
 
 
@@ -225,27 +226,15 @@
     )(*operands)
 
 
-def halves_kernel(before, after, first, second, arrived):
+def halves_kernel(whole, first, second):
     middle = first.shape[0]
-    copies = [
-        pltpu.make_async_copy(before.at[pl.ds(0, middle), :], first, arrived.at[0]),
-        pltpu.make_async_copy(after.at[pl.ds(middle, middle), :], second, arrived.at[1]),
-    ]
-    for copy in copies:
-        copy.start()
-    for copy in copies:
-        copy.wait()
-
-
-def far_halves(before, after):
-    half = jax.ShapeDtypeStruct((before.shape[0] // 2, before.shape[1]), before.dtype)
-    return pl.pallas_call(
-        halves_kernel,
-        out_shape=(half, half),
-        in_specs=[ANY, ANY],
-        out_specs=(ANY, ANY),
-        scratch_shapes=[pltpu.SemaphoreType.DMA((2,))],
-    )(before, after)
+    first[...] = whole[:middle, :]
+    second[...] = whole[middle:, :]
+
+
+def halves_of(array):
+    half = jax.ShapeDtypeStruct((array.shape[0] // 2, array.shape[1]), array.dtype)
+    return in_vmem(halves_kernel, (half, half), array)
 
 
 def select_kernel(experts, hidden_state, gain, index, normed, outgoing):
@@ -412,8 +401,7 @@
 
     before = shifted(chunk, "tp", 2)
     after = shifted(chunk, "tp", -2)
-    first, second = far_halves(before, after)
-    far = [shifted(first, "tp", 2), shifted(second, "tp", -2)]
+    far = [shifted(half, "tp", step) for half, step in zip(halves_of(chunk), (4, -4))]
     part_shape = jax.ShapeDtypeStruct((middle, 2 * units), jnp.bfloat16)
     hidden, hidden_first, hidden_second = fetching(
         hidden_kernel,
@@ -425,9 +413,9 @@
         own_in,
         partner_in,
     )
-    far = [shifted(hidden_first, "tp", 4), shifted(hidden_second, "tp", -4)]
     before = shifted(hidden, "tp", 2)
     after = shifted(hidden, "tp", -2)
+    far = [shifted(hidden_first, "tp", 4), shifted(hidden_second, "tp", -4)]
     answers = fetching(
         down_kernel,
         jax.ShapeDtypeStruct((chunk.shape[0], 2 * width_out), jnp.bfloat16),

time: 282 us -> 279 us (0.989)
  starting transfers between devices: 142 us -> 158 us
  Pallas kernels: 27.1 us -> 12 us
  waiting for transfers between devices: 81.2 us -> 75.5 us
  matrix products: 9.78 us -> 13.2 us
    pallas_call x1 -> x0, Pallas kernels: 17 us -> none  [far_halves(): pl.pallas_call(halves_kernel, out_shape=(half, half), in_specs=[ANY, ANY]...]
    ppermute x9, starting transfers between devices: 31.9 us -> 39.5 us  [swapped(): return lax.ppermute(array, axis, [(i, i ^ bit) for i in range(count)])]
    ppermute x8, starting transfers between devices: 31.6 us -> 37.9 us  [shifted(): lax.ppermute(array, axis, [(i, (i + step) % count) for i in range(count)])]
    all_to_all x4, waiting for transfers between devices: 44 us -> 40 us  [exchanged(): return lax.all_to_all(array, axis, split_axis=0, concat_axis=0, tiled=True)]
  transfers between devices with their start and end apart: 21 -> 21, of which waited for: 12 -> 12; matrix products, arithmetic and copies ran while one was open for 8% -> 9% of each run, Pallas kernels for 10% -> 4%
where the time goes in v6:
time: 279 us; the launch traced here: 278 us
  starting transfers between devices  158 us (57%)
  waiting for transfers between devices  75.5 us (27%)
  matrix products  13.2 us (5%)
  Pallas kernels  12 us (4%)
  other arithmetic  10.6 us (4%)
  local copies, waits for them, and re-layouts  7.23 us (3%)
    all_to_all x4, starting transfers between devices, exchanged(): return lax.all_to_all(array, axis, split_axis=0, concat_axis=0, tiled=True)  80.4 us
    all_to_all x4, waiting for transfers between devices, exchanged(): return lax.all_to_all(array, axis, split_axis=0, concat_axis=0, tiled=True)  40 us
    ppermute x9, starting transfers between devices, swapped(): return lax.ppermute(array, axis, [(i, i ^ bit) for i in range(count)])  39.5 us
    ppermute x8, starting transfers between devices, shifted(): lax.ppermute(array, axis, [(i, (i + step) % count) for i in range(count)])  37.9 us
    ppermute x8, waiting for transfers between devices, shifted(): lax.ppermute(array, axis, [(i, (i + step) % count) for i in range(count)])  24.6 us
    ppermute x9, waiting for transfers between devices, swapped(): return lax.ppermute(array, axis, [(i, i ^ bit) for i in range(count)])  10.9 us
    pallas_call x2, Pallas kernels, fetching(): pl.pallas_call(body, out_shape=shapes, in_specs=[ANY] * count, out_specs=...  7.68 us
  transfers between devices with their start and end apart: 21, of which 12 were waited for; matrix products, arithmetic and copies ran while one was open for 9% of the time, Pallas kernels for 4%

profile of v6, /device:TPU:65, one launch (start us, length us, event | category | flops | bytes accessed | tf_op | source)
XLA Modules:
  0.0 277.8 jit_solution(10717699345702671429)
XLA Ops:
  0.7 1.4 pad_maximum_fusion.refs_5_
  2.1 4.2 %collective-permute-start.10 = (bf16[2048,256]{1,0:T(8,128)(2,1)S(1)}, bf16[2048,256]{1,0:T(8,128)(2,1)}, u32[]{:S(2)}, u32[]{:S(2)}) collective-permute-start(bf16[2048,256]{1,0:T(8,128)(2,1)S(1)} %pad_maximum_fusion.refs_5_), channel_id=1, source_target_pairs={{0,1},{1,0},{2,3},{3,2},{4,5},{5,4},{6,7},{7,6},{8,9},{9,8},{10,11... | collective-permute-start | bytes 3145736 | tf_op jit(solution)/shard_map/ppermute | solution.py:31
  6.3 2.0 collective-permute-start.15
  10.1 1.7 while.13
  12.9 45.0 %all-to-all-start = ((bf16[32,8,256]{2,1,0:T(8,128)(2,1)}), bf16[32,8,256]{2,1,0:T(8,128)(2,1)S(1)}, u32[]{:S(2)}, u32[]{:S(2)}) async-start(bf16[32,8,256]{2,1,0:T(8,128)(2,1)} %fusion.31), calls=%async_computation | async-start | bytes 262144 | tf_op jit(solution)/shard_map/all_to_all | solution.py:35
  57.9 2.4 shard_map.185
  60.3 1.4 fusion.80
  61.8 2.0 fusion.7
  63.9 7.7 %collective-permute-start.3 = (bf16[128,128]{0,1:T(8,128)(2,1)}, bf16[128,128]{0,1:T(8,128)(2,1)}, u32[]{:S(2)}, u32[]{:S(2)}) collective-permute-start(bf16[128,128]{0,1:T(8,128)(2,1)} %fusion.7), channel_id=1, source_target_pairs={{0,4},{1,5},{2,6},{3,7},{4,0},{5,1},{6,2},{7,3},{8,12},{9,13},{10,... | collective-permute-start | bytes 98312 | tf_op jit(solution)/shard_map/ppermute | solution.py:31
  71.6 1.1 copy.201
  74.4 12.3 %all-to-all-start.2 = ((bf16[32,16,512]{2,1,0:T(8,128)(2,1)}), bf16[32,16,512]{2,1,0:T(8,128)(2,1)S(1)}, u32[]{:S(2)}, u32[]{:S(2)}) async-start(bf16[32,16,512]{2,1,0:T(8,128)(2,1)} %bitcast.131), calls=%async_computation.2 | async-start | bytes 1048576 | tf_op jit(solution)/shard_map/all_to_all | solution.py:35
  88.9 1.1 convolution_select_fusion
  89.9 1.0 fusion.63
  91.1 1.2 fusion.4
  93.1 26.9 %all-to-all-done.2 = bf16[32,16,512]{2,1,0:T(8,128)(2,1)S(1)} async-done(((bf16[32,16,512]{2,1,0:T(8,128)(2,1)}), bf16[32,16,512]{2,1,0:T(8,128)(2,1)S(1)}, u32[]{:S(2)}, u32[]{:S(2)}) %all-to-all-start.2) | async-done | bytes 524320 | tf_op jit(solution)/shard_map/all_to_all | solution.py:35
  120.1 4.8 %all-to-all-start.1 = ((bf16[32,8,128]{2,1,0:T(8,128)(2,1)}), bf16[32,8,128]{2,1,0:T(8,128)(2,1)}, u32[]{:S(2)}, u32[]{:S(2)}) async-start(bf16[32,8,128]{2,1,0:T(8,128)(2,1)} %copy.195), calls=%async_computation.1 | async-start | bytes 131072 | tf_op jit(solution)/shard_map/all_to_all | solution.py:35
  126.4 2.5 collective-permute-start.6
  128.9 4.9 %collective-permute-start.7 = (bf16[512,512]{1,0:T(8,128)(2,1)S(1)}, bf16[512,512]{1,0:T(8,128)(2,1)}, u32[]{:S(2)}, u32[]{:S(2)}) collective-permute-start(bf16[512,512]{1,0:T(8,128)(2,1)S(1)} %bitcast.120), channel_id=1, source_target_pairs={{0,6},{1,7},{2,0},{3,1},{4,2},{5,3},{6,4},{7,5},{8,14},{9,15},{10,... | collective-permute-start | bytes 1572872 | tf_op jit(solution)/shard_map/ppermute | solution.py:26
  133.9 4.6 %all-to-all-done.1 = bf16[32,8,128]{2,1,0:T(8,128)(2,1)} async-done(((bf16[32,8,128]{2,1,0:T(8,128)(2,1)}), bf16[32,8,128]{2,1,0:T(8,128)(2,1)}, u32[]{:S(2)}, u32[]{:S(2)}) %all-to-all-start.1) | async-done | bytes 65568 | tf_op jit(solution)/shard_map/all_to_all | solution.py:35
  138.4 1.5 bitcast_convert_fusion
  140.0 1.9 shard_map.186
  141.9 1.9 collective-permute-start.8
  143.8 7.3 %collective-permute-start.9 = (bf16[256,512]{1,0:T(8,128)(2,1)}, bf16[256,512]{1,0:T(8,128)(2,1)S(1)}, u32[]{:S(2)}, u32[]{:S(2)}) collective-permute-start(bf16[256,512]{1,0:T(8,128)(2,1)} %get-tuple-element.42), channel_id=1, source_target_pairs={{0,4},{1,5},{2,6},{3,7},{4,0},{5,1},{6,2},{7,3},{8,12},{9,13},{10,... | collective-permute-start | bytes 786440 | tf_op jit(solution)/shard_map/ppermute | solution.py:26
  151.1 1.6 multiply_reduce_fusion
  152.9 9.6 %collective-permute-done.8.refs_3_ = bf16[256,512]{1,0:T(8,128)(2,1)} collective-permute-done((bf16[256,512]{1,0:T(8,128)(2,1)}, bf16[256,512]{1,0:T(8,128)(2,1)}, u32[]{:S(2)}, u32[]{:S(2)}) %collective-permute-start.8) | collective-permute-done | bytes 262176 | tf_op jit(solution)/shard_map/ppermute | solution.py:26
  162.6 8.2 %collective-permute-done.9.refs_4_ = bf16[256,512]{1,0:T(8,128)(2,1)S(1)} collective-permute-done((bf16[256,512]{1,0:T(8,128)(2,1)}, bf16[256,512]{1,0:T(8,128)(2,1)S(1)}, u32[]{:S(2)}, u32[]{:S(2)}) %collective-permute-start.9) | collective-permute-done | bytes 262176 | tf_op jit(solution)/shard_map/ppermute | solution.py:26
  171.4 4.5 %shard_map.187 = (bf16[512,256]{1,0:T(8,128)(2,1)}, bf16[256,256]{1,0:T(8,128)(2,1)}, bf16[256,256]{1,0:T(8,128)(2,1)}) custom-call(bf16[512,512]{1,0:T(8,128)(2,1)} %bitcast.122, bf16[512,512]{1,0:T(8,128)(2,1)} %collective-permute-done.6.refs_1_, bf16[512,512]{1,0:T(8,128)(2,1)} %collective-permute-done.7.refs_2_, ...), custom_call_target="tpu_custom_call" | custom-call | tf_op jit(solution)/shard_map/pallas_call | solution.py:219
  175.9 10.0 %collective-permute-start.11 = (bf16[512,256]{1,0:T(8,128)(2,1)}, bf16[512,256]{1,0:T(8,128)(2,1)S(1)}, u32[]{:S(2)}, u32[]{:S(2)}) collective-permute-start(bf16[512,256]{1,0:T(8,128)(2,1)} %get-tuple-element.43.refs_0_), channel_id=1, source_target_pairs={{0,2},{1,3},{2,4},{3,5},{4,6},{5,7},{6,0},{7,1},{8,10},{9,11},{10,... | collective-permute-start | bytes 786440 | tf_op jit(solution)/shard_map/ppermute | solution.py:26
  185.9 2.0 collective-permute-start.12
  187.9 5.2 %collective-permute-start.13 = (bf16[256,256]{1,0:T(8,128)(2,1)}, bf16[256,256]{1,0:T(8,128)(2,1)S(1)}, u32[]{:S(2)}, u32[]{:S(2)}) collective-permute-start(bf16[256,256]{1,0:T(8,128)(2,1)} %get-tuple-element.44), channel_id=1, source_target_pairs={{0,4},{1,5},{2,6},{3,7},{4,0},{5,1},{6,2},{7,3},{8,12},{9,13},{10,... | collective-permute-start | bytes 393224 | tf_op jit(solution)/shard_map/ppermute | solution.py:26
  193.1 4.0 %collective-permute-start.14 = (bf16[256,256]{1,0:T(8,128)(2,1)}, bf16[256,256]{1,0:T(8,128)(2,1)S(1)}, u32[]{:S(2)}, u32[]{:S(2)}) collective-permute-start(bf16[256,256]{1,0:T(8,128)(2,1)} %get-tuple-element.45), channel_id=1, source_target_pairs={{0,4},{1,5},{2,6},{3,7},{4,0},{5,1},{6,2},{7,3},{8,12},{9,13},{10,... | collective-permute-start | bytes 393224 | tf_op jit(solution)/shard_map/ppermute | solution.py:26
  197.4 1.2 fusion.59
  198.6 4.3 %collective-permute-start.4 = (bf16[128,256]{0,1:T(8,128)(2,1)}, bf16[128,256]{0,1:T(8,128)(2,1)}, u32[]{:S(2)}, u32[]{:S(2)}) collective-permute-start(bf16[128,256]{0,1:T(8,128)(2,1)} %pad_maximum_fusion.2), channel_id=1, source_target_pairs={{0,2},{1,3},{2,0},{3,1},{4,6},{5,7},{6,4},{7,5},{8,10},{9,11},{10,... | collective-permute-start | bytes 196616 | tf_op jit(solution)/shard_map/ppermute | solution.py:31
  202.9 1.9 collective-permute-done.13.refs_3_
  204.8 4.8 %collective-permute-done.14.refs_4_ = bf16[256,256]{1,0:T(8,128)(2,1)S(1)} collective-permute-done((bf16[256,256]{1,0:T(8,128)(2,1)}, bf16[256,256]{1,0:T(8,128)(2,1)S(1)}, u32[]{:S(2)}, u32[]{:S(2)}) %collective-permute-start.14) | collective-permute-done | bytes 131104 | tf_op jit(solution)/shard_map/ppermute | solution.py:26
  211.7 3.2 %shard_map.188 = bf16[512,512]{1,0:T(8,128)(2,1)} custom-call(bf16[512,256]{1,0:T(8,128)(2,1)} %get-tuple-element.43.refs_0_, bf16[512,256]{1,0:T(8,128)(2,1)} %copy-done.12, bf16[512,256]{1,0:T(8,128)(2,1)} %copy-done.14, bf16[256,256]{1,0:T(8,128)(2,1)} %copy-done.15, bf16[256,256]{1,0:T(8,128)(2,1)} %copy-done.16, bf16[1024,256]{1,0:T(8,128)(2,1)} %bitcast.31.refs_5_, ...), custom_call_target="tpu_custom_call" | custom-call | tf_op jit(solution)/shard_map/pallas_call | solution.py:219
  214.9 18.2 %all-to-all-start.3 = ((bf16[32,16,512]{2,1,0:T(8,128)(2,1)}), bf16[32,16,512]{2,1,0:T(8,128)(2,1)S(1)}, u32[]{:S(2)}, u32[]{:S(2)}) async-start(bf16[32,16,512]{2,1,0:T(8,128)(2,1)} %bitcast.125), calls=%async_computation.3 | async-start | bytes 1048576 | tf_op jit(solution)/shard_map/all_to_all | solution.py:35
  233.2 7.0 %collective-permute-start = (bf16[2,2,16,2048]{3,2,0,1:T(8,128)(2,1)S(1)}, bf16[2,2,16,2048]{3,2,0,1:T(8,128)(2,1)S(1)}, u32[]{:S(2)}, u32[]{:S(2)}) collective-permute-start(bf16[2,2,16,2048]{3,2,0,1:T(8,128)(2,1)S(1)} %fusion.15), channel_id=1, source_target_pairs={{0,1},{1,0},{2,3},{3,2},{4,5},{5,4},{6,7},{7,6},{8,9},{9,8},{10,11... | collective-permute-start | bytes 786440 | tf_op jit(solution)/shard_map/ppermute | solution.py:31
  240.2 0.9 broadcast_select_fusion.3
  241.1 2.0 collective-permute-start.5
  243.1 3.1 %collective-permute-done = bf16[2,2,16,2048]{3,2,0,1:T(8,128)(2,1)S(1)} collective-permute-done((bf16[2,2,16,2048]{3,2,0,1:T(8,128)(2,1)S(1)}, bf16[2,2,16,2048]{3,2,0,1:T(8,128)(2,1)S(1)}, u32[]{:S(2)}, u32[]{:S(2)}) %collective-permute-start) | collective-permute-done | bytes 262176 | tf_op jit(solution)/shard_map/ppermute | solution.py:31
  246.3 2.0 collective-permute-start.1
  249.0 5.8 %collective-permute-done.1 = bf16[2,16,2048]{2,1,0:T(8,128)(2,1)S(1)} collective-permute-done((bf16[2,16,2048]{2,1,0:T(8,128)(2,1)S(1)}, bf16[2,16,2048]{2,1,0:T(8,128)(2,1)S(1)}, u32[]{:S(2)}, u32[]{:S(2)}) %collective-permute-start.1) | collective-permute-done | bytes 131104 | tf_op jit(solution)/shard_map/ppermute | solution.py:31
  254.9 3.5 %collective-permute-start.2 = (bf16[16,2048]{1,0:T(8,128)(2,1)S(1)}, bf16[16,2048]{1,0:T(8,128)(2,1)S(1)}, u32[]{:S(2)}, u32[]{:S(2)}) collective-permute-start(bf16[16,2048]{1,0:T(8,128)(2,1)S(1)} %fusion.61), channel_id=1, source_target_pairs={{0,4},{1,5},{2,6},{3,7},{4,0},{5,1},{6,2},{7,3},{8,12},{9,13},{10,... | collective-permute-start | bytes 196616 | tf_op jit(solution)/shard_map/ppermute | solution.py:31
  258.4 8.1 %all-to-all-done.3 = bf16[32,16,512]{2,1,0:T(8,128)(2,1)S(1)} async-done(((bf16[32,16,512]{2,1,0:T(8,128)(2,1)}), bf16[32,16,512]{2,1,0:T(8,128)(2,1)S(1)}, u32[]{:S(2)}, u32[]{:S(2)}) %all-to-all-start.3) | async-done | bytes 524320 | tf_op jit(solution)/shard_map/all_to_all | solution.py:35
  268.0 7.0 %collective-permute-start.16 = (bf16[128,256]{1,0:T(8,128)(2,1)S(1)}, bf16[128,256]{1,0:T(8,128)(2,1)S(1)}, u32[]{:S(2)}, u32[]{:S(2)}) collective-permute-start(bf16[128,256]{1,0:T(8,128)(2,1)S(1)} %slice.40), channel_id=1, source_target_pairs={{0,1},{1,0},{2,3},{3,2},{4,5},{5,4},{6,7},{7,6},{8,9},{9,8},{10,11... | collective-permute-start | bytes 196616 | tf_op jit(solution)/shard_map/ppermute | solution.py:31
  275.6 1.3 collective-permute-done.16
  276.9 0.9 fusion.5
  (124 shorter events, 16.9 us)
Async XLA Ops:
  0.6 196.7 %copy-start = (bf16[256,2048]{1,0:T(8,128)(2,1)S(1)}, bf16[256,2048]{1,0:T(8,128)(2,1)}, u32[]{:S(2)}) copy-start(bf16[256,2048]{1,0:T(8,128)(2,1)} %param.27) | copy-start | bytes 3145732
  0.6 7.7 %copy-start.23 = (f32[128,2]{0,1:T(2,128)S(1)}, f32[128,2]{0,1:T(2,128)}, u32[]{:S(2)}) copy-start(f32[128,2]{0,1:T(2,128)} %param.25) | copy-start | bytes 3076
  0.7 8.0 %copy-start.17 = (bf16[128,256]{1,0:T(8,128)(2,1)S(1)}, bf16[128,256]{1,0:T(8,128)(2,1)}, u32[]{:S(2)}) copy-start(bf16[128,256]{1,0:T(8,128)(2,1)} %param.21) | copy-start | bytes 196612
  0.7 8.0 %copy-start.24 = (f32[256]{0:T(256)S(1)}, f32[256]{0:T(256)}, u32[]{:S(2)}) copy-start(f32[256]{0:T(256)} %param.24) | copy-start | bytes 3076
  2.1 8.1 %copy-start.2 = (bf16[2048,256]{1,0:T(8,128)(2,1)}, bf16[2048,256]{1,0:T(8,128)(2,1)S(1)}, u32[]{:S(2)}) copy-start(bf16[2048,256]{1,0:T(8,128)(2,1)S(1)} %pad_maximum_fusion.refs_5_) | copy-start | bytes 3145732
  2.1 7.6 %copy-start.19 = (bf16[128,256]{1,0:T(8,128)(2,1)S(1)}, bf16[128,256]{1,0:T(8,128)(2,1)}, u32[]{:S(2)}) copy-start(bf16[128,256]{1,0:T(8,128)(2,1)} %param.22) | copy-start | bytes 196612
  2.1 141.7 %collective-permute-start.10 = (bf16[2048,256]{1,0:T(8,128)(2,1)S(1)}, bf16[2048,256]{1,0:T(8,128)(2,1)}, u32[]{:S(2)}, u32[]{:S(2)}) collective-permute-start(bf16[2048,256]{1,0:T(8,128)(2,1)S(1)} %pad_maximum_fusion.refs_5_), channel_id=1, source_target_pairs={{0,1},{1,0},{2,3},{3,2},{4,5},{5,4},{6,7},{7,6},{8,9},{9,8},{10,11... | collective-permute-start | bytes 3145736 | tf_op jit(solution)/shard_map/ppermute | solution.py:31
  6.3 192.2 %collective-permute-start.15 = (bf16[1024,256]{1,0:T(8,128)(2,1)}, bf16[1024,256]{1,0:T(8,128)(2,1)}, u32[]{:S(2)}, u32[]{:S(2)}) collective-permute-start(bf16[1024,256]{1,0:T(8,128)(2,1)} %bitcast.31.refs_5_), channel_id=1, source_target_pairs={{0,1},{1,0},{2,3},{3,2},{4,5},{5,4},{6,7},{7,6},{8,9},{9,8},{10,11... | collective-permute-start | bytes 1572872 | tf_op jit(solution)/shard_map/ppermute | solution.py:31
  9.7 52.1 %copy-start.4 = (bf16[2,64,2,128]{3,2,1,0:T(2,128)(2,1)}, bf16[2,64,2,128]{3,2,1,0:T(2,128)(2,1)S(1)}, u32[]{:S(2)}) copy-start(bf16[2,64,2,128]{3,2,1,0:T(2,128)(2,1)S(1)} %reshape.214) | copy-start | bytes 196612
  11.8 48.5 %copy-start.5 = (bf16[2048,128]{1,0:T(8,128)(2,1)S(1)}, bf16[2048,128]{1,0:T(8,128)(2,1)}, u32[]{:S(2)}) copy-start(bf16[2048,128]{1,0:T(8,128)(2,1)} %param.35) | copy-start | bytes 1572868
  12.9 60.9 %all-to-all-start = ((bf16[32,8,256]{2,1,0:T(8,128)(2,1)}), bf16[32,8,256]{2,1,0:T(8,128)(2,1)S(1)}, u32[]{:S(2)}, u32[]{:S(2)}) async-start(bf16[32,8,256]{2,1,0:T(8,128)(2,1)} %fusion.31), calls=%async_computation | async-start | bytes 262144 | tf_op jit(solution)/shard_map/all_to_all | solution.py:35
  60.3 1.5 copy-start.3
  60.3 11.2 %copy-start.22 = (f32[128,4]{0,1:T(4,128)S(1)}, f32[128,4]{0,1:T(4,128)}, u32[]{:S(2)}) copy-start(f32[128,4]{0,1:T(4,128)} %param.30) | copy-start | bytes 6148
  61.8 11.5 %copy-start.18 = (bf16[128,256]{1,0:T(8,128)(2,1)S(1)}, bf16[128,256]{1,0:T(8,128)(2,1)}, u32[]{:S(2)}) copy-start(bf16[128,256]{1,0:T(8,128)(2,1)} %param.20) | copy-start | bytes 196612
  63.9 61.1 %collective-permute-start.3 = (bf16[128,128]{0,1:T(8,128)(2,1)}, bf16[128,128]{0,1:T(8,128)(2,1)}, u32[]{:S(2)}, u32[]{:S(2)}) collective-permute-start(bf16[128,128]{0,1:T(8,128)(2,1)} %fusion.7), channel_id=1, source_target_pairs={{0,4},{1,5},{2,6},{3,7},{4,0},{5,1},{6,2},{7,3},{8,12},{9,13},{10,... | collective-permute-start | bytes 98312 | tf_op jit(solution)/shard_map/ppermute | solution.py:31
  71.6 15.8 %copy-start.20 = (s32[128,4]{0,1:T(4,128)S(1)}, s32[128,4]{0,1:T(4,128)}, u32[]{:S(2)}) copy-start(s32[128,4]{0,1:T(4,128)} %param.29) | copy-start | bytes 6148
  73.8 0.7 copy-start.6
  74.4 45.6 %all-to-all-start.2 = ((bf16[32,16,512]{2,1,0:T(8,128)(2,1)}), bf16[32,16,512]{2,1,0:T(8,128)(2,1)S(1)}, u32[]{:S(2)}, u32[]{:S(2)}) async-start(bf16[32,16,512]{2,1,0:T(8,128)(2,1)} %bitcast.131), calls=%async_computation.2 | async-start | bytes 1048576 | tf_op jit(solution)/shard_map/all_to_all | solution.py:35
  86.8 4.2 %copy-start.7 = (bf16[32,8,256]{2,1,0:T(8,128)(2,1)S(1)}, bf16[32,8,256]{2,1,0:T(8,128)(2,1)}, u32[]{:S(2)}) copy-start(bf16[32,8,256]{2,1,0:T(8,128)(2,1)} %copy-done.6) | copy-start | bytes 393220
  86.8 5.5 %slice-start = ((bf16[32,8,256]{2,1,0:T(8,128)(2,1)}), bf16[32,8,128]{2,1,0:T(8,128)(2,1)S(1)}, s32[]{:S(2)}) async-start(bf16[32,8,256]{2,1,0:T(8,128)(2,1)} %copy-done.6), calls=%async_computation.4 | async-start | bytes 131072 | tf_op jit(solution)/shard_map/slice | solution.py:94
  120.1 19.9 %copy-start.1 = (bf16[32,16,512]{2,1,0:T(8,128)(2,1)}, bf16[32,16,512]{2,1,0:T(8,128)(2,1)S(1)}, u32[]{:S(2)}) copy-start(bf16[32,16,512]{2,1,0:T(8,128)(2,1)S(1)} %all-to-all-done.2) | copy-start | bytes 1572868
  120.1 18.3 %all-to-all-start.1 = ((bf16[32,8,128]{2,1,0:T(8,128)(2,1)}), bf16[32,8,128]{2,1,0:T(8,128)(2,1)}, u32[]{:S(2)}, u32[]{:S(2)}) async-start(bf16[32,8,128]{2,1,0:T(8,128)(2,1)} %copy.195), calls=%async_computation.1 | async-start | bytes 131072 | tf_op jit(solution)/shard_map/all_to_all | solution.py:35
  125.7 0.7 copy-start.8
  125.7 3.2 %copy-start.10 = (bf16[128,128]{0,1:T(8,128)(2,1)}, bf16[128,128]{0,1:T(8,128)(2,1)S(1)}, u32[]{:S(2)}) copy-start(bf16[128,128]{0,1:T(8,128)(2,1)S(1)} %get-tuple-element.124) | copy-start | bytes 98308
  126.4 44.3 %collective-permute-start.6 = (bf16[512,512]{1,0:T(8,128)(2,1)S(1)}, bf16[512,512]{1,0:T(8,128)(2,1)}, u32[]{:S(2)}, u32[]{:S(2)}) collective-permute-start(bf16[512,512]{1,0:T(8,128)(2,1)S(1)} %bitcast.119), channel_id=1, source_target_pairs={{0,2},{1,3},{2,4},{3,5},{4,6},{5,7},{6,0},{7,1},{8,10},{9,11},{10,... | collective-permute-start | bytes 1572872 | tf_op jit(solution)/shard_map/ppermute | solution.py:26
  128.9 41.8 %collective-permute-start.7 = (bf16[512,512]{1,0:T(8,128)(2,1)S(1)}, bf16[512,512]{1,0:T(8,128)(2,1)}, u32[]{:S(2)}, u32[]{:S(2)}) collective-permute-start(bf16[512,512]{1,0:T(8,128)(2,1)S(1)} %bitcast.120), channel_id=1, source_target_pairs={{0,6},{1,7},{2,0},{3,1},{4,2},{5,3},{6,4},{7,5},{8,14},{9,15},{10,... | collective-permute-start | bytes 1572872 | tf_op jit(solution)/shard_map/ppermute | solution.py:26
  141.9 20.7 %collective-permute-start.8 = (bf16[256,512]{1,0:T(8,128)(2,1)}, bf16[256,512]{1,0:T(8,128)(2,1)}, u32[]{:S(2)}, u32[]{:S(2)}) collective-permute-start(bf16[256,512]{1,0:T(8,128)(2,1)} %get-tuple-element.41), channel_id=1, source_target_pairs={{0,4},{1,5},{2,6},{3,7},{4,0},{5,1},{6,2},{7,3},{8,12},{9,13},{10,... | collective-permute-start | bytes 786440 | tf_op jit(solution)/shard_map/ppermute | solution.py:26
  143.8 26.9 %collective-permute-start.9 = (bf16[256,512]{1,0:T(8,128)(2,1)}, bf16[256,512]{1,0:T(8,128)(2,1)S(1)}, u32[]{:S(2)}, u32[]{:S(2)}) collective-permute-start(bf16[256,512]{1,0:T(8,128)(2,1)} %get-tuple-element.42), channel_id=1, source_target_pairs={{0,4},{1,5},{2,6},{3,7},{4,0},{5,1},{6,2},{7,3},{8,12},{9,13},{10,... | collective-permute-start | bytes 786440 | tf_op jit(solution)/shard_map/ppermute | solution.py:26
  170.7 0.7 copy-start.13
  175.9 33.7 %collective-permute-start.11 = (bf16[512,256]{1,0:T(8,128)(2,1)}, bf16[512,256]{1,0:T(8,128)(2,1)S(1)}, u32[]{:S(2)}, u32[]{:S(2)}) collective-permute-start(bf16[512,256]{1,0:T(8,128)(2,1)} %get-tuple-element.43.refs_0_), channel_id=1, source_target_pairs={{0,2},{1,3},{2,4},{3,5},{4,6},{5,7},{6,0},{7,1},{8,10},{9,11},{10,... | collective-permute-start | bytes 786440 | tf_op jit(solution)/shard_map/ppermute | solution.py:26
  185.9 24.4 %collective-permute-start.12 = (bf16[512,256]{1,0:T(8,128)(2,1)}, bf16[512,256]{1,0:T(8,128)(2,1)S(1)}, u32[]{:S(2)}, u32[]{:S(2)}) collective-permute-start(bf16[512,256]{1,0:T(8,128)(2,1)} %get-tuple-element.43.refs_0_), channel_id=1, source_target_pairs={{0,6},{1,7},{2,0},{3,1},{4,2},{5,3},{6,4},{7,5},{8,14},{9,15},{10,... | collective-permute-start | bytes 786440 | tf_op jit(solution)/shard_map/ppermute | solution.py:26
  187.9 16.9 %collective-permute-start.13 = (bf16[256,256]{1,0:T(8,128)(2,1)}, bf16[256,256]{1,0:T(8,128)(2,1)S(1)}, u32[]{:S(2)}, u32[]{:S(2)}) collective-permute-start(bf16[256,256]{1,0:T(8,128)(2,1)} %get-tuple-element.44), channel_id=1, source_target_pairs={{0,4},{1,5},{2,6},{3,7},{4,0},{5,1},{6,2},{7,3},{8,12},{9,13},{10,... | collective-permute-start | bytes 393224 | tf_op jit(solution)/shard_map/ppermute | solution.py:26
  193.1 16.5 %collective-permute-start.14 = (bf16[256,256]{1,0:T(8,128)(2,1)}, bf16[256,256]{1,0:T(8,128)(2,1)S(1)}, u32[]{:S(2)}, u32[]{:S(2)}) collective-permute-start(bf16[256,256]{1,0:T(8,128)(2,1)} %get-tuple-element.45), channel_id=1, source_target_pairs={{0,4},{1,5},{2,6},{3,7},{4,0},{5,1},{6,2},{7,3},{8,12},{9,13},{10,... | collective-permute-start | bytes 393224 | tf_op jit(solution)/shard_map/ppermute | solution.py:26
  198.6 41.6 %collective-permute-start.4 = (bf16[128,256]{0,1:T(8,128)(2,1)}, bf16[128,256]{0,1:T(8,128)(2,1)}, u32[]{:S(2)}, u32[]{:S(2)}) collective-permute-start(bf16[128,256]{0,1:T(8,128)(2,1)} %pad_maximum_fusion.2), channel_id=1, source_target_pairs={{0,2},{1,3},{2,0},{3,1},{4,6},{5,7},{6,4},{7,5},{8,10},{9,11},{10,... | collective-permute-start | bytes 196616 | tf_op jit(solution)/shard_map/ppermute | solution.py:31
  204.8 5.5 %copy-start.15 = (bf16[256,256]{1,0:T(8,128)(2,1)}, bf16[256,256]{1,0:T(8,128)(2,1)S(1)}, u32[]{:S(2)}) copy-start(bf16[256,256]{1,0:T(8,128)(2,1)S(1)} %collective-permute-done.13.refs_3_) | copy-start | bytes 393220
  209.6 0.7 copy-start.16
  210.3 0.7 copy-start.12
  211.0 0.7 copy-start.14
  214.9 25.3 %copy-start.9 = (bf16[128,128]{0,1:T(8,128)(2,1)S(1)}, bf16[128,128]{0,1:T(8,128)(2,1)}, u32[]{:S(2)}) copy-start(bf16[128,128]{0,1:T(8,128)(2,1)} %copy-done.8) | copy-start | bytes 98308
  214.9 25.3 %copy-start.11 = (bf16[128,128]{0,1:T(8,128)(2,1)S(1)}, bf16[128,128]{0,1:T(8,128)(2,1)}, u32[]{:S(2)}) copy-start(bf16[128,128]{0,1:T(8,128)(2,1)} %copy-done.10) | copy-start | bytes 98308
  214.9 51.5 %all-to-all-start.3 = ((bf16[32,16,512]{2,1,0:T(8,128)(2,1)}), bf16[32,16,512]{2,1,0:T(8,128)(2,1)S(1)}, u32[]{:S(2)}, u32[]{:S(2)}) async-start(bf16[32,16,512]{2,1,0:T(8,128)(2,1)} %bitcast.125), calls=%async_computation.3 | async-start | bytes 1048576 | tf_op jit(solution)/shard_map/all_to_all | solution.py:35
  233.2 13.0 %collective-permute-start = (bf16[2,2,16,2048]{3,2,0,1:T(8,128)(2,1)S(1)}, bf16[2,2,16,2048]{3,2,0,1:T(8,128)(2,1)S(1)}, u32[]{:S(2)}, u32[]{:S(2)}) collective-permute-start(bf16[2,2,16,2048]{3,2,0,1:T(8,128)(2,1)S(1)} %fusion.15), channel_id=1, source_target_pairs={{0,1},{1,0},{2,3},{3,2},{4,5},{5,4},{6,7},{7,6},{8,9},{9,8},{10,11... | collective-permute-start | bytes 786440 | tf_op jit(solution)/shard_map/ppermute | solution.py:31
  241.1 7.9 %collective-permute-start.5 = (bf16[128,512]{0,1:T(8,128)(2,1)S(1)}, bf16[128,512]{0,1:T(8,128)(2,1)S(1)}, u32[]{:S(2)}, u32[]{:S(2)}) collective-permute-start(bf16[128,512]{0,1:T(8,128)(2,1)S(1)} %pad_maximum_fusion.1), channel_id=1, source_target_pairs={{0,1},{1,0},{2,3},{3,2},{4,5},{5,4},{6,7},{7,6},{8,9},{9,8},{10,11... | collective-permute-start | bytes 393224 | tf_op jit(solution)/shard_map/ppermute | solution.py:31
  246.2 20.2 %copy-start.21 = (s32[128,32]{0,1:T(8,128)S(1)}, s32[128,32]{0,1:T(8,128)}, u32[]{:S(2)}) copy-start(s32[128,32]{0,1:T(8,128)} %fusion.8) | copy-start | bytes 49156
  246.2 20.2 %copy-start.25 = (s32[16]{0:T(128)S(1)}, s32[16]{0:T(128)}, u32[]{:S(2)}) copy-start(s32[16]{0:T(128)} %iota_add_fusion) | copy-start | bytes 196
  246.3 8.5 %collective-permute-start.1 = (bf16[2,16,2048]{2,1,0:T(8,128)(2,1)S(1)}, bf16[2,16,2048]{2,1,0:T(8,128)(2,1)S(1)}, u32[]{:S(2)}, u32[]{:S(2)}) collective-permute-start(bf16[2,16,2048]{2,1,0:T(8,128)(2,1)S(1)} %fusion.32), channel_id=1, source_target_pairs={{0,2},{1,3},{2,0},{3,1},{4,6},{5,7},{6,4},{7,5},{8,10},{9,11},{10,... | collective-permute-start | bytes 393224 | tf_op jit(solution)/shard_map/ppermute | solution.py:31
  254.9 20.1 %collective-permute-start.2 = (bf16[16,2048]{1,0:T(8,128)(2,1)S(1)}, bf16[16,2048]{1,0:T(8,128)(2,1)S(1)}, u32[]{:S(2)}, u32[]{:S(2)}) collective-permute-start(bf16[16,2048]{1,0:T(8,128)(2,1)S(1)} %fusion.61), channel_id=1, source_target_pairs={{0,4},{1,5},{2,6},{3,7},{4,0},{5,1},{6,2},{7,3},{8,12},{9,13},{10,... | collective-permute-start | bytes 196616 | tf_op jit(solution)/shard_map/ppermute | solution.py:31
  268.0 8.9 %collective-permute-start.16 = (bf16[128,256]{1,0:T(8,128)(2,1)S(1)}, bf16[128,256]{1,0:T(8,128)(2,1)S(1)}, u32[]{:S(2)}, u32[]{:S(2)}) collective-permute-start(bf16[128,256]{1,0:T(8,128)(2,1)S(1)} %slice.40), channel_id=1, source_target_pairs={{0,1},{1,0},{2,3},{3,2},{4,5},{5,4},{6,7},{7,6},{8,9},{9,8},{10,11... | collective-permute-start | bytes 196616 | tf_op jit(solution)/shard_map/ppermute | solution.py:31

commit v7 on v6

--- a/solution.py
+++ b/solution.py
@@ -13,7 +13,9 @@
 BLK = 64
 EP = ("ep_0", "ep_1")
 GRP_EP = ("grp", "ep_0", "ep_1")
-GRP_EP_TP = ("grp", "ep_0", "ep_1", "tp")
+TP = ("tp_quad", "tp_pair")
+EP_PAIR = ("ep_0", "ep_1", "tp_pair")
+GRP_EP_TP = ("grp", "ep_0", "ep_1", "tp_quad", "tp_pair")
 
 
 EPSILON = 1e-06
@@ -178,7 +180,7 @@
     ]
     gated_rows = (normed * jax.nn.silu(output_gate_input.astype(jnp.float32))).astype(jnp.bfloat16)
     partial = jnp.dot(gated_rows, recurrence_out_weight, preferred_element_type=jnp.float32)
-    return summed_to_owners(partial, "tp").astype(jnp.bfloat16)
+    return summed_to_owners(partial, TP).astype(jnp.bfloat16)
 
 
 VMEM = pl.BlockSpec(memory_space=pltpu.VMEM)
@@ -241,7 +243,6 @@
     top, tokens = index.shape
     slots, width = outgoing.shape
     half = slots // experts
-    member = lax.axis_index("tp")
     features = hidden_state[...].astype(jnp.float32)
     factor = lax.rsqrt(jnp.mean(features * features, axis=1, keepdims=True) + EPSILON)
     normed[...] = (features * factor * gain[...]).astype(jnp.bfloat16)
@@ -265,16 +266,16 @@
         slot // half == lax.broadcasted_iota(jnp.int32, (slots, experts), 1), one, zero
     ).astype(jnp.bfloat16)
     wanted = jnp.dot(spread, places, preferred_element_type=jnp.float32).astype(jnp.int32)
-    own = lax.broadcasted_iota(jnp.int32, (slots, tokens), 0) % half + (member & 1) * half
+    own = lax.broadcasted_iota(jnp.int32, (slots, tokens), 0) % half + lax.axis_index("tp_pair") * half
     filled = jnp.where(wanted == own, one, zero).astype(jnp.bfloat16)
-    start = pl.multiple_of((member >> 1) * width, width)
+    start = pl.multiple_of(lax.axis_index("tp_quad") * width, width)
     outgoing[...] = jnp.dot(
         filled, normed[:, pl.ds(start, width)], preferred_element_type=jnp.float32
     ).astype(jnp.bfloat16)
 
 
 def around_products(pieces, matrices):
-    quad = lax.axis_index("tp") >> 1
+    quad = lax.axis_index("tp_quad")
     held = []
 
     def dot(piece, matrix, step):
@@ -313,7 +314,7 @@
         ]
         for halves in around_products(pieces, (own_in, partner_in))
     ]
-    even = (lax.axis_index("tp") & 1) == 0
+    even = lax.axis_index("tp_pair") == 0
     for k, part in enumerate((hidden_first, hidden_second)):
         part[:, :units] = jnp.where(even, sides[0][k], sides[1][k])
         part[:, units:] = jnp.where(even, sides[1][k], sides[0][k])
@@ -322,11 +323,15 @@
 
 def down_kernel(own, before, after, far_first, far_second, own_down, partner_down, answers):
     pieces = (own, before, after, far_first, far_second)
-    middle, width = (answers.shape[0] // 2, answers.shape[1] // 2)
-    for side, halves in enumerate(around_products(pieces, (own_down, partner_down))):
+    sources, _, slots, width = answers.shape
+    count = sources // 2
+    place = lax.axis_index("tp_pair")
+    for side, halves in zip(
+        (place, 1 - place), around_products(pieces, (own_down, partner_down))
+    ):
         for k, part in enumerate(halves):
-            answers[pl.ds(k * middle, middle), pl.ds(side * width, width)] = part.astype(
-                jnp.bfloat16
+            answers[pl.ds(k * count, count), side] = part.astype(jnp.bfloat16).reshape(
+                count, slots, width
             )
 
 
@@ -348,18 +353,16 @@
     experts = local_experts * devices
     capacity = min(tokens, 2 * tokens * top // experts)
     width_out = routed_down_weight.shape[2]
-    members = lax.axis_size("tp")
+    members = lax.axis_size(TP)
     quads = members // 2
-    member = lax.axis_index("tp")
-    parity = member & 1
     half = capacity // 2
     width_in = routed_gate_weight.shape[1] // quads
     units = routed_gate_weight.shape[2]
 
     own_in = jnp.concatenate([routed_gate_weight[0], routed_up_weight[0]], axis=1)
     own_down = routed_down_weight[0]
-    partner_in = swapped(own_in, "tp", 1)
-    partner_down = swapped(own_down, "tp", 1)
+    partner_in = swapped(own_in, TP, 1)
+    partner_down = swapped(own_down, TP, 1)
 
     normed, outgoing = in_vmem(
         functools.partial(select_kernel, experts),
@@ -386,22 +389,20 @@
         preferred_element_type=jnp.float32,
     )
     places = jnp.where(chosen, places.astype(jnp.int32), -1)
-    filled = places[:, :, None] == parity * half + jnp.arange(half)[None, None, :]
-    filled = filled.reshape(tokens, experts * half)
     shared_hidden = (
         jax.nn.silu(jnp.dot(normed, shared_gate_weight, preferred_element_type=jnp.float32))
         * jnp.dot(normed, shared_up_weight, preferred_element_type=jnp.float32)
     ).astype(jnp.bfloat16)
-    shared_piece = gathered_columns(shared_hidden, "tp")
+    shared_piece = gathered_columns(shared_hidden, TP)
     shared = jnp.dot(
         shared_piece,
         rows_by_reversed_bits(shared_down_weight, members),
         preferred_element_type=jnp.float32,
     )
 
-    before = shifted(chunk, "tp", 2)
-    after = shifted(chunk, "tp", -2)
-    far = [shifted(half, "tp", step) for half, step in zip(halves_of(chunk), (4, -4))]
+    before = shifted(chunk, TP, 2)
+    after = shifted(chunk, TP, -2)
+    far = [shifted(half, TP, step) for half, step in zip(halves_of(chunk), (4, -4))]
     part_shape = jax.ShapeDtypeStruct((middle, 2 * units), jnp.bfloat16)
     hidden, hidden_first, hidden_second = fetching(
         hidden_kernel,
@@ -413,12 +414,12 @@
         own_in,
         partner_in,
     )
-    before = shifted(hidden, "tp", 2)
-    after = shifted(hidden, "tp", -2)
-    far = [shifted(hidden_first, "tp", 4), shifted(hidden_second, "tp", -4)]
+    before = shifted(hidden, TP, 2)
+    after = shifted(hidden, TP, -2)
+    far = [shifted(hidden_first, TP, 4), shifted(hidden_second, TP, -4)]
     answers = fetching(
         down_kernel,
-        jax.ShapeDtypeStruct((chunk.shape[0], 2 * width_out), jnp.bfloat16),
+        jax.ShapeDtypeStruct((devices, 2, half, width_out), jnp.bfloat16),
         hidden,
         before,
         after,
@@ -426,16 +427,13 @@
         own_down,
         partner_down,
     )
-    returned = exchanged(answers.reshape(devices, half, 2 * width_out), EP)
-    returned = returned.reshape(experts * half, 2 * width_out)
-    mixing = jnp.where(filled.reshape(tokens, experts, half), gate_of[:, :, None], 0.0)
-    mixing = mixing.reshape(tokens, experts * half)
-    combined = sum(
-        jnp.dot(part, returned, preferred_element_type=jnp.float32) for part in in_parts(mixing, 3)
-    )
-    other = swapped(combined[:, width_out:].astype(jnp.bfloat16), "tp", 1)
-    combined = shared + combined[:, :width_out] + other.astype(jnp.float32)
-    return combined.astype(jnp.bfloat16)
+    returned = exchanged(answers.reshape(2 * devices, half, width_out), EP_PAIR)
+    returned = returned.reshape(experts * capacity, width_out)
+    filled = places[:, :, None] == jnp.arange(capacity)[None, None, :]
+    mixing = jnp.where(filled, gate_of[:, :, None], 0.0).reshape(tokens, experts * capacity)
+    for part in in_parts(mixing, 3):
+        shared = shared + jnp.dot(part, returned, preferred_element_type=jnp.float32)
+    return shared.astype(jnp.bfloat16)
 
 
 def per_device(
@@ -485,30 +483,30 @@
 
 def solution(mesh):
     split = Mesh(
-        mesh.devices.reshape(mesh.shape["grp"], 16, 2, mesh.shape["tp"]),
-        ("grp", "ep_0", "ep_1", "tp"),
+        mesh.devices.reshape(mesh.shape["grp"], -1, 2, mesh.shape["tp"] // 2, 2),
+        ("grp", "ep_0", "ep_1", "tp_quad", "tp_pair"),
     )
     in_specs = (
-        P(GRP_EP, "tp"),
-        P(GRP_EP, "tp"),
-        P(GRP_EP, "tp"),
-        P(GRP_EP, "tp"),
-        P("tp"),
-        P(GRP_EP, "tp"),
-        P("tp"),
-        P("tp", None),
+        P(GRP_EP, TP),
+        P(GRP_EP, TP),
+        P(GRP_EP, TP),
+        P(GRP_EP, TP),
+        P(TP),
+        P(GRP_EP, TP),
+        P(TP),
+        P(TP, None),
         P(GRP_EP, None),
         P(GRP_EP, None),
         P(GRP_EP, None),
         P(),
-        P(EP, None, "tp"),
-        P(EP, None, "tp"),
-        P(EP, None, "tp"),
-        P(None, "tp"),
-        P(None, "tp"),
-        P(None, "tp"),
-    )
-    out_specs = (P(GRP_EP_TP, None), P(GRP_EP, "tp"))
+        P(EP, None, TP),
+        P(EP, None, TP),
+        P(EP, None, TP),
+        P(None, TP),
+        P(None, TP),
+        P(None, TP),
+    )
+    out_specs = (P(GRP_EP_TP, None), P(GRP_EP, TP))
 
     return jax.shard_map(
         per_device, mesh=split, in_specs=in_specs, out_specs=out_specs, check_vma=False

time: 279 us -> 273 us (0.978)
  starting transfers between devices: 158 us -> 145 us
  waiting for transfers between devices: 75.5 us -> 81.6 us
  local copies, waits for them, and re-layouts: 7.23 us -> 10.4 us
    all_to_all x4, waiting for transfers between devices: 40 us -> 56.6 us  [exchanged(): return lax.all_to_all(array, axis, split_axis=0, concat_axis=0, tiled=True)]
    all_to_all x4, starting transfers between devices: 80.4 us -> 68.9 us  [exchanged(): return lax.all_to_all(array, axis, split_axis=0, concat_axis=0, tiled=True)]
    ppermute x9 -> x8, waiting for transfers between devices: 10.9 us -> 4.45 us  [swapped(): return lax.ppermute(array, axis, [(i, i ^ bit) for i in range(count)])]
    ppermute x8, waiting for transfers between devices: 24.6 us -> 20.6 us  [shifted(): lax.ppermute(array, axis, [(i, (i + step) % count) for i in range(count)])]
    ppermute x8, starting transfers between devices: 37.9 us -> 33.9 us  [shifted(): lax.ppermute(array, axis, [(i, (i + step) % count) for i in range(count)])]
    ppermute x9 -> x8, starting transfers between devices: 39.5 us -> 42.7 us  [swapped(): return lax.ppermute(array, axis, [(i, i ^ bit) for i in range(count)])]
  transfers between devices with their start and end apart: 21 -> 20, of which waited for: 12 -> 10; matrix products, arithmetic and copies ran while one was open for 9% -> 8% of each run, Pallas kernels for 4% -> 4%
where the time goes in v7:
time: 273 us; the launch traced here: 272 us
  starting transfers between devices  145 us (53%)
  waiting for transfers between devices  81.6 us (30%)
  Pallas kernels  11.9 us (4%)
  matrix products  11.1 us (4%)
  local copies, waits for them, and re-layouts  10.4 us (4%)
  other arithmetic  9.6 us (4%)
    all_to_all x4, starting transfers between devices, exchanged(): return lax.all_to_all(array, axis, split_axis=0, concat_axis=0, tiled=True)  68.9 us
    all_to_all x4, waiting for transfers between devices, exchanged(): return lax.all_to_all(array, axis, split_axis=0, concat_axis=0, tiled=True)  56.6 us
    ppermute x8, starting transfers between devices, swapped(): return lax.ppermute(array, axis, [(i, i ^ bit) for i in range(count)])  42.7 us
    ppermute x8, starting transfers between devices, shifted(): lax.ppermute(array, axis, [(i, (i + step) % count) for i in range(count)])  33.9 us
    ppermute x8, waiting for transfers between devices, shifted(): lax.ppermute(array, axis, [(i, (i + step) % count) for i in range(count)])  20.6 us
    pallas_call x2, Pallas kernels, fetching(): pl.pallas_call(body, out_shape=shapes, in_specs=[ANY] * count, out_specs=...  7.63 us
  transfers between devices with their start and end apart: 20, of which 10 were waited for; matrix products, arithmetic and copies ran while one was open for 8% of the time, Pallas kernels for 4%

profile of v7, /device:TPU:65, one launch (start us, length us, event | category | flops | bytes accessed | tf_op | source)
XLA Modules:
  0.0 271.6 jit_solution(4455726228116132649)
XLA Ops:
  1.7 0.9 divide_multiply_fusion
  6.3 45.2 %all-to-all-start = ((bf16[32,8,256]{2,1,0:T(8,128)(2,1)}), bf16[32,8,256]{2,1,0:T(8,128)(2,1)S(1)}, u32[]{:S(2)}, u32[]{:S(2)}) async-start(bf16[32,8,256]{2,1,0:T(8,128)(2,1)} %fusion.25), calls=%async_computation | async-start | bytes 262144 | tf_op jit(solution)/shard_map/all_to_all | solution.py:37
  51.7 3.4 %collective-permute-start.10 = (bf16[2048,256]{1,0:T(8,128)(2,1)S(1)}, bf16[2048,256]{1,0:T(8,128)(2,1)}, u32[]{:S(2)}, u32[]{:S(2)}) collective-permute-start(bf16[2048,256]{1,0:T(8,128)(2,1)S(1)} %pad_maximum_fusion.refs_5_), channel_id=1, source_target_pairs={{0,1},{1,0},{2,3},{3,2},{4,5},{5,4},{6,7},{7,6},{8,9},{9,8},{10,11... | collective-permute-start | bytes 3145736 | tf_op jit(solution)/shard_map/ppermute | solution.py:33
  55.1 2.1 collective-permute-start.15
  57.2 0.9 convert_multiply_fusion.1
  58.1 9.3 %all-to-all-done = bf16[32,8,256]{2,1,0:T(8,128)(2,1)S(1)} async-done(((bf16[32,8,256]{2,1,0:T(8,128)(2,1)}), bf16[32,8,256]{2,1,0:T(8,128)(2,1)S(1)}, u32[]{:S(2)}, u32[]{:S(2)}) %all-to-all-start) | async-done | bytes 131104 | tf_op jit(solution)/shard_map/all_to_all | solution.py:37
  67.5 1.2 fusion.2
  69.6 5.2 %all-to-all-start.1 = ((bf16[32,8,128]{2,1,0:T(8,128)(2,1)}), bf16[32,8,128]{2,1,0:T(8,128)(2,1)S(1)}, u32[]{:S(2)}, u32[]{:S(2)}) async-start(bf16[32,8,128]{2,1,0:T(8,128)(2,1)} %copy.181), calls=%async_computation.1 | async-start | bytes 131072 | tf_op jit(solution)/shard_map/all_to_all | solution.py:37
  74.9 2.4 shard_map.185
  77.9 10.3 %all-to-all-done.1 = bf16[32,8,128]{2,1,0:T(8,128)(2,1)S(1)} async-done(((bf16[32,8,128]{2,1,0:T(8,128)(2,1)}), bf16[32,8,128]{2,1,0:T(8,128)(2,1)S(1)}, u32[]{:S(2)}, u32[]{:S(2)}) %all-to-all-start.1) | async-done | bytes 65568 | tf_op jit(solution)/shard_map/all_to_all | solution.py:37
  88.8 5.1 %all-to-all-start.2 = ((bf16[32,16,512]{2,1,0:T(8,128)(2,1)}), bf16[32,16,512]{2,1,0:T(8,128)(2,1)S(1)}, u32[]{:S(2)}, u32[]{:S(2)}) async-start(bf16[32,16,512]{2,1,0:T(8,128)(2,1)} %bitcast.137), calls=%async_computation.2 | async-start | bytes 1048576 | tf_op jit(solution)/shard_map/all_to_all | solution.py:37
  94.0 0.9 fusion.6
  94.9 1.1 convolution_select_fusion
  96.0 1.1 fusion.8
  97.1 1.0 fusion.59
  98.3 1.1 copy.187
  99.5 2.2 fusion.5
  101.7 1.1 multiply_reduce_fusion
  102.8 24.6 %all-to-all-done.2 = bf16[32,16,512]{2,1,0:T(8,128)(2,1)S(1)} async-done(((bf16[32,16,512]{2,1,0:T(8,128)(2,1)}), bf16[32,16,512]{2,1,0:T(8,128)(2,1)S(1)}, u32[]{:S(2)}, u32[]{:S(2)}) %all-to-all-start.2) | async-done | bytes 524320 | tf_op jit(solution)/shard_map/all_to_all | solution.py:37
  127.4 4.1 %collective-permute-start.6 = (bf16[512,512]{1,0:T(8,128)(2,1)S(1)}, bf16[512,512]{1,0:T(8,128)(2,1)}, u32[]{:S(2)}, u32[]{:S(2)}) collective-permute-start(bf16[512,512]{1,0:T(8,128)(2,1)S(1)} %bitcast.122), channel_id=1, source_target_pairs={{0,2},{1,3},{2,4},{3,5},{4,6},{5,7},{6,0},{7,1},{8,10},{9,11},{10,... | collective-permute-start | bytes 1572872 | tf_op jit(solution)/shard_map/ppermute | solution.py:28
  131.5 3.8 %collective-permute-start.7 = (bf16[512,512]{1,0:T(8,128)(2,1)S(1)}, bf16[512,512]{1,0:T(8,128)(2,1)}, u32[]{:S(2)}, u32[]{:S(2)}) collective-permute-start(bf16[512,512]{1,0:T(8,128)(2,1)S(1)} %bitcast.123), channel_id=1, source_target_pairs={{0,6},{1,7},{2,0},{3,1},{4,2},{5,3},{6,4},{7,5},{8,14},{9,15},{10,... | collective-permute-start | bytes 1572872 | tf_op jit(solution)/shard_map/ppermute | solution.py:28
  136.1 1.0 copy.183
  137.1 1.9 shard_map.186
  139.0 7.0 %collective-permute-start.8 = (bf16[256,512]{1,0:T(8,128)(2,1)}, bf16[256,512]{1,0:T(8,128)(2,1)S(1)}, u32[]{:S(2)}, u32[]{:S(2)}) collective-permute-start(bf16[256,512]{1,0:T(8,128)(2,1)} %get-tuple-element.41), channel_id=1, source_target_pairs={{0,4},{1,5},{2,6},{3,7},{4,0},{5,1},{6,2},{7,3},{8,12},{9,13},{10,... | collective-permute-start | bytes 786440 | tf_op jit(solution)/shard_map/ppermute | solution.py:28
  146.0 2.3 collective-permute-start.9
  148.3 1.0 mul.111
  149.3 1.2 fusion.41
  150.5 13.5 %collective-permute-done.8.refs_3_ = bf16[256,512]{1,0:T(8,128)(2,1)S(1)} collective-permute-done((bf16[256,512]{1,0:T(8,128)(2,1)}, bf16[256,512]{1,0:T(8,128)(2,1)S(1)}, u32[]{:S(2)}, u32[]{:S(2)}) %collective-permute-start.8) | collective-permute-done | bytes 262176 | tf_op jit(solution)/shard_map/ppermute | solution.py:28
  164.1 4.9 %collective-permute-start.3 = (bf16[128,128]{0,1:T(8,128)(2,1)}, bf16[128,128]{0,1:T(8,128)(2,1)S(1)}, u32[]{:S(2)}, u32[]{:S(2)}) collective-permute-start(bf16[128,128]{0,1:T(8,128)(2,1)} %fusion.5), channel_id=1, source_target_pairs={{0,4},{1,5},{2,6},{3,7},{4,0},{5,1},{6,2},{7,3},{8,12},{9,13},{10,... | collective-permute-start | bytes 98312 | tf_op jit(solution)/shard_map/ppermute | solution.py:33
  169.7 1.5 collective-permute-done.9.refs_4_
  171.2 17.0 %collective-permute-start = (bf16[2,2,16,2048]{3,2,0,1:T(8,128)(2,1)}, bf16[2,2,16,2048]{3,2,0,1:T(8,128)(2,1)}, u32[]{:S(2)}, u32[]{:S(2)}) collective-permute-start(bf16[2,2,16,2048]{3,2,0,1:T(8,128)(2,1)} %fusion.10), channel_id=1, source_target_pairs={{0,1},{1,0},{2,3},{3,2},{4,5},{5,4},{6,7},{7,6},{8,9},{9,8},{10,11... | collective-permute-start | bytes 786440 | tf_op jit(solution)/shard_map/ppermute | solution.py:33
  188.3 4.4 %shard_map.187 = (bf16[512,256]{1,0:T(8,128)(2,1)}, bf16[256,256]{1,0:T(8,128)(2,1)}, bf16[256,256]{1,0:T(8,128)(2,1)}) custom-call(bf16[512,512]{1,0:T(8,128)(2,1)} %bitcast.125, bf16[512,512]{1,0:T(8,128)(2,1)} %collective-permute-done.6.refs_1_, bf16[512,512]{1,0:T(8,128)(2,1)} %collective-permute-done.7.refs_2_, bf16[256,512]{1,0:T(8,128)(2,1)} %copy-done.13, ...), custom_call_target="tpu_custom_call" | custom-call | tf_op jit(solution)/shard_map/pallas_call | solution.py:221
  192.8 2.0 collective-permute-start.11
  194.7 5.5 %collective-permute-start.12 = (bf16[512,256]{1,0:T(8,128)(2,1)}, bf16[512,256]{1,0:T(8,128)(2,1)S(1)}, u32[]{:S(2)}, u32[]{:S(2)}) collective-permute-start(bf16[512,256]{1,0:T(8,128)(2,1)} %get-tuple-element.43.refs_0_), channel_id=1, source_target_pairs={{0,6},{1,7},{2,0},{3,1},{4,2},{5,3},{6,4},{7,5},{8,14},{9,15},{10,... | collective-permute-start | bytes 786440 | tf_op jit(solution)/shard_map/ppermute | solution.py:28
  200.8 4.4 %collective-permute-start.13 = (bf16[256,256]{1,0:T(8,128)(2,1)}, bf16[256,256]{1,0:T(8,128)(2,1)S(1)}, u32[]{:S(2)}, u32[]{:S(2)}) collective-permute-start(bf16[256,256]{1,0:T(8,128)(2,1)} %get-tuple-element.44), channel_id=1, source_target_pairs={{0,4},{1,5},{2,6},{3,7},{4,0},{5,1},{6,2},{7,3},{8,12},{9,13},{10,... | collective-permute-start | bytes 393224 | tf_op jit(solution)/shard_map/ppermute | solution.py:28
  205.2 4.9 %collective-permute-start.14 = (bf16[256,256]{1,0:T(8,128)(2,1)}, bf16[256,256]{1,0:T(8,128)(2,1)S(1)}, u32[]{:S(2)}, u32[]{:S(2)}) collective-permute-start(bf16[256,256]{1,0:T(8,128)(2,1)} %get-tuple-element.45), channel_id=1, source_target_pairs={{0,4},{1,5},{2,6},{3,7},{4,0},{5,1},{6,2},{7,3},{8,12},{9,13},{10,... | collective-permute-start | bytes 393224 | tf_op jit(solution)/shard_map/ppermute | solution.py:28
  210.9 2.9 %collective-permute-done.13.refs_3_ = bf16[256,256]{1,0:T(8,128)(2,1)S(1)} collective-permute-done((bf16[256,256]{1,0:T(8,128)(2,1)}, bf16[256,256]{1,0:T(8,128)(2,1)S(1)}, u32[]{:S(2)}, u32[]{:S(2)}) %collective-permute-start.13) | collective-permute-done | bytes 131104 | tf_op jit(solution)/shard_map/ppermute | solution.py:28
  213.8 2.3 collective-permute-start.4
  216.1 2.6 collective-permute-done.14.refs_4_
  220.2 3.2 %shard_map.188 = bf16[32,2,16,256]{3,2,1,0:T(8,128)(2,1)} custom-call(bf16[512,256]{1,0:T(8,128)(2,1)} %get-tuple-element.43.refs_0_, bf16[512,256]{1,0:T(8,128)(2,1)} %copy-done.12, bf16[512,256]{1,0:T(8,128)(2,1)} %copy-done.14, bf16[256,256]{1,0:T(8,128)(2,1)} %copy-done.20, bf16[256,256]{1,0:T(8,128)(2,1)} %copy-done.21, ...), custom_call_target="tpu_custom_call" | custom-call | tf_op jit(solution)/shard_map/pallas_call | solution.py:221
  223.4 13.4 %all-to-all-start.3 = ((bf16[64,16,256]{2,1,0:T(8,128)(2,1)}), bf16[64,16,256]{2,1,0:T(8,128)(2,1)S(1)}, u32[]{:S(2)}, u32[]{:S(2)}) async-start(bf16[64,16,256]{2,1,0:T(8,128)(2,1)} %bitcast.128), calls=%async_computation.3 | async-start | bytes 1048576 | tf_op jit(solution)/shard_map/all_to_all | solution.py:37
  236.8 1.0 bitcast_add_fusion.1
  237.8 4.7 %collective-permute-start.1 = (bf16[2,16,2048]{2,1,0:T(8,128)(2,1)S(1)}, bf16[2,16,2048]{2,1,0:T(8,128)(2,1)S(1)}, u32[]{:S(2)}, u32[]{:S(2)}) collective-permute-start(bf16[2,16,2048]{2,1,0:T(8,128)(2,1)S(1)} %fusion.26), channel_id=1, source_target_pairs={{0,2},{1,3},{2,0},{3,1},{4,6},{5,7},{6,4},{7,5},{8,10},{9,11},{10,... | collective-permute-start | bytes 393224 | tf_op jit(solution)/shard_map/ppermute | solution.py:33
  243.4 3.3 %collective-permute-start.5 = (bf16[128,512]{0,1:T(8,128)(2,1)S(1)}, bf16[128,512]{0,1:T(8,128)(2,1)S(1)}, u32[]{:S(2)}, u32[]{:S(2)}) collective-permute-start(bf16[128,512]{0,1:T(8,128)(2,1)S(1)} %pad_maximum_fusion.1), channel_id=1, source_target_pairs={{0,1},{1,0},{2,3},{3,2},{4,5},{5,4},{6,7},{7,6},{8,9},{9,8},{10,11... | collective-permute-start | bytes 393224 | tf_op jit(solution)/shard_map/ppermute | solution.py:33
  246.8 5.0 %collective-permute-start.2 = (bf16[16,2048]{1,0:T(8,128)(2,1)S(1)}, bf16[16,2048]{1,0:T(8,128)(2,1)S(1)}, u32[]{:S(2)}, u32[]{:S(2)}) collective-permute-start(bf16[16,2048]{1,0:T(8,128)(2,1)S(1)} %fusion.43), channel_id=1, source_target_pairs={{0,4},{1,5},{2,6},{3,7},{4,0},{5,1},{6,2},{7,3},{8,12},{9,13},{10,... | collective-permute-start | bytes 196616 | tf_op jit(solution)/shard_map/ppermute | solution.py:33
  252.4 4.0 %collective-permute-done.2 = bf16[16,2048]{1,0:T(8,128)(2,1)S(1)} collective-permute-done((bf16[16,2048]{1,0:T(8,128)(2,1)S(1)}, bf16[16,2048]{1,0:T(8,128)(2,1)S(1)}, u32[]{:S(2)}, u32[]{:S(2)}) %collective-permute-start.2) | collective-permute-done | bytes 65568 | tf_op jit(solution)/shard_map/ppermute | solution.py:33
  257.0 12.5 %all-to-all-done.3 = bf16[64,16,256]{2,1,0:T(8,128)(2,1)S(1)} async-done(((bf16[64,16,256]{2,1,0:T(8,128)(2,1)}), bf16[64,16,256]{2,1,0:T(8,128)(2,1)S(1)}, u32[]{:S(2)}, u32[]{:S(2)}) %all-to-all-start.3) | async-done | bytes 524320 | tf_op jit(solution)/shard_map/all_to_all | solution.py:37
  270.7 0.9 fusion.3
  (124 shorter events, 15.3 us)
Async XLA Ops:
  0.6 148.7 %copy-start = (bf16[256,2048]{1,0:T(8,128)(2,1)S(1)}, bf16[256,2048]{1,0:T(8,128)(2,1)}, u32[]{:S(2)}) copy-start(bf16[256,2048]{1,0:T(8,128)(2,1)} %param.27) | copy-start | bytes 3145732
  0.6 3.6 %copy-start.22 = (bf16[128,256]{1,0:T(8,128)(2,1)S(1)}, bf16[128,256]{1,0:T(8,128)(2,1)}, u32[]{:S(2)}) copy-start(bf16[128,256]{1,0:T(8,128)(2,1)} %param.22) | copy-start | bytes 196612
  4.3 0.6 copy-start.7
  4.7 46.8 %copy-start.11 = (bf16[1,2048,128]{2,1,0:T(8,128)(2,1)S(1)}, bf16[1,2048,128]{2,1,0:T(8,128)(2,1)}, u32[]{:S(2)}) copy-start(bf16[1,2048,128]{2,1,0:T(8,128)(2,1)} %param.32) | copy-start | bytes 1572868
  5.2 46.2 %copy-start.16 = (f32[2,2,128,128]{3,2,1,0:T(8,128)}, f32[2,2,128,128]{3,2,1,0:T(8,128)S(1)}, u32[]{:S(2)}) copy-start(f32[2,2,128,128]{3,2,1,0:T(8,128)S(1)} %get-tuple-element.37) | copy-start | bytes 786436
  5.3 46.3 %copy-start.10 = (bf16[1,2048,128]{2,1,0:T(8,128)(2,1)S(1)}, bf16[1,2048,128]{2,1,0:T(8,128)(2,1)}, u32[]{:S(2)}) copy-start(bf16[1,2048,128]{2,1,0:T(8,128)(2,1)} %param.33) | copy-start | bytes 1572868
  6.3 61.1 %all-to-all-start = ((bf16[32,8,256]{2,1,0:T(8,128)(2,1)}), bf16[32,8,256]{2,1,0:T(8,128)(2,1)S(1)}, u32[]{:S(2)}, u32[]{:S(2)}) async-start(bf16[32,8,256]{2,1,0:T(8,128)(2,1)} %fusion.25), calls=%async_computation | async-start | bytes 262144 | tf_op jit(solution)/shard_map/all_to_all | solution.py:37
  51.5 5.7 %copy-start.25 = (f32[128,4]{0,1:T(4,128)S(1)}, f32[128,4]{0,1:T(4,128)}, u32[]{:S(2)}) copy-start(f32[128,4]{0,1:T(4,128)} %param.30) | copy-start | bytes 6148
  51.7 37.2 %copy-start.2 = (bf16[2048,256]{1,0:T(8,128)(2,1)}, bf16[2048,256]{1,0:T(8,128)(2,1)S(1)}, u32[]{:S(2)}) copy-start(bf16[2048,256]{1,0:T(8,128)(2,1)S(1)} %pad_maximum_fusion.refs_5_) | copy-start | bytes 3145732
  51.7 25.6 %copy-start.24 = (s32[128,4]{0,1:T(4,128)S(1)}, s32[128,4]{0,1:T(4,128)}, u32[]{:S(2)}) copy-start(s32[128,4]{0,1:T(4,128)} %param.29) | copy-start | bytes 6148
  51.7 94.3 %collective-permute-start.10 = (bf16[2048,256]{1,0:T(8,128)(2,1)S(1)}, bf16[2048,256]{1,0:T(8,128)(2,1)}, u32[]{:S(2)}, u32[]{:S(2)}) collective-permute-start(bf16[2048,256]{1,0:T(8,128)(2,1)S(1)} %pad_maximum_fusion.refs_5_), channel_id=1, source_target_pairs={{0,1},{1,0},{2,3},{3,2},{4,5},{5,4},{6,7},{7,6},{8,9},{9,8},{10,11... | collective-permute-start | bytes 3145736 | tf_op jit(solution)/shard_map/ppermute | solution.py:33
  55.1 150.1 %collective-permute-start.15 = (bf16[1024,256]{1,0:T(8,128)(2,1)}, bf16[1024,256]{1,0:T(8,128)(2,1)}, u32[]{:S(2)}, u32[]{:S(2)}) collective-permute-start(bf16[1024,256]{1,0:T(8,128)(2,1)} %bitcast.32.refs_5_), channel_id=1, source_target_pairs={{0,1},{1,0},{2,3},{3,2},{4,5},{5,4},{6,7},{7,6},{8,9},{9,8},{10,11... | collective-permute-start | bytes 1572872 | tf_op jit(solution)/shard_map/ppermute | solution.py:33
  69.6 18.6 %all-to-all-start.1 = ((bf16[32,8,128]{2,1,0:T(8,128)(2,1)}), bf16[32,8,128]{2,1,0:T(8,128)(2,1)S(1)}, u32[]{:S(2)}, u32[]{:S(2)}) async-start(bf16[32,8,128]{2,1,0:T(8,128)(2,1)} %copy.181), calls=%async_computation.1 | async-start | bytes 131072 | tf_op jit(solution)/shard_map/all_to_all | solution.py:37
  88.2 0.6 copy-start.18
  88.8 8.3 %copy-start.3 = (bf16[128,2048]{1,0:T(8,128)(2,1)S(1)}, bf16[128,2048]{1,0:T(8,128)(2,1)}, u32[]{:S(2)}) copy-start(bf16[128,2048]{1,0:T(8,128)(2,1)} %get-tuple-element.39) | copy-start | bytes 1572868
  88.8 38.6 %all-to-all-start.2 = ((bf16[32,16,512]{2,1,0:T(8,128)(2,1)}), bf16[32,16,512]{2,1,0:T(8,128)(2,1)S(1)}, u32[]{:S(2)}, u32[]{:S(2)}) async-start(bf16[32,16,512]{2,1,0:T(8,128)(2,1)} %bitcast.137), calls=%async_computation.2 | async-start | bytes 1048576 | tf_op jit(solution)/shard_map/all_to_all | solution.py:37
  94.0 3.2 %copy-start.9 = (bf16[2048,128]{1,0:T(8,128)(2,1)S(1)}, bf16[2048,128]{1,0:T(8,128)(2,1)}, u32[]{:S(2)}) copy-start(bf16[2048,128]{1,0:T(8,128)(2,1)} %param.35) | copy-start | bytes 1572868
  96.0 2.1 copy-start.8
  97.1 2.3 copy-start.26
  99.5 2.2 copy-start.19
  99.5 2.2 copy-start.17
  101.7 47.6 %copy-start.27 = (f32[256]{0:T(256)S(1)}, f32[256]{0:T(256)}, u32[]{:S(2)}) copy-start(f32[256]{0:T(256)} %param.26) | copy-start | bytes 3076
  127.4 9.8 %copy-start.1 = (bf16[32,16,512]{2,1,0:T(8,128)(2,1)}, bf16[32,16,512]{2,1,0:T(8,128)(2,1)S(1)}, u32[]{:S(2)}) copy-start(bf16[32,16,512]{2,1,0:T(8,128)(2,1)S(1)} %all-to-all-done.2) | copy-start | bytes 1572868
  127.4 60.9 %collective-permute-start.6 = (bf16[512,512]{1,0:T(8,128)(2,1)S(1)}, bf16[512,512]{1,0:T(8,128)(2,1)}, u32[]{:S(2)}, u32[]{:S(2)}) collective-permute-start(bf16[512,512]{1,0:T(8,128)(2,1)S(1)} %bitcast.122), channel_id=1, source_target_pairs={{0,2},{1,3},{2,4},{3,5},{4,6},{5,7},{6,0},{7,1},{8,10},{9,11},{10,... | collective-permute-start | bytes 1572872 | tf_op jit(solution)/shard_map/ppermute | solution.py:28
  131.5 56.7 %collective-permute-start.7 = (bf16[512,512]{1,0:T(8,128)(2,1)S(1)}, bf16[512,512]{1,0:T(8,128)(2,1)}, u32[]{:S(2)}, u32[]{:S(2)}) collective-permute-start(bf16[512,512]{1,0:T(8,128)(2,1)S(1)} %bitcast.123), channel_id=1, source_target_pairs={{0,6},{1,7},{2,0},{3,1},{4,2},{5,3},{6,4},{7,5},{8,14},{9,15},{10,... | collective-permute-start | bytes 1572872 | tf_op jit(solution)/shard_map/ppermute | solution.py:28
  139.0 25.1 %collective-permute-start.8 = (bf16[256,512]{1,0:T(8,128)(2,1)}, bf16[256,512]{1,0:T(8,128)(2,1)S(1)}, u32[]{:S(2)}, u32[]{:S(2)}) collective-permute-start(bf16[256,512]{1,0:T(8,128)(2,1)} %get-tuple-element.41), channel_id=1, source_target_pairs={{0,4},{1,5},{2,6},{3,7},{4,0},{5,1},{6,2},{7,3},{8,12},{9,13},{10,... | collective-permute-start | bytes 786440 | tf_op jit(solution)/shard_map/ppermute | solution.py:28
  146.0 25.2 %collective-permute-start.9 = (bf16[256,512]{1,0:T(8,128)(2,1)}, bf16[256,512]{1,0:T(8,128)(2,1)S(1)}, u32[]{:S(2)}, u32[]{:S(2)}) collective-permute-start(bf16[256,512]{1,0:T(8,128)(2,1)} %get-tuple-element.42), channel_id=1, source_target_pairs={{0,4},{1,5},{2,6},{3,7},{4,0},{5,1},{6,2},{7,3},{8,12},{9,13},{10,... | collective-permute-start | bytes 786440 | tf_op jit(solution)/shard_map/ppermute | solution.py:28
  164.1 24.2 %copy-start.13 = (bf16[256,512]{1,0:T(8,128)(2,1)}, bf16[256,512]{1,0:T(8,128)(2,1)S(1)}, u32[]{:S(2)}) copy-start(bf16[256,512]{1,0:T(8,128)(2,1)S(1)} %collective-permute-done.8.refs_3_) | copy-start | bytes 786436
  164.1 36.2 %collective-permute-start.3 = (bf16[128,128]{0,1:T(8,128)(2,1)}, bf16[128,128]{0,1:T(8,128)(2,1)S(1)}, u32[]{:S(2)}, u32[]{:S(2)}) collective-permute-start(bf16[128,128]{0,1:T(8,128)(2,1)} %fusion.5), channel_id=1, source_target_pairs={{0,4},{1,5},{2,6},{3,7},{4,0},{5,1},{6,2},{7,3},{8,12},{9,13},{10,... | collective-permute-start | bytes 98312 | tf_op jit(solution)/shard_map/ppermute | solution.py:33
  171.2 17.0 %copy-start.15 = (bf16[256,512]{1,0:T(8,128)(2,1)}, bf16[256,512]{1,0:T(8,128)(2,1)S(1)}, u32[]{:S(2)}) copy-start(bf16[256,512]{1,0:T(8,128)(2,1)S(1)} %collective-permute-done.9.refs_4_) | copy-start | bytes 786436
  171.2 65.5 %collective-permute-start = (bf16[2,2,16,2048]{3,2,0,1:T(8,128)(2,1)}, bf16[2,2,16,2048]{3,2,0,1:T(8,128)(2,1)}, u32[]{:S(2)}, u32[]{:S(2)}) collective-permute-start(bf16[2,2,16,2048]{3,2,0,1:T(8,128)(2,1)} %fusion.10), channel_id=1, source_target_pairs={{0,1},{1,0},{2,3},{3,2},{4,5},{5,4},{6,7},{7,6},{8,9},{9,8},{10,11... | collective-permute-start | bytes 786440 | tf_op jit(solution)/shard_map/ppermute | solution.py:33
  192.8 26.0 %collective-permute-start.11 = (bf16[512,256]{1,0:T(8,128)(2,1)}, bf16[512,256]{1,0:T(8,128)(2,1)S(1)}, u32[]{:S(2)}, u32[]{:S(2)}) collective-permute-start(bf16[512,256]{1,0:T(8,128)(2,1)} %get-tuple-element.43.refs_0_), channel_id=1, source_target_pairs={{0,2},{1,3},{2,4},{3,5},{4,6},{5,7},{6,0},{7,1},{8,10},{9,11},{10,... | collective-permute-start | bytes 786440 | tf_op jit(solution)/shard_map/ppermute | solution.py:28
  194.7 24.0 %collective-permute-start.12 = (bf16[512,256]{1,0:T(8,128)(2,1)}, bf16[512,256]{1,0:T(8,128)(2,1)S(1)}, u32[]{:S(2)}, u32[]{:S(2)}) collective-permute-start(bf16[512,256]{1,0:T(8,128)(2,1)} %get-tuple-element.43.refs_0_), channel_id=1, source_target_pairs={{0,6},{1,7},{2,0},{3,1},{4,2},{5,3},{6,4},{7,5},{8,14},{9,15},{10,... | collective-permute-start | bytes 786440 | tf_op jit(solution)/shard_map/ppermute | solution.py:28
  200.2 0.6 copy-start.23
  200.8 13.0 %collective-permute-start.13 = (bf16[256,256]{1,0:T(8,128)(2,1)}, bf16[256,256]{1,0:T(8,128)(2,1)S(1)}, u32[]{:S(2)}, u32[]{:S(2)}) collective-permute-start(bf16[256,256]{1,0:T(8,128)(2,1)} %get-tuple-element.44), channel_id=1, source_target_pairs={{0,4},{1,5},{2,6},{3,7},{4,0},{5,1},{6,2},{7,3},{8,12},{9,13},{10,... | collective-permute-start | bytes 393224 | tf_op jit(solution)/shard_map/ppermute | solution.py:28
  205.2 13.5 %collective-permute-start.14 = (bf16[256,256]{1,0:T(8,128)(2,1)}, bf16[256,256]{1,0:T(8,128)(2,1)S(1)}, u32[]{:S(2)}, u32[]{:S(2)}) collective-permute-start(bf16[256,256]{1,0:T(8,128)(2,1)} %get-tuple-element.45), channel_id=1, source_target_pairs={{0,4},{1,5},{2,6},{3,7},{4,0},{5,1},{6,2},{7,3},{8,12},{9,13},{10,... | collective-permute-start | bytes 393224 | tf_op jit(solution)/shard_map/ppermute | solution.py:28
  213.8 4.9 %copy-start.20 = (bf16[256,256]{1,0:T(8,128)(2,1)}, bf16[256,256]{1,0:T(8,128)(2,1)S(1)}, u32[]{:S(2)}) copy-start(bf16[256,256]{1,0:T(8,128)(2,1)S(1)} %collective-permute-done.13.refs_3_) | copy-start | bytes 393220
  213.8 28.7 %collective-permute-start.4 = (bf16[128,256]{0,1:T(8,128)(2,1)S(1)}, bf16[128,256]{0,1:T(8,128)(2,1)}, u32[]{:S(2)}, u32[]{:S(2)}) collective-permute-start(bf16[128,256]{0,1:T(8,128)(2,1)S(1)} %pad_maximum_fusion.2), channel_id=1, source_target_pairs={{0,2},{1,3},{2,0},{3,1},{4,6},{5,7},{6,4},{7,5},{8,10},{9,11},{10,... | collective-permute-start | bytes 196616 | tf_op jit(solution)/shard_map/ppermute | solution.py:33
  218.7 0.7 copy-start.21
  218.7 0.8 copy-start.12
  219.5 0.7 copy-start.14
  223.4 46.1 %all-to-all-start.3 = ((bf16[64,16,256]{2,1,0:T(8,128)(2,1)}), bf16[64,16,256]{2,1,0:T(8,128)(2,1)S(1)}, u32[]{:S(2)}, u32[]{:S(2)}) async-start(bf16[64,16,256]{2,1,0:T(8,128)(2,1)} %bitcast.128), calls=%async_computation.3 | async-start | bytes 1048576 | tf_op jit(solution)/shard_map/all_to_all | solution.py:37
  237.8 31.7 %copy-start.5 = (bf16[128,32,32]{0,2,1:T(8,128)(2,1)S(1)}, bf16[128,32,32]{0,2,1:T(8,128)(2,1)}, u32[]{:S(2)}) copy-start(bf16[128,32,32]{0,2,1:T(8,128)(2,1)} %get-tuple-element.127) | copy-start | bytes 786436
  237.8 8.9 %collective-permute-start.1 = (bf16[2,16,2048]{2,1,0:T(8,128)(2,1)S(1)}, bf16[2,16,2048]{2,1,0:T(8,128)(2,1)S(1)}, u32[]{:S(2)}, u32[]{:S(2)}) collective-permute-start(bf16[2,16,2048]{2,1,0:T(8,128)(2,1)S(1)} %fusion.26), channel_id=1, source_target_pairs={{0,2},{1,3},{2,0},{3,1},{4,6},{5,7},{6,4},{7,5},{8,10},{9,11},{10,... | collective-permute-start | bytes 393224 | tf_op jit(solution)/shard_map/ppermute | solution.py:33
  243.4 8.8 %collective-permute-start.5 = (bf16[128,512]{0,1:T(8,128)(2,1)S(1)}, bf16[128,512]{0,1:T(8,128)(2,1)S(1)}, u32[]{:S(2)}, u32[]{:S(2)}) collective-permute-start(bf16[128,512]{0,1:T(8,128)(2,1)S(1)} %pad_maximum_fusion.1), channel_id=1, source_target_pairs={{0,1},{1,0},{2,3},{3,2},{4,5},{5,4},{6,7},{7,6},{8,9},{9,8},{10,11... | collective-permute-start | bytes 393224 | tf_op jit(solution)/shard_map/ppermute | solution.py:33
  246.8 23.0 %copy-start.4 = (bf16[128,32,32]{0,2,1:T(8,128)(2,1)S(1)}, bf16[128,32,32]{0,2,1:T(8,128)(2,1)}, u32[]{:S(2)}) copy-start(bf16[128,32,32]{0,2,1:T(8,128)(2,1)} %get-tuple-element.126) | copy-start | bytes 786436
  246.8 9.5 %collective-permute-start.2 = (bf16[16,2048]{1,0:T(8,128)(2,1)S(1)}, bf16[16,2048]{1,0:T(8,128)(2,1)S(1)}, u32[]{:S(2)}, u32[]{:S(2)}) collective-permute-start(bf16[16,2048]{1,0:T(8,128)(2,1)S(1)} %fusion.43), channel_id=1, source_target_pairs={{0,4},{1,5},{2,6},{3,7},{4,0},{5,1},{6,2},{7,3},{8,12},{9,13},{10,... | collective-permute-start | bytes 196616 | tf_op jit(solution)/shard_map/ppermute | solution.py:33
  269.8 1.0 copy-start.6

commit v8 on v7

--- a/solution.py
+++ b/solution.py
@@ -394,11 +394,8 @@
         * jnp.dot(normed, shared_up_weight, preferred_element_type=jnp.float32)
     ).astype(jnp.bfloat16)
     shared_piece = gathered_columns(shared_hidden, TP)
-    shared = jnp.dot(
-        shared_piece,
-        rows_by_reversed_bits(shared_down_weight, members),
-        preferred_element_type=jnp.float32,
-    )
+    shared_down = rows_by_reversed_bits(shared_down_weight, members)
+    shared = jnp.dot(shared_piece, shared_down, preferred_element_type=jnp.float32)
 
     before = shifted(chunk, TP, 2)
     after = shifted(chunk, TP, -2)

time: 273 us -> 273 us (level)
  no operation moved by 1% of the time
where the time goes in v8:
time: 273 us; the launch traced here: 272 us
  starting transfers between devices  145 us (53%)
  waiting for transfers between devices  81.6 us (30%)
  Pallas kernels  11.9 us (4%)
  matrix products  11.1 us (4%)
  local copies, waits for them, and re-layouts  10.4 us (4%)
  other arithmetic  9.6 us (4%)
    all_to_all x4, starting transfers between devices, exchanged(): return lax.all_to_all(array, axis, split_axis=0, concat_axis=0, tiled=True)  68.9 us
    all_to_all x4, waiting for transfers between devices, exchanged(): return lax.all_to_all(array, axis, split_axis=0, concat_axis=0, tiled=True)  56.6 us
    ppermute x8, starting transfers between devices, swapped(): return lax.ppermute(array, axis, [(i, i ^ bit) for i in range(count)])  42.7 us
    ppermute x8, starting transfers between devices, shifted(): lax.ppermute(array, axis, [(i, (i + step) % count) for i in range(count)])  33.9 us
    ppermute x8, waiting for transfers between devices, shifted(): lax.ppermute(array, axis, [(i, (i + step) % count) for i in range(count)])  20.6 us
    pallas_call x2, Pallas kernels, fetching(): pl.pallas_call(body, out_shape=shapes, in_specs=[ANY] * count, out_specs=...  7.63 us
  transfers between devices with their start and end apart: 20, of which 10 were waited for; matrix products, arithmetic and copies ran while one was open for 8% of the time, Pallas kernels for 4%

profile of v8, /device:TPU:65, one launch (start us, length us, event | category | flops | bytes accessed | tf_op | source)
XLA Modules:
  0.0 271.6 jit_solution(4455726228116132649)
XLA Ops:
  1.7 0.9 divide_multiply_fusion
  6.3 45.2 %all-to-all-start = ((bf16[32,8,256]{2,1,0:T(8,128)(2,1)}), bf16[32,8,256]{2,1,0:T(8,128)(2,1)S(1)}, u32[]{:S(2)}, u32[]{:S(2)}) async-start(bf16[32,8,256]{2,1,0:T(8,128)(2,1)} %fusion.25), calls=%async_computation | async-start | bytes 262144 | tf_op jit(solution)/shard_map/all_to_all | solution.py:37
  51.7 3.4 %collective-permute-start.10 = (bf16[2048,256]{1,0:T(8,128)(2,1)S(1)}, bf16[2048,256]{1,0:T(8,128)(2,1)}, u32[]{:S(2)}, u32[]{:S(2)}) collective-permute-start(bf16[2048,256]{1,0:T(8,128)(2,1)S(1)} %pad_maximum_fusion.refs_5_), channel_id=1, source_target_pairs={{0,1},{1,0},{2,3},{3,2},{4,5},{5,4},{6,7},{7,6},{8,9},{9,8},{10,11... | collective-permute-start | bytes 3145736 | tf_op jit(solution)/shard_map/ppermute | solution.py:33
  55.1 2.1 collective-permute-start.15
  57.2 0.9 convert_multiply_fusion.1
  58.1 9.3 %all-to-all-done = bf16[32,8,256]{2,1,0:T(8,128)(2,1)S(1)} async-done(((bf16[32,8,256]{2,1,0:T(8,128)(2,1)}), bf16[32,8,256]{2,1,0:T(8,128)(2,1)S(1)}, u32[]{:S(2)}, u32[]{:S(2)}) %all-to-all-start) | async-done | bytes 131104 | tf_op jit(solution)/shard_map/all_to_all | solution.py:37
  67.5 1.2 fusion.2
  69.6 5.2 %all-to-all-start.1 = ((bf16[32,8,128]{2,1,0:T(8,128)(2,1)}), bf16[32,8,128]{2,1,0:T(8,128)(2,1)S(1)}, u32[]{:S(2)}, u32[]{:S(2)}) async-start(bf16[32,8,128]{2,1,0:T(8,128)(2,1)} %copy.181), calls=%async_computation.1 | async-start | bytes 131072 | tf_op jit(solution)/shard_map/all_to_all | solution.py:37
  74.9 2.4 shard_map.185
  77.9 10.3 %all-to-all-done.1 = bf16[32,8,128]{2,1,0:T(8,128)(2,1)S(1)} async-done(((bf16[32,8,128]{2,1,0:T(8,128)(2,1)}), bf16[32,8,128]{2,1,0:T(8,128)(2,1)S(1)}, u32[]{:S(2)}, u32[]{:S(2)}) %all-to-all-start.1) | async-done | bytes 65568 | tf_op jit(solution)/shard_map/all_to_all | solution.py:37
  88.8 5.1 %all-to-all-start.2 = ((bf16[32,16,512]{2,1,0:T(8,128)(2,1)}), bf16[32,16,512]{2,1,0:T(8,128)(2,1)S(1)}, u32[]{:S(2)}, u32[]{:S(2)}) async-start(bf16[32,16,512]{2,1,0:T(8,128)(2,1)} %bitcast.137), calls=%async_computation.2 | async-start | bytes 1048576 | tf_op jit(solution)/shard_map/all_to_all | solution.py:37
  94.0 0.9 fusion.6
  94.9 1.1 convolution_select_fusion
  96.0 1.1 fusion.8
  97.1 1.0 fusion.59
  98.3 1.1 copy.187
  99.5 2.2 fusion.5
  101.7 1.1 multiply_reduce_fusion
  102.8 24.6 %all-to-all-done.2 = bf16[32,16,512]{2,1,0:T(8,128)(2,1)S(1)} async-done(((bf16[32,16,512]{2,1,0:T(8,128)(2,1)}), bf16[32,16,512]{2,1,0:T(8,128)(2,1)S(1)}, u32[]{:S(2)}, u32[]{:S(2)}) %all-to-all-start.2) | async-done | bytes 524320 | tf_op jit(solution)/shard_map/all_to_all | solution.py:37
  127.4 4.1 %collective-permute-start.6 = (bf16[512,512]{1,0:T(8,128)(2,1)S(1)}, bf16[512,512]{1,0:T(8,128)(2,1)}, u32[]{:S(2)}, u32[]{:S(2)}) collective-permute-start(bf16[512,512]{1,0:T(8,128)(2,1)S(1)} %bitcast.122), channel_id=1, source_target_pairs={{0,2},{1,3},{2,4},{3,5},{4,6},{5,7},{6,0},{7,1},{8,10},{9,11},{10,... | collective-permute-start | bytes 1572872 | tf_op jit(solution)/shard_map/ppermute | solution.py:28
  131.5 3.8 %collective-permute-start.7 = (bf16[512,512]{1,0:T(8,128)(2,1)S(1)}, bf16[512,512]{1,0:T(8,128)(2,1)}, u32[]{:S(2)}, u32[]{:S(2)}) collective-permute-start(bf16[512,512]{1,0:T(8,128)(2,1)S(1)} %bitcast.123), channel_id=1, source_target_pairs={{0,6},{1,7},{2,0},{3,1},{4,2},{5,3},{6,4},{7,5},{8,14},{9,15},{10,... | collective-permute-start | bytes 1572872 | tf_op jit(solution)/shard_map/ppermute | solution.py:28
  136.1 1.0 copy.183
  137.1 1.9 shard_map.186
  139.0 7.0 %collective-permute-start.8 = (bf16[256,512]{1,0:T(8,128)(2,1)}, bf16[256,512]{1,0:T(8,128)(2,1)S(1)}, u32[]{:S(2)}, u32[]{:S(2)}) collective-permute-start(bf16[256,512]{1,0:T(8,128)(2,1)} %get-tuple-element.41), channel_id=1, source_target_pairs={{0,4},{1,5},{2,6},{3,7},{4,0},{5,1},{6,2},{7,3},{8,12},{9,13},{10,... | collective-permute-start | bytes 786440 | tf_op jit(solution)/shard_map/ppermute | solution.py:28
  146.0 2.3 collective-permute-start.9
  148.3 1.0 mul.111
  149.3 1.2 fusion.41
  150.5 13.5 %collective-permute-done.8.refs_3_ = bf16[256,512]{1,0:T(8,128)(2,1)S(1)} collective-permute-done((bf16[256,512]{1,0:T(8,128)(2,1)}, bf16[256,512]{1,0:T(8,128)(2,1)S(1)}, u32[]{:S(2)}, u32[]{:S(2)}) %collective-permute-start.8) | collective-permute-done | bytes 262176 | tf_op jit(solution)/shard_map/ppermute | solution.py:28
  164.1 4.9 %collective-permute-start.3 = (bf16[128,128]{0,1:T(8,128)(2,1)}, bf16[128,128]{0,1:T(8,128)(2,1)S(1)}, u32[]{:S(2)}, u32[]{:S(2)}) collective-permute-start(bf16[128,128]{0,1:T(8,128)(2,1)} %fusion.5), channel_id=1, source_target_pairs={{0,4},{1,5},{2,6},{3,7},{4,0},{5,1},{6,2},{7,3},{8,12},{9,13},{10,... | collective-permute-start | bytes 98312 | tf_op jit(solution)/shard_map/ppermute | solution.py:33
  169.7 1.5 collective-permute-done.9.refs_4_
  171.2 17.0 %collective-permute-start = (bf16[2,2,16,2048]{3,2,0,1:T(8,128)(2,1)}, bf16[2,2,16,2048]{3,2,0,1:T(8,128)(2,1)}, u32[]{:S(2)}, u32[]{:S(2)}) collective-permute-start(bf16[2,2,16,2048]{3,2,0,1:T(8,128)(2,1)} %fusion.10), channel_id=1, source_target_pairs={{0,1},{1,0},{2,3},{3,2},{4,5},{5,4},{6,7},{7,6},{8,9},{9,8},{10,11... | collective-permute-start | bytes 786440 | tf_op jit(solution)/shard_map/ppermute | solution.py:33
  188.3 4.4 %shard_map.187 = (bf16[512,256]{1,0:T(8,128)(2,1)}, bf16[256,256]{1,0:T(8,128)(2,1)}, bf16[256,256]{1,0:T(8,128)(2,1)}) custom-call(bf16[512,512]{1,0:T(8,128)(2,1)} %bitcast.125, bf16[512,512]{1,0:T(8,128)(2,1)} %collective-permute-done.6.refs_1_, bf16[512,512]{1,0:T(8,128)(2,1)} %collective-permute-done.7.refs_2_, bf16[256,512]{1,0:T(8,128)(2,1)} %copy-done.13, ...), custom_call_target="tpu_custom_call" | custom-call | tf_op jit(solution)/shard_map/pallas_call | solution.py:221
  192.8 2.0 collective-permute-start.11
  194.7 5.5 %collective-permute-start.12 = (bf16[512,256]{1,0:T(8,128)(2,1)}, bf16[512,256]{1,0:T(8,128)(2,1)S(1)}, u32[]{:S(2)}, u32[]{:S(2)}) collective-permute-start(bf16[512,256]{1,0:T(8,128)(2,1)} %get-tuple-element.43.refs_0_), channel_id=1, source_target_pairs={{0,6},{1,7},{2,0},{3,1},{4,2},{5,3},{6,4},{7,5},{8,14},{9,15},{10,... | collective-permute-start | bytes 786440 | tf_op jit(solution)/shard_map/ppermute | solution.py:28
  200.8 4.4 %collective-permute-start.13 = (bf16[256,256]{1,0:T(8,128)(2,1)}, bf16[256,256]{1,0:T(8,128)(2,1)S(1)}, u32[]{:S(2)}, u32[]{:S(2)}) collective-permute-start(bf16[256,256]{1,0:T(8,128)(2,1)} %get-tuple-element.44), channel_id=1, source_target_pairs={{0,4},{1,5},{2,6},{3,7},{4,0},{5,1},{6,2},{7,3},{8,12},{9,13},{10,... | collective-permute-start | bytes 393224 | tf_op jit(solution)/shard_map/ppermute | solution.py:28
  205.2 4.9 %collective-permute-start.14 = (bf16[256,256]{1,0:T(8,128)(2,1)}, bf16[256,256]{1,0:T(8,128)(2,1)S(1)}, u32[]{:S(2)}, u32[]{:S(2)}) collective-permute-start(bf16[256,256]{1,0:T(8,128)(2,1)} %get-tuple-element.45), channel_id=1, source_target_pairs={{0,4},{1,5},{2,6},{3,7},{4,0},{5,1},{6,2},{7,3},{8,12},{9,13},{10,... | collective-permute-start | bytes 393224 | tf_op jit(solution)/shard_map/ppermute | solution.py:28
  210.9 2.9 %collective-permute-done.13.refs_3_ = bf16[256,256]{1,0:T(8,128)(2,1)S(1)} collective-permute-done((bf16[256,256]{1,0:T(8,128)(2,1)}, bf16[256,256]{1,0:T(8,128)(2,1)S(1)}, u32[]{:S(2)}, u32[]{:S(2)}) %collective-permute-start.13) | collective-permute-done | bytes 131104 | tf_op jit(solution)/shard_map/ppermute | solution.py:28
  213.8 2.3 collective-permute-start.4
  216.1 2.6 collective-permute-done.14.refs_4_
  220.2 3.2 %shard_map.188 = bf16[32,2,16,256]{3,2,1,0:T(8,128)(2,1)} custom-call(bf16[512,256]{1,0:T(8,128)(2,1)} %get-tuple-element.43.refs_0_, bf16[512,256]{1,0:T(8,128)(2,1)} %copy-done.12, bf16[512,256]{1,0:T(8,128)(2,1)} %copy-done.14, bf16[256,256]{1,0:T(8,128)(2,1)} %copy-done.20, bf16[256,256]{1,0:T(8,128)(2,1)} %copy-done.21, ...), custom_call_target="tpu_custom_call" | custom-call | tf_op jit(solution)/shard_map/pallas_call | solution.py:221
  223.4 13.4 %all-to-all-start.3 = ((bf16[64,16,256]{2,1,0:T(8,128)(2,1)}), bf16[64,16,256]{2,1,0:T(8,128)(2,1)S(1)}, u32[]{:S(2)}, u32[]{:S(2)}) async-start(bf16[64,16,256]{2,1,0:T(8,128)(2,1)} %bitcast.128), calls=%async_computation.3 | async-start | bytes 1048576 | tf_op jit(solution)/shard_map/all_to_all | solution.py:37
  236.8 1.0 bitcast_add_fusion.1
  237.8 4.7 %collective-permute-start.1 = (bf16[2,16,2048]{2,1,0:T(8,128)(2,1)S(1)}, bf16[2,16,2048]{2,1,0:T(8,128)(2,1)S(1)}, u32[]{:S(2)}, u32[]{:S(2)}) collective-permute-start(bf16[2,16,2048]{2,1,0:T(8,128)(2,1)S(1)} %fusion.26), channel_id=1, source_target_pairs={{0,2},{1,3},{2,0},{3,1},{4,6},{5,7},{6,4},{7,5},{8,10},{9,11},{10,... | collective-permute-start | bytes 393224 | tf_op jit(solution)/shard_map/ppermute | solution.py:33
  243.4 3.3 %collective-permute-start.5 = (bf16[128,512]{0,1:T(8,128)(2,1)S(1)}, bf16[128,512]{0,1:T(8,128)(2,1)S(1)}, u32[]{:S(2)}, u32[]{:S(2)}) collective-permute-start(bf16[128,512]{0,1:T(8,128)(2,1)S(1)} %pad_maximum_fusion.1), channel_id=1, source_target_pairs={{0,1},{1,0},{2,3},{3,2},{4,5},{5,4},{6,7},{7,6},{8,9},{9,8},{10,11... | collective-permute-start | bytes 393224 | tf_op jit(solution)/shard_map/ppermute | solution.py:33
  246.8 5.0 %collective-permute-start.2 = (bf16[16,2048]{1,0:T(8,128)(2,1)S(1)}, bf16[16,2048]{1,0:T(8,128)(2,1)S(1)}, u32[]{:S(2)}, u32[]{:S(2)}) collective-permute-start(bf16[16,2048]{1,0:T(8,128)(2,1)S(1)} %fusion.43), channel_id=1, source_target_pairs={{0,4},{1,5},{2,6},{3,7},{4,0},{5,1},{6,2},{7,3},{8,12},{9,13},{10,... | collective-permute-start | bytes 196616 | tf_op jit(solution)/shard_map/ppermute | solution.py:33
  252.4 4.0 %collective-permute-done.2 = bf16[16,2048]{1,0:T(8,128)(2,1)S(1)} collective-permute-done((bf16[16,2048]{1,0:T(8,128)(2,1)S(1)}, bf16[16,2048]{1,0:T(8,128)(2,1)S(1)}, u32[]{:S(2)}, u32[]{:S(2)}) %collective-permute-start.2) | collective-permute-done | bytes 65568 | tf_op jit(solution)/shard_map/ppermute | solution.py:33
  257.0 12.5 %all-to-all-done.3 = bf16[64,16,256]{2,1,0:T(8,128)(2,1)S(1)} async-done(((bf16[64,16,256]{2,1,0:T(8,128)(2,1)}), bf16[64,16,256]{2,1,0:T(8,128)(2,1)S(1)}, u32[]{:S(2)}, u32[]{:S(2)}) %all-to-all-start.3) | async-done | bytes 524320 | tf_op jit(solution)/shard_map/all_to_all | solution.py:37
  270.7 0.9 fusion.3
  (124 shorter events, 15.3 us)
Async XLA Ops:
  0.6 148.7 %copy-start = (bf16[256,2048]{1,0:T(8,128)(2,1)S(1)}, bf16[256,2048]{1,0:T(8,128)(2,1)}, u32[]{:S(2)}) copy-start(bf16[256,2048]{1,0:T(8,128)(2,1)} %param.27) | copy-start | bytes 3145732
  0.6 3.6 %copy-start.22 = (bf16[128,256]{1,0:T(8,128)(2,1)S(1)}, bf16[128,256]{1,0:T(8,128)(2,1)}, u32[]{:S(2)}) copy-start(bf16[128,256]{1,0:T(8,128)(2,1)} %param.22) | copy-start | bytes 196612
  4.3 0.6 copy-start.7
  4.7 46.8 %copy-start.11 = (bf16[1,2048,128]{2,1,0:T(8,128)(2,1)S(1)}, bf16[1,2048,128]{2,1,0:T(8,128)(2,1)}, u32[]{:S(2)}) copy-start(bf16[1,2048,128]{2,1,0:T(8,128)(2,1)} %param.32) | copy-start | bytes 1572868
  5.2 46.2 %copy-start.16 = (f32[2,2,128,128]{3,2,1,0:T(8,128)}, f32[2,2,128,128]{3,2,1,0:T(8,128)S(1)}, u32[]{:S(2)}) copy-start(f32[2,2,128,128]{3,2,1,0:T(8,128)S(1)} %get-tuple-element.37) | copy-start | bytes 786436
  5.3 46.3 %copy-start.10 = (bf16[1,2048,128]{2,1,0:T(8,128)(2,1)S(1)}, bf16[1,2048,128]{2,1,0:T(8,128)(2,1)}, u32[]{:S(2)}) copy-start(bf16[1,2048,128]{2,1,0:T(8,128)(2,1)} %param.33) | copy-start | bytes 1572868
  6.3 61.1 %all-to-all-start = ((bf16[32,8,256]{2,1,0:T(8,128)(2,1)}), bf16[32,8,256]{2,1,0:T(8,128)(2,1)S(1)}, u32[]{:S(2)}, u32[]{:S(2)}) async-start(bf16[32,8,256]{2,1,0:T(8,128)(2,1)} %fusion.25), calls=%async_computation | async-start | bytes 262144 | tf_op jit(solution)/shard_map/all_to_all | solution.py:37
  51.5 5.7 %copy-start.25 = (f32[128,4]{0,1:T(4,128)S(1)}, f32[128,4]{0,1:T(4,128)}, u32[]{:S(2)}) copy-start(f32[128,4]{0,1:T(4,128)} %param.30) | copy-start | bytes 6148
  51.7 37.2 %copy-start.2 = (bf16[2048,256]{1,0:T(8,128)(2,1)}, bf16[2048,256]{1,0:T(8,128)(2,1)S(1)}, u32[]{:S(2)}) copy-start(bf16[2048,256]{1,0:T(8,128)(2,1)S(1)} %pad_maximum_fusion.refs_5_) | copy-start | bytes 3145732
  51.7 25.6 %copy-start.24 = (s32[128,4]{0,1:T(4,128)S(1)}, s32[128,4]{0,1:T(4,128)}, u32[]{:S(2)}) copy-start(s32[128,4]{0,1:T(4,128)} %param.29) | copy-start | bytes 6148
  51.7 94.3 %collective-permute-start.10 = (bf16[2048,256]{1,0:T(8,128)(2,1)S(1)}, bf16[2048,256]{1,0:T(8,128)(2,1)}, u32[]{:S(2)}, u32[]{:S(2)}) collective-permute-start(bf16[2048,256]{1,0:T(8,128)(2,1)S(1)} %pad_maximum_fusion.refs_5_), channel_id=1, source_target_pairs={{0,1},{1,0},{2,3},{3,2},{4,5},{5,4},{6,7},{7,6},{8,9},{9,8},{10,11... | collective-permute-start | bytes 3145736 | tf_op jit(solution)/shard_map/ppermute | solution.py:33
  55.1 150.1 %collective-permute-start.15 = (bf16[1024,256]{1,0:T(8,128)(2,1)}, bf16[1024,256]{1,0:T(8,128)(2,1)}, u32[]{:S(2)}, u32[]{:S(2)}) collective-permute-start(bf16[1024,256]{1,0:T(8,128)(2,1)} %bitcast.32.refs_5_), channel_id=1, source_target_pairs={{0,1},{1,0},{2,3},{3,2},{4,5},{5,4},{6,7},{7,6},{8,9},{9,8},{10,11... | collective-permute-start | bytes 1572872 | tf_op jit(solution)/shard_map/ppermute | solution.py:33
  69.6 18.6 %all-to-all-start.1 = ((bf16[32,8,128]{2,1,0:T(8,128)(2,1)}), bf16[32,8,128]{2,1,0:T(8,128)(2,1)S(1)}, u32[]{:S(2)}, u32[]{:S(2)}) async-start(bf16[32,8,128]{2,1,0:T(8,128)(2,1)} %copy.181), calls=%async_computation.1 | async-start | bytes 131072 | tf_op jit(solution)/shard_map/all_to_all | solution.py:37
  88.2 0.6 copy-start.18
  88.8 8.3 %copy-start.3 = (bf16[128,2048]{1,0:T(8,128)(2,1)S(1)}, bf16[128,2048]{1,0:T(8,128)(2,1)}, u32[]{:S(2)}) copy-start(bf16[128,2048]{1,0:T(8,128)(2,1)} %get-tuple-element.39) | copy-start | bytes 1572868
  88.8 38.6 %all-to-all-start.2 = ((bf16[32,16,512]{2,1,0:T(8,128)(2,1)}), bf16[32,16,512]{2,1,0:T(8,128)(2,1)S(1)}, u32[]{:S(2)}, u32[]{:S(2)}) async-start(bf16[32,16,512]{2,1,0:T(8,128)(2,1)} %bitcast.137), calls=%async_computation.2 | async-start | bytes 1048576 | tf_op jit(solution)/shard_map/all_to_all | solution.py:37
  94.0 3.2 %copy-start.9 = (bf16[2048,128]{1,0:T(8,128)(2,1)S(1)}, bf16[2048,128]{1,0:T(8,128)(2,1)}, u32[]{:S(2)}) copy-start(bf16[2048,128]{1,0:T(8,128)(2,1)} %param.35) | copy-start | bytes 1572868
  96.0 2.1 copy-start.8
  97.1 2.3 copy-start.26
  99.5 2.2 copy-start.19
  99.5 2.2 copy-start.17
  101.7 47.6 %copy-start.27 = (f32[256]{0:T(256)S(1)}, f32[256]{0:T(256)}, u32[]{:S(2)}) copy-start(f32[256]{0:T(256)} %param.26) | copy-start | bytes 3076
  127.4 9.8 %copy-start.1 = (bf16[32,16,512]{2,1,0:T(8,128)(2,1)}, bf16[32,16,512]{2,1,0:T(8,128)(2,1)S(1)}, u32[]{:S(2)}) copy-start(bf16[32,16,512]{2,1,0:T(8,128)(2,1)S(1)} %all-to-all-done.2) | copy-start | bytes 1572868
  127.4 60.9 %collective-permute-start.6 = (bf16[512,512]{1,0:T(8,128)(2,1)S(1)}, bf16[512,512]{1,0:T(8,128)(2,1)}, u32[]{:S(2)}, u32[]{:S(2)}) collective-permute-start(bf16[512,512]{1,0:T(8,128)(2,1)S(1)} %bitcast.122), channel_id=1, source_target_pairs={{0,2},{1,3},{2,4},{3,5},{4,6},{5,7},{6,0},{7,1},{8,10},{9,11},{10,... | collective-permute-start | bytes 1572872 | tf_op jit(solution)/shard_map/ppermute | solution.py:28
  131.5 56.7 %collective-permute-start.7 = (bf16[512,512]{1,0:T(8,128)(2,1)S(1)}, bf16[512,512]{1,0:T(8,128)(2,1)}, u32[]{:S(2)}, u32[]{:S(2)}) collective-permute-start(bf16[512,512]{1,0:T(8,128)(2,1)S(1)} %bitcast.123), channel_id=1, source_target_pairs={{0,6},{1,7},{2,0},{3,1},{4,2},{5,3},{6,4},{7,5},{8,14},{9,15},{10,... | collective-permute-start | bytes 1572872 | tf_op jit(solution)/shard_map/ppermute | solution.py:28
  139.0 25.1 %collective-permute-start.8 = (bf16[256,512]{1,0:T(8,128)(2,1)}, bf16[256,512]{1,0:T(8,128)(2,1)S(1)}, u32[]{:S(2)}, u32[]{:S(2)}) collective-permute-start(bf16[256,512]{1,0:T(8,128)(2,1)} %get-tuple-element.41), channel_id=1, source_target_pairs={{0,4},{1,5},{2,6},{3,7},{4,0},{5,1},{6,2},{7,3},{8,12},{9,13},{10,... | collective-permute-start | bytes 786440 | tf_op jit(solution)/shard_map/ppermute | solution.py:28
  146.0 25.2 %collective-permute-start.9 = (bf16[256,512]{1,0:T(8,128)(2,1)}, bf16[256,512]{1,0:T(8,128)(2,1)S(1)}, u32[]{:S(2)}, u32[]{:S(2)}) collective-permute-start(bf16[256,512]{1,0:T(8,128)(2,1)} %get-tuple-element.42), channel_id=1, source_target_pairs={{0,4},{1,5},{2,6},{3,7},{4,0},{5,1},{6,2},{7,3},{8,12},{9,13},{10,... | collective-permute-start | bytes 786440 | tf_op jit(solution)/shard_map/ppermute | solution.py:28
  164.1 24.2 %copy-start.13 = (bf16[256,512]{1,0:T(8,128)(2,1)}, bf16[256,512]{1,0:T(8,128)(2,1)S(1)}, u32[]{:S(2)}) copy-start(bf16[256,512]{1,0:T(8,128)(2,1)S(1)} %collective-permute-done.8.refs_3_) | copy-start | bytes 786436
  164.1 36.2 %collective-permute-start.3 = (bf16[128,128]{0,1:T(8,128)(2,1)}, bf16[128,128]{0,1:T(8,128)(2,1)S(1)}, u32[]{:S(2)}, u32[]{:S(2)}) collective-permute-start(bf16[128,128]{0,1:T(8,128)(2,1)} %fusion.5), channel_id=1, source_target_pairs={{0,4},{1,5},{2,6},{3,7},{4,0},{5,1},{6,2},{7,3},{8,12},{9,13},{10,... | collective-permute-start | bytes 98312 | tf_op jit(solution)/shard_map/ppermute | solution.py:33
  171.2 17.0 %copy-start.15 = (bf16[256,512]{1,0:T(8,128)(2,1)}, bf16[256,512]{1,0:T(8,128)(2,1)S(1)}, u32[]{:S(2)}) copy-start(bf16[256,512]{1,0:T(8,128)(2,1)S(1)} %collective-permute-done.9.refs_4_) | copy-start | bytes 786436
  171.2 65.5 %collective-permute-start = (bf16[2,2,16,2048]{3,2,0,1:T(8,128)(2,1)}, bf16[2,2,16,2048]{3,2,0,1:T(8,128)(2,1)}, u32[]{:S(2)}, u32[]{:S(2)}) collective-permute-start(bf16[2,2,16,2048]{3,2,0,1:T(8,128)(2,1)} %fusion.10), channel_id=1, source_target_pairs={{0,1},{1,0},{2,3},{3,2},{4,5},{5,4},{6,7},{7,6},{8,9},{9,8},{10,11... | collective-permute-start | bytes 786440 | tf_op jit(solution)/shard_map/ppermute | solution.py:33
  192.8 26.0 %collective-permute-start.11 = (bf16[512,256]{1,0:T(8,128)(2,1)}, bf16[512,256]{1,0:T(8,128)(2,1)S(1)}, u32[]{:S(2)}, u32[]{:S(2)}) collective-permute-start(bf16[512,256]{1,0:T(8,128)(2,1)} %get-tuple-element.43.refs_0_), channel_id=1, source_target_pairs={{0,2},{1,3},{2,4},{3,5},{4,6},{5,7},{6,0},{7,1},{8,10},{9,11},{10,... | collective-permute-start | bytes 786440 | tf_op jit(solution)/shard_map/ppermute | solution.py:28
  194.7 24.0 %collective-permute-start.12 = (bf16[512,256]{1,0:T(8,128)(2,1)}, bf16[512,256]{1,0:T(8,128)(2,1)S(1)}, u32[]{:S(2)}, u32[]{:S(2)}) collective-permute-start(bf16[512,256]{1,0:T(8,128)(2,1)} %get-tuple-element.43.refs_0_), channel_id=1, source_target_pairs={{0,6},{1,7},{2,0},{3,1},{4,2},{5,3},{6,4},{7,5},{8,14},{9,15},{10,... | collective-permute-start | bytes 786440 | tf_op jit(solution)/shard_map/ppermute | solution.py:28
  200.2 0.6 copy-start.23
  200.8 13.0 %collective-permute-start.13 = (bf16[256,256]{1,0:T(8,128)(2,1)}, bf16[256,256]{1,0:T(8,128)(2,1)S(1)}, u32[]{:S(2)}, u32[]{:S(2)}) collective-permute-start(bf16[256,256]{1,0:T(8,128)(2,1)} %get-tuple-element.44), channel_id=1, source_target_pairs={{0,4},{1,5},{2,6},{3,7},{4,0},{5,1},{6,2},{7,3},{8,12},{9,13},{10,... | collective-permute-start | bytes 393224 | tf_op jit(solution)/shard_map/ppermute | solution.py:28
  205.2 13.5 %collective-permute-start.14 = (bf16[256,256]{1,0:T(8,128)(2,1)}, bf16[256,256]{1,0:T(8,128)(2,1)S(1)}, u32[]{:S(2)}, u32[]{:S(2)}) collective-permute-start(bf16[256,256]{1,0:T(8,128)(2,1)} %get-tuple-element.45), channel_id=1, source_target_pairs={{0,4},{1,5},{2,6},{3,7},{4,0},{5,1},{6,2},{7,3},{8,12},{9,13},{10,... | collective-permute-start | bytes 393224 | tf_op jit(solution)/shard_map/ppermute | solution.py:28
  213.8 4.9 %copy-start.20 = (bf16[256,256]{1,0:T(8,128)(2,1)}, bf16[256,256]{1,0:T(8,128)(2,1)S(1)}, u32[]{:S(2)}) copy-start(bf16[256,256]{1,0:T(8,128)(2,1)S(1)} %collective-permute-done.13.refs_3_) | copy-start | bytes 393220
  213.8 28.7 %collective-permute-start.4 = (bf16[128,256]{0,1:T(8,128)(2,1)S(1)}, bf16[128,256]{0,1:T(8,128)(2,1)}, u32[]{:S(2)}, u32[]{:S(2)}) collective-permute-start(bf16[128,256]{0,1:T(8,128)(2,1)S(1)} %pad_maximum_fusion.2), channel_id=1, source_target_pairs={{0,2},{1,3},{2,0},{3,1},{4,6},{5,7},{6,4},{7,5},{8,10},{9,11},{10,... | collective-permute-start | bytes 196616 | tf_op jit(solution)/shard_map/ppermute | solution.py:33
  218.7 0.7 copy-start.21
  218.7 0.8 copy-start.12
  219.5 0.7 copy-start.14
  223.4 46.1 %all-to-all-start.3 = ((bf16[64,16,256]{2,1,0:T(8,128)(2,1)}), bf16[64,16,256]{2,1,0:T(8,128)(2,1)S(1)}, u32[]{:S(2)}, u32[]{:S(2)}) async-start(bf16[64,16,256]{2,1,0:T(8,128)(2,1)} %bitcast.128), calls=%async_computation.3 | async-start | bytes 1048576 | tf_op jit(solution)/shard_map/all_to_all | solution.py:37
  237.8 31.7 %copy-start.5 = (bf16[128,32,32]{0,2,1:T(8,128)(2,1)S(1)}, bf16[128,32,32]{0,2,1:T(8,128)(2,1)}, u32[]{:S(2)}) copy-start(bf16[128,32,32]{0,2,1:T(8,128)(2,1)} %get-tuple-element.127) | copy-start | bytes 786436
  237.8 8.9 %collective-permute-start.1 = (bf16[2,16,2048]{2,1,0:T(8,128)(2,1)S(1)}, bf16[2,16,2048]{2,1,0:T(8,128)(2,1)S(1)}, u32[]{:S(2)}, u32[]{:S(2)}) collective-permute-start(bf16[2,16,2048]{2,1,0:T(8,128)(2,1)S(1)} %fusion.26), channel_id=1, source_target_pairs={{0,2},{1,3},{2,0},{3,1},{4,6},{5,7},{6,4},{7,5},{8,10},{9,11},{10,... | collective-permute-start | bytes 393224 | tf_op jit(solution)/shard_map/ppermute | solution.py:33
  243.4 8.8 %collective-permute-start.5 = (bf16[128,512]{0,1:T(8,128)(2,1)S(1)}, bf16[128,512]{0,1:T(8,128)(2,1)S(1)}, u32[]{:S(2)}, u32[]{:S(2)}) collective-permute-start(bf16[128,512]{0,1:T(8,128)(2,1)S(1)} %pad_maximum_fusion.1), channel_id=1, source_target_pairs={{0,1},{1,0},{2,3},{3,2},{4,5},{5,4},{6,7},{7,6},{8,9},{9,8},{10,11... | collective-permute-start | bytes 393224 | tf_op jit(solution)/shard_map/ppermute | solution.py:33
  246.8 23.0 %copy-start.4 = (bf16[128,32,32]{0,2,1:T(8,128)(2,1)S(1)}, bf16[128,32,32]{0,2,1:T(8,128)(2,1)}, u32[]{:S(2)}) copy-start(bf16[128,32,32]{0,2,1:T(8,128)(2,1)} %get-tuple-element.126) | copy-start | bytes 786436
  246.8 9.5 %collective-permute-start.2 = (bf16[16,2048]{1,0:T(8,128)(2,1)S(1)}, bf16[16,2048]{1,0:T(8,128)(2,1)S(1)}, u32[]{:S(2)}, u32[]{:S(2)}) collective-permute-start(bf16[16,2048]{1,0:T(8,128)(2,1)S(1)} %fusion.43), channel_id=1, source_target_pairs={{0,4},{1,5},{2,6},{3,7},{4,0},{5,1},{6,2},{7,3},{8,12},{9,13},{10,... | collective-permute-start | bytes 196616 | tf_op jit(solution)/shard_map/ppermute | solution.py:33
  269.8 1.0 copy-start.6

commit v9 on v8

--- a/solution.py
+++ b/solution.py
@@ -13,9 +13,10 @@
 BLK = 64
 EP = ("ep_0", "ep_1")
 GRP_EP = ("grp", "ep_0", "ep_1")
-TP = ("tp_quad", "tp_pair")
-EP_PAIR = ("ep_0", "ep_1", "tp_pair")
-GRP_EP_TP = ("grp", "ep_0", "ep_1", "tp_quad", "tp_pair")
+QUAD, PAIR = ("tq", "tb")
+TP = (QUAD, PAIR)
+EP_PAIR = (*EP, PAIR)
+GRP_EP_TP = (*GRP_EP, *TP)
 
 
 EPSILON = 1e-06
@@ -266,16 +267,16 @@
         slot // half == lax.broadcasted_iota(jnp.int32, (slots, experts), 1), one, zero
     ).astype(jnp.bfloat16)
     wanted = jnp.dot(spread, places, preferred_element_type=jnp.float32).astype(jnp.int32)
-    own = lax.broadcasted_iota(jnp.int32, (slots, tokens), 0) % half + lax.axis_index("tp_pair") * half
+    own = lax.broadcasted_iota(jnp.int32, (slots, tokens), 0) % half + lax.axis_index(PAIR) * half
     filled = jnp.where(wanted == own, one, zero).astype(jnp.bfloat16)
-    start = pl.multiple_of(lax.axis_index("tp_quad") * width, width)
+    start = pl.multiple_of(lax.axis_index(QUAD) * width, width)
     outgoing[...] = jnp.dot(
         filled, normed[:, pl.ds(start, width)], preferred_element_type=jnp.float32
     ).astype(jnp.bfloat16)
 
 
 def around_products(pieces, matrices):
-    quad = lax.axis_index("tp_quad")
+    quad = lax.axis_index(QUAD)
     held = []
 
     def dot(piece, matrix, step):
@@ -314,7 +315,7 @@
         ]
         for halves in around_products(pieces, (own_in, partner_in))
     ]
-    even = lax.axis_index("tp_pair") == 0
+    even = lax.axis_index(PAIR) == 0
     for k, part in enumerate((hidden_first, hidden_second)):
         part[:, :units] = jnp.where(even, sides[0][k], sides[1][k])
         part[:, units:] = jnp.where(even, sides[1][k], sides[0][k])
@@ -325,7 +326,7 @@
     pieces = (own, before, after, far_first, far_second)
     sources, _, slots, width = answers.shape
     count = sources // 2
-    place = lax.axis_index("tp_pair")
+    place = lax.axis_index(PAIR)
     for side, halves in zip(
         (place, 1 - place), around_products(pieces, (own_down, partner_down))
     ):
@@ -481,7 +482,7 @@
 def solution(mesh):
     split = Mesh(
         mesh.devices.reshape(mesh.shape["grp"], -1, 2, mesh.shape["tp"] // 2, 2),
-        ("grp", "ep_0", "ep_1", "tp_quad", "tp_pair"),
+        GRP_EP_TP,
     )
     in_specs = (
         P(GRP_EP, TP),

time: 273 us -> 273 us (level)
  no operation moved by 1% of the time
where the time goes in v9:
time: 273 us; the launch traced here: 272 us
  starting transfers between devices  145 us (53%)
  waiting for transfers between devices  81.6 us (30%)
  Pallas kernels  11.9 us (4%)
  matrix products  11.1 us (4%)
  local copies, waits for them, and re-layouts  10.4 us (4%)
  other arithmetic  9.6 us (4%)
    all_to_all x4, starting transfers between devices, exchanged(): return lax.all_to_all(array, axis, split_axis=0, concat_axis=0, tiled=True)  68.9 us
    all_to_all x4, waiting for transfers between devices, exchanged(): return lax.all_to_all(array, axis, split_axis=0, concat_axis=0, tiled=True)  56.6 us
    ppermute x8, starting transfers between devices, swapped(): return lax.ppermute(array, axis, [(i, i ^ bit) for i in range(count)])  42.7 us
    ppermute x8, starting transfers between devices, shifted(): lax.ppermute(array, axis, [(i, (i + step) % count) for i in range(count)])  33.9 us
    ppermute x8, waiting for transfers between devices, shifted(): lax.ppermute(array, axis, [(i, (i + step) % count) for i in range(count)])  20.6 us
    pallas_call x2, Pallas kernels, fetching(): pl.pallas_call(body, out_shape=shapes, in_specs=[ANY] * count, out_specs=...  7.63 us
  transfers between devices with their start and end apart: 20, of which 10 were waited for; matrix products, arithmetic and copies ran while one was open for 8% of the time, Pallas kernels for 4%

profile of v9, /device:TPU:65, one launch (start us, length us, event | category | flops | bytes accessed | tf_op | source)
XLA Modules:
  0.0 271.6 jit_solution(4455726228116132649)
XLA Ops:
  1.7 0.9 divide_multiply_fusion
  6.3 45.2 %all-to-all-start = ((bf16[32,8,256]{2,1,0:T(8,128)(2,1)}), bf16[32,8,256]{2,1,0:T(8,128)(2,1)S(1)}, u32[]{:S(2)}, u32[]{:S(2)}) async-start(bf16[32,8,256]{2,1,0:T(8,128)(2,1)} %fusion.25), calls=%async_computation | async-start | bytes 262144 | tf_op jit(solution)/shard_map/all_to_all | solution.py:38
  51.7 3.4 %collective-permute-start.10 = (bf16[2048,256]{1,0:T(8,128)(2,1)S(1)}, bf16[2048,256]{1,0:T(8,128)(2,1)}, u32[]{:S(2)}, u32[]{:S(2)}) collective-permute-start(bf16[2048,256]{1,0:T(8,128)(2,1)S(1)} %pad_maximum_fusion.refs_5_), channel_id=1, source_target_pairs={{0,1},{1,0},{2,3},{3,2},{4,5},{5,4},{6,7},{7,6},{8,9},{9,8},{10,11... | collective-permute-start | bytes 3145736 | tf_op jit(solution)/shard_map/ppermute | solution.py:34
  55.1 2.1 collective-permute-start.15
  57.2 0.9 convert_multiply_fusion.1
  58.1 9.3 %all-to-all-done = bf16[32,8,256]{2,1,0:T(8,128)(2,1)S(1)} async-done(((bf16[32,8,256]{2,1,0:T(8,128)(2,1)}), bf16[32,8,256]{2,1,0:T(8,128)(2,1)S(1)}, u32[]{:S(2)}, u32[]{:S(2)}) %all-to-all-start) | async-done | bytes 131104 | tf_op jit(solution)/shard_map/all_to_all | solution.py:38
  67.5 1.2 fusion.2
  69.6 5.2 %all-to-all-start.1 = ((bf16[32,8,128]{2,1,0:T(8,128)(2,1)}), bf16[32,8,128]{2,1,0:T(8,128)(2,1)S(1)}, u32[]{:S(2)}, u32[]{:S(2)}) async-start(bf16[32,8,128]{2,1,0:T(8,128)(2,1)} %copy.181), calls=%async_computation.1 | async-start | bytes 131072 | tf_op jit(solution)/shard_map/all_to_all | solution.py:38
  74.9 2.4 shard_map.185
  77.9 10.3 %all-to-all-done.1 = bf16[32,8,128]{2,1,0:T(8,128)(2,1)S(1)} async-done(((bf16[32,8,128]{2,1,0:T(8,128)(2,1)}), bf16[32,8,128]{2,1,0:T(8,128)(2,1)S(1)}, u32[]{:S(2)}, u32[]{:S(2)}) %all-to-all-start.1) | async-done | bytes 65568 | tf_op jit(solution)/shard_map/all_to_all | solution.py:38
  88.8 5.1 %all-to-all-start.2 = ((bf16[32,16,512]{2,1,0:T(8,128)(2,1)}), bf16[32,16,512]{2,1,0:T(8,128)(2,1)S(1)}, u32[]{:S(2)}, u32[]{:S(2)}) async-start(bf16[32,16,512]{2,1,0:T(8,128)(2,1)} %bitcast.137), calls=%async_computation.2 | async-start | bytes 1048576 | tf_op jit(solution)/shard_map/all_to_all | solution.py:38
  94.0 0.9 fusion.6
  94.9 1.1 convolution_select_fusion
  96.0 1.1 fusion.8
  97.1 1.0 fusion.59
  98.3 1.1 copy.187
  99.5 2.2 fusion.5
  101.7 1.1 multiply_reduce_fusion
  102.8 24.6 %all-to-all-done.2 = bf16[32,16,512]{2,1,0:T(8,128)(2,1)S(1)} async-done(((bf16[32,16,512]{2,1,0:T(8,128)(2,1)}), bf16[32,16,512]{2,1,0:T(8,128)(2,1)S(1)}, u32[]{:S(2)}, u32[]{:S(2)}) %all-to-all-start.2) | async-done | bytes 524320 | tf_op jit(solution)/shard_map/all_to_all | solution.py:38
  127.4 4.1 %collective-permute-start.6 = (bf16[512,512]{1,0:T(8,128)(2,1)S(1)}, bf16[512,512]{1,0:T(8,128)(2,1)}, u32[]{:S(2)}, u32[]{:S(2)}) collective-permute-start(bf16[512,512]{1,0:T(8,128)(2,1)S(1)} %bitcast.122), channel_id=1, source_target_pairs={{0,2},{1,3},{2,4},{3,5},{4,6},{5,7},{6,0},{7,1},{8,10},{9,11},{10,... | collective-permute-start | bytes 1572872 | tf_op jit(solution)/shard_map/ppermute | solution.py:29
  131.5 3.8 %collective-permute-start.7 = (bf16[512,512]{1,0:T(8,128)(2,1)S(1)}, bf16[512,512]{1,0:T(8,128)(2,1)}, u32[]{:S(2)}, u32[]{:S(2)}) collective-permute-start(bf16[512,512]{1,0:T(8,128)(2,1)S(1)} %bitcast.123), channel_id=1, source_target_pairs={{0,6},{1,7},{2,0},{3,1},{4,2},{5,3},{6,4},{7,5},{8,14},{9,15},{10,... | collective-permute-start | bytes 1572872 | tf_op jit(solution)/shard_map/ppermute | solution.py:29
  136.1 1.0 copy.183
  137.1 1.9 shard_map.186
  139.0 7.0 %collective-permute-start.8 = (bf16[256,512]{1,0:T(8,128)(2,1)}, bf16[256,512]{1,0:T(8,128)(2,1)S(1)}, u32[]{:S(2)}, u32[]{:S(2)}) collective-permute-start(bf16[256,512]{1,0:T(8,128)(2,1)} %get-tuple-element.41), channel_id=1, source_target_pairs={{0,4},{1,5},{2,6},{3,7},{4,0},{5,1},{6,2},{7,3},{8,12},{9,13},{10,... | collective-permute-start | bytes 786440 | tf_op jit(solution)/shard_map/ppermute | solution.py:29
  146.0 2.3 collective-permute-start.9
  148.3 1.0 mul.111
  149.3 1.2 fusion.41
  150.5 13.5 %collective-permute-done.8.refs_3_ = bf16[256,512]{1,0:T(8,128)(2,1)S(1)} collective-permute-done((bf16[256,512]{1,0:T(8,128)(2,1)}, bf16[256,512]{1,0:T(8,128)(2,1)S(1)}, u32[]{:S(2)}, u32[]{:S(2)}) %collective-permute-start.8) | collective-permute-done | bytes 262176 | tf_op jit(solution)/shard_map/ppermute | solution.py:29
  164.1 4.9 %collective-permute-start.3 = (bf16[128,128]{0,1:T(8,128)(2,1)}, bf16[128,128]{0,1:T(8,128)(2,1)S(1)}, u32[]{:S(2)}, u32[]{:S(2)}) collective-permute-start(bf16[128,128]{0,1:T(8,128)(2,1)} %fusion.5), channel_id=1, source_target_pairs={{0,4},{1,5},{2,6},{3,7},{4,0},{5,1},{6,2},{7,3},{8,12},{9,13},{10,... | collective-permute-start | bytes 98312 | tf_op jit(solution)/shard_map/ppermute | solution.py:34
  169.7 1.5 collective-permute-done.9.refs_4_
  171.2 17.0 %collective-permute-start = (bf16[2,2,16,2048]{3,2,0,1:T(8,128)(2,1)}, bf16[2,2,16,2048]{3,2,0,1:T(8,128)(2,1)}, u32[]{:S(2)}, u32[]{:S(2)}) collective-permute-start(bf16[2,2,16,2048]{3,2,0,1:T(8,128)(2,1)} %fusion.10), channel_id=1, source_target_pairs={{0,1},{1,0},{2,3},{3,2},{4,5},{5,4},{6,7},{7,6},{8,9},{9,8},{10,11... | collective-permute-start | bytes 786440 | tf_op jit(solution)/shard_map/ppermute | solution.py:34
  188.3 4.4 %shard_map.187 = (bf16[512,256]{1,0:T(8,128)(2,1)}, bf16[256,256]{1,0:T(8,128)(2,1)}, bf16[256,256]{1,0:T(8,128)(2,1)}) custom-call(bf16[512,512]{1,0:T(8,128)(2,1)} %bitcast.125, bf16[512,512]{1,0:T(8,128)(2,1)} %collective-permute-done.6.refs_1_, bf16[512,512]{1,0:T(8,128)(2,1)} %collective-permute-done.7.refs_2_, bf16[256,512]{1,0:T(8,128)(2,1)} %copy-done.13, ...), custom_call_target="tpu_custom_call" | custom-call | tf_op jit(solution)/shard_map/pallas_call | solution.py:222
  192.8 2.0 collective-permute-start.11
  194.7 5.5 %collective-permute-start.12 = (bf16[512,256]{1,0:T(8,128)(2,1)}, bf16[512,256]{1,0:T(8,128)(2,1)S(1)}, u32[]{:S(2)}, u32[]{:S(2)}) collective-permute-start(bf16[512,256]{1,0:T(8,128)(2,1)} %get-tuple-element.43.refs_0_), channel_id=1, source_target_pairs={{0,6},{1,7},{2,0},{3,1},{4,2},{5,3},{6,4},{7,5},{8,14},{9,15},{10,... | collective-permute-start | bytes 786440 | tf_op jit(solution)/shard_map/ppermute | solution.py:29
  200.8 4.4 %collective-permute-start.13 = (bf16[256,256]{1,0:T(8,128)(2,1)}, bf16[256,256]{1,0:T(8,128)(2,1)S(1)}, u32[]{:S(2)}, u32[]{:S(2)}) collective-permute-start(bf16[256,256]{1,0:T(8,128)(2,1)} %get-tuple-element.44), channel_id=1, source_target_pairs={{0,4},{1,5},{2,6},{3,7},{4,0},{5,1},{6,2},{7,3},{8,12},{9,13},{10,... | collective-permute-start | bytes 393224 | tf_op jit(solution)/shard_map/ppermute | solution.py:29
  205.2 4.9 %collective-permute-start.14 = (bf16[256,256]{1,0:T(8,128)(2,1)}, bf16[256,256]{1,0:T(8,128)(2,1)S(1)}, u32[]{:S(2)}, u32[]{:S(2)}) collective-permute-start(bf16[256,256]{1,0:T(8,128)(2,1)} %get-tuple-element.45), channel_id=1, source_target_pairs={{0,4},{1,5},{2,6},{3,7},{4,0},{5,1},{6,2},{7,3},{8,12},{9,13},{10,... | collective-permute-start | bytes 393224 | tf_op jit(solution)/shard_map/ppermute | solution.py:29
  210.9 2.9 %collective-permute-done.13.refs_3_ = bf16[256,256]{1,0:T(8,128)(2,1)S(1)} collective-permute-done((bf16[256,256]{1,0:T(8,128)(2,1)}, bf16[256,256]{1,0:T(8,128)(2,1)S(1)}, u32[]{:S(2)}, u32[]{:S(2)}) %collective-permute-start.13) | collective-permute-done | bytes 131104 | tf_op jit(solution)/shard_map/ppermute | solution.py:29
  213.8 2.3 collective-permute-start.4
  216.1 2.6 collective-permute-done.14.refs_4_
  220.2 3.2 %shard_map.188 = bf16[32,2,16,256]{3,2,1,0:T(8,128)(2,1)} custom-call(bf16[512,256]{1,0:T(8,128)(2,1)} %get-tuple-element.43.refs_0_, bf16[512,256]{1,0:T(8,128)(2,1)} %copy-done.12, bf16[512,256]{1,0:T(8,128)(2,1)} %copy-done.14, bf16[256,256]{1,0:T(8,128)(2,1)} %copy-done.20, bf16[256,256]{1,0:T(8,128)(2,1)} %copy-done.21, ...), custom_call_target="tpu_custom_call" | custom-call | tf_op jit(solution)/shard_map/pallas_call | solution.py:222
  223.4 13.4 %all-to-all-start.3 = ((bf16[64,16,256]{2,1,0:T(8,128)(2,1)}), bf16[64,16,256]{2,1,0:T(8,128)(2,1)S(1)}, u32[]{:S(2)}, u32[]{:S(2)}) async-start(bf16[64,16,256]{2,1,0:T(8,128)(2,1)} %bitcast.128), calls=%async_computation.3 | async-start | bytes 1048576 | tf_op jit(solution)/shard_map/all_to_all | solution.py:38
  236.8 1.0 bitcast_add_fusion.1
  237.8 4.7 %collective-permute-start.1 = (bf16[2,16,2048]{2,1,0:T(8,128)(2,1)S(1)}, bf16[2,16,2048]{2,1,0:T(8,128)(2,1)S(1)}, u32[]{:S(2)}, u32[]{:S(2)}) collective-permute-start(bf16[2,16,2048]{2,1,0:T(8,128)(2,1)S(1)} %fusion.26), channel_id=1, source_target_pairs={{0,2},{1,3},{2,0},{3,1},{4,6},{5,7},{6,4},{7,5},{8,10},{9,11},{10,... | collective-permute-start | bytes 393224 | tf_op jit(solution)/shard_map/ppermute | solution.py:34
  243.4 3.3 %collective-permute-start.5 = (bf16[128,512]{0,1:T(8,128)(2,1)S(1)}, bf16[128,512]{0,1:T(8,128)(2,1)S(1)}, u32[]{:S(2)}, u32[]{:S(2)}) collective-permute-start(bf16[128,512]{0,1:T(8,128)(2,1)S(1)} %pad_maximum_fusion.1), channel_id=1, source_target_pairs={{0,1},{1,0},{2,3},{3,2},{4,5},{5,4},{6,7},{7,6},{8,9},{9,8},{10,11... | collective-permute-start | bytes 393224 | tf_op jit(solution)/shard_map/ppermute | solution.py:34
  246.8 5.0 %collective-permute-start.2 = (bf16[16,2048]{1,0:T(8,128)(2,1)S(1)}, bf16[16,2048]{1,0:T(8,128)(2,1)S(1)}, u32[]{:S(2)}, u32[]{:S(2)}) collective-permute-start(bf16[16,2048]{1,0:T(8,128)(2,1)S(1)} %fusion.43), channel_id=1, source_target_pairs={{0,4},{1,5},{2,6},{3,7},{4,0},{5,1},{6,2},{7,3},{8,12},{9,13},{10,... | collective-permute-start | bytes 196616 | tf_op jit(solution)/shard_map/ppermute | solution.py:34
  252.4 4.0 %collective-permute-done.2 = bf16[16,2048]{1,0:T(8,128)(2,1)S(1)} collective-permute-done((bf16[16,2048]{1,0:T(8,128)(2,1)S(1)}, bf16[16,2048]{1,0:T(8,128)(2,1)S(1)}, u32[]{:S(2)}, u32[]{:S(2)}) %collective-permute-start.2) | collective-permute-done | bytes 65568 | tf_op jit(solution)/shard_map/ppermute | solution.py:34
  257.0 12.5 %all-to-all-done.3 = bf16[64,16,256]{2,1,0:T(8,128)(2,1)S(1)} async-done(((bf16[64,16,256]{2,1,0:T(8,128)(2,1)}), bf16[64,16,256]{2,1,0:T(8,128)(2,1)S(1)}, u32[]{:S(2)}, u32[]{:S(2)}) %all-to-all-start.3) | async-done | bytes 524320 | tf_op jit(solution)/shard_map/all_to_all | solution.py:38
  270.7 0.9 fusion.3
  (124 shorter events, 15.3 us)
Async XLA Ops:
  0.6 148.7 %copy-start = (bf16[256,2048]{1,0:T(8,128)(2,1)S(1)}, bf16[256,2048]{1,0:T(8,128)(2,1)}, u32[]{:S(2)}) copy-start(bf16[256,2048]{1,0:T(8,128)(2,1)} %param.27) | copy-start | bytes 3145732
  0.6 3.6 %copy-start.22 = (bf16[128,256]{1,0:T(8,128)(2,1)S(1)}, bf16[128,256]{1,0:T(8,128)(2,1)}, u32[]{:S(2)}) copy-start(bf16[128,256]{1,0:T(8,128)(2,1)} %param.22) | copy-start | bytes 196612
  4.3 0.6 copy-start.7
  4.7 46.8 %copy-start.11 = (bf16[1,2048,128]{2,1,0:T(8,128)(2,1)S(1)}, bf16[1,2048,128]{2,1,0:T(8,128)(2,1)}, u32[]{:S(2)}) copy-start(bf16[1,2048,128]{2,1,0:T(8,128)(2,1)} %param.32) | copy-start | bytes 1572868
  5.2 46.2 %copy-start.16 = (f32[2,2,128,128]{3,2,1,0:T(8,128)}, f32[2,2,128,128]{3,2,1,0:T(8,128)S(1)}, u32[]{:S(2)}) copy-start(f32[2,2,128,128]{3,2,1,0:T(8,128)S(1)} %get-tuple-element.37) | copy-start | bytes 786436
  5.3 46.3 %copy-start.10 = (bf16[1,2048,128]{2,1,0:T(8,128)(2,1)S(1)}, bf16[1,2048,128]{2,1,0:T(8,128)(2,1)}, u32[]{:S(2)}) copy-start(bf16[1,2048,128]{2,1,0:T(8,128)(2,1)} %param.33) | copy-start | bytes 1572868
  6.3 61.1 %all-to-all-start = ((bf16[32,8,256]{2,1,0:T(8,128)(2,1)}), bf16[32,8,256]{2,1,0:T(8,128)(2,1)S(1)}, u32[]{:S(2)}, u32[]{:S(2)}) async-start(bf16[32,8,256]{2,1,0:T(8,128)(2,1)} %fusion.25), calls=%async_computation | async-start | bytes 262144 | tf_op jit(solution)/shard_map/all_to_all | solution.py:38
  51.5 5.7 %copy-start.25 = (f32[128,4]{0,1:T(4,128)S(1)}, f32[128,4]{0,1:T(4,128)}, u32[]{:S(2)}) copy-start(f32[128,4]{0,1:T(4,128)} %param.30) | copy-start | bytes 6148
  51.7 37.2 %copy-start.2 = (bf16[2048,256]{1,0:T(8,128)(2,1)}, bf16[2048,256]{1,0:T(8,128)(2,1)S(1)}, u32[]{:S(2)}) copy-start(bf16[2048,256]{1,0:T(8,128)(2,1)S(1)} %pad_maximum_fusion.refs_5_) | copy-start | bytes 3145732
  51.7 25.6 %copy-start.24 = (s32[128,4]{0,1:T(4,128)S(1)}, s32[128,4]{0,1:T(4,128)}, u32[]{:S(2)}) copy-start(s32[128,4]{0,1:T(4,128)} %param.29) | copy-start | bytes 6148
  51.7 94.3 %collective-permute-start.10 = (bf16[2048,256]{1,0:T(8,128)(2,1)S(1)}, bf16[2048,256]{1,0:T(8,128)(2,1)}, u32[]{:S(2)}, u32[]{:S(2)}) collective-permute-start(bf16[2048,256]{1,0:T(8,128)(2,1)S(1)} %pad_maximum_fusion.refs_5_), channel_id=1, source_target_pairs={{0,1},{1,0},{2,3},{3,2},{4,5},{5,4},{6,7},{7,6},{8,9},{9,8},{10,11... | collective-permute-start | bytes 3145736 | tf_op jit(solution)/shard_map/ppermute | solution.py:34
  55.1 150.1 %collective-permute-start.15 = (bf16[1024,256]{1,0:T(8,128)(2,1)}, bf16[1024,256]{1,0:T(8,128)(2,1)}, u32[]{:S(2)}, u32[]{:S(2)}) collective-permute-start(bf16[1024,256]{1,0:T(8,128)(2,1)} %bitcast.32.refs_5_), channel_id=1, source_target_pairs={{0,1},{1,0},{2,3},{3,2},{4,5},{5,4},{6,7},{7,6},{8,9},{9,8},{10,11... | collective-permute-start | bytes 1572872 | tf_op jit(solution)/shard_map/ppermute | solution.py:34
  69.6 18.6 %all-to-all-start.1 = ((bf16[32,8,128]{2,1,0:T(8,128)(2,1)}), bf16[32,8,128]{2,1,0:T(8,128)(2,1)S(1)}, u32[]{:S(2)}, u32[]{:S(2)}) async-start(bf16[32,8,128]{2,1,0:T(8,128)(2,1)} %copy.181), calls=%async_computation.1 | async-start | bytes 131072 | tf_op jit(solution)/shard_map/all_to_all | solution.py:38
  88.2 0.6 copy-start.18
  88.8 8.3 %copy-start.3 = (bf16[128,2048]{1,0:T(8,128)(2,1)S(1)}, bf16[128,2048]{1,0:T(8,128)(2,1)}, u32[]{:S(2)}) copy-start(bf16[128,2048]{1,0:T(8,128)(2,1)} %get-tuple-element.39) | copy-start | bytes 1572868
  88.8 38.6 %all-to-all-start.2 = ((bf16[32,16,512]{2,1,0:T(8,128)(2,1)}), bf16[32,16,512]{2,1,0:T(8,128)(2,1)S(1)}, u32[]{:S(2)}, u32[]{:S(2)}) async-start(bf16[32,16,512]{2,1,0:T(8,128)(2,1)} %bitcast.137), calls=%async_computation.2 | async-start | bytes 1048576 | tf_op jit(solution)/shard_map/all_to_all | solution.py:38
  94.0 3.2 %copy-start.9 = (bf16[2048,128]{1,0:T(8,128)(2,1)S(1)}, bf16[2048,128]{1,0:T(8,128)(2,1)}, u32[]{:S(2)}) copy-start(bf16[2048,128]{1,0:T(8,128)(2,1)} %param.35) | copy-start | bytes 1572868
  96.0 2.1 copy-start.8
  97.1 2.3 copy-start.26
  99.5 2.2 copy-start.19
  99.5 2.2 copy-start.17
  101.7 47.6 %copy-start.27 = (f32[256]{0:T(256)S(1)}, f32[256]{0:T(256)}, u32[]{:S(2)}) copy-start(f32[256]{0:T(256)} %param.26) | copy-start | bytes 3076
  127.4 9.8 %copy-start.1 = (bf16[32,16,512]{2,1,0:T(8,128)(2,1)}, bf16[32,16,512]{2,1,0:T(8,128)(2,1)S(1)}, u32[]{:S(2)}) copy-start(bf16[32,16,512]{2,1,0:T(8,128)(2,1)S(1)} %all-to-all-done.2) | copy-start | bytes 1572868
  127.4 60.9 %collective-permute-start.6 = (bf16[512,512]{1,0:T(8,128)(2,1)S(1)}, bf16[512,512]{1,0:T(8,128)(2,1)}, u32[]{:S(2)}, u32[]{:S(2)}) collective-permute-start(bf16[512,512]{1,0:T(8,128)(2,1)S(1)} %bitcast.122), channel_id=1, source_target_pairs={{0,2},{1,3},{2,4},{3,5},{4,6},{5,7},{6,0},{7,1},{8,10},{9,11},{10,... | collective-permute-start | bytes 1572872 | tf_op jit(solution)/shard_map/ppermute | solution.py:29
  131.5 56.7 %collective-permute-start.7 = (bf16[512,512]{1,0:T(8,128)(2,1)S(1)}, bf16[512,512]{1,0:T(8,128)(2,1)}, u32[]{:S(2)}, u32[]{:S(2)}) collective-permute-start(bf16[512,512]{1,0:T(8,128)(2,1)S(1)} %bitcast.123), channel_id=1, source_target_pairs={{0,6},{1,7},{2,0},{3,1},{4,2},{5,3},{6,4},{7,5},{8,14},{9,15},{10,... | collective-permute-start | bytes 1572872 | tf_op jit(solution)/shard_map/ppermute | solution.py:29
  139.0 25.1 %collective-permute-start.8 = (bf16[256,512]{1,0:T(8,128)(2,1)}, bf16[256,512]{1,0:T(8,128)(2,1)S(1)}, u32[]{:S(2)}, u32[]{:S(2)}) collective-permute-start(bf16[256,512]{1,0:T(8,128)(2,1)} %get-tuple-element.41), channel_id=1, source_target_pairs={{0,4},{1,5},{2,6},{3,7},{4,0},{5,1},{6,2},{7,3},{8,12},{9,13},{10,... | collective-permute-start | bytes 786440 | tf_op jit(solution)/shard_map/ppermute | solution.py:29
  146.0 25.2 %collective-permute-start.9 = (bf16[256,512]{1,0:T(8,128)(2,1)}, bf16[256,512]{1,0:T(8,128)(2,1)S(1)}, u32[]{:S(2)}, u32[]{:S(2)}) collective-permute-start(bf16[256,512]{1,0:T(8,128)(2,1)} %get-tuple-element.42), channel_id=1, source_target_pairs={{0,4},{1,5},{2,6},{3,7},{4,0},{5,1},{6,2},{7,3},{8,12},{9,13},{10,... | collective-permute-start | bytes 786440 | tf_op jit(solution)/shard_map/ppermute | solution.py:29
  164.1 24.2 %copy-start.13 = (bf16[256,512]{1,0:T(8,128)(2,1)}, bf16[256,512]{1,0:T(8,128)(2,1)S(1)}, u32[]{:S(2)}) copy-start(bf16[256,512]{1,0:T(8,128)(2,1)S(1)} %collective-permute-done.8.refs_3_) | copy-start | bytes 786436
  164.1 36.2 %collective-permute-start.3 = (bf16[128,128]{0,1:T(8,128)(2,1)}, bf16[128,128]{0,1:T(8,128)(2,1)S(1)}, u32[]{:S(2)}, u32[]{:S(2)}) collective-permute-start(bf16[128,128]{0,1:T(8,128)(2,1)} %fusion.5), channel_id=1, source_target_pairs={{0,4},{1,5},{2,6},{3,7},{4,0},{5,1},{6,2},{7,3},{8,12},{9,13},{10,... | collective-permute-start | bytes 98312 | tf_op jit(solution)/shard_map/ppermute | solution.py:34
  171.2 17.0 %copy-start.15 = (bf16[256,512]{1,0:T(8,128)(2,1)}, bf16[256,512]{1,0:T(8,128)(2,1)S(1)}, u32[]{:S(2)}) copy-start(bf16[256,512]{1,0:T(8,128)(2,1)S(1)} %collective-permute-done.9.refs_4_) | copy-start | bytes 786436
  171.2 65.5 %collective-permute-start = (bf16[2,2,16,2048]{3,2,0,1:T(8,128)(2,1)}, bf16[2,2,16,2048]{3,2,0,1:T(8,128)(2,1)}, u32[]{:S(2)}, u32[]{:S(2)}) collective-permute-start(bf16[2,2,16,2048]{3,2,0,1:T(8,128)(2,1)} %fusion.10), channel_id=1, source_target_pairs={{0,1},{1,0},{2,3},{3,2},{4,5},{5,4},{6,7},{7,6},{8,9},{9,8},{10,11... | collective-permute-start | bytes 786440 | tf_op jit(solution)/shard_map/ppermute | solution.py:34
  192.8 26.0 %collective-permute-start.11 = (bf16[512,256]{1,0:T(8,128)(2,1)}, bf16[512,256]{1,0:T(8,128)(2,1)S(1)}, u32[]{:S(2)}, u32[]{:S(2)}) collective-permute-start(bf16[512,256]{1,0:T(8,128)(2,1)} %get-tuple-element.43.refs_0_), channel_id=1, source_target_pairs={{0,2},{1,3},{2,4},{3,5},{4,6},{5,7},{6,0},{7,1},{8,10},{9,11},{10,... | collective-permute-start | bytes 786440 | tf_op jit(solution)/shard_map/ppermute | solution.py:29
  194.7 24.0 %collective-permute-start.12 = (bf16[512,256]{1,0:T(8,128)(2,1)}, bf16[512,256]{1,0:T(8,128)(2,1)S(1)}, u32[]{:S(2)}, u32[]{:S(2)}) collective-permute-start(bf16[512,256]{1,0:T(8,128)(2,1)} %get-tuple-element.43.refs_0_), channel_id=1, source_target_pairs={{0,6},{1,7},{2,0},{3,1},{4,2},{5,3},{6,4},{7,5},{8,14},{9,15},{10,... | collective-permute-start | bytes 786440 | tf_op jit(solution)/shard_map/ppermute | solution.py:29
  200.2 0.6 copy-start.23
  200.8 13.0 %collective-permute-start.13 = (bf16[256,256]{1,0:T(8,128)(2,1)}, bf16[256,256]{1,0:T(8,128)(2,1)S(1)}, u32[]{:S(2)}, u32[]{:S(2)}) collective-permute-start(bf16[256,256]{1,0:T(8,128)(2,1)} %get-tuple-element.44), channel_id=1, source_target_pairs={{0,4},{1,5},{2,6},{3,7},{4,0},{5,1},{6,2},{7,3},{8,12},{9,13},{10,... | collective-permute-start | bytes 393224 | tf_op jit(solution)/shard_map/ppermute | solution.py:29
  205.2 13.5 %collective-permute-start.14 = (bf16[256,256]{1,0:T(8,128)(2,1)}, bf16[256,256]{1,0:T(8,128)(2,1)S(1)}, u32[]{:S(2)}, u32[]{:S(2)}) collective-permute-start(bf16[256,256]{1,0:T(8,128)(2,1)} %get-tuple-element.45), channel_id=1, source_target_pairs={{0,4},{1,5},{2,6},{3,7},{4,0},{5,1},{6,2},{7,3},{8,12},{9,13},{10,... | collective-permute-start | bytes 393224 | tf_op jit(solution)/shard_map/ppermute | solution.py:29
  213.8 4.9 %copy-start.20 = (bf16[256,256]{1,0:T(8,128)(2,1)}, bf16[256,256]{1,0:T(8,128)(2,1)S(1)}, u32[]{:S(2)}) copy-start(bf16[256,256]{1,0:T(8,128)(2,1)S(1)} %collective-permute-done.13.refs_3_) | copy-start | bytes 393220
  213.8 28.7 %collective-permute-start.4 = (bf16[128,256]{0,1:T(8,128)(2,1)S(1)}, bf16[128,256]{0,1:T(8,128)(2,1)}, u32[]{:S(2)}, u32[]{:S(2)}) collective-permute-start(bf16[128,256]{0,1:T(8,128)(2,1)S(1)} %pad_maximum_fusion.2), channel_id=1, source_target_pairs={{0,2},{1,3},{2,0},{3,1},{4,6},{5,7},{6,4},{7,5},{8,10},{9,11},{10,... | collective-permute-start | bytes 196616 | tf_op jit(solution)/shard_map/ppermute | solution.py:34
  218.7 0.7 copy-start.21
  218.7 0.8 copy-start.12
  219.5 0.7 copy-start.14
  223.4 46.1 %all-to-all-start.3 = ((bf16[64,16,256]{2,1,0:T(8,128)(2,1)}), bf16[64,16,256]{2,1,0:T(8,128)(2,1)S(1)}, u32[]{:S(2)}, u32[]{:S(2)}) async-start(bf16[64,16,256]{2,1,0:T(8,128)(2,1)} %bitcast.128), calls=%async_computation.3 | async-start | bytes 1048576 | tf_op jit(solution)/shard_map/all_to_all | solution.py:38
  237.8 31.7 %copy-start.5 = (bf16[128,32,32]{0,2,1:T(8,128)(2,1)S(1)}, bf16[128,32,32]{0,2,1:T(8,128)(2,1)}, u32[]{:S(2)}) copy-start(bf16[128,32,32]{0,2,1:T(8,128)(2,1)} %get-tuple-element.127) | copy-start | bytes 786436
  237.8 8.9 %collective-permute-start.1 = (bf16[2,16,2048]{2,1,0:T(8,128)(2,1)S(1)}, bf16[2,16,2048]{2,1,0:T(8,128)(2,1)S(1)}, u32[]{:S(2)}, u32[]{:S(2)}) collective-permute-start(bf16[2,16,2048]{2,1,0:T(8,128)(2,1)S(1)} %fusion.26), channel_id=1, source_target_pairs={{0,2},{1,3},{2,0},{3,1},{4,6},{5,7},{6,4},{7,5},{8,10},{9,11},{10,... | collective-permute-start | bytes 393224 | tf_op jit(solution)/shard_map/ppermute | solution.py:34
  243.4 8.8 %collective-permute-start.5 = (bf16[128,512]{0,1:T(8,128)(2,1)S(1)}, bf16[128,512]{0,1:T(8,128)(2,1)S(1)}, u32[]{:S(2)}, u32[]{:S(2)}) collective-permute-start(bf16[128,512]{0,1:T(8,128)(2,1)S(1)} %pad_maximum_fusion.1), channel_id=1, source_target_pairs={{0,1},{1,0},{2,3},{3,2},{4,5},{5,4},{6,7},{7,6},{8,9},{9,8},{10,11... | collective-permute-start | bytes 393224 | tf_op jit(solution)/shard_map/ppermute | solution.py:34
  246.8 23.0 %copy-start.4 = (bf16[128,32,32]{0,2,1:T(8,128)(2,1)S(1)}, bf16[128,32,32]{0,2,1:T(8,128)(2,1)}, u32[]{:S(2)}) copy-start(bf16[128,32,32]{0,2,1:T(8,128)(2,1)} %get-tuple-element.126) | copy-start | bytes 786436
  246.8 9.5 %collective-permute-start.2 = (bf16[16,2048]{1,0:T(8,128)(2,1)S(1)}, bf16[16,2048]{1,0:T(8,128)(2,1)S(1)}, u32[]{:S(2)}, u32[]{:S(2)}) collective-permute-start(bf16[16,2048]{1,0:T(8,128)(2,1)S(1)} %fusion.43), channel_id=1, source_target_pairs={{0,4},{1,5},{2,6},{3,7},{4,0},{5,1},{6,2},{7,3},{8,12},{9,13},{10,... | collective-permute-start | bytes 196616 | tf_op jit(solution)/shard_map/ppermute | solution.py:34
  269.8 1.0 copy-start.6

commit v10 on v9

--- a/solution.py
+++ b/solution.py
@@ -428,8 +428,9 @@
     returned = exchanged(answers.reshape(2 * devices, half, width_out), EP_PAIR)
     returned = returned.reshape(experts * capacity, width_out)
     filled = places[:, :, None] == jnp.arange(capacity)[None, None, :]
-    mixing = jnp.where(filled, gate_of[:, :, None], 0.0).reshape(tokens, experts * capacity)
-    for part in in_parts(mixing, 3):
+    mixing = jnp.where(filled, gate_of[:, :, None], 0.0)
+    mixing_parts = in_parts(mixing.reshape(tokens, experts * capacity), 3)
+    for part in mixing_parts:
         shared = shared + jnp.dot(part, returned, preferred_element_type=jnp.float32)
     return shared.astype(jnp.bfloat16)
 

time: 273 us -> 273 us (level)
  no operation moved by 1% of the time
where the time goes in v10:
time: 273 us; the launch traced here: 272 us
  starting transfers between devices  145 us (53%)
  waiting for transfers between devices  81.6 us (30%)
  Pallas kernels  11.9 us (4%)
  matrix products  11.1 us (4%)
  local copies, waits for them, and re-layouts  10.4 us (4%)
  other arithmetic  9.6 us (4%)
    all_to_all x4, starting transfers between devices, exchanged(): return lax.all_to_all(array, axis, split_axis=0, concat_axis=0, tiled=True)  68.9 us
    all_to_all x4, waiting for transfers between devices, exchanged(): return lax.all_to_all(array, axis, split_axis=0, concat_axis=0, tiled=True)  56.6 us
    ppermute x8, starting transfers between devices, swapped(): return lax.ppermute(array, axis, [(i, i ^ bit) for i in range(count)])  42.7 us
    ppermute x8, starting transfers between devices, shifted(): lax.ppermute(array, axis, [(i, (i + step) % count) for i in range(count)])  33.9 us
    ppermute x8, waiting for transfers between devices, shifted(): lax.ppermute(array, axis, [(i, (i + step) % count) for i in range(count)])  20.6 us
    pallas_call x2, Pallas kernels, fetching(): pl.pallas_call(body, out_shape=shapes, in_specs=[ANY] * count, out_specs=...  7.63 us
  transfers between devices with their start and end apart: 20, of which 10 were waited for; matrix products, arithmetic and copies ran while one was open for 8% of the time, Pallas kernels for 4%

profile of v10, /device:TPU:65, one launch (start us, length us, event | category | flops | bytes accessed | tf_op | source)
XLA Modules:
  0.0 271.6 jit_solution(4455726228116132649)
XLA Ops:
  1.7 0.9 divide_multiply_fusion
  6.3 45.2 %all-to-all-start = ((bf16[32,8,256]{2,1,0:T(8,128)(2,1)}), bf16[32,8,256]{2,1,0:T(8,128)(2,1)S(1)}, u32[]{:S(2)}, u32[]{:S(2)}) async-start(bf16[32,8,256]{2,1,0:T(8,128)(2,1)} %fusion.25), calls=%async_computation | async-start | bytes 262144 | tf_op jit(solution)/shard_map/all_to_all | solution.py:38
  51.7 3.4 %collective-permute-start.10 = (bf16[2048,256]{1,0:T(8,128)(2,1)S(1)}, bf16[2048,256]{1,0:T(8,128)(2,1)}, u32[]{:S(2)}, u32[]{:S(2)}) collective-permute-start(bf16[2048,256]{1,0:T(8,128)(2,1)S(1)} %pad_maximum_fusion.refs_5_), channel_id=1, source_target_pairs={{0,1},{1,0},{2,3},{3,2},{4,5},{5,4},{6,7},{7,6},{8,9},{9,8},{10,11... | collective-permute-start | bytes 3145736 | tf_op jit(solution)/shard_map/ppermute | solution.py:34
  55.1 2.1 collective-permute-start.15
  57.2 0.9 convert_multiply_fusion.1
  58.1 9.3 %all-to-all-done = bf16[32,8,256]{2,1,0:T(8,128)(2,1)S(1)} async-done(((bf16[32,8,256]{2,1,0:T(8,128)(2,1)}), bf16[32,8,256]{2,1,0:T(8,128)(2,1)S(1)}, u32[]{:S(2)}, u32[]{:S(2)}) %all-to-all-start) | async-done | bytes 131104 | tf_op jit(solution)/shard_map/all_to_all | solution.py:38
  67.5 1.2 fusion.2
  69.6 5.2 %all-to-all-start.1 = ((bf16[32,8,128]{2,1,0:T(8,128)(2,1)}), bf16[32,8,128]{2,1,0:T(8,128)(2,1)S(1)}, u32[]{:S(2)}, u32[]{:S(2)}) async-start(bf16[32,8,128]{2,1,0:T(8,128)(2,1)} %copy.181), calls=%async_computation.1 | async-start | bytes 131072 | tf_op jit(solution)/shard_map/all_to_all | solution.py:38
  74.9 2.4 shard_map.185
  77.9 10.3 %all-to-all-done.1 = bf16[32,8,128]{2,1,0:T(8,128)(2,1)S(1)} async-done(((bf16[32,8,128]{2,1,0:T(8,128)(2,1)}), bf16[32,8,128]{2,1,0:T(8,128)(2,1)S(1)}, u32[]{:S(2)}, u32[]{:S(2)}) %all-to-all-start.1) | async-done | bytes 65568 | tf_op jit(solution)/shard_map/all_to_all | solution.py:38
  88.8 5.1 %all-to-all-start.2 = ((bf16[32,16,512]{2,1,0:T(8,128)(2,1)}), bf16[32,16,512]{2,1,0:T(8,128)(2,1)S(1)}, u32[]{:S(2)}, u32[]{:S(2)}) async-start(bf16[32,16,512]{2,1,0:T(8,128)(2,1)} %bitcast.137), calls=%async_computation.2 | async-start | bytes 1048576 | tf_op jit(solution)/shard_map/all_to_all | solution.py:38
  94.0 0.9 fusion.6
  94.9 1.1 convolution_select_fusion
  96.0 1.1 fusion.8
  97.1 1.0 fusion.59
  98.3 1.1 copy.187
  99.5 2.2 fusion.5
  101.7 1.1 multiply_reduce_fusion
  102.8 24.6 %all-to-all-done.2 = bf16[32,16,512]{2,1,0:T(8,128)(2,1)S(1)} async-done(((bf16[32,16,512]{2,1,0:T(8,128)(2,1)}), bf16[32,16,512]{2,1,0:T(8,128)(2,1)S(1)}, u32[]{:S(2)}, u32[]{:S(2)}) %all-to-all-start.2) | async-done | bytes 524320 | tf_op jit(solution)/shard_map/all_to_all | solution.py:38
  127.4 4.1 %collective-permute-start.6 = (bf16[512,512]{1,0:T(8,128)(2,1)S(1)}, bf16[512,512]{1,0:T(8,128)(2,1)}, u32[]{:S(2)}, u32[]{:S(2)}) collective-permute-start(bf16[512,512]{1,0:T(8,128)(2,1)S(1)} %bitcast.122), channel_id=1, source_target_pairs={{0,2},{1,3},{2,4},{3,5},{4,6},{5,7},{6,0},{7,1},{8,10},{9,11},{10,... | collective-permute-start | bytes 1572872 | tf_op jit(solution)/shard_map/ppermute | solution.py:29
  131.5 3.8 %collective-permute-start.7 = (bf16[512,512]{1,0:T(8,128)(2,1)S(1)}, bf16[512,512]{1,0:T(8,128)(2,1)}, u32[]{:S(2)}, u32[]{:S(2)}) collective-permute-start(bf16[512,512]{1,0:T(8,128)(2,1)S(1)} %bitcast.123), channel_id=1, source_target_pairs={{0,6},{1,7},{2,0},{3,1},{4,2},{5,3},{6,4},{7,5},{8,14},{9,15},{10,... | collective-permute-start | bytes 1572872 | tf_op jit(solution)/shard_map/ppermute | solution.py:29
  136.1 1.0 copy.183
  137.1 1.9 shard_map.186
  139.0 7.0 %collective-permute-start.8 = (bf16[256,512]{1,0:T(8,128)(2,1)}, bf16[256,512]{1,0:T(8,128)(2,1)S(1)}, u32[]{:S(2)}, u32[]{:S(2)}) collective-permute-start(bf16[256,512]{1,0:T(8,128)(2,1)} %get-tuple-element.41), channel_id=1, source_target_pairs={{0,4},{1,5},{2,6},{3,7},{4,0},{5,1},{6,2},{7,3},{8,12},{9,13},{10,... | collective-permute-start | bytes 786440 | tf_op jit(solution)/shard_map/ppermute | solution.py:29
  146.0 2.3 collective-permute-start.9
  148.3 1.0 mul.111
  149.3 1.2 fusion.41
  150.5 13.5 %collective-permute-done.8.refs_3_ = bf16[256,512]{1,0:T(8,128)(2,1)S(1)} collective-permute-done((bf16[256,512]{1,0:T(8,128)(2,1)}, bf16[256,512]{1,0:T(8,128)(2,1)S(1)}, u32[]{:S(2)}, u32[]{:S(2)}) %collective-permute-start.8) | collective-permute-done | bytes 262176 | tf_op jit(solution)/shard_map/ppermute | solution.py:29
  164.1 4.9 %collective-permute-start.3 = (bf16[128,128]{0,1:T(8,128)(2,1)}, bf16[128,128]{0,1:T(8,128)(2,1)S(1)}, u32[]{:S(2)}, u32[]{:S(2)}) collective-permute-start(bf16[128,128]{0,1:T(8,128)(2,1)} %fusion.5), channel_id=1, source_target_pairs={{0,4},{1,5},{2,6},{3,7},{4,0},{5,1},{6,2},{7,3},{8,12},{9,13},{10,... | collective-permute-start | bytes 98312 | tf_op jit(solution)/shard_map/ppermute | solution.py:34
  169.7 1.5 collective-permute-done.9.refs_4_
  171.2 17.0 %collective-permute-start = (bf16[2,2,16,2048]{3,2,0,1:T(8,128)(2,1)}, bf16[2,2,16,2048]{3,2,0,1:T(8,128)(2,1)}, u32[]{:S(2)}, u32[]{:S(2)}) collective-permute-start(bf16[2,2,16,2048]{3,2,0,1:T(8,128)(2,1)} %fusion.10), channel_id=1, source_target_pairs={{0,1},{1,0},{2,3},{3,2},{4,5},{5,4},{6,7},{7,6},{8,9},{9,8},{10,11... | collective-permute-start | bytes 786440 | tf_op jit(solution)/shard_map/ppermute | solution.py:34
  188.3 4.4 %shard_map.187 = (bf16[512,256]{1,0:T(8,128)(2,1)}, bf16[256,256]{1,0:T(8,128)(2,1)}, bf16[256,256]{1,0:T(8,128)(2,1)}) custom-call(bf16[512,512]{1,0:T(8,128)(2,1)} %bitcast.125, bf16[512,512]{1,0:T(8,128)(2,1)} %collective-permute-done.6.refs_1_, bf16[512,512]{1,0:T(8,128)(2,1)} %collective-permute-done.7.refs_2_, bf16[256,512]{1,0:T(8,128)(2,1)} %copy-done.13, ...), custom_call_target="tpu_custom_call" | custom-call | tf_op jit(solution)/shard_map/pallas_call | solution.py:222
  192.8 2.0 collective-permute-start.11
  194.7 5.5 %collective-permute-start.12 = (bf16[512,256]{1,0:T(8,128)(2,1)}, bf16[512,256]{1,0:T(8,128)(2,1)S(1)}, u32[]{:S(2)}, u32[]{:S(2)}) collective-permute-start(bf16[512,256]{1,0:T(8,128)(2,1)} %get-tuple-element.43.refs_0_), channel_id=1, source_target_pairs={{0,6},{1,7},{2,0},{3,1},{4,2},{5,3},{6,4},{7,5},{8,14},{9,15},{10,... | collective-permute-start | bytes 786440 | tf_op jit(solution)/shard_map/ppermute | solution.py:29
  200.8 4.4 %collective-permute-start.13 = (bf16[256,256]{1,0:T(8,128)(2,1)}, bf16[256,256]{1,0:T(8,128)(2,1)S(1)}, u32[]{:S(2)}, u32[]{:S(2)}) collective-permute-start(bf16[256,256]{1,0:T(8,128)(2,1)} %get-tuple-element.44), channel_id=1, source_target_pairs={{0,4},{1,5},{2,6},{3,7},{4,0},{5,1},{6,2},{7,3},{8,12},{9,13},{10,... | collective-permute-start | bytes 393224 | tf_op jit(solution)/shard_map/ppermute | solution.py:29
  205.2 4.9 %collective-permute-start.14 = (bf16[256,256]{1,0:T(8,128)(2,1)}, bf16[256,256]{1,0:T(8,128)(2,1)S(1)}, u32[]{:S(2)}, u32[]{:S(2)}) collective-permute-start(bf16[256,256]{1,0:T(8,128)(2,1)} %get-tuple-element.45), channel_id=1, source_target_pairs={{0,4},{1,5},{2,6},{3,7},{4,0},{5,1},{6,2},{7,3},{8,12},{9,13},{10,... | collective-permute-start | bytes 393224 | tf_op jit(solution)/shard_map/ppermute | solution.py:29
  210.9 2.9 %collective-permute-done.13.refs_3_ = bf16[256,256]{1,0:T(8,128)(2,1)S(1)} collective-permute-done((bf16[256,256]{1,0:T(8,128)(2,1)}, bf16[256,256]{1,0:T(8,128)(2,1)S(1)}, u32[]{:S(2)}, u32[]{:S(2)}) %collective-permute-start.13) | collective-permute-done | bytes 131104 | tf_op jit(solution)/shard_map/ppermute | solution.py:29
  213.8 2.3 collective-permute-start.4
  216.1 2.6 collective-permute-done.14.refs_4_
  220.2 3.2 %shard_map.188 = bf16[32,2,16,256]{3,2,1,0:T(8,128)(2,1)} custom-call(bf16[512,256]{1,0:T(8,128)(2,1)} %get-tuple-element.43.refs_0_, bf16[512,256]{1,0:T(8,128)(2,1)} %copy-done.12, bf16[512,256]{1,0:T(8,128)(2,1)} %copy-done.14, bf16[256,256]{1,0:T(8,128)(2,1)} %copy-done.20, bf16[256,256]{1,0:T(8,128)(2,1)} %copy-done.21, ...), custom_call_target="tpu_custom_call" | custom-call | tf_op jit(solution)/shard_map/pallas_call | solution.py:222
  223.4 13.4 %all-to-all-start.3 = ((bf16[64,16,256]{2,1,0:T(8,128)(2,1)}), bf16[64,16,256]{2,1,0:T(8,128)(2,1)S(1)}, u32[]{:S(2)}, u32[]{:S(2)}) async-start(bf16[64,16,256]{2,1,0:T(8,128)(2,1)} %bitcast.128), calls=%async_computation.3 | async-start | bytes 1048576 | tf_op jit(solution)/shard_map/all_to_all | solution.py:38
  236.8 1.0 bitcast_add_fusion.1
  237.8 4.7 %collective-permute-start.1 = (bf16[2,16,2048]{2,1,0:T(8,128)(2,1)S(1)}, bf16[2,16,2048]{2,1,0:T(8,128)(2,1)S(1)}, u32[]{:S(2)}, u32[]{:S(2)}) collective-permute-start(bf16[2,16,2048]{2,1,0:T(8,128)(2,1)S(1)} %fusion.26), channel_id=1, source_target_pairs={{0,2},{1,3},{2,0},{3,1},{4,6},{5,7},{6,4},{7,5},{8,10},{9,11},{10,... | collective-permute-start | bytes 393224 | tf_op jit(solution)/shard_map/ppermute | solution.py:34
  243.4 3.3 %collective-permute-start.5 = (bf16[128,512]{0,1:T(8,128)(2,1)S(1)}, bf16[128,512]{0,1:T(8,128)(2,1)S(1)}, u32[]{:S(2)}, u32[]{:S(2)}) collective-permute-start(bf16[128,512]{0,1:T(8,128)(2,1)S(1)} %pad_maximum_fusion.1), channel_id=1, source_target_pairs={{0,1},{1,0},{2,3},{3,2},{4,5},{5,4},{6,7},{7,6},{8,9},{9,8},{10,11... | collective-permute-start | bytes 393224 | tf_op jit(solution)/shard_map/ppermute | solution.py:34
  246.8 5.0 %collective-permute-start.2 = (bf16[16,2048]{1,0:T(8,128)(2,1)S(1)}, bf16[16,2048]{1,0:T(8,128)(2,1)S(1)}, u32[]{:S(2)}, u32[]{:S(2)}) collective-permute-start(bf16[16,2048]{1,0:T(8,128)(2,1)S(1)} %fusion.43), channel_id=1, source_target_pairs={{0,4},{1,5},{2,6},{3,7},{4,0},{5,1},{6,2},{7,3},{8,12},{9,13},{10,... | collective-permute-start | bytes 196616 | tf_op jit(solution)/shard_map/ppermute | solution.py:34
  252.4 4.0 %collective-permute-done.2 = bf16[16,2048]{1,0:T(8,128)(2,1)S(1)} collective-permute-done((bf16[16,2048]{1,0:T(8,128)(2,1)S(1)}, bf16[16,2048]{1,0:T(8,128)(2,1)S(1)}, u32[]{:S(2)}, u32[]{:S(2)}) %collective-permute-start.2) | collective-permute-done | bytes 65568 | tf_op jit(solution)/shard_map/ppermute | solution.py:34
  257.0 12.5 %all-to-all-done.3 = bf16[64,16,256]{2,1,0:T(8,128)(2,1)S(1)} async-done(((bf16[64,16,256]{2,1,0:T(8,128)(2,1)}), bf16[64,16,256]{2,1,0:T(8,128)(2,1)S(1)}, u32[]{:S(2)}, u32[]{:S(2)}) %all-to-all-start.3) | async-done | bytes 524320 | tf_op jit(solution)/shard_map/all_to_all | solution.py:38
  270.7 0.9 fusion.3
  (124 shorter events, 15.3 us)
Async XLA Ops:
  0.6 148.7 %copy-start = (bf16[256,2048]{1,0:T(8,128)(2,1)S(1)}, bf16[256,2048]{1,0:T(8,128)(2,1)}, u32[]{:S(2)}) copy-start(bf16[256,2048]{1,0:T(8,128)(2,1)} %param.27) | copy-start | bytes 3145732
  0.6 3.6 %copy-start.22 = (bf16[128,256]{1,0:T(8,128)(2,1)S(1)}, bf16[128,256]{1,0:T(8,128)(2,1)}, u32[]{:S(2)}) copy-start(bf16[128,256]{1,0:T(8,128)(2,1)} %param.22) | copy-start | bytes 196612
  4.3 0.6 copy-start.7
  4.7 46.8 %copy-start.11 = (bf16[1,2048,128]{2,1,0:T(8,128)(2,1)S(1)}, bf16[1,2048,128]{2,1,0:T(8,128)(2,1)}, u32[]{:S(2)}) copy-start(bf16[1,2048,128]{2,1,0:T(8,128)(2,1)} %param.32) | copy-start | bytes 1572868
  5.2 46.2 %copy-start.16 = (f32[2,2,128,128]{3,2,1,0:T(8,128)}, f32[2,2,128,128]{3,2,1,0:T(8,128)S(1)}, u32[]{:S(2)}) copy-start(f32[2,2,128,128]{3,2,1,0:T(8,128)S(1)} %get-tuple-element.37) | copy-start | bytes 786436
  5.3 46.3 %copy-start.10 = (bf16[1,2048,128]{2,1,0:T(8,128)(2,1)S(1)}, bf16[1,2048,128]{2,1,0:T(8,128)(2,1)}, u32[]{:S(2)}) copy-start(bf16[1,2048,128]{2,1,0:T(8,128)(2,1)} %param.33) | copy-start | bytes 1572868
  6.3 61.1 %all-to-all-start = ((bf16[32,8,256]{2,1,0:T(8,128)(2,1)}), bf16[32,8,256]{2,1,0:T(8,128)(2,1)S(1)}, u32[]{:S(2)}, u32[]{:S(2)}) async-start(bf16[32,8,256]{2,1,0:T(8,128)(2,1)} %fusion.25), calls=%async_computation | async-start | bytes 262144 | tf_op jit(solution)/shard_map/all_to_all | solution.py:38
  51.5 5.7 %copy-start.25 = (f32[128,4]{0,1:T(4,128)S(1)}, f32[128,4]{0,1:T(4,128)}, u32[]{:S(2)}) copy-start(f32[128,4]{0,1:T(4,128)} %param.30) | copy-start | bytes 6148
  51.7 37.2 %copy-start.2 = (bf16[2048,256]{1,0:T(8,128)(2,1)}, bf16[2048,256]{1,0:T(8,128)(2,1)S(1)}, u32[]{:S(2)}) copy-start(bf16[2048,256]{1,0:T(8,128)(2,1)S(1)} %pad_maximum_fusion.refs_5_) | copy-start | bytes 3145732
  51.7 25.6 %copy-start.24 = (s32[128,4]{0,1:T(4,128)S(1)}, s32[128,4]{0,1:T(4,128)}, u32[]{:S(2)}) copy-start(s32[128,4]{0,1:T(4,128)} %param.29) | copy-start | bytes 6148
  51.7 94.3 %collective-permute-start.10 = (bf16[2048,256]{1,0:T(8,128)(2,1)S(1)}, bf16[2048,256]{1,0:T(8,128)(2,1)}, u32[]{:S(2)}, u32[]{:S(2)}) collective-permute-start(bf16[2048,256]{1,0:T(8,128)(2,1)S(1)} %pad_maximum_fusion.refs_5_), channel_id=1, source_target_pairs={{0,1},{1,0},{2,3},{3,2},{4,5},{5,4},{6,7},{7,6},{8,9},{9,8},{10,11... | collective-permute-start | bytes 3145736 | tf_op jit(solution)/shard_map/ppermute | solution.py:34
  55.1 150.1 %collective-permute-start.15 = (bf16[1024,256]{1,0:T(8,128)(2,1)}, bf16[1024,256]{1,0:T(8,128)(2,1)}, u32[]{:S(2)}, u32[]{:S(2)}) collective-permute-start(bf16[1024,256]{1,0:T(8,128)(2,1)} %bitcast.32.refs_5_), channel_id=1, source_target_pairs={{0,1},{1,0},{2,3},{3,2},{4,5},{5,4},{6,7},{7,6},{8,9},{9,8},{10,11... | collective-permute-start | bytes 1572872 | tf_op jit(solution)/shard_map/ppermute | solution.py:34
  69.6 18.6 %all-to-all-start.1 = ((bf16[32,8,128]{2,1,0:T(8,128)(2,1)}), bf16[32,8,128]{2,1,0:T(8,128)(2,1)S(1)}, u32[]{:S(2)}, u32[]{:S(2)}) async-start(bf16[32,8,128]{2,1,0:T(8,128)(2,1)} %copy.181), calls=%async_computation.1 | async-start | bytes 131072 | tf_op jit(solution)/shard_map/all_to_all | solution.py:38
  88.2 0.6 copy-start.18
  88.8 8.3 %copy-start.3 = (bf16[128,2048]{1,0:T(8,128)(2,1)S(1)}, bf16[128,2048]{1,0:T(8,128)(2,1)}, u32[]{:S(2)}) copy-start(bf16[128,2048]{1,0:T(8,128)(2,1)} %get-tuple-element.39) | copy-start | bytes 1572868
  88.8 38.6 %all-to-all-start.2 = ((bf16[32,16,512]{2,1,0:T(8,128)(2,1)}), bf16[32,16,512]{2,1,0:T(8,128)(2,1)S(1)}, u32[]{:S(2)}, u32[]{:S(2)}) async-start(bf16[32,16,512]{2,1,0:T(8,128)(2,1)} %bitcast.137), calls=%async_computation.2 | async-start | bytes 1048576 | tf_op jit(solution)/shard_map/all_to_all | solution.py:38
  94.0 3.2 %copy-start.9 = (bf16[2048,128]{1,0:T(8,128)(2,1)S(1)}, bf16[2048,128]{1,0:T(8,128)(2,1)}, u32[]{:S(2)}) copy-start(bf16[2048,128]{1,0:T(8,128)(2,1)} %param.35) | copy-start | bytes 1572868
  96.0 2.1 copy-start.8
  97.1 2.3 copy-start.26
  99.5 2.2 copy-start.19
  99.5 2.2 copy-start.17
  101.7 47.6 %copy-start.27 = (f32[256]{0:T(256)S(1)}, f32[256]{0:T(256)}, u32[]{:S(2)}) copy-start(f32[256]{0:T(256)} %param.26) | copy-start | bytes 3076
  127.4 9.8 %copy-start.1 = (bf16[32,16,512]{2,1,0:T(8,128)(2,1)}, bf16[32,16,512]{2,1,0:T(8,128)(2,1)S(1)}, u32[]{:S(2)}) copy-start(bf16[32,16,512]{2,1,0:T(8,128)(2,1)S(1)} %all-to-all-done.2) | copy-start | bytes 1572868
  127.4 60.9 %collective-permute-start.6 = (bf16[512,512]{1,0:T(8,128)(2,1)S(1)}, bf16[512,512]{1,0:T(8,128)(2,1)}, u32[]{:S(2)}, u32[]{:S(2)}) collective-permute-start(bf16[512,512]{1,0:T(8,128)(2,1)S(1)} %bitcast.122), channel_id=1, source_target_pairs={{0,2},{1,3},{2,4},{3,5},{4,6},{5,7},{6,0},{7,1},{8,10},{9,11},{10,... | collective-permute-start | bytes 1572872 | tf_op jit(solution)/shard_map/ppermute | solution.py:29
  131.5 56.7 %collective-permute-start.7 = (bf16[512,512]{1,0:T(8,128)(2,1)S(1)}, bf16[512,512]{1,0:T(8,128)(2,1)}, u32[]{:S(2)}, u32[]{:S(2)}) collective-permute-start(bf16[512,512]{1,0:T(8,128)(2,1)S(1)} %bitcast.123), channel_id=1, source_target_pairs={{0,6},{1,7},{2,0},{3,1},{4,2},{5,3},{6,4},{7,5},{8,14},{9,15},{10,... | collective-permute-start | bytes 1572872 | tf_op jit(solution)/shard_map/ppermute | solution.py:29
  139.0 25.1 %collective-permute-start.8 = (bf16[256,512]{1,0:T(8,128)(2,1)}, bf16[256,512]{1,0:T(8,128)(2,1)S(1)}, u32[]{:S(2)}, u32[]{:S(2)}) collective-permute-start(bf16[256,512]{1,0:T(8,128)(2,1)} %get-tuple-element.41), channel_id=1, source_target_pairs={{0,4},{1,5},{2,6},{3,7},{4,0},{5,1},{6,2},{7,3},{8,12},{9,13},{10,... | collective-permute-start | bytes 786440 | tf_op jit(solution)/shard_map/ppermute | solution.py:29
  146.0 25.2 %collective-permute-start.9 = (bf16[256,512]{1,0:T(8,128)(2,1)}, bf16[256,512]{1,0:T(8,128)(2,1)S(1)}, u32[]{:S(2)}, u32[]{:S(2)}) collective-permute-start(bf16[256,512]{1,0:T(8,128)(2,1)} %get-tuple-element.42), channel_id=1, source_target_pairs={{0,4},{1,5},{2,6},{3,7},{4,0},{5,1},{6,2},{7,3},{8,12},{9,13},{10,... | collective-permute-start | bytes 786440 | tf_op jit(solution)/shard_map/ppermute | solution.py:29
  164.1 24.2 %copy-start.13 = (bf16[256,512]{1,0:T(8,128)(2,1)}, bf16[256,512]{1,0:T(8,128)(2,1)S(1)}, u32[]{:S(2)}) copy-start(bf16[256,512]{1,0:T(8,128)(2,1)S(1)} %collective-permute-done.8.refs_3_) | copy-start | bytes 786436
  164.1 36.2 %collective-permute-start.3 = (bf16[128,128]{0,1:T(8,128)(2,1)}, bf16[128,128]{0,1:T(8,128)(2,1)S(1)}, u32[]{:S(2)}, u32[]{:S(2)}) collective-permute-start(bf16[128,128]{0,1:T(8,128)(2,1)} %fusion.5), channel_id=1, source_target_pairs={{0,4},{1,5},{2,6},{3,7},{4,0},{5,1},{6,2},{7,3},{8,12},{9,13},{10,... | collective-permute-start | bytes 98312 | tf_op jit(solution)/shard_map/ppermute | solution.py:34
  171.2 17.0 %copy-start.15 = (bf16[256,512]{1,0:T(8,128)(2,1)}, bf16[256,512]{1,0:T(8,128)(2,1)S(1)}, u32[]{:S(2)}) copy-start(bf16[256,512]{1,0:T(8,128)(2,1)S(1)} %collective-permute-done.9.refs_4_) | copy-start | bytes 786436
  171.2 65.5 %collective-permute-start = (bf16[2,2,16,2048]{3,2,0,1:T(8,128)(2,1)}, bf16[2,2,16,2048]{3,2,0,1:T(8,128)(2,1)}, u32[]{:S(2)}, u32[]{:S(2)}) collective-permute-start(bf16[2,2,16,2048]{3,2,0,1:T(8,128)(2,1)} %fusion.10), channel_id=1, source_target_pairs={{0,1},{1,0},{2,3},{3,2},{4,5},{5,4},{6,7},{7,6},{8,9},{9,8},{10,11... | collective-permute-start | bytes 786440 | tf_op jit(solution)/shard_map/ppermute | solution.py:34
  192.8 26.0 %collective-permute-start.11 = (bf16[512,256]{1,0:T(8,128)(2,1)}, bf16[512,256]{1,0:T(8,128)(2,1)S(1)}, u32[]{:S(2)}, u32[]{:S(2)}) collective-permute-start(bf16[512,256]{1,0:T(8,128)(2,1)} %get-tuple-element.43.refs_0_), channel_id=1, source_target_pairs={{0,2},{1,3},{2,4},{3,5},{4,6},{5,7},{6,0},{7,1},{8,10},{9,11},{10,... | collective-permute-start | bytes 786440 | tf_op jit(solution)/shard_map/ppermute | solution.py:29
  194.7 24.0 %collective-permute-start.12 = (bf16[512,256]{1,0:T(8,128)(2,1)}, bf16[512,256]{1,0:T(8,128)(2,1)S(1)}, u32[]{:S(2)}, u32[]{:S(2)}) collective-permute-start(bf16[512,256]{1,0:T(8,128)(2,1)} %get-tuple-element.43.refs_0_), channel_id=1, source_target_pairs={{0,6},{1,7},{2,0},{3,1},{4,2},{5,3},{6,4},{7,5},{8,14},{9,15},{10,... | collective-permute-start | bytes 786440 | tf_op jit(solution)/shard_map/ppermute | solution.py:29
  200.2 0.6 copy-start.23
  200.8 13.0 %collective-permute-start.13 = (bf16[256,256]{1,0:T(8,128)(2,1)}, bf16[256,256]{1,0:T(8,128)(2,1)S(1)}, u32[]{:S(2)}, u32[]{:S(2)}) collective-permute-start(bf16[256,256]{1,0:T(8,128)(2,1)} %get-tuple-element.44), channel_id=1, source_target_pairs={{0,4},{1,5},{2,6},{3,7},{4,0},{5,1},{6,2},{7,3},{8,12},{9,13},{10,... | collective-permute-start | bytes 393224 | tf_op jit(solution)/shard_map/ppermute | solution.py:29
  205.2 13.5 %collective-permute-start.14 = (bf16[256,256]{1,0:T(8,128)(2,1)}, bf16[256,256]{1,0:T(8,128)(2,1)S(1)}, u32[]{:S(2)}, u32[]{:S(2)}) collective-permute-start(bf16[256,256]{1,0:T(8,128)(2,1)} %get-tuple-element.45), channel_id=1, source_target_pairs={{0,4},{1,5},{2,6},{3,7},{4,0},{5,1},{6,2},{7,3},{8,12},{9,13},{10,... | collective-permute-start | bytes 393224 | tf_op jit(solution)/shard_map/ppermute | solution.py:29
  213.8 4.9 %copy-start.20 = (bf16[256,256]{1,0:T(8,128)(2,1)}, bf16[256,256]{1,0:T(8,128)(2,1)S(1)}, u32[]{:S(2)}) copy-start(bf16[256,256]{1,0:T(8,128)(2,1)S(1)} %collective-permute-done.13.refs_3_) | copy-start | bytes 393220
  213.8 28.7 %collective-permute-start.4 = (bf16[128,256]{0,1:T(8,128)(2,1)S(1)}, bf16[128,256]{0,1:T(8,128)(2,1)}, u32[]{:S(2)}, u32[]{:S(2)}) collective-permute-start(bf16[128,256]{0,1:T(8,128)(2,1)S(1)} %pad_maximum_fusion.2), channel_id=1, source_target_pairs={{0,2},{1,3},{2,0},{3,1},{4,6},{5,7},{6,4},{7,5},{8,10},{9,11},{10,... | collective-permute-start | bytes 196616 | tf_op jit(solution)/shard_map/ppermute | solution.py:34
  218.7 0.7 copy-start.21
  218.7 0.8 copy-start.12
  219.5 0.7 copy-start.14
  223.4 46.1 %all-to-all-start.3 = ((bf16[64,16,256]{2,1,0:T(8,128)(2,1)}), bf16[64,16,256]{2,1,0:T(8,128)(2,1)S(1)}, u32[]{:S(2)}, u32[]{:S(2)}) async-start(bf16[64,16,256]{2,1,0:T(8,128)(2,1)} %bitcast.128), calls=%async_computation.3 | async-start | bytes 1048576 | tf_op jit(solution)/shard_map/all_to_all | solution.py:38
  237.8 31.7 %copy-start.5 = (bf16[128,32,32]{0,2,1:T(8,128)(2,1)S(1)}, bf16[128,32,32]{0,2,1:T(8,128)(2,1)}, u32[]{:S(2)}) copy-start(bf16[128,32,32]{0,2,1:T(8,128)(2,1)} %get-tuple-element.127) | copy-start | bytes 786436
  237.8 8.9 %collective-permute-start.1 = (bf16[2,16,2048]{2,1,0:T(8,128)(2,1)S(1)}, bf16[2,16,2048]{2,1,0:T(8,128)(2,1)S(1)}, u32[]{:S(2)}, u32[]{:S(2)}) collective-permute-start(bf16[2,16,2048]{2,1,0:T(8,128)(2,1)S(1)} %fusion.26), channel_id=1, source_target_pairs={{0,2},{1,3},{2,0},{3,1},{4,6},{5,7},{6,4},{7,5},{8,10},{9,11},{10,... | collective-permute-start | bytes 393224 | tf_op jit(solution)/shard_map/ppermute | solution.py:34
  243.4 8.8 %collective-permute-start.5 = (bf16[128,512]{0,1:T(8,128)(2,1)S(1)}, bf16[128,512]{0,1:T(8,128)(2,1)S(1)}, u32[]{:S(2)}, u32[]{:S(2)}) collective-permute-start(bf16[128,512]{0,1:T(8,128)(2,1)S(1)} %pad_maximum_fusion.1), channel_id=1, source_target_pairs={{0,1},{1,0},{2,3},{3,2},{4,5},{5,4},{6,7},{7,6},{8,9},{9,8},{10,11... | collective-permute-start | bytes 393224 | tf_op jit(solution)/shard_map/ppermute | solution.py:34
  246.8 23.0 %copy-start.4 = (bf16[128,32,32]{0,2,1:T(8,128)(2,1)S(1)}, bf16[128,32,32]{0,2,1:T(8,128)(2,1)}, u32[]{:S(2)}) copy-start(bf16[128,32,32]{0,2,1:T(8,128)(2,1)} %get-tuple-element.126) | copy-start | bytes 786436
  246.8 9.5 %collective-permute-start.2 = (bf16[16,2048]{1,0:T(8,128)(2,1)S(1)}, bf16[16,2048]{1,0:T(8,128)(2,1)S(1)}, u32[]{:S(2)}, u32[]{:S(2)}) collective-permute-start(bf16[16,2048]{1,0:T(8,128)(2,1)S(1)} %fusion.43), channel_id=1, source_target_pairs={{0,4},{1,5},{2,6},{3,7},{4,0},{5,1},{6,2},{7,3},{8,12},{9,13},{10,... | collective-permute-start | bytes 196616 | tf_op jit(solution)/shard_map/ppermute | solution.py:34
  269.8 1.0 copy-start.6
